TPU v7x, 32 devices: a whole 2x2x4 slice. The times are simulated.
32 devices in a mesh: ep: 8 (over z, x), tp: 4 (over y, core).
Axes of the slice: x: 2, y: 2, z: 4, core: 2. Of those that a mesh axis runs over, the one named last changes fastest.
Arguments:
- mixer_input: bfloat16 [2048, 2048], P('ep', 'tp'), may hold values from -80 to 80
- mixer_gain: float32 [2048], P('tp'), may hold values from 0.1 to 1.9
- time_step: float32 [2048, 128], P('ep', 'tp'), may hold values from 0.25 to 4
- pole_real: float32 [128, 32], P('tp'), may hold values from -0.1 to 0, as said below
- pole_imag: float32 [128, 32], P('tp'), may hold values from 0.25 to 3
- input_real: float32 [128, 32, 16], P('tp'), may hold values from -1 to 1
- input_imag: float32 [128, 32, 16], P('tp'), may hold values from -1 to 1
- read_real: float32 [128, 16, 32], P('tp'), may hold values from -1 to 1
- read_imag: float32 [128, 16, 32], P('tp'), may hold values from -1 to 1
- out_value: bfloat16 [2048, 2048], P(None, 'tp'), may hold values from -0.125 to 0.125
- out_gate: bfloat16 [2048, 2048], P(None, 'tp'), may hold values from -0.125 to 0.125
- expert_input: bfloat16 [1024, 2048], P('ep', 'tp'), may hold values from -80 to 80
- expert_gain: float32 [2048], P('tp'), may hold values from 0.1 to 1.9
- routes: int32 [1024, 2], P('ep'), may hold values from 0 to 7, all different within a row; in each aligned block of 128 rows (0 to 127, 128 to 255, ...) at most 64 rows name the same one
- route_weight: float32 [1024, 2], P('ep'), may hold values from 0.2 to 1
- expert_gate: bfloat16 [8, 2048, 4096], P('ep', None, 'tp'), may hold values from -0.125 to 0.125
- expert_up: bfloat16 [8, 2048, 4096], P('ep', None, 'tp'), may hold values from -0.125 to 0.125
- expert_down: bfloat16 [8, 4096, 2048], P('ep', 'tp'), may hold values from -0.125 to 0.125
Outputs:
- mixer_output: bfloat16 [2048, 2048], P('ep', 'tp')
- expert_output: bfloat16 [1024, 2048], P('ep', 'tp')
Inputs may be any that keep to these rules, and one draw needn't show every extreme that they name: `routes`: each row names 2 different experts. Among the 128 rows of one index of ep, no expert is named more than 64 times, a bound that some block reaches in some of them. `pole_real`: every rate is negative.
All inputs are finite; a program needn't handle non-finite values.
Results may differ from a plain program's by a relative error of at most 0.02.
Values may be sent and summed in bfloat16 or wider, within the bound.
No kernel may reach another device: no remote copies, remote signals or barrier semaphores. Data moves between devices by JAX's collectives and lax.ppermute only.
A program may use at most 128 MiB of HBM per device.

v0:
```python
import functools

import jax
import jax.numpy as jnp
from jax import lax
from jax.experimental import pallas as pl
from jax.experimental.pallas import tpu as pltpu
from jax.sharding import PartitionSpec as P


f32 = jnp.float32
bf16 = jnp.bfloat16
norm_eps = 1e-05
LANES = 8
NN = (((1,), (0,)), ((), ()))
NT = (((1,), (1,)), ((), ()))
TN = (((0,), (0,)), ((), ()))


def iota(shape, dim):
    return lax.broadcasted_iota(jnp.int32, shape, dim)


def ones_where(mask):
    return jnp.where(mask, 1.0, 0.0).astype(bf16)


def split2(value):
    high = value.astype(bf16)
    return high, (value - high.astype(f32)).astype(bf16)


def split3(value):
    high = value.astype(bf16)
    rest = value - high.astype(f32)
    mid = rest.astype(bf16)
    return high, mid, (rest - mid.astype(f32)).astype(bf16)


def mm(left, right, dims=NN):
    return lax.dot_general(left, right, dims, preferred_element_type=f32)


def mm3(left, right, dims):
    lh, ll = left
    rh, rl = right
    return mm(lh, rh, dims) + (mm(ll, rh, dims) + mm(lh, rl, dims))


def mul(ar, ai, br, bi):
    return ar * br - ai * bi, ar * bi + ai * br


def slot_keys(routes_t, experts):
    top, tokens = routes_t.shape
    number = iota((experts, tokens), 0)
    hit = routes_t[0:1, :] == number
    for k in range(1, top):
        hit = hit | (routes_t[k : k + 1, :] == number)
    before = ones_where(iota((tokens, tokens), 0) < iota((tokens, tokens), 1))
    place = mm(ones_where(hit), before)
    return jnp.where(hit, place, -1.0)


def send_kernel(experts, capacity, routes_ref, rows_ref, out_ref):
    keys = slot_keys(routes_ref[...], experts)
    tokens = keys.shape[1]
    slot = iota((capacity, tokens), 0).astype(f32)
    chosen = [ones_where(slot == keys[e : e + 1, :]) for e in range(experts)]
    out_ref[...] = mm(jnp.concatenate(chosen, axis=0), rows_ref[...]).astype(bf16)


def share_kernel(experts, capacity, routes_ref, weight_ref, out_ref):
    routes_t = routes_ref[...]
    weight_t = weight_ref[...]
    keys = slot_keys(routes_t, experts)
    tokens = keys.shape[1]
    number = iota((experts, tokens), 0)
    share = jnp.zeros((experts, tokens), f32)
    for k in range(routes_t.shape[0]):
        share = share + jnp.where(routes_t[k : k + 1, :] == number, weight_t[k : k + 1, :], 0.0)
    slot = iota((capacity, tokens), 0).astype(f32)
    spread = [
        jnp.where(slot == keys[e : e + 1, :], share[e : e + 1, :], 0.0) for e in range(experts)
    ]
    same = ones_where(iota((tokens, tokens), 0) == iota((tokens, tokens), 1))
    for n, term in enumerate(split3(jnp.concatenate(spread, axis=0))):
        out_ref[n] = mm(same, term, NT).astype(bf16)


def combine_kernel(share_ref, back_ref, out_ref):
    back = back_ref[...]
    out = mm(share_ref[0], back) + (mm(share_ref[1], back) + mm(share_ref[2], back))
    out_ref[...] = out.astype(bf16)


def hidden_kernel(parts, blocks_of, me_ref, packed_ref, *refs):
    blocks = refs[:parts]
    gate_ref, up_ref, down_ref, hidden_ref, far_ref, normed_ref = refs[parts:]
    rows, feats = blocks[0].shape
    width = parts * feats
    chunk = 64
    step = pl.program_id(0)

    @pl.when(step == 0)
    def _():
        me = me_ref[0]
        lead = packed_ref.shape[1] - feats
        number = iota((parts, feats), 0)
        gains = [
            jnp.sum(jnp.where(number == me ^ k, packed_ref[:, lead:], 0.0), axis=0, keepdims=True)
            for k in range(parts)
        ]

        def body(step, unused):
            at = pl.ds(pl.multiple_of(step * chunk, chunk), chunk)
            total = jnp.zeros((chunk, 1), f32)
            square = jnp.zeros((chunk, 1), f32)
            for block in blocks:
                wide = block[at, :].astype(f32)
                total = total + jnp.sum(wide, axis=1, keepdims=True)
                square = square + jnp.sum(wide * wide, axis=1, keepdims=True)
            mean = total / width
            scale = lax.rsqrt(square / width - mean * mean + norm_eps)
            for k, block in enumerate(blocks):
                which = me ^ k
                value = (block[at, :].astype(f32) - mean) * scale * gains[k]
                cols = pl.ds(pl.multiple_of(which * feats, feats), feats)
                normed_ref[at, cols] = value.astype(bf16)
            return unused

        lax.fori_loop(0, rows // chunk, body, 0, unroll=2)

    @pl.when(step < blocks_of)
    def _():
        normed = normed_ref[...]
        gate = mm(normed, gate_ref[0])
        up = mm(normed, up_ref[0])
        size = gate_ref.shape[2]
        cols = pl.ds(pl.multiple_of(step * size, size), size)
        hidden_ref[:, cols] = (gate * jax.nn.sigmoid(gate) * up).astype(bf16)

    @pl.when(step >= blocks_of)
    def _():
        far_ref[0] = mm(hidden_ref[...], down_ref[0]).astype(bf16)


def down_kernel(me_ref, hidden_ref, weight_ref, out_ref):
    out_ref[0] = mm(hidden_ref[...], weight_ref[0]).astype(bf16)


def reorder(rows, back):
    steps = rows // LANES
    row, col = iota((rows, rows), 1 if back else 0), iota((rows, rows), 0 if back else 1)
    return ones_where(col == (row % LANES) * steps + row // LANES)


def sums_kernel(x_ref, gain_ref, out_ref):
    rows = x_ref[...]
    count = rows.shape[0]
    ones = jnp.ones((8, rows.shape[1]), bf16)
    wide = rows.astype(f32)
    high, low = split2(wide * wide)
    out_ref[:, :count] = mm(ones, rows, NT)[0:1]
    out_ref[:, count : 2 * count] = (mm(ones, high, NT) + mm(ones, low, NT))[0:1]
    out_ref[:, 2 * count :] = gain_ref[...]


def in_line(table, width):
    states = table.shape[1]
    wide = spread_table(table, states, 1, states, width)
    return jnp.sum(wide, axis=0, keepdims=True)


def sin_cos(angle):
    turns = jnp.floor(angle * 0.6366197723675814 + 0.5)
    rest = angle - turns * 1.5703125
    rest = rest - turns * 4.83751296997070312e-4
    rest = rest - turns * 7.54978995489188e-8
    z = rest * rest
    sine = rest + rest * z * (
        -1.6666654611e-1 + z * (8.3321608736e-3 + z * -1.9515295891e-4)
    )
    cosine = 1.0 - 0.5 * z + z * z * (
        4.166664568298827e-2 + z * (-1.388731625493765e-3 + z * 2.443315711809948e-5)
    )
    quarter = turns.astype(jnp.int32)
    odd = (quarter & 1) != 0
    first = jnp.where(odd, cosine, sine)
    second = jnp.where(odd, sine, cosine)
    first = jnp.where((quarter & 2) != 0, -first, first)
    second = jnp.where(((quarter + 1) & 2) != 0, -second, second)
    return first, second


def spread_table(table, inner, outer_rows, outer_cols, width):
    rows = table.shape[0]
    pick = ones_where(iota((inner, width), 1) % inner == iota((inner, width), 0))
    high, mid, low = split3(table)
    wide = mm(high, pick) + (mm(mid, pick) + mm(low, pick))
    same = iota((rows, width), 0) // outer_rows == iota((rows, width), 1) // outer_cols
    return jnp.where(same, wide, 0.0)


def scan_kernel(
    total, x_ref, packed_ref, gain_ref, step_ref, pr_ref, pi_ref, ir_ref, ii_ref,
    hr_ref, hi_ref, cr_ref, ci_ref, end_ref, ar_ref, ai_ref,
):
    rows, feats = x_ref.shape
    groups, states = pr_ref.shape
    flat = groups * states
    inner = feats // groups
    steps = rows // LANES
    order = reorder(rows, False)
    mean = jnp.sum(packed_ref[:, :rows], axis=0, keepdims=True) / total
    square = jnp.sum(packed_ref[:, rows : 2 * rows], axis=0, keepdims=True) / total
    scale = lax.rsqrt(square - mean * mean + norm_eps)
    match = iota((rows, rows), 1) == (iota((rows, rows), 0) % LANES) * steps + iota(
        (rows, rows), 0
    ) // LANES
    mean_col = jnp.sum(jnp.where(match, mean, 0.0), axis=1, keepdims=True)
    scale_col = jnp.sum(jnp.where(match, scale, 0.0), axis=1, keepdims=True)
    poles_re = in_line(pr_ref[...], flat)
    poles_im = in_line(pi_ref[...], flat)
    size = poles_re * poles_re + poles_im * poles_im
    over_re, over_im = poles_re / size, -poles_im / size
    d_high, d_mid, d_low = (
        mm(part, order, NT).astype(bf16) for part in split3(step_ref[...])
    )
    piece = min(flat, 256)
    for at in range(0, flat, piece):
        cols = pl.ds(at, piece)
        expand = ones_where(
            iota((groups, piece), 0) == (iota((groups, piece), 1) + at) // states
        )
        delta = mm(d_high, expand, TN) + (mm(d_mid, expand, TN) + mm(d_low, expand, TN))
        size = jnp.exp(poles_re[:, at : at + piece] * delta)
        sine, cosine = sin_cos(poles_im[:, at : at + piece] * delta)
        ar_ref[:, cols] = size * cosine
        ai_ref[:, cols] = size * sine
    cw = min(feats, 256)
    sw = cw // inner * states
    for b in range(feats // cw):
        chans = pl.ds(b * cw, cw)
        cols = pl.ds(b * sw, sw)
        rows_in = mm(order, x_ref[:, chans])
        normed = split2((rows_in - mean_col) * scale_col * gain_ref[:, chans])
        real = split2(spread_table(ir_ref[chans, :], states, inner, states, sw))
        imag = split2(spread_table(ii_ref[chans, :], states, inner, states, sw))
        hr_ref[:, cols], hi_ref[:, cols] = mul(
            mm3(normed, real, NN), mm3(normed, imag, NN),
            over_re[:, b * sw : b * sw + sw], over_im[:, b * sw : b * sw + sw],
        )
    span = min(flat, 512)
    for at in range(0, flat, span):
        cols = pl.ds(at, span)

        def body(j, carry):
            h_re, h_im, c_re, c_im = carry
            here = pl.ds(pl.multiple_of(j * LANES, LANES), LANES)
            a_re, a_im = ar_ref[here, cols], ai_ref[here, cols]
            d_re, d_im = hr_ref[here, cols], hi_ref[here, cols]
            h_re, h_im = mul(a_re, a_im, h_re + d_re, h_im + d_im)
            h_re, h_im = h_re - d_re, h_im - d_im
            c_re, c_im = mul(a_re, a_im, c_re, c_im)
            hr_ref[here, cols], hi_ref[here, cols] = h_re, h_im
            cr_ref[here, cols], ci_ref[here, cols] = c_re, c_im
            return h_re, h_im, c_re, c_im

        zero = jnp.zeros((LANES, span), f32)
        lax.fori_loop(0, steps, body, (zero, zero, zero + 1.0, zero))
    last = pl.ds(rows - LANES, LANES)
    h_re, h_im, c_re, c_im = hr_ref[last, :], hi_ref[last, :], cr_ref[last, :], ci_ref[last, :]
    p_re, p_im = c_re[0:1], c_im[0:1]
    s_re, s_im = h_re[0:1], h_im[0:1]
    for c in range(1, LANES):
        k_re, k_im = c_re[c : c + 1], c_im[c : c + 1]
        p_re, p_im = mul(k_re, k_im, p_re, p_im)
        s_re, s_im = mul(k_re, k_im, s_re, s_im)
        s_re, s_im = s_re + h_re[c : c + 1], s_im + h_im[c : c + 1]
    ends = jnp.concatenate([p_re, p_im, s_re, s_im], axis=0)
    for i in range(end_ref.shape[0]):
        end_ref[i] = ends


def read_kernel(
    me_ref, got_ref, hr_ref, hi_ref, cr_ref, ci_ref, rr_ref, ri_ref, out_ref,
):
    rows, flat = hr_ref.shape
    feats = out_ref.shape[1]
    states = rr_ref.shape[1]
    inner = feats // (flat // states)
    steps = rows // LANES
    me = me_ref[0]
    s_re = jnp.zeros((1, flat), f32)
    s_im = jnp.zeros((1, flat), f32)
    for i in range(got_ref.shape[0] - 1):
        ends = got_ref[i]
        n_re, n_im = mul(ends[0:1], ends[1:2], s_re, s_im)
        s_re = jnp.where(i < me, n_re + ends[2:3], s_re)
        s_im = jnp.where(i < me, n_im + ends[3:4], s_im)
    last = pl.ds(rows - LANES, LANES)
    h_re, h_im, c_re, c_im = hr_ref[last, :], hi_ref[last, :], cr_ref[last, :], ci_ref[last, :]
    in_re, in_im = [s_re], [s_im]
    for c in range(LANES - 1):
        n_re, n_im = mul(c_re[c : c + 1], c_im[c : c + 1], in_re[-1], in_im[-1])
        in_re.append(n_re + h_re[c : c + 1])
        in_im.append(n_im + h_im[c : c + 1])
    in_re = jnp.concatenate(in_re, axis=0)[None]
    in_im = jnp.concatenate(in_im, axis=0)[None]
    back = reorder(rows, True)
    cw = min(feats, 256)
    sw = cw // inner * states
    for b in range(feats // cw):
        chans = pl.ds(b * cw, cw)
        lo = b * sw
        cols = pl.ds(lo, sw)
        shape = (steps, LANES, sw)
        c_re, c_im = cr_ref[:, cols].reshape(shape), ci_ref[:, cols].reshape(shape)
        g_re, g_im = in_re[:, :, lo : lo + sw], in_im[:, :, lo : lo + sw]
        f_re = hr_ref[:, cols].reshape(shape) + (c_re * g_re - c_im * g_im)
        f_im = hi_ref[:, cols].reshape(shape) + (c_re * g_im + c_im * g_re)
        real = split2(spread_table(rr_ref[chans, :], states, inner, states, sw))
        imag = split2(spread_table(ri_ref[chans, :], states, inner, states, sw))
        response = mm3(split2(f_re.reshape(rows, sw)), real, NT) - mm3(
            split2(f_im.reshape(rows, sw)), imag, NT
        )
        cube = response + 0.044715 * (response * response * response)
        mixed = 0.5 * response * (1.0 + jnp.tanh(0.7978845608028654 * cube))
        out_ref[:, chans] = mm(back, mixed.astype(bf16)).astype(bf16)


def output_kernel(parts, me_ref, *refs):
    pieces = refs[:parts]
    value_ref, gate_ref, out_ref = refs[parts:]
    feats = pieces[0].shape[1]
    value = gate = None
    for k, piece in enumerate(pieces):
        at = pl.ds(pl.multiple_of((me_ref[0] ^ k) * feats, feats), feats)
        rows = piece[...]
        v, g = mm(rows, value_ref[at, :]), mm(rows, gate_ref[at, :])
        value, gate = (v, g) if value is None else (value + v, gate + g)
    out_ref[...] = (value * jax.nn.sigmoid(gate)).astype(bf16)


vmem = pl.BlockSpec(memory_space=pltpu.VMEM)
smem = pl.BlockSpec(memory_space=pltpu.SMEM)


def params(mib):
    return pltpu.CompilerParams(vmem_limit_bytes=mib << 20)


def swap(value, bit):
    count = lax.axis_size("tp")
    return lax.ppermute(value, "tp", [(i, i ^ bit) for i in range(count)])


def gather_tp(value):
    count = lax.axis_size("tp")
    blocks = {0: value}
    bit = count // 2
    while bit >= 1:
        blocks.update({k ^ bit: swap(block, bit) for k, block in list(blocks.items())})
        bit //= 2
    return [blocks[k] for k in range(count)]


def shards(
    mixer_input, mixer_gain, time_step, pole_real, pole_imag, input_real, input_imag,
    read_real, read_imag, out_value, out_gate, expert_input, expert_gain, routes,
    route_weight, expert_gate, expert_up, expert_down,
):
    n_tp, n_ep = lax.axis_size("tp"), lax.axis_size("ep")
    tp_at = lax.axis_index("tp").astype(jnp.int32).reshape(1)
    ep_at = lax.axis_index("ep").astype(jnp.int32).reshape(1)
    tokens, feats = expert_input.shape
    top = routes.shape[1]
    capacity = 2 * top * tokens // n_ep
    slots = n_ep * capacity
    routes_t = routes.T
    weight_t = route_weight.T

    send = pl.pallas_call(
        functools.partial(send_kernel, n_ep, capacity),
        out_shape=jax.ShapeDtypeStruct((slots, feats), bf16),
        in_specs=[vmem, vmem], out_specs=vmem, compiler_params=params(8), name="send_rows",
    )(routes_t, expert_input)
    arrived = lax.all_to_all(send, "ep", split_axis=0, concat_axis=0, tiled=True)

    rows, chans = mixer_input.shape
    mixer_input, send = lax.optimization_barrier((mixer_input, send))
    packed = pl.pallas_call(
        sums_kernel,
        out_shape=jax.ShapeDtypeStruct((1, 2 * rows + feats), f32),
        in_specs=[vmem, vmem], out_specs=vmem, compiler_params=params(8), name="mixer_sums",
    )(mixer_input, expert_gain.reshape(1, feats))
    packed = lax.all_gather(packed, "tp", axis=0, tiled=True)

    groups, states = pole_real.shape
    flat = groups * states
    big = jax.ShapeDtypeStruct((rows, flat), f32)
    h_re, h_im, c_re, c_im, ends = pl.pallas_call(
        functools.partial(scan_kernel, float(chans * n_tp)),
        out_shape=(big, big, big, big, jax.ShapeDtypeStruct((n_ep, 4, flat), f32)),
        in_specs=[vmem] * 8, out_specs=(vmem,) * 5,
        scratch_shapes=[pltpu.VMEM((rows, flat), f32)] * 2,
        compiler_params=params(28), name="mixer_scan",
    )(
        mixer_input, packed, mixer_gain.reshape(1, chans), time_step.T,
        pole_real, pole_imag,
        jnp.swapaxes(input_real, 1, 2).reshape(chans, states),
        jnp.swapaxes(input_imag, 1, 2).reshape(chans, states),
    )
    got = lax.all_to_all(ends, "ep", split_axis=0, concat_axis=0)

    blocks = gather_tp(arrived)
    share = pl.pallas_call(
        functools.partial(share_kernel, n_ep, capacity),
        out_shape=jax.ShapeDtypeStruct((3, tokens, slots), bf16),
        in_specs=[vmem, vmem], out_specs=vmem, compiler_params=params(8), name="route_share",
    )(routes_t, weight_t)
    units = expert_gate.shape[2]
    unit_block = min(units, 256)
    n_unit = units // unit_block
    n_far = n_tp // 2 - 1
    hidden, odd_far = pl.pallas_call(
        functools.partial(hidden_kernel, n_tp, n_unit),
        grid_spec=pltpu.PrefetchScalarGridSpec(
            num_scalar_prefetch=1,
            grid=(n_unit + n_far,),
            in_specs=[vmem] * (n_tp + 1) + [
                pl.BlockSpec(
                    (1, n_tp * feats, unit_block),
                    lambda j, me: (0, 0, jnp.minimum(j, n_unit - 1)),
                ),
                pl.BlockSpec(
                    (1, n_tp * feats, unit_block),
                    lambda j, me: (0, 0, jnp.minimum(j, n_unit - 1)),
                ),
                pl.BlockSpec(
                    (1, units, feats),
                    lambda j, me: (0, 0, me[0] ^ (2 * jnp.maximum(j - n_unit, 0) + 3)),
                ),
            ],
            out_specs=(
                pl.BlockSpec((slots, units), lambda j, me: (0, 0)),
                pl.BlockSpec(
                    (1, slots, feats), lambda j, me: (jnp.maximum(j - n_unit, 0), 0, 0)
                ),
            ),
            scratch_shapes=[pltpu.VMEM((slots, n_tp * feats), bf16)],
        ),
        out_shape=(
            jax.ShapeDtypeStruct((slots, units), bf16),
            jax.ShapeDtypeStruct((n_far, slots, feats), bf16),
        ),
        compiler_params=params(28), name="expert_hidden",
    )(tp_at, packed, *blocks, expert_gate, expert_up, expert_down)

    def down(count, offset):
        return pl.pallas_call(
            down_kernel,
            grid_spec=pltpu.PrefetchScalarGridSpec(
                num_scalar_prefetch=1,
                grid=(count,),
                in_specs=[
                    pl.BlockSpec((slots, units), lambda i, me: (0, 0)),
                    pl.BlockSpec((1, units, feats), lambda i, me: (0, 0, me[0] ^ offset(i))),
                ],
                out_specs=pl.BlockSpec((1, slots, feats), lambda i, me: (i, 0, 0)),
            ),
            out_shape=jax.ShapeDtypeStruct((count, slots, feats), bf16),
            compiler_params=params(10),
        )(tp_at, hidden, expert_down)

    theirs = swap(odd_far, 1)
    far = down(n_far, lambda i: 2 * i + 2).astype(f32) + theirs.astype(f32)
    parts = [swap(down(1, lambda i: i + 1)[0], 1), down(1, lambda i: i)[0]]
    bit = n_tp // 4
    while bit >= 1:
        come = swap(far[bit - 1 :].astype(bf16), 2 * bit).astype(f32)
        parts.append(come[0])
        far = far[: bit - 1] + come[1:]
        bit //= 2
    result = sum(part.astype(f32) for part in parts).astype(bf16)
    back = lax.all_to_all(result, "ep", split_axis=0, concat_axis=0, tiled=True)

    mixed = pl.pallas_call(
        read_kernel,
        out_shape=jax.ShapeDtypeStruct((rows, chans), bf16),
        in_specs=[smem] + [vmem] * 7, out_specs=vmem, compiler_params=params(28),
        name="mixer_read",
    )(
        ep_at, got, h_re, h_im, c_re, c_im,
        read_real.reshape(chans, states), read_imag.reshape(chans, states),
    )
    pieces = gather_tp(mixed)
    mixer_output = pl.pallas_call(
        functools.partial(output_kernel, n_tp),
        out_shape=jax.ShapeDtypeStruct((rows, out_value.shape[1]), bf16),
        in_specs=[smem] + [vmem] * (n_tp + 2), out_specs=vmem, compiler_params=params(20),
        name="mixer_out",
    )(tp_at, *pieces, out_value, out_gate)
    expert_output = pl.pallas_call(
        combine_kernel,
        out_shape=jax.ShapeDtypeStruct((tokens, feats), bf16),
        in_specs=[vmem] * 2, out_specs=vmem, compiler_params=params(8), name="combine",
    )(share, back)
    return mixer_output, expert_output


def solution(mesh):
    return jax.shard_map(
        shards,
        mesh=mesh,
        in_specs=(
            P("ep", "tp"), P("tp"), P("ep", "tp"), P("tp", None), P("tp", None),
            P("tp", None, None), P("tp", None, None), P("tp", None, None), P("tp", None, None),
            P(None, "tp"), P(None, "tp"), P("ep", "tp"), P("tp"), P("ep", None), P("ep", None),
            P("ep", None, "tp"), P("ep", None, "tp"), P("ep", "tp", None),
        ),
        out_specs=(P("ep", "tp"), P("ep", "tp")),
        check_vma=False,
    )
```

profile of v0, /device:TPU:0, one launch (start us, length us, event | category | flops | bytes accessed | tf_op | source)
XLA Modules:
  0.0 108.9 jit_solution(11110360165244996356)
XLA Ops:
  0.6 0.9 copy-done.20
  1.5 0.7 copy-done.24
  2.2 0.4 send_rows.1
  2.6 21.6 %all_to_all.27 = bf16[8,64,512]{2,1,0:T(8,128)(2,1)S(1)} all-to-all(bf16[8,64,512]{2,1,0:T(8,128)(2,1)S(1)} %bitcast.33), channel_id=1, replica_groups=mesh['ep'=8,'tp'=4] {'ep'}, dimensions={0} | all-to-all | bytes 1048576 | tf_op jit(solution)/shard_map/all_to_all | solution.py:389
  24.2 1.5 %collective-permute-start.4 = (bf16[512,512]{1,0:T(8,128)(2,1)S(1)}, bf16[512,512]{1,0:T(8,128)(2,1)S(1)}, u32[]{:S(2)}, u32[]{:S(2)}) collective-permute-start(bf16[512,512]{1,0:T(8,128)(2,1)S(1)} %bitcast.30), channel_id=1, source_target_pairs={{0,2},{1,3},{2,0},{3,1},{4,6},{5,7},{6,4},{7,5},{8,10},{9,11},{10,... | collective-permute-start | bytes 1572872 | tf_op jit(solution)/shard_map/ppermute | solution.py:356
  25.7 0.0 collective-permute-start.3
  25.8 11.0 %collective-permute-done.4.refs_2_ = bf16[512,512]{1,0:T(8,128)(2,1)S(1)} collective-permute-done((bf16[512,512]{1,0:T(8,128)(2,1)S(1)}, bf16[512,512]{1,0:T(8,128)(2,1)S(1)}, u32[]{:S(2)}, u32[]{:S(2)}) %collective-permute-start.4) | collective-permute-done | bytes 524320 | tf_op jit(solution)/shard_map/ppermute | solution.py:356
  36.8 0.0 collective-permute-start.5
  36.8 0.9 copy-done.6
  37.7 0.7 copy-done.26
  38.4 0.3 mixer_sums.1
  38.7 5.2 %all-gather = f32[4,1,1024]{2,1,0:T(1,128)S(1)} all-gather(f32[1,1,1024]{2,1,0:T(1,128)S(1)} %bitcast.43), channel_id=1, replica_groups=mesh['ep'=8,'tp'=4] {'tp'}, dimensions={0}, use_global_device_ids=true | all-gather | bytes 20480 | tf_op jit(solution)/shard_map/all_gather | solution.py:398
  43.9 0.0 collective-permute-done.3.refs_1_
  43.9 0.0 collective-permute-done.5.refs_3_
  43.9 0.0 copy-start
  44.0 2.2 %copy-done = bf16[1,1024,2048]{2,1,0:T(8,128)(2,1)S(1)} copy-done((bf16[1,1024,2048]{2,1,0:T(8,128)(2,1)S(1)}, bf16[1,1024,2048]{2,1,0:T(8,128)(2,1)}, u32[]{:S(2)}) %copy-start) | copy-done | bytes 4194328
  46.1 2.2 %copy-done.2 = bf16[1,2048,1024]{2,1,0:T(8,128)(2,1)S(1)} copy-done((bf16[1,2048,1024]{2,1,0:T(8,128)(2,1)S(1)}, bf16[1,2048,1024]{2,1,0:T(8,128)(2,1)}, u32[]{:S(2)}) %copy-start.2) | copy-done | bytes 4194328
  48.3 2.2 %copy-done.3 = bf16[1,2048,1024]{2,1,0:T(8,128)(2,1)S(1)} copy-done((bf16[1,2048,1024]{2,1,0:T(8,128)(2,1)S(1)}, bf16[1,2048,1024]{2,1,0:T(8,128)(2,1)}, u32[]{:S(2)}) %copy-start.3) | copy-done | bytes 4194328
  50.5 8.6 %expert_hidden.1 = (bf16[512,1024]{1,0:T(8,128)(2,1)S(1)}, bf16[1,512,512]{2,1,0:T(8,128)(2,1)S(1)}) custom-call(s32[1]{0:T(128)} %bitcast.me_ref, f32[4,1024]{1,0:T(4,128)S(1)} %bitcast.40, bf16[512,512]{1,0:T(8,128)(2,1)S(1)} %bitcast.32, bf16[512,512]{1,0:T(8,128)(2,1)S(1)} %collective-permute-done.3.refs_1_, ...), custom_call_target="tpu_custom_call" | custom-call | tf_op jit(solution)/shard_map/expert_hidden/pallas_call | solution.py:427
  59.1 0.4 collective-permute-start.7
  59.6 0.7 shard_map.187
  60.3 0.0 copy-start.7
  60.3 0.0 copy-start.16
  60.3 0.0 copy-start.17
  60.3 0.0 copy-start.21
  60.3 0.0 copy-start.22
  60.3 0.0 copy-start.23
  60.3 0.0 copy-start.27
  60.4 0.7 shard_map.185
  61.1 0.2 collective-permute-start.6
  61.3 0.0 collective-permute-done.7
  61.3 0.9 add_convert_fusion
  62.2 1.5 %collective-permute-start.8 = (bf16[1,512,512]{2,1,0:T(8,128)(2,1)}, bf16[1,512,512]{2,1,0:T(8,128)(2,1)}, u32[]{:S(2)}, u32[]{:S(2)}) collective-permute-start(bf16[1,512,512]{2,1,0:T(8,128)(2,1)} %add_convert_fusion), channel_id=1, source_target_pairs={{0,2},{1,3},{2,0},{3,1},{4,6},{5,7},{6,4},{7,5},{8,10},{9,11},{10,... | collective-permute-start | bytes 1572872 | tf_op jit(solution)/shard_map/ppermute | solution.py:356
  63.8 5.8 %mixer_scan.1 = (f32[256,1024]{1,0:T(8,128)S(1)}, f32[256,1024]{1,0:T(8,128)S(1)}, f32[256,1024]{1,0:T(8,128)S(1)}, f32[256,1024]{1,0:T(8,128)S(1)}, f32[8,4,1024]{2,1,0:T(4,128)}) custom-call(bf16[256,512]{1,0:T(8,128)(2,1)S(1)} %copy-done.7, f32[4,1024]{1,0:T(4,128)S(1)} %bitcast.41, f32[1,512]{1,0:T(1,128)S(1)} %bitcast.47, f32[32,256]{1,0:T(8,128)S(1)} %bitcast.42, ...), custom_call_target="tpu_custom_call" | custom-call | tf_op jit(solution)/shard_map/mixer_scan/pallas_call | solution.py:403
  69.6 1.0 copy-done.8
  70.6 1.0 copy-done.10
  71.6 1.0 copy-done.12
  72.6 1.0 copy-done.14
  73.6 4.4 %all-to-all-start = ((f32[8,4,1024]{2,1,0:T(4,128)}), f32[8,4,1024]{2,1,0:T(4,128)S(1)}, u32[]{:S(2)}, u32[]{:S(2)}) async-start(f32[8,4,1024]{2,1,0:T(4,128)} %get-tuple-element.11), calls=%async_computation | async-start | bytes 262144 | tf_op jit(solution)/shard_map/all_to_all | solution.py:415
  77.9 2.2 %copy-done.1 = bf16[1,1024,2048]{2,1,0:T(8,128)(2,1)S(1)} copy-done((bf16[1,1024,2048]{2,1,0:T(8,128)(2,1)S(1)}, bf16[1,1024,2048]{2,1,0:T(8,128)(2,1)}, u32[]{:S(2)}) %copy-start.1) | copy-done | bytes 4194328
  80.1 0.7 shard_map.186
  80.8 0.0 copy-start.25
  80.8 0.0 copy-start.28
  80.9 0.0 copy-start.4
  80.9 0.0 collective-permute-done.6
  80.9 0.0 collective-permute-done.8
  80.9 2.3 %fusion = bf16[512,512]{1,0:T(8,128)(2,1)} fusion(bf16[512,512]{1,0:T(8,128)(2,1)} %collective-permute-done.6, bf16[1,512,512]{2,1,0:T(8,128)(2,1)} %collective-permute-done.8, bf16[1,512,512]{2,1,0:T(8,128)(2,1)S(1)} %shard_map.186), kind=kLoop, calls=%fused_computation.1 | loop fusion | flops 1572864 | bytes 2097152 | tf_op jit(solution)/shard_map/convert_element_type | solution.py:486
  83.2 2.0 %all-to-all-done.got_ref = f32[8,4,1024]{2,1,0:T(4,128)S(1)} async-done(((f32[8,4,1024]{2,1,0:T(4,128)}), f32[8,4,1024]{2,1,0:T(4,128)S(1)}, u32[]{:S(2)}, u32[]{:S(2)}) %all-to-all-start) | async-done | bytes 131104 | tf_op jit(solution)/shard_map/all_to_all | solution.py:415
  85.3 4.0 %all-to-all-start.2 = ((bf16[8,64,512]{2,1,0:T(8,128)(2,1)}), bf16[8,64,512]{2,1,0:T(8,128)(2,1)S(1)}, u32[]{:S(2)}, u32[]{:S(2)}) async-start(bf16[8,64,512]{2,1,0:T(8,128)(2,1)} %bitcast.49), calls=%async_computation.2 | async-start | bytes 1048576 | tf_op jit(solution)/shard_map/all_to_all | solution.py:487
  89.3 1.4 %copy-done.9 = f32[256,1024]{1,0:T(8,128)S(1)} copy-done((f32[256,1024]{1,0:T(8,128)S(1)}, f32[256,1024]{1,0:T(8,128)}, u32[]{:S(2)}) %copy-start.9) | copy-done | bytes 1048600
  90.6 1.2 %copy-done.11 = f32[256,1024]{1,0:T(8,128)S(1)} copy-done((f32[256,1024]{1,0:T(8,128)S(1)}, f32[256,1024]{1,0:T(8,128)}, u32[]{:S(2)}) %copy-start.11) | copy-done | bytes 1048600
  91.8 1.2 %copy-done.13 = f32[256,1024]{1,0:T(8,128)S(1)} copy-done((f32[256,1024]{1,0:T(8,128)S(1)}, f32[256,1024]{1,0:T(8,128)}, u32[]{:S(2)}) %copy-start.13) | copy-done | bytes 1048600
  93.1 1.2 %copy-done.15 = f32[256,1024]{1,0:T(8,128)S(1)} copy-done((f32[256,1024]{1,0:T(8,128)S(1)}, f32[256,1024]{1,0:T(8,128)}, u32[]{:S(2)}) %copy-start.15) | copy-done | bytes 1048600
  94.3 2.5 %mixer_read.1.refs_0_ = bf16[256,512]{1,0:T(8,128)(2,1)S(1)} custom-call(s32[1]{0:T(128)} %bitcast.1.me_ref, f32[8,4,1024]{2,1,0:T(4,128)S(1)} %all-to-all-done.got_ref, f32[256,1024]{1,0:T(8,128)S(1)} %copy-done.9, f32[256,1024]{1,0:T(8,128)S(1)} %copy-done.11, f32[256,1024]{1,0:T(8,128)S(1)} %copy-done.13, f32[256,1024]{1,0:T(8,128)S(1)} %copy-done.15, ...), custom_call_target="tpu_custom_call" | custom-call | tf_op jit(solution)/shard_map/mixer_read/pallas_call | solution.py:489
  96.8 0.6 collective-permute-start.1
  97.4 0.0 collective-permute-start
  97.4 6.9 %collective-permute-done.1.refs_2_ = bf16[256,512]{1,0:T(8,128)(2,1)S(1)} collective-permute-done((bf16[256,512]{1,0:T(8,128)(2,1)S(1)}, bf16[256,512]{1,0:T(8,128)(2,1)S(1)}, u32[]{:S(2)}, u32[]{:S(2)}) %collective-permute-start.1) | collective-permute-done | bytes 262176 | tf_op jit(solution)/shard_map/ppermute | solution.py:356
  104.3 0.0 collective-permute-start.2
  104.3 0.4 route_share.1.share_ref
  104.8 0.0 collective-permute-done.refs_1_
  104.8 1.1 %collective-permute-done.2.refs_3_ = bf16[256,512]{1,0:T(8,128)(2,1)S(1)} collective-permute-done((bf16[256,512]{1,0:T(8,128)(2,1)S(1)}, bf16[256,512]{1,0:T(8,128)(2,1)S(1)}, u32[]{:S(2)}, u32[]{:S(2)}) %collective-permute-start.2) | collective-permute-done | bytes 262176 | tf_op jit(solution)/shard_map/ppermute | solution.py:356
  105.9 2.0 %mixer_out.1 = bf16[256,512]{1,0:T(8,128)(2,1)} custom-call(s32[1]{0:T(128)} %bitcast.me_ref, bf16[256,512]{1,0:T(8,128)(2,1)S(1)} %mixer_read.1.refs_0_, bf16[256,512]{1,0:T(8,128)(2,1)S(1)} %collective-permute-done.refs_1_, bf16[256,512]{1,0:T(8,128)(2,1)S(1)} %collective-permute-done.1.refs_2_, bf16[256,512]{1,0:T(8,128)(2,1)S(1)} %collective-permute-done.2.refs_3_, ...), custom_call_target="tpu_custom_call" | custom-call | tf_op jit(solution)/shard_map/mixer_out/pallas_call | solution.py:499
  107.8 0.0 all-to-all-done.2
  107.8 1.0 combine.1
  (32 shorter events, 0.1 us)
Async XLA Ops:
  0.6 0.9 copy-start.20
  1.5 0.7 copy-start.24
  24.2 12.5 %collective-permute-start.4 = (bf16[512,512]{1,0:T(8,128)(2,1)S(1)}, bf16[512,512]{1,0:T(8,128)(2,1)S(1)}, u32[]{:S(2)}, u32[]{:S(2)}) collective-permute-start(bf16[512,512]{1,0:T(8,128)(2,1)S(1)} %bitcast.30), channel_id=1, source_target_pairs={{0,2},{1,3},{2,0},{3,1},{4,6},{5,7},{6,4},{7,5},{8,10},{9,11},{10,... | collective-permute-start | bytes 1572872 | tf_op jit(solution)/shard_map/ppermute | solution.py:356
  25.7 18.2 %collective-permute-start.3 = (bf16[512,512]{1,0:T(8,128)(2,1)S(1)}, bf16[512,512]{1,0:T(8,128)(2,1)S(1)}, u32[]{:S(2)}, u32[]{:S(2)}) collective-permute-start(bf16[512,512]{1,0:T(8,128)(2,1)S(1)} %bitcast.31), channel_id=1, source_target_pairs={{0,1},{1,0},{2,3},{3,2},{4,5},{5,4},{6,7},{7,6},{8,9},{9,8},{10,11... | collective-permute-start | bytes 1572872 | tf_op jit(solution)/shard_map/ppermute | solution.py:356
  36.8 7.2 %collective-permute-start.5 = (bf16[512,512]{1,0:T(8,128)(2,1)S(1)}, bf16[512,512]{1,0:T(8,128)(2,1)S(1)}, u32[]{:S(2)}, u32[]{:S(2)}) collective-permute-start(bf16[512,512]{1,0:T(8,128)(2,1)S(1)} %collective-permute-done.4.refs_2_), channel_id=1, source_target_pairs={{0,1},{1,0},{2,3},{3,2},{4,5},{5,4},{6,7},{7,6},{8,9},{9,8},{10,11... | collective-permute-start | bytes 1572872 | tf_op jit(solution)/shard_map/ppermute | solution.py:356
  36.8 1.0 copy-start.6
  37.7 0.7 copy-start.26
  43.9 2.2 %copy-start = (bf16[1,1024,2048]{2,1,0:T(8,128)(2,1)S(1)}, bf16[1,1024,2048]{2,1,0:T(8,128)(2,1)}, u32[]{:S(2)}) copy-start(bf16[1,1024,2048]{2,1,0:T(8,128)(2,1)} %weight_ref.5) | copy-start | bytes 12582916
  46.1 2.2 %copy-start.2 = (bf16[1,2048,1024]{2,1,0:T(8,128)(2,1)S(1)}, bf16[1,2048,1024]{2,1,0:T(8,128)(2,1)}, u32[]{:S(2)}) copy-start(bf16[1,2048,1024]{2,1,0:T(8,128)(2,1)} %refs_4_.3) | copy-start | bytes 12582916
  48.3 2.2 %copy-start.3 = (bf16[1,2048,1024]{2,1,0:T(8,128)(2,1)S(1)}, bf16[1,2048,1024]{2,1,0:T(8,128)(2,1)}, u32[]{:S(2)}) copy-start(bf16[1,2048,1024]{2,1,0:T(8,128)(2,1)} %refs_5_.3) | copy-start | bytes 12582916
  59.1 2.2 %collective-permute-start.7 = (bf16[1,512,512]{2,1,0:T(8,128)(2,1)S(1)}, bf16[1,512,512]{2,1,0:T(8,128)(2,1)S(1)}, u32[]{:S(2)}, u32[]{:S(2)}) collective-permute-start(bf16[1,512,512]{2,1,0:T(8,128)(2,1)S(1)} %get-tuple-element.17), channel_id=1, source_target_pairs={{0,1},{1,0},{2,3},{3,2},{4,5},{5,4},{6,7},{7,6},{8,9},{9,8},{10,11... | collective-permute-start | bytes 1572872 | tf_op jit(solution)/shard_map/ppermute | solution.py:356
  60.3 3.5 %copy-start.7 = (bf16[256,512]{1,0:T(8,128)(2,1)S(1)}, bf16[256,512]{1,0:T(8,128)(2,1)}, u32[]{:S(2)}) copy-start(bf16[256,512]{1,0:T(8,128)(2,1)} %x_ref.1) | copy-start | bytes 786436
  60.3 3.5 %copy-start.16 = (f32[32,32,16]{1,2,0:T(8,128)S(1)}, f32[32,32,16]{1,2,0:T(8,128)}, u32[]{:S(2)}) copy-start(f32[32,32,16]{1,2,0:T(8,128)} %param.23) | copy-start | bytes 196612
  60.3 3.5 %copy-start.17 = (f32[32,32,16]{1,2,0:T(8,128)S(1)}, f32[32,32,16]{1,2,0:T(8,128)}, u32[]{:S(2)}) copy-start(f32[32,32,16]{1,2,0:T(8,128)} %param.24) | copy-start | bytes 196612
  60.3 3.4 %copy-start.21 = (f32[256,32]{0,1:T(8,128)S(1)}, f32[256,32]{0,1:T(8,128)}, u32[]{:S(2)}) copy-start(f32[256,32]{0,1:T(8,128)} %param.20) | copy-start | bytes 98308
  60.3 3.4 %copy-start.22 = (f32[32,32]{1,0:T(8,128)S(1)}, f32[32,32]{1,0:T(8,128)}, u32[]{:S(2)}) copy-start(f32[32,32]{1,0:T(8,128)} %pr_ref.1) | copy-start | bytes 12292
  60.3 3.4 %copy-start.23 = (f32[32,32]{1,0:T(8,128)S(1)}, f32[32,32]{1,0:T(8,128)}, u32[]{:S(2)}) copy-start(f32[32,32]{1,0:T(8,128)} %pi_ref.1) | copy-start | bytes 12292
  60.3 3.4 %copy-start.27 = (f32[512]{0:T(512)S(1)}, f32[512]{0:T(512)}, u32[]{:S(2)}) copy-start(f32[512]{0:T(512)} %param.19) | copy-start | bytes 6148
  61.1 19.8 %collective-permute-start.6 = (bf16[512,512]{1,0:T(8,128)(2,1)S(1)}, bf16[512,512]{1,0:T(8,128)(2,1)}, u32[]{:S(2)}, u32[]{:S(2)}) collective-permute-start(bf16[512,512]{1,0:T(8,128)(2,1)S(1)} %bitcast.35), channel_id=1, source_target_pairs={{0,1},{1,0},{2,3},{3,2},{4,5},{5,4},{6,7},{7,6},{8,9},{9,8},{10,11... | collective-permute-start | bytes 1572872 | tf_op jit(solution)/shard_map/ppermute | solution.py:356
  62.2 18.7 %collective-permute-start.8 = (bf16[1,512,512]{2,1,0:T(8,128)(2,1)}, bf16[1,512,512]{2,1,0:T(8,128)(2,1)}, u32[]{:S(2)}, u32[]{:S(2)}) collective-permute-start(bf16[1,512,512]{2,1,0:T(8,128)(2,1)} %add_convert_fusion), channel_id=1, source_target_pairs={{0,2},{1,3},{2,0},{3,1},{4,6},{5,7},{6,4},{7,5},{8,10},{9,11},{10,... | collective-permute-start | bytes 1572872 | tf_op jit(solution)/shard_map/ppermute | solution.py:356
  69.6 1.0 copy-start.8
  70.6 1.0 copy-start.10
  71.6 1.0 copy-start.12
  72.6 1.0 copy-start.14
  73.6 11.7 %all-to-all-start = ((f32[8,4,1024]{2,1,0:T(4,128)}), f32[8,4,1024]{2,1,0:T(4,128)S(1)}, u32[]{:S(2)}, u32[]{:S(2)}) async-start(f32[8,4,1024]{2,1,0:T(4,128)} %get-tuple-element.11), calls=%async_computation | async-start | bytes 262144 | tf_op jit(solution)/shard_map/all_to_all | solution.py:415
  77.9 2.2 %copy-start.1 = (bf16[1,1024,2048]{2,1,0:T(8,128)(2,1)S(1)}, bf16[1,1024,2048]{2,1,0:T(8,128)(2,1)}, u32[]{:S(2)}) copy-start(bf16[1,1024,2048]{2,1,0:T(8,128)(2,1)} %weight_ref.5) | copy-start | bytes 12582916
  80.1 9.1 %copy-start.18 = (f32[32,16,32]{2,1,0:T(8,128)S(1)}, f32[32,16,32]{2,1,0:T(8,128)}, u32[]{:S(2)}) copy-start(f32[32,16,32]{2,1,0:T(8,128)} %param.25) | copy-start | bytes 196612
  80.1 9.1 %copy-start.19 = (f32[32,16,32]{2,1,0:T(8,128)S(1)}, f32[32,16,32]{2,1,0:T(8,128)}, u32[]{:S(2)}) copy-start(f32[32,16,32]{2,1,0:T(8,128)} %param.26) | copy-start | bytes 196612
  80.8 23.5 %copy-start.25 = (s32[128,2]{0,1:T(2,128)S(1)}, s32[128,2]{0,1:T(2,128)}, u32[]{:S(2)}) copy-start(s32[128,2]{0,1:T(2,128)} %param.31) | copy-start | bytes 3076
  80.8 23.5 %copy-start.28 = (f32[128,2]{0,1:T(2,128)S(1)}, f32[128,2]{0,1:T(2,128)}, u32[]{:S(2)}) copy-start(f32[128,2]{0,1:T(2,128)} %param.32) | copy-start | bytes 3076
  80.9 25.0 %copy-start.4 = (bf16[2048,512]{1,0:T(8,128)(2,1)S(1)}, bf16[2048,512]{1,0:T(8,128)(2,1)}, u32[]{:S(2)}) copy-start(bf16[2048,512]{1,0:T(8,128)(2,1)} %refs_4_.2) | copy-start | bytes 6291460
  85.3 22.6 %all-to-all-start.2 = ((bf16[8,64,512]{2,1,0:T(8,128)(2,1)}), bf16[8,64,512]{2,1,0:T(8,128)(2,1)S(1)}, u32[]{:S(2)}, u32[]{:S(2)}) async-start(bf16[8,64,512]{2,1,0:T(8,128)(2,1)} %bitcast.49), calls=%async_computation.2 | async-start | bytes 1048576 | tf_op jit(solution)/shard_map/all_to_all | solution.py:487
  89.2 16.7 %copy-start.5 = (bf16[2048,512]{1,0:T(8,128)(2,1)S(1)}, bf16[2048,512]{1,0:T(8,128)(2,1)}, u32[]{:S(2)}) copy-start(bf16[2048,512]{1,0:T(8,128)(2,1)} %refs_5_.2) | copy-start | bytes 6291460
  89.2 1.4 %copy-start.9 = (f32[256,1024]{1,0:T(8,128)S(1)}, f32[256,1024]{1,0:T(8,128)}, u32[]{:S(2)}) copy-start(f32[256,1024]{1,0:T(8,128)} %copy-done.8) | copy-start | bytes 3145732
  90.6 1.2 %copy-start.11 = (f32[256,1024]{1,0:T(8,128)S(1)}, f32[256,1024]{1,0:T(8,128)}, u32[]{:S(2)}) copy-start(f32[256,1024]{1,0:T(8,128)} %copy-done.10) | copy-start | bytes 3145732
  91.8 1.2 %copy-start.13 = (f32[256,1024]{1,0:T(8,128)S(1)}, f32[256,1024]{1,0:T(8,128)}, u32[]{:S(2)}) copy-start(f32[256,1024]{1,0:T(8,128)} %copy-done.12) | copy-start | bytes 3145732
  93.1 1.2 %copy-start.15 = (f32[256,1024]{1,0:T(8,128)S(1)}, f32[256,1024]{1,0:T(8,128)}, u32[]{:S(2)}) copy-start(f32[256,1024]{1,0:T(8,128)} %copy-done.14) | copy-start | bytes 3145732
  96.8 7.5 %collective-permute-start.1 = (bf16[256,512]{1,0:T(8,128)(2,1)S(1)}, bf16[256,512]{1,0:T(8,128)(2,1)S(1)}, u32[]{:S(2)}, u32[]{:S(2)}) collective-permute-start(bf16[256,512]{1,0:T(8,128)(2,1)S(1)} %mixer_read.1.refs_0_), channel_id=1, source_target_pairs={{0,2},{1,3},{2,0},{3,1},{4,6},{5,7},{6,4},{7,5},{8,10},{9,11},{10,... | collective-permute-start | bytes 786440 | tf_op jit(solution)/shard_map/ppermute | solution.py:356
  97.4 7.4 %collective-permute-start = (bf16[256,512]{1,0:T(8,128)(2,1)S(1)}, bf16[256,512]{1,0:T(8,128)(2,1)S(1)}, u32[]{:S(2)}, u32[]{:S(2)}) collective-permute-start(bf16[256,512]{1,0:T(8,128)(2,1)S(1)} %mixer_read.1.refs_0_), channel_id=1, source_target_pairs={{0,1},{1,0},{2,3},{3,2},{4,5},{5,4},{6,7},{7,6},{8,9},{9,8},{10,11... | collective-permute-start | bytes 786440 | tf_op jit(solution)/shard_map/ppermute | solution.py:356
  104.3 1.5 %collective-permute-start.2 = (bf16[256,512]{1,0:T(8,128)(2,1)S(1)}, bf16[256,512]{1,0:T(8,128)(2,1)S(1)}, u32[]{:S(2)}, u32[]{:S(2)}) collective-permute-start(bf16[256,512]{1,0:T(8,128)(2,1)S(1)} %collective-permute-done.1.refs_2_), channel_id=1, source_target_pairs={{0,1},{1,0},{2,3},{3,2},{4,5},{5,4},{6,7},{7,6},{8,9},{9,8},{10,11... | collective-permute-start | bytes 786440 | tf_op jit(solution)/shard_map/ppermute | solution.py:356
where the time goes:
time: 110 us; the launch traced here: 109 us
  blocking collectives  26.8 us (24%)
  Pallas kernels  23.2 us (21%)
  waiting for transfers between devices  21.1 us (19%)
  local copies, waits for them, and re-layouts  21 us (19%)
  starting transfers between devices  12.6 us (11%)
  other arithmetic  3.25 us (3%)
    all_to_all x1, blocking collectives, shards(): lax.all_to_all(send, 'ep', split_axis=0, concat_axis=0, tiled=True)  21.6 us
    unnamed x59, local copies, waits for them, and re-layouts  21 us
    ppermute x9, waiting for transfers between devices, swap(): return lax.ppermute(value, 'tp', [(i, i ^ bit) for i in range(count)])  19.1 us
    pallas_call x1, Pallas kernels, shards(): pl.pallas_call(functools.partial(hidden_kernel, n_tp, n_unit), grid_spec=...  8.62 us
    pallas_call x1, Pallas kernels, shards(): pl.pallas_call(functools.partial(scan_kernel, float(chans * n_tp)), out_s...  5.82 us
    all_gather x1, blocking collectives, shards(): packed = lax.all_gather(packed, 'tp', axis=0, tiled=True)  5.22 us
    all_to_all x1, starting transfers between devices, shards(): got = lax.all_to_all(ends, 'ep', split_axis=0, concat_axis=0)  4.37 us
    ppermute x9, starting transfers between devices, swap(): return lax.ppermute(value, 'tp', [(i, i ^ bit) for i in range(count)])  4.27 us
  transfers between devices with their start and end apart: 11, of which 4 were waited for; matrix products, arithmetic and copies ran while one was open for 3% of the time, Pallas kernels for 12%

commit v1 on v0

--- a/solution.py
+++ b/solution.py
@@ -70,7 +70,16 @@
     out_ref[...] = mm(jnp.concatenate(chosen, axis=0), rows_ref[...]).astype(bf16)
 
 
-def share_kernel(experts, capacity, routes_ref, weight_ref, out_ref):
+def share_kernel(
+    experts, capacity, routes_ref, weight_ref, value_ref, gate_ref,
+    out_ref, value_out, gate_out, sems,
+):
+    copies = [
+        pltpu.make_async_copy(value_ref, value_out, sems.at[0]),
+        pltpu.make_async_copy(gate_ref, gate_out, sems.at[1]),
+    ]
+    for copy in copies:
+        copy.start()
     routes_t = routes_ref[...]
     weight_t = weight_ref[...]
     keys = slot_keys(routes_t, experts)
@@ -86,6 +95,20 @@
     same = ones_where(iota((tokens, tokens), 0) == iota((tokens, tokens), 1))
     for n, term in enumerate(split3(jnp.concatenate(spread, axis=0))):
         out_ref[n] = mm(same, term, NT).astype(bf16)
+    for copy in copies:
+        copy.wait()
+
+
+def fetch_kernel(*refs):
+    count = (len(refs) - 1) // 2
+    sems = refs[-1]
+    copies = [
+        pltpu.make_async_copy(refs[n], refs[count + n], sems.at[n]) for n in range(count)
+    ]
+    for copy in copies:
+        copy.start()
+    for copy in copies:
+        copy.wait()
 
 
 def combine_kernel(share_ref, back_ref, out_ref):
@@ -94,59 +117,59 @@
     out_ref[...] = out.astype(bf16)
 
 
-def hidden_kernel(parts, blocks_of, me_ref, packed_ref, *refs):
+def hidden_kernel(parts, me_ref, packed_ref, *refs):
     blocks = refs[:parts]
     gate_ref, up_ref, down_ref, hidden_ref, far_ref, normed_ref = refs[parts:]
     rows, feats = blocks[0].shape
     width = parts * feats
     chunk = 64
-    step = pl.program_id(0)
-
-    @pl.when(step == 0)
-    def _():
-        me = me_ref[0]
-        lead = packed_ref.shape[1] - feats
-        number = iota((parts, feats), 0)
-        gains = [
-            jnp.sum(jnp.where(number == me ^ k, packed_ref[:, lead:], 0.0), axis=0, keepdims=True)
-            for k in range(parts)
-        ]
-
-        def body(step, unused):
-            at = pl.ds(pl.multiple_of(step * chunk, chunk), chunk)
-            total = jnp.zeros((chunk, 1), f32)
-            square = jnp.zeros((chunk, 1), f32)
-            for block in blocks:
-                wide = block[at, :].astype(f32)
-                total = total + jnp.sum(wide, axis=1, keepdims=True)
-                square = square + jnp.sum(wide * wide, axis=1, keepdims=True)
-            mean = total / width
-            scale = lax.rsqrt(square / width - mean * mean + norm_eps)
-            for k, block in enumerate(blocks):
-                which = me ^ k
-                value = (block[at, :].astype(f32) - mean) * scale * gains[k]
-                cols = pl.ds(pl.multiple_of(which * feats, feats), feats)
-                normed_ref[at, cols] = value.astype(bf16)
-            return unused
-
-        lax.fori_loop(0, rows // chunk, body, 0, unroll=2)
-
-    @pl.when(step < blocks_of)
-    def _():
+    me = me_ref[0]
+    lead = packed_ref.shape[1] - feats
+    number = iota((parts, feats), 0)
+    gains = [
+        jnp.sum(jnp.where(number == me ^ k, packed_ref[:, lead:], 0.0), axis=0, keepdims=True)
+        for k in range(parts)
+    ]
+
+    def body(step, unused):
+        at = pl.ds(pl.multiple_of(step * chunk, chunk), chunk)
+        total = jnp.zeros((chunk, 1), f32)
+        square = jnp.zeros((chunk, 1), f32)
+        for block in blocks:
+            wide = block[at, :].astype(f32)
+            total = total + jnp.sum(wide, axis=1, keepdims=True)
+            square = square + jnp.sum(wide * wide, axis=1, keepdims=True)
+        mean = total / width
+        scale = lax.rsqrt(square / width - mean * mean + norm_eps)
+        for k, block in enumerate(blocks):
+            value = (block[at, :].astype(f32) - mean) * scale * gains[k]
+            cols = pl.ds(pl.multiple_of((me ^ k) * feats, feats), feats)
+            normed_ref[at, cols] = value.astype(bf16)
+        return unused
+
+    lax.fori_loop(0, rows // chunk, body, 0, unroll=2)
+    units = gate_ref.shape[2]
+    size = min(units, 256)
+    for at in range(0, units, size):
+        cols = pl.ds(at, size)
         normed = normed_ref[...]
-        gate = mm(normed, gate_ref[0])
-        up = mm(normed, up_ref[0])
-        size = gate_ref.shape[2]
-        cols = pl.ds(pl.multiple_of(step * size, size), size)
+        gate = mm(normed, gate_ref[0, :, cols])
+        up = mm(normed, up_ref[0, :, cols])
         hidden_ref[:, cols] = (gate * jax.nn.sigmoid(gate) * up).astype(bf16)
-
-    @pl.when(step >= blocks_of)
-    def _():
-        far_ref[0] = mm(hidden_ref[...], down_ref[0]).astype(bf16)
-
-
-def down_kernel(me_ref, hidden_ref, weight_ref, out_ref):
-    out_ref[0] = mm(hidden_ref[...], weight_ref[0]).astype(bf16)
+    for n in range(far_ref.shape[0]):
+        far_ref[n] = down_part(me ^ (2 * n + 3), hidden_ref, down_ref, feats)
+
+
+def down_part(which, hidden_ref, weight_ref, feats):
+    cols = pl.ds(pl.multiple_of(which * feats, feats), feats)
+    return mm(hidden_ref[...], weight_ref[0, :, cols]).astype(bf16)
+
+
+def down_kernel(offsets, me_ref, hidden_ref, weight_ref, out_ref):
+    for n, offset in enumerate(offsets):
+        out_ref[n] = down_part(
+            me_ref[0] ^ offset, hidden_ref, weight_ref, out_ref.shape[2]
+        )
 
 
 def reorder(rows, back):
@@ -344,7 +367,12 @@
 
 
 vmem = pl.BlockSpec(memory_space=pltpu.VMEM)
+hbm = pl.BlockSpec(memory_space=pltpu.HBM)
 smem = pl.BlockSpec(memory_space=pltpu.SMEM)
+
+
+def stay(value):
+    return pltpu.with_memory_space_constraint(value, pltpu.HBM)
 
 
 def params(mib):
@@ -384,16 +412,18 @@
     send = pl.pallas_call(
         functools.partial(send_kernel, n_ep, capacity),
         out_shape=jax.ShapeDtypeStruct((slots, feats), bf16),
-        in_specs=[vmem, vmem], out_specs=vmem, compiler_params=params(8), name="send_rows",
+        in_specs=[vmem, vmem], out_specs=vmem, compiler_params=params(60), name="send_rows",
     )(routes_t, expert_input)
     arrived = lax.all_to_all(send, "ep", split_axis=0, concat_axis=0, tiled=True)
 
     rows, chans = mixer_input.shape
-    mixer_input, send = lax.optimization_barrier((mixer_input, send))
+    mixer_input, send, tp_at, ep_at = lax.optimization_barrier(
+        (mixer_input, send, tp_at, ep_at)
+    )
     packed = pl.pallas_call(
         sums_kernel,
         out_shape=jax.ShapeDtypeStruct((1, 2 * rows + feats), f32),
-        in_specs=[vmem, vmem], out_specs=vmem, compiler_params=params(8), name="mixer_sums",
+        in_specs=[vmem, vmem], out_specs=vmem, compiler_params=params(60), name="mixer_sums",
     )(mixer_input, expert_gain.reshape(1, feats))
     packed = lax.all_gather(packed, "tp", axis=0, tiled=True)
 
@@ -405,7 +435,7 @@
         out_shape=(big, big, big, big, jax.ShapeDtypeStruct((n_ep, 4, flat), f32)),
         in_specs=[vmem] * 8, out_specs=(vmem,) * 5,
         scratch_shapes=[pltpu.VMEM((rows, flat), f32)] * 2,
-        compiler_params=params(28), name="mixer_scan",
+        compiler_params=params(60), name="mixer_scan",
     )(
         mixer_input, packed, mixer_gain.reshape(1, chans), time_step.T,
         pole_real, pole_imag,
@@ -415,68 +445,39 @@
     got = lax.all_to_all(ends, "ep", split_axis=0, concat_axis=0)
 
     blocks = gather_tp(arrived)
-    share = pl.pallas_call(
-        functools.partial(share_kernel, n_ep, capacity),
-        out_shape=jax.ShapeDtypeStruct((3, tokens, slots), bf16),
-        in_specs=[vmem, vmem], out_specs=vmem, compiler_params=params(8), name="route_share",
-    )(routes_t, weight_t)
+    weights = tuple(stay(w) for w in (expert_gate, expert_up, expert_down))
+    gate_w, up_w, down_w = pl.pallas_call(
+        fetch_kernel,
+        out_shape=tuple(jax.ShapeDtypeStruct(w.shape, w.dtype) for w in weights),
+        in_specs=[hbm] * 3, out_specs=(vmem,) * 3,
+        scratch_shapes=[pltpu.SemaphoreType.DMA((3,))],
+        compiler_params=params(16), name="expert_fetch",
+    )(*weights)
     units = expert_gate.shape[2]
-    unit_block = min(units, 256)
-    n_unit = units // unit_block
     n_far = n_tp // 2 - 1
     hidden, odd_far = pl.pallas_call(
-        functools.partial(hidden_kernel, n_tp, n_unit),
-        grid_spec=pltpu.PrefetchScalarGridSpec(
-            num_scalar_prefetch=1,
-            grid=(n_unit + n_far,),
-            in_specs=[vmem] * (n_tp + 1) + [
-                pl.BlockSpec(
-                    (1, n_tp * feats, unit_block),
-                    lambda j, me: (0, 0, jnp.minimum(j, n_unit - 1)),
-                ),
-                pl.BlockSpec(
-                    (1, n_tp * feats, unit_block),
-                    lambda j, me: (0, 0, jnp.minimum(j, n_unit - 1)),
-                ),
-                pl.BlockSpec(
-                    (1, units, feats),
-                    lambda j, me: (0, 0, me[0] ^ (2 * jnp.maximum(j - n_unit, 0) + 3)),
-                ),
-            ],
-            out_specs=(
-                pl.BlockSpec((slots, units), lambda j, me: (0, 0)),
-                pl.BlockSpec(
-                    (1, slots, feats), lambda j, me: (jnp.maximum(j - n_unit, 0), 0, 0)
-                ),
-            ),
-            scratch_shapes=[pltpu.VMEM((slots, n_tp * feats), bf16)],
-        ),
+        functools.partial(hidden_kernel, n_tp),
+        in_specs=[smem] + [vmem] * (n_tp + 4), out_specs=(vmem, vmem),
+        scratch_shapes=[pltpu.VMEM((slots, n_tp * feats), bf16)],
         out_shape=(
             jax.ShapeDtypeStruct((slots, units), bf16),
             jax.ShapeDtypeStruct((n_far, slots, feats), bf16),
         ),
-        compiler_params=params(28), name="expert_hidden",
-    )(tp_at, packed, *blocks, expert_gate, expert_up, expert_down)
-
-    def down(count, offset):
+        compiler_params=params(16), name="expert_hidden",
+    )(tp_at, packed, *blocks, gate_w, up_w, down_w)
+
+    def down(offsets):
         return pl.pallas_call(
-            down_kernel,
-            grid_spec=pltpu.PrefetchScalarGridSpec(
-                num_scalar_prefetch=1,
-                grid=(count,),
-                in_specs=[
-                    pl.BlockSpec((slots, units), lambda i, me: (0, 0)),
-                    pl.BlockSpec((1, units, feats), lambda i, me: (0, 0, me[0] ^ offset(i))),
-                ],
-                out_specs=pl.BlockSpec((1, slots, feats), lambda i, me: (i, 0, 0)),
-            ),
-            out_shape=jax.ShapeDtypeStruct((count, slots, feats), bf16),
+            functools.partial(down_kernel, offsets),
+            in_specs=[smem, vmem, vmem], out_specs=vmem,
+            out_shape=jax.ShapeDtypeStruct((len(offsets), slots, feats), bf16),
             compiler_params=params(10),
-        )(tp_at, hidden, expert_down)
+        )(tp_at, hidden, down_w)
 
     theirs = swap(odd_far, 1)
-    far = down(n_far, lambda i: 2 * i + 2).astype(f32) + theirs.astype(f32)
-    parts = [swap(down(1, lambda i: i + 1)[0], 1), down(1, lambda i: i)[0]]
+    even_far = down(tuple(range(2, n_tp, 2)))
+    far = even_far.astype(f32) + theirs.astype(f32)
+    parts = [swap(down((1,))[0], 1), down((0,))[0]]
     bit = n_tp // 4
     while bit >= 1:
         come = swap(far[bit - 1 :].astype(bf16), 2 * bit).astype(f32)
@@ -489,19 +490,30 @@
     mixed = pl.pallas_call(
         read_kernel,
         out_shape=jax.ShapeDtypeStruct((rows, chans), bf16),
-        in_specs=[smem] + [vmem] * 7, out_specs=vmem, compiler_params=params(28),
+        in_specs=[smem] + [vmem] * 7, out_specs=vmem, compiler_params=params(60),
         name="mixer_read",
     )(
         ep_at, got, h_re, h_im, c_re, c_im,
         read_real.reshape(chans, states), read_imag.reshape(chans, states),
     )
     pieces = gather_tp(mixed)
+    share, value_w, gate_w = pl.pallas_call(
+        functools.partial(share_kernel, n_ep, capacity),
+        out_shape=(
+            jax.ShapeDtypeStruct((3, tokens, slots), bf16),
+            jax.ShapeDtypeStruct(out_value.shape, bf16),
+            jax.ShapeDtypeStruct(out_gate.shape, bf16),
+        ),
+        in_specs=[vmem, vmem, hbm, hbm], out_specs=(vmem,) * 3,
+        scratch_shapes=[pltpu.SemaphoreType.DMA((2,))],
+        compiler_params=params(10), name="out_fetch",
+    )(routes_t, weight_t, stay(out_value), stay(out_gate))
     mixer_output = pl.pallas_call(
         functools.partial(output_kernel, n_tp),
         out_shape=jax.ShapeDtypeStruct((rows, out_value.shape[1]), bf16),
-        in_specs=[smem] + [vmem] * (n_tp + 2), out_specs=vmem, compiler_params=params(20),
+        in_specs=[smem] + [vmem] * (n_tp + 2), out_specs=vmem, compiler_params=params(10),
         name="mixer_out",
-    )(tp_at, *pieces, out_value, out_gate)
+    )(tp_at, *pieces, value_w, gate_w)
     expert_output = pl.pallas_call(
         combine_kernel,
         out_shape=jax.ShapeDtypeStruct((tokens, feats), bf16),

time: 110 us -> 102 us (0.927)
  local copies, waits for them, and re-layouts: 21 us -> 2.22 us
  Pallas kernels: 23.2 us -> 36.4 us
    unnamed x59 -> x15, local copies, waits for them, and re-layouts: 21 us -> 2.22 us
    pallas_call x1, Pallas kernels: 2.52 us -> 5.55 us  [shards(): pl.pallas_call(read_kernel, out_shape=jax.ShapeDtypeStruct((rows, chans),...]
    pallas_call x4 -> x5, Pallas kernels: 10.7 us -> 13.4 us  [the longest x1 6.54 us: shards(): pl.pallas_call(functools.partial(hidden_kernel, n_tp), in_specs=[smem] +...]
    pallas_call x1, Pallas kernels: 5.82 us -> 8.27 us  [shards(): pl.pallas_call(functools.partial(scan_kernel, float(chans * n_tp)), out_s...]
    pallas_call x1, Pallas kernels: 0.41 us -> 2.24 us  [shards(): pl.pallas_call(functools.partial(share_kernel, n_ep, capacity), out_shape...]
    pallas_call x1, Pallas kernels: 0.4 us -> 2.13 us  [shards(): pl.pallas_call(functools.partial(send_kernel, n_ep, capacity), out_shape=...]
    pallas_call x1, Pallas kernels: 0.3 us -> 1.87 us  [shards(): pl.pallas_call(sums_kernel, out_shape=jax.ShapeDtypeStruct((1, 2 * rows +...]
  transfers between devices with their start and end apart: 11 -> 11, of which waited for: 4 -> 3; matrix products, arithmetic and copies ran while one was open for 3% -> 2% of each run, Pallas kernels for 12% -> 26%
where the time goes in v1:
time: 102 us
  Pallas kernels  36.4 us (36%)
  blocking collectives  27.1 us (27%)
  waiting for transfers between devices  20.5 us (20%)
  starting transfers between devices  12.3 us (12%)
  local copies, waits for them, and re-layouts  2.22 us (2%)
  other arithmetic  2.18 us (2%)
    all_to_all x1, blocking collectives, shards(): lax.all_to_all(send, 'ep', split_axis=0, concat_axis=0, tiled=True)  21.8 us
    ppermute x9, waiting for transfers between devices, swap(): return lax.ppermute(value, 'tp', [(i, i ^ bit) for i in range(count)])  18.1 us
    pallas_call x1, Pallas kernels, shards(): pl.pallas_call(functools.partial(scan_kernel, float(chans * n_tp)), out_s...  8.27 us
    pallas_call x1, Pallas kernels, shards(): pl.pallas_call(functools.partial(hidden_kernel, n_tp), in_specs=[smem] +...  6.54 us
    pallas_call x1, Pallas kernels, shards(): pl.pallas_call(read_kernel, out_shape=jax.ShapeDtypeStruct((rows, chans),...  5.55 us
    all_gather x1, blocking collectives, shards(): packed = lax.all_gather(packed, 'tp', axis=0, tiled=True)  5.32 us
    pallas_call x1, Pallas kernels, shards(): pl.pallas_call(fetch_kernel, out_shape=tuple((jax.ShapeDtypeStruct(w.shap...  4.69 us
    all_to_all x1, starting transfers between devices, shards(): got = lax.all_to_all(ends, 'ep', split_axis=0, concat_axis=0)  4.37 us
  transfers between devices with their start and end apart: 11, of which 3 were waited for; matrix products, arithmetic and copies ran while one was open for 2% of the time, Pallas kernels for 26%

profile of v1, /device:TPU:0, one launch (start us, length us, event | category | flops | bytes accessed | tf_op | source)
XLA Modules:
  0.0 101.6 jit_solution(13871684719384974644)
XLA Ops:
  0.6 2.1 %send_rows.1 = bf16[512,512]{1,0:T(8,128)(2,1)} custom-call(s32[2,128]{1,0:T(2,128)} %bitcast.37, bf16[128,512]{1,0:T(8,128)(2,1)} %rows_ref.1), custom_call_target="tpu_custom_call" | custom-call | tf_op jit(solution)/shard_map/send_rows/pallas_call | solution.py:412
  2.8 21.8 %all_to_all.27 = bf16[8,64,512]{2,1,0:T(8,128)(2,1)S(1)} all-to-all(bf16[8,64,512]{2,1,0:T(8,128)(2,1)} %bitcast.40), channel_id=1, replica_groups=mesh['ep'=8,'tp'=4] {'ep'}, dimensions={0} | all-to-all | bytes 1048576 | tf_op jit(solution)/shard_map/all_to_all | solution.py:417
  24.6 1.5 %collective-permute-start.4 = (bf16[512,512]{1,0:T(8,128)(2,1)S(1)}, bf16[512,512]{1,0:T(8,128)(2,1)S(1)}, u32[]{:S(2)}, u32[]{:S(2)}) collective-permute-start(bf16[512,512]{1,0:T(8,128)(2,1)S(1)} %bitcast.30), channel_id=1, source_target_pairs={{0,2},{1,3},{2,0},{3,1},{4,6},{5,7},{6,4},{7,5},{8,10},{9,11},{10,... | collective-permute-start | bytes 1572872 | tf_op jit(solution)/shard_map/ppermute | solution.py:384
  26.1 0.0 collective-permute-start.3
  26.1 11.0 %collective-permute-done.4.refs_2_ = bf16[512,512]{1,0:T(8,128)(2,1)S(1)} collective-permute-done((bf16[512,512]{1,0:T(8,128)(2,1)S(1)}, bf16[512,512]{1,0:T(8,128)(2,1)S(1)}, u32[]{:S(2)}, u32[]{:S(2)}) %collective-permute-start.4) | collective-permute-done | bytes 524320 | tf_op jit(solution)/shard_map/ppermute | solution.py:384
  37.1 0.0 collective-permute-start.5
  37.1 1.9 %mixer_sums.1 = f32[1,1024]{1,0:T(1,128)} custom-call(bf16[256,512]{1,0:T(8,128)(2,1)} %x_ref.1, f32[1,512]{1,0:T(1,128)} %bitcast.47), custom_call_target="tpu_custom_call" | custom-call | tf_op jit(solution)/shard_map/mixer_sums/pallas_call | solution.py:423
  39.0 5.3 %all-gather = f32[4,1,1024]{2,1,0:T(1,128)S(1)} all-gather(f32[1,1,1024]{2,1,0:T(1,128)} %bitcast.46), channel_id=1, replica_groups=mesh['ep'=8,'tp'=4] {'tp'}, dimensions={0}, use_global_device_ids=true | all-gather | bytes 20480 | tf_op jit(solution)/shard_map/all_gather | solution.py:428
  44.3 0.0 copy-start.3
  44.3 4.7 %expert_fetch.1 = (bf16[1,2048,1024]{2,1,0:T(8,128)(2,1)S(1)}, bf16[1,2048,1024]{2,1,0:T(8,128)(2,1)S(1)}, bf16[1,1024,2048]{2,1,0:T(8,128)(2,1)S(1)}) custom-call(bf16[1,2048,1024]{2,1,0:T(8,128)(2,1)} %refs_0_.1, bf16[1,2048,1024]{2,1,0:T(8,128)(2,1)} %refs_1_.1, bf16[1,1024,2048]{2,1,0:T(8,128)(2,1)} %refs_2_.1), custom_call_target="tpu_custom_call" | custom-call | tf_op jit(solution)/shard_map/expert_fetch/pallas_call | solution.py:449
  49.0 0.0 copy-start
  49.0 0.0 collective-permute-done.3.refs_1_
  49.0 0.0 collective-permute-done.5.refs_3_
  49.0 0.0 copy-done.3
  49.1 6.5 %expert_hidden.1 = (bf16[512,1024]{1,0:T(8,128)(2,1)S(1)}, bf16[1,512,512]{2,1,0:T(8,128)(2,1)S(1)}) custom-call(s32[1]{0:T(128)} %bitcast.1.me_ref, f32[4,1024]{1,0:T(4,128)S(1)} %bitcast.35, bf16[512,512]{1,0:T(8,128)(2,1)S(1)} %bitcast.32, bf16[512,512]{1,0:T(8,128)(2,1)S(1)} %collective-permute-done.3.refs_1_, ...), custom_call_target="tpu_custom_call" | custom-call | tf_op jit(solution)/shard_map/expert_hidden/pallas_call | solution.py:458
  55.6 0.4 collective-permute-start.7
  56.0 0.7 shard_map.187
  56.7 0.0 copy-done
  56.7 0.7 shard_map.185
  57.5 0.2 collective-permute-start.6
  57.7 0.0 collective-permute-done.7
  57.7 0.1 add_convert_fusion
  57.8 1.6 %collective-permute-start.8 = (bf16[1,512,512]{2,1,0:T(8,128)(2,1)S(1)}, bf16[1,512,512]{2,1,0:T(8,128)(2,1)}, u32[]{:S(2)}, u32[]{:S(2)}) collective-permute-start(bf16[1,512,512]{2,1,0:T(8,128)(2,1)S(1)} %add_convert_fusion), channel_id=1, source_target_pairs={{0,2},{1,3},{2,0},{3,1},{4,6},{5,7},{6,4},{7,5},{8,10},{9,11},{10,... | collective-permute-start | bytes 1572872 | tf_op jit(solution)/shard_map/ppermute | solution.py:384
  59.4 8.3 %mixer_scan.1 = (f32[256,1024]{1,0:T(8,128)}, f32[256,1024]{1,0:T(8,128)}, f32[256,1024]{1,0:T(8,128)}, f32[256,1024]{1,0:T(8,128)}, f32[8,4,1024]{2,1,0:T(4,128)}) custom-call(bf16[256,512]{1,0:T(8,128)(2,1)} %x_ref.1, f32[4,1024]{1,0:T(4,128)} %bitcast.36, f32[1,512]{1,0:T(1,128)} %bitcast.48, f32[32,256]{1,0:T(8,128)} %bitcast.45, f32[32,32]{1,0:T(8,128)} %pr_ref.1, ...), custom_call_target="tpu_custom_call" | custom-call | tf_op jit(solution)/shard_map/mixer_scan/pallas_call | solution.py:433
  67.7 4.4 %all-to-all-start = ((f32[8,4,1024]{2,1,0:T(4,128)}), f32[8,4,1024]{2,1,0:T(4,128)S(1)}, u32[]{:S(2)}, u32[]{:S(2)}) async-start(f32[8,4,1024]{2,1,0:T(4,128)} %get-tuple-element.21), calls=%async_computation | async-start | bytes 262144 | tf_op jit(solution)/shard_map/all_to_all | solution.py:445
  72.1 0.0 copy-start.1
  72.1 2.2 %copy-done.1 = bf16[1,1024,2048]{2,1,0:T(8,128)(2,1)S(1)} copy-done((bf16[1,1024,2048]{2,1,0:T(8,128)(2,1)S(1)}, bf16[1,1024,2048]{2,1,0:T(8,128)(2,1)}, u32[]{:S(2)}) %copy-start.1) | copy-done | bytes 4194328
  74.2 0.7 shard_map.186
  75.0 0.0 copy-start.4
  75.0 0.0 copy-start.5
  75.0 0.0 collective-permute-done.6
  75.0 0.0 collective-permute-done.8
  75.0 2.0 %fusion = bf16[512,512]{1,0:T(8,128)(2,1)} fusion(bf16[512,512]{1,0:T(8,128)(2,1)S(1)} %collective-permute-done.6, bf16[1,512,512]{2,1,0:T(8,128)(2,1)} %collective-permute-done.8, bf16[1,512,512]{2,1,0:T(8,128)(2,1)S(1)} %shard_map.186), kind=kLoop, calls=%fused_computation.1 | loop fusion | flops 1572864 | bytes 2097152 | tf_op jit(solution)/shard_map/convert_element_type | solution.py:487
  77.1 2.4 %all-to-all-done.got_ref = f32[8,4,1024]{2,1,0:T(4,128)S(1)} async-done(((f32[8,4,1024]{2,1,0:T(4,128)}), f32[8,4,1024]{2,1,0:T(4,128)S(1)}, u32[]{:S(2)}, u32[]{:S(2)}) %all-to-all-start) | async-done | bytes 131104 | tf_op jit(solution)/shard_map/all_to_all | solution.py:445
  79.4 0.0 copy-start.6
  79.4 3.7 %all-to-all-start.2 = ((bf16[8,64,512]{2,1,0:T(8,128)(2,1)}), bf16[8,64,512]{2,1,0:T(8,128)(2,1)S(1)}, u32[]{:S(2)}, u32[]{:S(2)}) async-start(bf16[8,64,512]{2,1,0:T(8,128)(2,1)} %bitcast.19), calls=%async_computation.2 | async-start | bytes 1048576 | tf_op jit(solution)/shard_map/all_to_all | solution.py:488
  83.1 0.0 copy-done.6
  83.1 5.5 %mixer_read.1.refs_0_ = bf16[256,512]{1,0:T(8,128)(2,1)} custom-call(s32[1]{0:T(128)} %bitcast.2.me_ref, f32[8,4,1024]{2,1,0:T(4,128)} %copy-done.6, f32[256,1024]{1,0:T(8,128)} %get-tuple-element.22.hr_ref, f32[256,1024]{1,0:T(8,128)} %get-tuple-element.23.hi_ref, f32[256,1024]{1,0:T(8,128)} %get-tuple-element.24.cr_ref, ...), custom_call_target="tpu_custom_call" | custom-call | tf_op jit(solution)/shard_map/mixer_read/pallas_call | solution.py:490
  88.6 0.0 copy-start.2
  88.7 0.5 collective-permute-start.1
  89.2 0.0 collective-permute-start
  89.2 7.1 %collective-permute-done.1.refs_2_ = bf16[256,512]{1,0:T(8,128)(2,1)S(1)} collective-permute-done((bf16[256,512]{1,0:T(8,128)(2,1)}, bf16[256,512]{1,0:T(8,128)(2,1)S(1)}, u32[]{:S(2)}, u32[]{:S(2)}) %collective-permute-start.1) | collective-permute-done | bytes 262176 | tf_op jit(solution)/shard_map/ppermute | solution.py:384
  96.3 0.0 collective-permute-start.2
  96.3 0.0 copy-done.4
  96.3 0.0 copy-done.5
  96.3 2.2 %out_fetch.1 = (bf16[3,128,512]{2,1,0:T(8,128)(2,1)S(1)}, bf16[2048,512]{1,0:T(8,128)(2,1)S(1)}, bf16[2048,512]{1,0:T(8,128)(2,1)S(1)}) custom-call(s32[2,128]{1,0:T(2,128)S(1)} %bitcast.38, f32[2,128]{1,0:T(2,128)S(1)} %bitcast.39, bf16[2048,512]{1,0:T(8,128)(2,1)} %value_ref.1, bf16[2048,512]{1,0:T(8,128)(2,1)} %gate_ref.1), custom_call_target="tpu_custom_call" | custom-call | tf_op jit(solution)/shard_map/out_fetch/pallas_call | solution.py:500
  98.5 0.0 collective-permute-done.refs_1_
  98.5 0.0 collective-permute-done.2.refs_3_
  98.5 0.0 copy-done.2
  98.6 2.0 %mixer_out.1 = bf16[256,512]{1,0:T(8,128)(2,1)} custom-call(s32[1]{0:T(128)} %bitcast.1.me_ref, bf16[256,512]{1,0:T(8,128)(2,1)S(1)} %copy-done.2, bf16[256,512]{1,0:T(8,128)(2,1)S(1)} %collective-permute-done.refs_1_, bf16[256,512]{1,0:T(8,128)(2,1)S(1)} %collective-permute-done.1.refs_2_, bf16[256,512]{1,0:T(8,128)(2,1)S(1)} %collective-permute-done.2.refs_3_, ...), custom_call_target="tpu_custom_call" | custom-call | tf_op jit(solution)/shard_map/mixer_out/pallas_call | solution.py:511
  100.5 0.0 all-to-all-done.2
  100.5 1.0 %combine.1 = bf16[128,512]{1,0:T(8,128)(2,1)} custom-call(bf16[3,128,512]{2,1,0:T(8,128)(2,1)S(1)} %get-tuple-element.28.share_ref, bf16[512,512]{1,0:T(8,128)(2,1)S(1)} %bitcast.33), custom_call_target="tpu_custom_call" | custom-call | tf_op jit(solution)/shard_map/combine/pallas_call | solution.py:517
  (1 shorter events, 0.0 us)
Async XLA Ops:
  24.6 12.5 %collective-permute-start.4 = (bf16[512,512]{1,0:T(8,128)(2,1)S(1)}, bf16[512,512]{1,0:T(8,128)(2,1)S(1)}, u32[]{:S(2)}, u32[]{:S(2)}) collective-permute-start(bf16[512,512]{1,0:T(8,128)(2,1)S(1)} %bitcast.30), channel_id=1, source_target_pairs={{0,2},{1,3},{2,0},{3,1},{4,6},{5,7},{6,4},{7,5},{8,10},{9,11},{10,... | collective-permute-start | bytes 1572872 | tf_op jit(solution)/shard_map/ppermute | solution.py:384
  26.1 22.9 %collective-permute-start.3 = (bf16[512,512]{1,0:T(8,128)(2,1)S(1)}, bf16[512,512]{1,0:T(8,128)(2,1)S(1)}, u32[]{:S(2)}, u32[]{:S(2)}) collective-permute-start(bf16[512,512]{1,0:T(8,128)(2,1)S(1)} %bitcast.31), channel_id=1, source_target_pairs={{0,1},{1,0},{2,3},{3,2},{4,5},{5,4},{6,7},{7,6},{8,9},{9,8},{10,11... | collective-permute-start | bytes 1572872 | tf_op jit(solution)/shard_map/ppermute | solution.py:384
  37.1 11.9 %collective-permute-start.5 = (bf16[512,512]{1,0:T(8,128)(2,1)S(1)}, bf16[512,512]{1,0:T(8,128)(2,1)S(1)}, u32[]{:S(2)}, u32[]{:S(2)}) collective-permute-start(bf16[512,512]{1,0:T(8,128)(2,1)S(1)} %collective-permute-done.4.refs_2_), channel_id=1, source_target_pairs={{0,1},{1,0},{2,3},{3,2},{4,5},{5,4},{6,7},{7,6},{8,9},{9,8},{10,11... | collective-permute-start | bytes 1572872 | tf_op jit(solution)/shard_map/ppermute | solution.py:384
  44.3 4.7 %copy-start.3 = (f32[4,1,1024]{2,0,1:T(4,128)}, f32[4,1,1024]{2,0,1:T(4,128)S(1)}, u32[]{:S(2)}) copy-start(f32[4,1,1024]{2,0,1:T(4,128)S(1)} %copy.22) | copy-start | bytes 49156
  49.0 7.7 %copy-start = (bf16[1,1024,2048]{2,1,0:T(8,128)(2,1)}, bf16[1,1024,2048]{2,1,0:T(8,128)(2,1)S(1)}, u32[]{:S(2)}) copy-start(bf16[1,1024,2048]{2,1,0:T(8,128)(2,1)S(1)} %get-tuple-element.31.refs_6_.weight_ref) | copy-start | bytes 12582916
  55.6 2.1 %collective-permute-start.7 = (bf16[1,512,512]{2,1,0:T(8,128)(2,1)S(1)}, bf16[1,512,512]{2,1,0:T(8,128)(2,1)S(1)}, u32[]{:S(2)}, u32[]{:S(2)}) collective-permute-start(bf16[1,512,512]{2,1,0:T(8,128)(2,1)S(1)} %get-tuple-element.33), channel_id=1, source_target_pairs={{0,1},{1,0},{2,3},{3,2},{4,5},{5,4},{6,7},{7,6},{8,9},{9,8},{10,11... | collective-permute-start | bytes 1572872 | tf_op jit(solution)/shard_map/ppermute | solution.py:384
  57.5 17.5 %collective-permute-start.6 = (bf16[512,512]{1,0:T(8,128)(2,1)S(1)}, bf16[512,512]{1,0:T(8,128)(2,1)S(1)}, u32[]{:S(2)}, u32[]{:S(2)}) collective-permute-start(bf16[512,512]{1,0:T(8,128)(2,1)S(1)} %bitcast.34), channel_id=1, source_target_pairs={{0,1},{1,0},{2,3},{3,2},{4,5},{5,4},{6,7},{7,6},{8,9},{9,8},{10,11... | collective-permute-start | bytes 1572872 | tf_op jit(solution)/shard_map/ppermute | solution.py:384
  57.8 17.2 %collective-permute-start.8 = (bf16[1,512,512]{2,1,0:T(8,128)(2,1)S(1)}, bf16[1,512,512]{2,1,0:T(8,128)(2,1)}, u32[]{:S(2)}, u32[]{:S(2)}) collective-permute-start(bf16[1,512,512]{2,1,0:T(8,128)(2,1)S(1)} %add_convert_fusion), channel_id=1, source_target_pairs={{0,2},{1,3},{2,0},{3,1},{4,6},{5,7},{6,4},{7,5},{8,10},{9,11},{10,... | collective-permute-start | bytes 1572872 | tf_op jit(solution)/shard_map/ppermute | solution.py:384
  67.7 11.7 %all-to-all-start = ((f32[8,4,1024]{2,1,0:T(4,128)}), f32[8,4,1024]{2,1,0:T(4,128)S(1)}, u32[]{:S(2)}, u32[]{:S(2)}) async-start(f32[8,4,1024]{2,1,0:T(4,128)} %get-tuple-element.21), calls=%async_computation | async-start | bytes 262144 | tf_op jit(solution)/shard_map/all_to_all | solution.py:445
  72.1 2.2 %copy-start.1 = (bf16[1,1024,2048]{2,1,0:T(8,128)(2,1)S(1)}, bf16[1,1024,2048]{2,1,0:T(8,128)(2,1)}, u32[]{:S(2)}) copy-start(bf16[1,1024,2048]{2,1,0:T(8,128)(2,1)} %copy-done) | copy-start | bytes 12582916
  75.0 21.3 %copy-start.4 = (s32[128,2]{0,1:T(2,128)S(1)}, s32[128,2]{0,1:T(2,128)}, u32[]{:S(2)}) copy-start(s32[128,2]{0,1:T(2,128)} %param.31) | copy-start | bytes 3076
  75.0 21.3 %copy-start.5 = (f32[128,2]{0,1:T(2,128)S(1)}, f32[128,2]{0,1:T(2,128)}, u32[]{:S(2)}) copy-start(f32[128,2]{0,1:T(2,128)} %param.32) | copy-start | bytes 3076
  79.4 3.7 %copy-start.6 = (f32[8,4,1024]{2,1,0:T(4,128)}, f32[8,4,1024]{2,1,0:T(4,128)S(1)}, u32[]{:S(2)}) copy-start(f32[8,4,1024]{2,1,0:T(4,128)S(1)} %all-to-all-done.got_ref) | copy-start | bytes 393220
  79.4 21.1 %all-to-all-start.2 = ((bf16[8,64,512]{2,1,0:T(8,128)(2,1)}), bf16[8,64,512]{2,1,0:T(8,128)(2,1)S(1)}, u32[]{:S(2)}, u32[]{:S(2)}) async-start(bf16[8,64,512]{2,1,0:T(8,128)(2,1)} %bitcast.19), calls=%async_computation.2 | async-start | bytes 1048576 | tf_op jit(solution)/shard_map/all_to_all | solution.py:488
  88.6 9.9 %copy-start.2 = (bf16[256,512]{1,0:T(8,128)(2,1)S(1)}, bf16[256,512]{1,0:T(8,128)(2,1)}, u32[]{:S(2)}) copy-start(bf16[256,512]{1,0:T(8,128)(2,1)} %mixer_read.1.refs_0_) | copy-start | bytes 786436
  88.7 7.6 %collective-permute-start.1 = (bf16[256,512]{1,0:T(8,128)(2,1)}, bf16[256,512]{1,0:T(8,128)(2,1)S(1)}, u32[]{:S(2)}, u32[]{:S(2)}) collective-permute-start(bf16[256,512]{1,0:T(8,128)(2,1)} %mixer_read.1.refs_0_), channel_id=1, source_target_pairs={{0,2},{1,3},{2,0},{3,1},{4,6},{5,7},{6,4},{7,5},{8,10},{9,11},{10,... | collective-permute-start | bytes 786440 | tf_op jit(solution)/shard_map/ppermute | solution.py:384
  89.2 9.4 %collective-permute-start = (bf16[256,512]{1,0:T(8,128)(2,1)}, bf16[256,512]{1,0:T(8,128)(2,1)S(1)}, u32[]{:S(2)}, u32[]{:S(2)}) collective-permute-start(bf16[256,512]{1,0:T(8,128)(2,1)} %mixer_read.1.refs_0_), channel_id=1, source_target_pairs={{0,1},{1,0},{2,3},{3,2},{4,5},{5,4},{6,7},{7,6},{8,9},{9,8},{10,11... | collective-permute-start | bytes 786440 | tf_op jit(solution)/shard_map/ppermute | solution.py:384
  96.3 2.3 %collective-permute-start.2 = (bf16[256,512]{1,0:T(8,128)(2,1)S(1)}, bf16[256,512]{1,0:T(8,128)(2,1)S(1)}, u32[]{:S(2)}, u32[]{:S(2)}) collective-permute-start(bf16[256,512]{1,0:T(8,128)(2,1)S(1)} %collective-permute-done.1.refs_2_), channel_id=1, source_target_pairs={{0,1},{1,0},{2,3},{3,2},{4,5},{5,4},{6,7},{7,6},{8,9},{9,8},{10,11... | collective-permute-start | bytes 786440 | tf_op jit(solution)/shard_map/ppermute | solution.py:384

commit v2 on v1

--- a/solution.py
+++ b/solution.py
@@ -99,77 +99,119 @@
         copy.wait()
 
 
-def fetch_kernel(*refs):
-    count = (len(refs) - 1) // 2
-    sems = refs[-1]
-    copies = [
-        pltpu.make_async_copy(refs[n], refs[count + n], sems.at[n]) for n in range(count)
-    ]
-    for copy in copies:
-        copy.start()
-    for copy in copies:
-        copy.wait()
-
-
 def combine_kernel(share_ref, back_ref, out_ref):
     back = back_ref[...]
     out = mm(share_ref[0], back) + (mm(share_ref[1], back) + mm(share_ref[2], back))
     out_ref[...] = out.astype(bf16)
 
 
-def hidden_kernel(parts, me_ref, packed_ref, *refs):
+def row_gain(packed_ref, which, lead):
+    gain = jnp.zeros_like(packed_ref[0][:, lead:])
+    for q in range(packed_ref.shape[0]):
+        gain = jnp.where(which == q, packed_ref[q][:, lead:], gain)
+    return gain
+
+
+def hidden_kernel(parts, senders, start, me_ref, packed_ref, *refs):
     blocks = refs[:parts]
-    gate_ref, up_ref, down_ref, hidden_ref, far_ref, normed_ref = refs[parts:]
-    rows, feats = blocks[0].shape
+    gate_hbm, up_hbm, down_hbm, hidden_ref, odd_ref, even_ref = refs[parts : parts + 6]
+    normed_ref, gate_ref, up_ref, down_ref, unit_sems, down_sems = refs[parts + 6 :]
+    rows = hidden_ref.shape[0]
+    full, feats = blocks[0].shape
     width = parts * feats
-    chunk = 64
+    chunk = rows // senders
     me = me_ref[0]
-    lead = packed_ref.shape[1] - feats
-    number = iota((parts, feats), 0)
-    gains = [
-        jnp.sum(jnp.where(number == me ^ k, packed_ref[:, lead:], 0.0), axis=0, keepdims=True)
-        for k in range(parts)
-    ]
-
-    def body(step, unused):
-        at = pl.ds(pl.multiple_of(step * chunk, chunk), chunk)
+    units = gate_ref.shape[1]
+    size = units // unit_sems.shape[1]
+    loads = []
+    for n in range(unit_sems.shape[1]):
+        cols = pl.ds(n * size, size)
+        loads.append([
+            pltpu.make_async_copy(hbm.at[0, :, cols], ref.at[:, cols], unit_sems.at[m, n])
+            for m, (hbm, ref) in enumerate(((gate_hbm, gate_ref), (up_hbm, up_ref)))
+        ])
+    downs = []
+    for n in range(down_ref.shape[0]):
+        which = me ^ (n + 2)
+        cols = pl.ds(pl.multiple_of(which * feats, feats), feats)
+        downs.append(
+            pltpu.make_async_copy(down_hbm.at[0, :, cols], down_ref.at[n], down_sems.at[n])
+        )
+    for pair in loads:
+        for copy in pair:
+            copy.start()
+    for copy in downs:
+        copy.start()
+    gains = [row_gain(packed_ref, me ^ k, packed_ref.shape[2] - feats) for k in range(parts)]
+
+    def body(sender, unused):
+        here = pl.ds(pl.multiple_of(sender * chunk, chunk), chunk)
+        there = pl.ds(pl.multiple_of(sender * (full // senders) + start, chunk), chunk)
+        at = [there if k < 2 else here for k in range(parts)]
         total = jnp.zeros((chunk, 1), f32)
         square = jnp.zeros((chunk, 1), f32)
-        for block in blocks:
-            wide = block[at, :].astype(f32)
+        for k, block in enumerate(blocks):
+            wide = block[at[k], :].astype(f32)
             total = total + jnp.sum(wide, axis=1, keepdims=True)
             square = square + jnp.sum(wide * wide, axis=1, keepdims=True)
         mean = total / width
         scale = lax.rsqrt(square / width - mean * mean + norm_eps)
         for k, block in enumerate(blocks):
-            value = (block[at, :].astype(f32) - mean) * scale * gains[k]
+            value = (block[at[k], :].astype(f32) - mean) * scale * gains[k]
             cols = pl.ds(pl.multiple_of((me ^ k) * feats, feats), feats)
-            normed_ref[at, cols] = value.astype(bf16)
+            normed_ref[here, cols] = value.astype(bf16)
         return unused
 
-    lax.fori_loop(0, rows // chunk, body, 0, unroll=2)
-    units = gate_ref.shape[2]
-    size = min(units, 256)
-    for at in range(0, units, size):
-        cols = pl.ds(at, size)
+    lax.fori_loop(0, senders, body, 0, unroll=2)
+    for n, pair in enumerate(loads):
+        cols = pl.ds(n * size, size)
+        for copy in pair:
+            copy.wait()
         normed = normed_ref[...]
-        gate = mm(normed, gate_ref[0, :, cols])
-        up = mm(normed, up_ref[0, :, cols])
+        gate = mm(normed, gate_ref[:, cols])
+        up = mm(normed, up_ref[:, cols])
         hidden_ref[:, cols] = (gate * jax.nn.sigmoid(gate) * up).astype(bf16)
-    for n in range(far_ref.shape[0]):
-        far_ref[n] = down_part(me ^ (2 * n + 3), hidden_ref, down_ref, feats)
-
-
-def down_part(which, hidden_ref, weight_ref, feats):
-    cols = pl.ds(pl.multiple_of(which * feats, feats), feats)
-    return mm(hidden_ref[...], weight_ref[0, :, cols]).astype(bf16)
-
-
-def down_kernel(offsets, me_ref, hidden_ref, weight_ref, out_ref):
-    for n, offset in enumerate(offsets):
-        out_ref[n] = down_part(
-            me_ref[0] ^ offset, hidden_ref, weight_ref, out_ref.shape[2]
+    order = [*range(1, len(downs), 2), *range(0, len(downs), 2)]
+    for copy in downs:
+        copy.wait()
+    for n in order:
+        out = odd_ref if n % 2 else even_ref
+        out[n // 2] = mm(hidden_ref[...], down_ref[n]).astype(bf16)
+
+
+def near_kernel(count, me_ref, *refs):
+    hiddens = refs[:count]
+    down_hbm, near_ref, *owns = refs[count : 2 * count + 2]
+    down_ref, sems = refs[2 * count + 2 :]
+    feats = near_ref.shape[1]
+    copies = []
+    for n in range(2):
+        cols = pl.ds(pl.multiple_of((me_ref[0] ^ n) * feats, feats), feats)
+        copies.append(
+            pltpu.make_async_copy(down_hbm.at[0, :, cols], down_ref.at[n], sems.at[n])
         )
+    for copy in copies:
+        copy.start()
+    for copy in copies:
+        copy.wait()
+    rows = near_ref.shape[0] // count
+    for c, hidden in enumerate(hiddens):
+        near_ref[pl.ds(c * rows, rows), :] = mm(hidden[...], down_ref[1]).astype(bf16)
+    for own, hidden in zip(owns, hiddens):
+        own[...] = mm(hidden[...], down_ref[0]).astype(bf16)
+
+
+def join_kernel(count, senders, near_ref, *refs):
+    out_ref = refs[-1]
+    terms = (len(refs) - 1) // count
+    part = near_ref.shape[0] // count
+    chunk = part // senders
+    for c in range(count):
+        for e in range(senders):
+            total = near_ref[pl.ds(c * part + e * chunk, chunk), :].astype(f32)
+            for ref in refs[c * terms : (c + 1) * terms]:
+                total = total + ref[pl.ds(e * chunk, chunk), :].astype(f32)
+            out_ref[pl.ds((e * count + c) * chunk, chunk), :] = total.astype(bf16)
 
 
 def reorder(rows, back):
@@ -235,8 +277,11 @@
     inner = feats // groups
     steps = rows // LANES
     order = reorder(rows, False)
-    mean = jnp.sum(packed_ref[:, :rows], axis=0, keepdims=True) / total
-    square = jnp.sum(packed_ref[:, rows : 2 * rows], axis=0, keepdims=True) / total
+    packed = packed_ref[0]
+    for q in range(1, packed_ref.shape[0]):
+        packed = packed + packed_ref[q]
+    mean = packed[:, :rows] / total
+    square = packed[:, rows : 2 * rows] / total
     scale = lax.rsqrt(square - mean * mean + norm_eps)
     match = iota((rows, rows), 1) == (iota((rows, rows), 0) % LANES) * steps + iota(
         (rows, rows), 0
@@ -425,7 +470,7 @@
         out_shape=jax.ShapeDtypeStruct((1, 2 * rows + feats), f32),
         in_specs=[vmem, vmem], out_specs=vmem, compiler_params=params(60), name="mixer_sums",
     )(mixer_input, expert_gain.reshape(1, feats))
-    packed = lax.all_gather(packed, "tp", axis=0, tiled=True)
+    packed = lax.all_gather(packed, "tp")
 
     groups, states = pole_real.shape
     flat = groups * states
@@ -444,47 +489,73 @@
     )
     got = lax.all_to_all(ends, "ep", split_axis=0, concat_axis=0)
 
-    blocks = gather_tp(arrived)
-    weights = tuple(stay(w) for w in (expert_gate, expert_up, expert_down))
-    gate_w, up_w, down_w = pl.pallas_call(
-        fetch_kernel,
-        out_shape=tuple(jax.ShapeDtypeStruct(w.shape, w.dtype) for w in weights),
-        in_specs=[hbm] * 3, out_specs=(vmem,) * 3,
-        scratch_shapes=[pltpu.SemaphoreType.DMA((3,))],
-        compiler_params=params(16), name="expert_fetch",
-    )(*weights)
     units = expert_gate.shape[2]
     n_far = n_tp // 2 - 1
-    hidden, odd_far = pl.pallas_call(
-        functools.partial(hidden_kernel, n_tp),
-        in_specs=[smem] + [vmem] * (n_tp + 4), out_specs=(vmem, vmem),
-        scratch_shapes=[pltpu.VMEM((slots, n_tp * feats), bf16)],
-        out_shape=(
-            jax.ShapeDtypeStruct((slots, units), bf16),
-            jax.ShapeDtypeStruct((n_far, slots, feats), bf16),
-        ),
-        compiler_params=params(16), name="expert_hidden",
-    )(tp_at, packed, *blocks, gate_w, up_w, down_w)
-
-    def down(offsets):
-        return pl.pallas_call(
-            functools.partial(down_kernel, offsets),
-            in_specs=[smem, vmem, vmem], out_specs=vmem,
-            out_shape=jax.ShapeDtypeStruct((len(offsets), slots, feats), bf16),
-            compiler_params=params(10),
-        )(tp_at, hidden, down_w)
-
-    theirs = swap(odd_far, 1)
-    even_far = down(tuple(range(2, n_tp, 2)))
-    far = even_far.astype(f32) + theirs.astype(f32)
-    parts = [swap(down((1,))[0], 1), down((0,))[0]]
-    bit = n_tp // 4
-    while bit >= 1:
-        come = swap(far[bit - 1 :].astype(bf16), 2 * bit).astype(f32)
-        parts.append(come[0])
-        far = far[: bit - 1] + come[1:]
-        bit //= 2
-    result = sum(part.astype(f32) for part in parts).astype(bf16)
+    n_half = 2 if capacity % 32 == 0 else 1
+    half = capacity // n_half
+    part = n_ep * half
+    by_sender = arrived.reshape(n_ep, capacity, feats)
+    halves = [by_sender[:, c * half : (c + 1) * half].reshape(part, feats) for c in range(n_half)]
+    far_blocks = []
+    for c in range(n_half):
+        evens = {0: halves[c]}
+        bit = n_tp // 2
+        while bit > 1:
+            evens.update({k ^ bit: swap(b, bit) for k, b in list(evens.items())})
+            bit //= 2
+        far_blocks.append(evens)
+    partner = swap(arrived, 1)
+    weights = [stay(w) for w in (expert_gate, expert_up, expert_down)]
+    n_unit = max(1, units // 256)
+    hiddens, sums = [], []
+    for c in range(n_half):
+        blocks = [arrived, partner]
+        for k in range(2, n_tp, 2):
+            blocks += [far_blocks[c][k], swap(far_blocks[c][k], 1)]
+        far_shape = jax.ShapeDtypeStruct((n_far, part, feats), bf16)
+        hidden, odd_far, even_far = pl.pallas_call(
+            functools.partial(hidden_kernel, n_tp, n_ep, c * half),
+            in_specs=[smem] + [vmem] * (n_tp + 1) + [hbm] * 3, out_specs=(vmem,) * 3,
+            scratch_shapes=[
+                pltpu.VMEM((part, n_tp * feats), bf16),
+                pltpu.VMEM((n_tp * feats, units), bf16),
+                pltpu.VMEM((n_tp * feats, units), bf16),
+                pltpu.VMEM((2 * n_far, units, feats), bf16),
+                pltpu.SemaphoreType.DMA((2, n_unit)),
+                pltpu.SemaphoreType.DMA((2 * n_far,)),
+            ],
+            out_shape=(jax.ShapeDtypeStruct((part, units), bf16), far_shape, far_shape),
+            compiler_params=params(20),
+        )(tp_at, packed, *blocks, *weights)
+        hiddens.append(hidden)
+        theirs = swap(odd_far, 1)
+        far = even_far.astype(f32) + theirs.astype(f32)
+        come = []
+        bit = n_tp // 4
+        while bit >= 1:
+            got_far = swap(far[bit - 1 :].astype(bf16), 2 * bit)
+            come.append(got_far[0])
+            far = far[: bit - 1] + got_far[1:].astype(f32)
+            bit //= 2
+        sums.append(come)
+    near, *owns = pl.pallas_call(
+        functools.partial(near_kernel, n_half),
+        in_specs=[smem] + [vmem] * n_half + [hbm], out_specs=(vmem,) * (n_half + 1),
+        out_shape=(jax.ShapeDtypeStruct((slots, feats), bf16),)
+        + (jax.ShapeDtypeStruct((part, feats), bf16),) * n_half,
+        scratch_shapes=[
+            pltpu.VMEM((2, units, feats), bf16), pltpu.SemaphoreType.DMA((2,)),
+        ],
+        compiler_params=params(10), name="expert_near",
+    )(tp_at, *hiddens, weights[2])
+    near = swap(near, 1)
+    terms = [term for own, come in zip(owns, sums) for term in (own, *come)]
+    result = pl.pallas_call(
+        functools.partial(join_kernel, n_half, n_ep),
+        out_shape=jax.ShapeDtypeStruct((slots, feats), bf16),
+        in_specs=[vmem] * (len(terms) + 1), out_specs=vmem, compiler_params=params(8),
+        name="expert_join",
+    )(near, *terms)
     back = lax.all_to_all(result, "ep", split_axis=0, concat_axis=0, tiled=True)
 
     mixed = pl.pallas_call(

time: 102 us -> 103 us (level)
  starting transfers between devices: 12.3 us -> 14.9 us
  local copies, waits for them, and re-layouts: 2.22 us -> 0.06 us
  other arithmetic: 2.18 us -> 0.13 us
  waiting for transfers between devices: 20.5 us -> 21.9 us
  Pallas kernels: 36.4 us -> 37.6 us
    all_to_all x1, waiting for transfers between devices: 2.35 us -> 6.32 us  [shards(): got = lax.all_to_all(ends, 'ep', split_axis=0, concat_axis=0)]
    ppermute x9 -> x13, starting transfers between devices: 4.27 us -> 6.84 us  [swap(): return lax.ppermute(value, 'tp', [(i, i ^ bit) for i in range(count)])]
    ppermute x9 -> x13, waiting for transfers between devices: 18.1 us -> 15.6 us  [swap(): return lax.ppermute(value, 'tp', [(i, i ^ bit) for i in range(count)])]
    unnamed x15 -> x10, local copies, waits for them, and re-layouts: 2.22 us -> 0.03 us
    convert_element_type x2, other arithmetic: 2.18 us -> 0.13 us  [shards(): got_far = swap(far[bit - 1:].astype(bf16), 2 * bit)]
    pallas_call x5 -> x4, Pallas kernels: 13.4 us -> 14.5 us  [the longest x2 10.7 us: shards(): pl.pallas_call(functools.partial(hidden_kernel, n_tp, n_ep, c * half), in...]
  transfers between devices with their start and end apart: 11 -> 15, of which waited for: 3 -> 4; matrix products, arithmetic and copies ran while one was open for 2% -> 0% of each run, Pallas kernels for 26% -> 34%
where the time goes in v2:
time: 103 us
  Pallas kernels  37.6 us (37%)
  blocking collectives  27.1 us (26%)
  waiting for transfers between devices  21.9 us (21%)
  starting transfers between devices  14.9 us (14%)
    all_to_all x1, blocking collectives, shards(): lax.all_to_all(send, 'ep', split_axis=0, concat_axis=0, tiled=True)  21.8 us
    ppermute x13, waiting for transfers between devices, swap(): return lax.ppermute(value, 'tp', [(i, i ^ bit) for i in range(count)])  15.6 us
    pallas_call x2, Pallas kernels, shards(): pl.pallas_call(functools.partial(hidden_kernel, n_tp, n_ep, c * half), in...  10.7 us
    pallas_call x1, Pallas kernels, shards(): pl.pallas_call(functools.partial(scan_kernel, float(chans * n_tp)), out_s...  8.25 us
    ppermute x13, starting transfers between devices, swap(): return lax.ppermute(value, 'tp', [(i, i ^ bit) for i in range(count)])  6.84 us
    all_to_all x1, waiting for transfers between devices, shards(): got = lax.all_to_all(ends, 'ep', split_axis=0, concat_axis=0)  6.32 us
    pallas_call x1, Pallas kernels, shards(): pl.pallas_call(read_kernel, out_shape=jax.ShapeDtypeStruct((rows, chans),...  5.55 us
    all_gather x1, blocking collectives, shards(): packed = lax.all_gather(packed, 'tp')  5.32 us
  transfers between devices with their start and end apart: 15, of which 4 were waited for; matrix products, arithmetic and copies ran while one was open for 0% of the time, Pallas kernels for 34%

profile of v2, /device:TPU:0, one launch (start us, length us, event | category | flops | bytes accessed | tf_op | source)
XLA Modules:
  0.0 102.5 jit_solution(6881522940013223391)
XLA Ops:
  0.6 2.1 %send_rows.1 = bf16[512,512]{1,0:T(8,128)(2,1)} custom-call(s32[2,128]{1,0:T(2,128)} %bitcast.30, bf16[128,512]{1,0:T(8,128)(2,1)} %rows_ref.1), custom_call_target="tpu_custom_call" | custom-call | tf_op jit(solution)/shard_map/send_rows/pallas_call | solution.py:457
  2.8 21.8 %all_to_all.27 = bf16[8,64,512]{2,1,0:T(8,128)(2,1)S(1)} all-to-all(bf16[8,64,512]{2,1,0:T(8,128)(2,1)} %bitcast.33), channel_id=1, replica_groups=mesh['ep'=8,'tp'=4] {'ep'}, dimensions={0} | all-to-all | bytes 1048576 | tf_op jit(solution)/shard_map/all_to_all | solution.py:462
  24.6 1.6 %collective-permute-start.6 = (bf16[256,512]{1,0:T(8,128)(2,1)S(1)}, bf16[256,512]{1,0:T(8,128)(2,1)S(1)}, u32[]{:S(2)}, u32[]{:S(2)}) collective-permute-start(bf16[256,512]{1,0:T(8,128)(2,1)S(1)} %bitcast.37), channel_id=1, source_target_pairs={{0,2},{1,3},{2,0},{3,1},{4,6},{5,7},{6,4},{7,5},{8,10},{9,11},{10,... | collective-permute-start | bytes 786440 | tf_op jit(solution)/shard_map/ppermute | solution.py:429
  26.2 0.0 collective-permute-start.3
  26.2 0.5 collective-permute-start.4
  26.7 7.1 %collective-permute-done.6.refs_2_ = bf16[256,512]{1,0:T(8,128)(2,1)S(1)} collective-permute-done((bf16[256,512]{1,0:T(8,128)(2,1)S(1)}, bf16[256,512]{1,0:T(8,128)(2,1)S(1)}, u32[]{:S(2)}, u32[]{:S(2)}) %collective-permute-start.6) | collective-permute-done | bytes 262176 | tf_op jit(solution)/shard_map/ppermute | solution.py:429
  33.9 0.0 collective-permute-start.7
  33.9 3.4 %collective-permute-done.4.refs_2_ = bf16[256,512]{1,0:T(8,128)(2,1)S(1)} collective-permute-done((bf16[256,512]{1,0:T(8,128)(2,1)S(1)}, bf16[256,512]{1,0:T(8,128)(2,1)S(1)}, u32[]{:S(2)}, u32[]{:S(2)}) %collective-permute-start.4) | collective-permute-done | bytes 262176 | tf_op jit(solution)/shard_map/ppermute | solution.py:429
  37.2 0.0 collective-permute-start.5
  37.2 1.9 %mixer_sums.1 = f32[1,1024]{1,0:T(1,128)} custom-call(bf16[256,512]{1,0:T(8,128)(2,1)} %x_ref.1, f32[1,512]{1,0:T(1,128)} %bitcast.42), custom_call_target="tpu_custom_call" | custom-call | tf_op jit(solution)/shard_map/mixer_sums/pallas_call | solution.py:468
  39.1 5.3 %all-gather.1.packed_ref = f32[4,1,1024]{2,1,0:T(1,128)S(1)} all-gather(f32[1,1,1024]{2,1,0:T(1,128)} %bitcast.41), channel_id=2, replica_groups=mesh['ep'=8,'tp'=4] {'tp'}, dimensions={0}, use_global_device_ids=true | all-gather | bytes 20480 | tf_op jit(solution)/shard_map/all_gather | solution.py:473
  44.4 0.0 copy-start.1
  44.4 0.0 collective-permute-done.7.refs_3_
  44.4 0.0 collective-permute-done.3.refs_1_
  44.4 5.4 %shard_map.186 = (bf16[256,1024]{1,0:T(8,128)(2,1)S(1)}, bf16[1,256,512]{2,1,0:T(8,128)(2,1)S(1)}, bf16[1,256,512]{2,1,0:T(8,128)(2,1)S(1)}) custom-call(s32[1]{0:T(128)} %bitcast.1.me_ref, f32[4,1,1024]{2,1,0:T(1,128)S(1)} %all-gather.1.packed_ref, bf16[512,512]{1,0:T(8,128)(2,1)S(1)} %bitcast.25, bf16[512,512]{1,0:T(8,128)(2,1)S(1)} %collective-permute-done.3.refs_1_, ...), custom_call_target="tpu_custom_call" | custom-call | tf_op jit(solution)/shard_map/pallas_call | solution.py:516
  49.8 0.4 collective-permute-start.11
  50.2 0.0 collective-permute-done.5.refs_3_
  50.2 0.0 copy-done.1
  50.2 5.3 %shard_map.185 = (bf16[256,1024]{1,0:T(8,128)(2,1)S(1)}, bf16[1,256,512]{2,1,0:T(8,128)(2,1)S(1)}, bf16[1,256,512]{2,1,0:T(8,128)(2,1)S(1)}) custom-call(s32[1]{0:T(128)} %bitcast.1.me_ref, f32[4,1,1024]{2,1,0:T(1,128)S(1)} %all-gather.1.packed_ref, bf16[512,512]{1,0:T(8,128)(2,1)S(1)} %bitcast.26, bf16[512,512]{1,0:T(8,128)(2,1)S(1)} %collective-permute-done.3.refs_1_, ...), custom_call_target="tpu_custom_call" | custom-call | tf_op jit(solution)/shard_map/pallas_call | solution.py:516
  55.6 0.2 collective-permute-start.9
  55.8 2.8 %expert_near.1 = (bf16[512,512]{1,0:T(8,128)(2,1)S(1)}, bf16[256,512]{1,0:T(8,128)(2,1)S(1)}, bf16[256,512]{1,0:T(8,128)(2,1)S(1)}) custom-call(s32[1]{0:T(128)} %bitcast.1.me_ref, bf16[256,1024]{1,0:T(8,128)(2,1)S(1)} %get-tuple-element.33.refs_0_, bf16[256,1024]{1,0:T(8,128)(2,1)S(1)} %get-tuple-element.34.refs_1_, bf16[1,1024,2048]{2,1,0:T(8,128)(2,1)} %refs_2_.1), custom_call_target="tpu_custom_call" | custom-call | tf_op jit(solution)/shard_map/expert_near/pallas_call | solution.py:541
  58.6 0.4 collective-permute-start.8
  59.0 0.0 collective-permute-done.11
  59.0 0.1 add_convert_fusion
  59.1 1.6 %collective-permute-start.12 = (bf16[1,256,512]{2,1,0:T(8,128)(2,1)S(1)}, bf16[1,256,512]{2,1,0:T(8,128)(2,1)S(1)}, u32[]{:S(2)}, u32[]{:S(2)}) collective-permute-start(bf16[1,256,512]{2,1,0:T(8,128)(2,1)S(1)} %add_convert_fusion), channel_id=1, source_target_pairs={{0,2},{1,3},{2,0},{3,1},{4,6},{5,7},{6,4},{7,5},{8,10},{9,11},{10,... | collective-permute-start | bytes 786440 | tf_op jit(solution)/shard_map/ppermute | solution.py:429
  60.7 0.0 collective-permute-done.9
  60.7 0.1 add_convert_fusion.1
  60.8 0.6 collective-permute-start.10
  61.3 8.3 %mixer_scan.1 = (f32[256,1024]{1,0:T(8,128)}, f32[256,1024]{1,0:T(8,128)}, f32[256,1024]{1,0:T(8,128)}, f32[256,1024]{1,0:T(8,128)}, f32[8,4,1024]{2,1,0:T(4,128)}) custom-call(bf16[256,512]{1,0:T(8,128)(2,1)} %x_ref.1, f32[4,1,1024]{2,1,0:T(1,128)} %copy-done.1, f32[1,512]{1,0:T(1,128)} %bitcast.43, f32[32,256]{1,0:T(8,128)} %bitcast.40, f32[32,32]{1,0:T(8,128)} %pr_ref.1, ...), custom_call_target="tpu_custom_call" | custom-call | tf_op jit(solution)/shard_map/mixer_scan/pallas_call | solution.py:478
  69.6 4.4 %all-to-all-start = ((f32[8,4,1024]{2,1,0:T(4,128)}), f32[8,4,1024]{2,1,0:T(4,128)S(1)}, u32[]{:S(2)}, u32[]{:S(2)}) async-start(f32[8,4,1024]{2,1,0:T(4,128)} %get-tuple-element.25), calls=%async_computation | async-start | bytes 262144 | tf_op jit(solution)/shard_map/all_to_all | solution.py:490
  73.9 0.0 collective-permute-done.12
  74.0 0.0 collective-permute-done.10
  74.0 0.0 collective-permute-done.8.near_ref
  74.0 1.0 expert_join.1
  75.0 6.3 %all-to-all-done.got_ref = f32[8,4,1024]{2,1,0:T(4,128)S(1)} async-done(((f32[8,4,1024]{2,1,0:T(4,128)}), f32[8,4,1024]{2,1,0:T(4,128)S(1)}, u32[]{:S(2)}, u32[]{:S(2)}) %all-to-all-start) | async-done | bytes 131104 | tf_op jit(solution)/shard_map/all_to_all | solution.py:490
  81.3 0.0 copy-start.4
  81.3 3.7 %all-to-all-start.2 = ((bf16[8,64,512]{2,1,0:T(8,128)(2,1)}), bf16[8,64,512]{2,1,0:T(8,128)(2,1)S(1)}, u32[]{:S(2)}, u32[]{:S(2)}) async-start(bf16[8,64,512]{2,1,0:T(8,128)(2,1)} %bitcast.20), calls=%async_computation.2 | async-start | bytes 1048576 | tf_op jit(solution)/shard_map/all_to_all | solution.py:559
  85.0 0.0 copy-done.4
  85.0 0.0 copy-start.2
  85.0 0.0 copy-start.3
  85.0 5.5 %mixer_read.1.refs_0_ = bf16[256,512]{1,0:T(8,128)(2,1)} custom-call(s32[1]{0:T(128)} %bitcast.2.me_ref, f32[8,4,1024]{2,1,0:T(4,128)} %copy-done.4, f32[256,1024]{1,0:T(8,128)} %get-tuple-element.26.hr_ref, f32[256,1024]{1,0:T(8,128)} %get-tuple-element.27.hi_ref, f32[256,1024]{1,0:T(8,128)} %get-tuple-element.28.cr_ref, ...), custom_call_target="tpu_custom_call" | custom-call | tf_op jit(solution)/shard_map/mixer_read/pallas_call | solution.py:561
  90.6 1.5 %collective-permute-start.1 = (bf16[256,512]{1,0:T(8,128)(2,1)}, bf16[256,512]{1,0:T(8,128)(2,1)S(1)}, u32[]{:S(2)}, u32[]{:S(2)}) collective-permute-start(bf16[256,512]{1,0:T(8,128)(2,1)} %mixer_read.1.refs_0_), channel_id=1, source_target_pairs={{0,2},{1,3},{2,0},{3,1},{4,6},{5,7},{6,4},{7,5},{8,10},{9,11},{10,... | collective-permute-start | bytes 786440 | tf_op jit(solution)/shard_map/ppermute | solution.py:429
  92.1 0.0 collective-permute-start
  92.1 5.1 %collective-permute-done.1.refs_2_ = bf16[256,512]{1,0:T(8,128)(2,1)S(1)} collective-permute-done((bf16[256,512]{1,0:T(8,128)(2,1)}, bf16[256,512]{1,0:T(8,128)(2,1)S(1)}, u32[]{:S(2)}, u32[]{:S(2)}) %collective-permute-start.1) | collective-permute-done | bytes 262176 | tf_op jit(solution)/shard_map/ppermute | solution.py:429
  97.2 0.0 collective-permute-start.2
  97.2 0.0 copy-done.2
  97.2 0.0 copy-done.3
  97.2 0.0 copy-start
  97.2 2.3 %out_fetch.1 = (bf16[3,128,512]{2,1,0:T(8,128)(2,1)S(1)}, bf16[2048,512]{1,0:T(8,128)(2,1)S(1)}, bf16[2048,512]{1,0:T(8,128)(2,1)S(1)}) custom-call(s32[2,128]{1,0:T(2,128)S(1)} %bitcast.31, f32[2,128]{1,0:T(2,128)S(1)} %bitcast.32, bf16[2048,512]{1,0:T(8,128)(2,1)} %value_ref.1, bf16[2048,512]{1,0:T(8,128)(2,1)} %gate_ref.1), custom_call_target="tpu_custom_call" | custom-call | tf_op jit(solution)/shard_map/out_fetch/pallas_call | solution.py:571
  99.5 0.0 collective-permute-done.refs_1_
  99.5 0.0 collective-permute-done.2.refs_3_
  99.5 0.0 copy-done
  99.5 2.0 %mixer_out.1 = bf16[256,512]{1,0:T(8,128)(2,1)} custom-call(s32[1]{0:T(128)} %bitcast.1.me_ref, bf16[256,512]{1,0:T(8,128)(2,1)S(1)} %copy-done, bf16[256,512]{1,0:T(8,128)(2,1)S(1)} %collective-permute-done.refs_1_, bf16[256,512]{1,0:T(8,128)(2,1)S(1)} %collective-permute-done.1.refs_2_, bf16[256,512]{1,0:T(8,128)(2,1)S(1)} %collective-permute-done.2.refs_3_, ...), custom_call_target="tpu_custom_call" | custom-call | tf_op jit(solution)/shard_map/mixer_out/pallas_call | solution.py:582
  101.5 0.0 all-to-all-done.2
  101.5 1.0 %combine.1 = bf16[128,512]{1,0:T(8,128)(2,1)} custom-call(bf16[3,128,512]{2,1,0:T(8,128)(2,1)S(1)} %get-tuple-element.32.share_ref, bf16[512,512]{1,0:T(8,128)(2,1)S(1)} %bitcast.27), custom_call_target="tpu_custom_call" | custom-call | tf_op jit(solution)/shard_map/combine/pallas_call | solution.py:588
  (1 shorter events, 0.0 us)
Async XLA Ops:
  24.6 9.2 %collective-permute-start.6 = (bf16[256,512]{1,0:T(8,128)(2,1)S(1)}, bf16[256,512]{1,0:T(8,128)(2,1)S(1)}, u32[]{:S(2)}, u32[]{:S(2)}) collective-permute-start(bf16[256,512]{1,0:T(8,128)(2,1)S(1)} %bitcast.37), channel_id=1, source_target_pairs={{0,2},{1,3},{2,0},{3,1},{4,6},{5,7},{6,4},{7,5},{8,10},{9,11},{10,... | collective-permute-start | bytes 786440 | tf_op jit(solution)/shard_map/ppermute | solution.py:429
  26.2 18.2 %collective-permute-start.3 = (bf16[512,512]{1,0:T(8,128)(2,1)S(1)}, bf16[512,512]{1,0:T(8,128)(2,1)S(1)}, u32[]{:S(2)}, u32[]{:S(2)}) collective-permute-start(bf16[512,512]{1,0:T(8,128)(2,1)S(1)} %bitcast.24), channel_id=1, source_target_pairs={{0,1},{1,0},{2,3},{3,2},{4,5},{5,4},{6,7},{7,6},{8,9},{9,8},{10,11... | collective-permute-start | bytes 1572872 | tf_op jit(solution)/shard_map/ppermute | solution.py:429
  26.2 11.0 %collective-permute-start.4 = (bf16[256,512]{1,0:T(8,128)(2,1)S(1)}, bf16[256,512]{1,0:T(8,128)(2,1)S(1)}, u32[]{:S(2)}, u32[]{:S(2)}) collective-permute-start(bf16[256,512]{1,0:T(8,128)(2,1)S(1)} %bitcast.36), channel_id=1, source_target_pairs={{0,2},{1,3},{2,0},{3,1},{4,6},{5,7},{6,4},{7,5},{8,10},{9,11},{10,... | collective-permute-start | bytes 786440 | tf_op jit(solution)/shard_map/ppermute | solution.py:429
  33.9 10.6 %collective-permute-start.7 = (bf16[256,512]{1,0:T(8,128)(2,1)S(1)}, bf16[256,512]{1,0:T(8,128)(2,1)S(1)}, u32[]{:S(2)}, u32[]{:S(2)}) collective-permute-start(bf16[256,512]{1,0:T(8,128)(2,1)S(1)} %collective-permute-done.6.refs_2_), channel_id=1, source_target_pairs={{0,1},{1,0},{2,3},{3,2},{4,5},{5,4},{6,7},{7,6},{8,9},{9,8},{10,11... | collective-permute-start | bytes 786440 | tf_op jit(solution)/shard_map/ppermute | solution.py:429
  37.2 13.0 %collective-permute-start.5 = (bf16[256,512]{1,0:T(8,128)(2,1)S(1)}, bf16[256,512]{1,0:T(8,128)(2,1)S(1)}, u32[]{:S(2)}, u32[]{:S(2)}) collective-permute-start(bf16[256,512]{1,0:T(8,128)(2,1)S(1)} %collective-permute-done.4.refs_2_), channel_id=1, source_target_pairs={{0,1},{1,0},{2,3},{3,2},{4,5},{5,4},{6,7},{7,6},{8,9},{9,8},{10,11... | collective-permute-start | bytes 786440 | tf_op jit(solution)/shard_map/ppermute | solution.py:429
  44.4 5.8 %copy-start.1 = (f32[4,1,1024]{2,1,0:T(1,128)}, f32[4,1,1024]{2,1,0:T(1,128)S(1)}, u32[]{:S(2)}) copy-start(f32[4,1,1024]{2,1,0:T(1,128)S(1)} %all-gather.1.packed_ref) | copy-start | bytes 49156
  49.8 9.2 %collective-permute-start.11 = (bf16[1,256,512]{2,1,0:T(8,128)(2,1)S(1)}, bf16[1,256,512]{2,1,0:T(8,128)(2,1)S(1)}, u32[]{:S(2)}, u32[]{:S(2)}) collective-permute-start(bf16[1,256,512]{2,1,0:T(8,128)(2,1)S(1)} %get-tuple-element.41), channel_id=1, source_target_pairs={{0,1},{1,0},{2,3},{3,2},{4,5},{5,4},{6,7},{7,6},{8,9},{9,8},{10,11... | collective-permute-start | bytes 786440 | tf_op jit(solution)/shard_map/ppermute | solution.py:429
  55.6 5.1 %collective-permute-start.9 = (bf16[1,256,512]{2,1,0:T(8,128)(2,1)S(1)}, bf16[1,256,512]{2,1,0:T(8,128)(2,1)S(1)}, u32[]{:S(2)}, u32[]{:S(2)}) collective-permute-start(bf16[1,256,512]{2,1,0:T(8,128)(2,1)S(1)} %get-tuple-element.38), channel_id=1, source_target_pairs={{0,1},{1,0},{2,3},{3,2},{4,5},{5,4},{6,7},{7,6},{8,9},{9,8},{10,11... | collective-permute-start | bytes 786440 | tf_op jit(solution)/shard_map/ppermute | solution.py:429
  58.6 15.4 %collective-permute-start.8 = (bf16[512,512]{1,0:T(8,128)(2,1)S(1)}, bf16[512,512]{1,0:T(8,128)(2,1)S(1)}, u32[]{:S(2)}, u32[]{:S(2)}) collective-permute-start(bf16[512,512]{1,0:T(8,128)(2,1)S(1)} %get-tuple-element.35), channel_id=1, source_target_pairs={{0,1},{1,0},{2,3},{3,2},{4,5},{5,4},{6,7},{7,6},{8,9},{9,8},{10,11... | collective-permute-start | bytes 1572872 | tf_op jit(solution)/shard_map/ppermute | solution.py:429
  59.1 14.9 %collective-permute-start.12 = (bf16[1,256,512]{2,1,0:T(8,128)(2,1)S(1)}, bf16[1,256,512]{2,1,0:T(8,128)(2,1)S(1)}, u32[]{:S(2)}, u32[]{:S(2)}) collective-permute-start(bf16[1,256,512]{2,1,0:T(8,128)(2,1)S(1)} %add_convert_fusion), channel_id=1, source_target_pairs={{0,2},{1,3},{2,0},{3,1},{4,6},{5,7},{6,4},{7,5},{8,10},{9,11},{10,... | collective-permute-start | bytes 786440 | tf_op jit(solution)/shard_map/ppermute | solution.py:429
  60.8 13.2 %collective-permute-start.10 = (bf16[1,256,512]{2,1,0:T(8,128)(2,1)S(1)}, bf16[1,256,512]{2,1,0:T(8,128)(2,1)S(1)}, u32[]{:S(2)}, u32[]{:S(2)}) collective-permute-start(bf16[1,256,512]{2,1,0:T(8,128)(2,1)S(1)} %add_convert_fusion.1), channel_id=1, source_target_pairs={{0,2},{1,3},{2,0},{3,1},{4,6},{5,7},{6,4},{7,5},{8,10},{9,11},{10,... | collective-permute-start | bytes 786440 | tf_op jit(solution)/shard_map/ppermute | solution.py:429
  69.6 11.7 %all-to-all-start = ((f32[8,4,1024]{2,1,0:T(4,128)}), f32[8,4,1024]{2,1,0:T(4,128)S(1)}, u32[]{:S(2)}, u32[]{:S(2)}) async-start(f32[8,4,1024]{2,1,0:T(4,128)} %get-tuple-element.25), calls=%async_computation | async-start | bytes 262144 | tf_op jit(solution)/shard_map/all_to_all | solution.py:490
  81.3 3.7 %copy-start.4 = (f32[8,4,1024]{2,1,0:T(4,128)}, f32[8,4,1024]{2,1,0:T(4,128)S(1)}, u32[]{:S(2)}) copy-start(f32[8,4,1024]{2,1,0:T(4,128)S(1)} %all-to-all-done.got_ref) | copy-start | bytes 393220
  81.3 20.2 %all-to-all-start.2 = ((bf16[8,64,512]{2,1,0:T(8,128)(2,1)}), bf16[8,64,512]{2,1,0:T(8,128)(2,1)S(1)}, u32[]{:S(2)}, u32[]{:S(2)}) async-start(bf16[8,64,512]{2,1,0:T(8,128)(2,1)} %bitcast.20), calls=%async_computation.2 | async-start | bytes 1048576 | tf_op jit(solution)/shard_map/all_to_all | solution.py:559
  85.0 12.2 %copy-start.2 = (s32[128,2]{0,1:T(2,128)S(1)}, s32[128,2]{0,1:T(2,128)}, u32[]{:S(2)}) copy-start(s32[128,2]{0,1:T(2,128)} %param.31) | copy-start | bytes 3076
  85.0 12.2 %copy-start.3 = (f32[128,2]{0,1:T(2,128)S(1)}, f32[128,2]{0,1:T(2,128)}, u32[]{:S(2)}) copy-start(f32[128,2]{0,1:T(2,128)} %param.32) | copy-start | bytes 3076
  90.6 6.6 %collective-permute-start.1 = (bf16[256,512]{1,0:T(8,128)(2,1)}, bf16[256,512]{1,0:T(8,128)(2,1)S(1)}, u32[]{:S(2)}, u32[]{:S(2)}) collective-permute-start(bf16[256,512]{1,0:T(8,128)(2,1)} %mixer_read.1.refs_0_), channel_id=1, source_target_pairs={{0,2},{1,3},{2,0},{3,1},{4,6},{5,7},{6,4},{7,5},{8,10},{9,11},{10,... | collective-permute-start | bytes 786440 | tf_op jit(solution)/shard_map/ppermute | solution.py:429
  92.1 7.4 %collective-permute-start = (bf16[256,512]{1,0:T(8,128)(2,1)}, bf16[256,512]{1,0:T(8,128)(2,1)S(1)}, u32[]{:S(2)}, u32[]{:S(2)}) collective-permute-start(bf16[256,512]{1,0:T(8,128)(2,1)} %mixer_read.1.refs_0_), channel_id=1, source_target_pairs={{0,1},{1,0},{2,3},{3,2},{4,5},{5,4},{6,7},{7,6},{8,9},{9,8},{10,11... | collective-permute-start | bytes 786440 | tf_op jit(solution)/shard_map/ppermute | solution.py:429
  97.2 2.3 %collective-permute-start.2 = (bf16[256,512]{1,0:T(8,128)(2,1)S(1)}, bf16[256,512]{1,0:T(8,128)(2,1)S(1)}, u32[]{:S(2)}, u32[]{:S(2)}) collective-permute-start(bf16[256,512]{1,0:T(8,128)(2,1)S(1)} %collective-permute-done.1.refs_2_), channel_id=1, source_target_pairs={{0,1},{1,0},{2,3},{3,2},{4,5},{5,4},{6,7},{7,6},{8,9},{9,8},{10,11... | collective-permute-start | bytes 786440 | tf_op jit(solution)/shard_map/ppermute | solution.py:429
  97.2 2.3 %copy-start = (bf16[256,512]{1,0:T(8,128)(2,1)S(1)}, bf16[256,512]{1,0:T(8,128)(2,1)}, u32[]{:S(2)}) copy-start(bf16[256,512]{1,0:T(8,128)(2,1)} %mixer_read.1.refs_0_) | copy-start | bytes 786436

commit v3 on v2

v3 whole, which is shorter than its diff:
```python
import functools

import jax
import jax.numpy as jnp
from jax import lax
from jax.experimental import pallas as pl
from jax.experimental.pallas import tpu as pltpu
from jax.sharding import PartitionSpec as P


f32 = jnp.float32
bf16 = jnp.bfloat16
norm_eps = 1e-05
LANES = 8
NN = (((1,), (0,)), ((), ()))
NT = (((1,), (1,)), ((), ()))
TN = (((0,), (0,)), ((), ()))


def iota(shape, dim):
    return lax.broadcasted_iota(jnp.int32, shape, dim)


def ones_where(mask):
    return jnp.where(mask, 1.0, 0.0).astype(bf16)


def split2(value):
    high = value.astype(bf16)
    return high, (value - high.astype(f32)).astype(bf16)


def split3(value):
    high = value.astype(bf16)
    rest = value - high.astype(f32)
    mid = rest.astype(bf16)
    return high, mid, (rest - mid.astype(f32)).astype(bf16)


def mm(left, right, dims=NN):
    return lax.dot_general(left, right, dims, preferred_element_type=f32)


def mm3(left, right, dims):
    lh, ll = left
    rh, rl = right
    return mm(lh, rh, dims) + (mm(ll, rh, dims) + mm(lh, rl, dims))


def mul(ar, ai, br, bi):
    return ar * br - ai * bi, ar * bi + ai * br


def slot_keys(routes_t, experts):
    top, tokens = routes_t.shape
    number = iota((experts, tokens), 0)
    hit = routes_t[0:1, :] == number
    for k in range(1, top):
        hit = hit | (routes_t[k : k + 1, :] == number)
    before = ones_where(iota((tokens, tokens), 0) < iota((tokens, tokens), 1))
    place = mm(ones_where(hit), before)
    return jnp.where(hit, place, -1.0)


def send_kernel(experts, capacity, routes_ref, rows_ref, x_ref, gain_ref, out_ref, sums_ref):
    keys = slot_keys(routes_ref[...], experts)
    tokens = keys.shape[1]
    slot = iota((capacity, tokens), 0).astype(f32)
    chosen = [ones_where(slot == keys[e : e + 1, :]) for e in range(experts)]
    out_ref[...] = mm(jnp.concatenate(chosen, axis=0), rows_ref[...]).astype(bf16)
    rows = x_ref[...]
    count = rows.shape[0]
    ones = jnp.ones((8, rows.shape[1]), bf16)
    wide = rows.astype(f32)
    high, low = split2(wide * wide)
    sums_ref[:, :count] = mm(ones, rows, NT)[0:1]
    sums_ref[:, count : 2 * count] = (mm(ones, high, NT) + mm(ones, low, NT))[0:1]
    sums_ref[:, 2 * count :] = gain_ref[...]


def share_kernel(experts, capacity, routes_ref, weight_ref, out_ref):
    routes_t = routes_ref[...]
    weight_t = weight_ref[...]
    keys = slot_keys(routes_t, experts)
    tokens = keys.shape[1]
    number = iota((experts, tokens), 0)
    share = jnp.zeros((experts, tokens), f32)
    for k in range(routes_t.shape[0]):
        share = share + jnp.where(routes_t[k : k + 1, :] == number, weight_t[k : k + 1, :], 0.0)
    slot = iota((capacity, tokens), 0).astype(f32)
    spread = [
        jnp.where(slot == keys[e : e + 1, :], share[e : e + 1, :], 0.0)
        for e in range(experts)
    ]
    same = ones_where(iota((tokens, tokens), 0) == iota((tokens, tokens), 1))
    for n, term in enumerate(split3(jnp.concatenate(spread, axis=0))):
        out_ref[n] = mm(same, term, NT).astype(bf16)


def fetch_kernel(*refs):
    count = (len(refs) - 1) // 2
    sems = refs[-1]
    copies = [
        pltpu.make_async_copy(refs[n], refs[count + n], sems.at[n]) for n in range(count)
    ]
    for copy in copies:
        copy.start()
    for copy in copies:
        copy.wait()


def combine_kernel(share_ref, back_ref, out_ref):
    back = back_ref[...]
    out = mm(share_ref[0], back) + (mm(share_ref[1], back) + mm(share_ref[2], back))
    out_ref[...] = out.astype(bf16)


def hidden_kernel(parts, senders, start, load, me_ref, *refs):
    packs = refs[:parts]
    blocks = refs[parts : 2 * parts]
    if load:
        sources = refs[2 * parts : 2 * parts + 3]
        hidden_ref, odd_ref, even_ref, gate_ref, up_ref, down_ref = refs[
            2 * parts + 3 : 2 * parts + 9
        ]
        normed_ref, sems = refs[2 * parts + 9 :]
    else:
        gate_ref, up_ref, down_ref, hidden_ref, odd_ref, even_ref, normed_ref = refs[
            2 * parts :
        ]
    rows, units = hidden_ref.shape
    full, feats = blocks[0].shape
    width = parts * feats
    chunk = rows // senders
    me = me_ref[0]
    lead = packs[0].shape[1] - feats
    size = min(units, 256)
    loads = []
    if load:
        for n in range(units // size):
            cols = pl.ds(n * size, size)
            loads.append([
                pltpu.make_async_copy(
                    sources[m].at[0, :, cols], ref.at[0, :, cols], sems.at[m, n]
                )
                for m, ref in enumerate((gate_ref, up_ref))
            ])
        loads.append([pltpu.make_async_copy(sources[2], down_ref, sems.at[2, 0])])
        for group in loads:
            for copy in group:
                copy.start()

    def body(sender, unused):
        here = pl.ds(pl.multiple_of(sender * chunk, chunk), chunk)
        there = pl.ds(pl.multiple_of(sender * (full // senders) + start, chunk), chunk)
        at = [there if k < 2 else here for k in range(parts)]
        total = jnp.zeros((chunk, 1), f32)
        square = jnp.zeros((chunk, 1), f32)
        for k, block in enumerate(blocks):
            wide = block[at[k], :].astype(f32)
            total = total + jnp.sum(wide, axis=1, keepdims=True)
            square = square + jnp.sum(wide * wide, axis=1, keepdims=True)
        mean = total / width
        scale = lax.rsqrt(square / width - mean * mean + norm_eps)
        for k, block in enumerate(blocks):
            gain = packs[k][:, lead:]
            value = (block[at[k], :].astype(f32) - mean) * scale * gain
            cols = pl.ds(pl.multiple_of((me ^ k) * feats, feats), feats)
            normed_ref[here, cols] = value.astype(bf16)
        return unused

    lax.fori_loop(0, senders, body, 0, unroll=2)
    for at in range(0, units, size):
        cols = pl.ds(at, size)
        if load:
            for copy in loads[at // size]:
                copy.wait()
        normed = normed_ref[...]
        gate = mm(normed, gate_ref[0, :, cols])
        up = mm(normed, up_ref[0, :, cols])
        hidden_ref[:, cols] = (gate * jax.nn.sigmoid(gate) * up).astype(bf16)
    if load:
        loads[-1][0].wait()
    for first, out in ((3, odd_ref), (2, even_ref)):
        for n in range(out.shape[0]):
            out[n] = down_part(me ^ (2 * n + first), hidden_ref, down_ref, feats)


def down_part(which, hidden_ref, weight_ref, feats):
    cols = pl.ds(pl.multiple_of(which * feats, feats), feats)
    return mm(hidden_ref[...], weight_ref[0, :, cols]).astype(bf16)


def near_kernel(count, me_ref, *refs):
    hiddens = refs[:count]
    down_ref, near_ref, *owns = refs[count:]
    feats = near_ref.shape[1]
    rows = near_ref.shape[0] // count
    for c, hidden in enumerate(hiddens):
        near_ref[pl.ds(c * rows, rows), :] = down_part(me_ref[0] ^ 1, hidden, down_ref, feats)
    for own, hidden in zip(owns, hiddens):
        own[...] = down_part(me_ref[0], hidden, down_ref, feats)


def join_kernel(count, senders, near_ref, *refs):
    out_ref = refs[-1]
    terms = (len(refs) - 1) // count
    part = near_ref.shape[0] // count
    chunk = part // senders
    for c in range(count):
        for e in range(senders):
            total = near_ref[pl.ds(c * part + e * chunk, chunk), :].astype(f32)
            for ref in refs[c * terms : (c + 1) * terms]:
                total = total + ref[pl.ds(e * chunk, chunk), :].astype(f32)
            out_ref[pl.ds((e * count + c) * chunk, chunk), :] = total.astype(bf16)


def reorder(rows, back):
    steps = rows // LANES
    row, col = iota((rows, rows), 1 if back else 0), iota((rows, rows), 0 if back else 1)
    return ones_where(col == (row % LANES) * steps + row // LANES)


def in_line(table, width):
    states = table.shape[1]
    wide = spread_table(table, states, 1, states, width)
    return jnp.sum(wide, axis=0, keepdims=True)


def sin_cos(angle):
    turns = jnp.floor(angle * 0.6366197723675814 + 0.5)
    rest = angle - turns * 1.5703125
    rest = rest - turns * 4.83751296997070312e-4
    rest = rest - turns * 7.54978995489188e-8
    z = rest * rest
    sine = rest + rest * z * (
        -1.6666654611e-1 + z * (8.3321608736e-3 + z * -1.9515295891e-4)
    )
    cosine = 1.0 - 0.5 * z + z * z * (
        4.166664568298827e-2 + z * (-1.388731625493765e-3 + z * 2.443315711809948e-5)
    )
    quarter = turns.astype(jnp.int32)
    odd = (quarter & 1) != 0
    first = jnp.where(odd, cosine, sine)
    second = jnp.where(odd, sine, cosine)
    first = jnp.where((quarter & 2) != 0, -first, first)
    second = jnp.where(((quarter + 1) & 2) != 0, -second, second)
    return first, second


def spread_table(table, inner, outer_rows, outer_cols, width):
    rows = table.shape[0]
    pick = ones_where(iota((inner, width), 1) % inner == iota((inner, width), 0))
    high, mid, low = split3(table)
    wide = mm(high, pick) + (mm(mid, pick) + mm(low, pick))
    same = iota((rows, width), 0) // outer_rows == iota((rows, width), 1) // outer_cols
    return jnp.where(same, wide, 0.0)


def poles_kernel(step_ref, pr_ref, pi_ref, ar_ref, ai_ref, over_ref):
    groups, states = pr_ref.shape
    rows, flat = ar_ref.shape
    order = reorder(rows, False)
    poles_re = in_line(pr_ref[...], flat)
    poles_im = in_line(pi_ref[...], flat)
    size = poles_re * poles_re + poles_im * poles_im
    over_ref[0:1, :] = poles_re / size
    over_ref[1:2, :] = -poles_im / size
    d_high, d_mid, d_low = (
        mm(part, order, NT).astype(bf16) for part in split3(step_ref[...])
    )
    piece = min(flat, 256)
    for at in range(0, flat, piece):
        cols = pl.ds(at, piece)
        expand = ones_where(
            iota((groups, piece), 0) == (iota((groups, piece), 1) + at) // states
        )
        delta = mm(d_high, expand, TN) + (mm(d_mid, expand, TN) + mm(d_low, expand, TN))
        size = jnp.exp(poles_re[:, at : at + piece] * delta)
        sine, cosine = sin_cos(poles_im[:, at : at + piece] * delta)
        ar_ref[:, cols] = size * cosine
        ai_ref[:, cols] = size * sine


def scan_kernel(
    total, parts, x_ref, gain_ref, ar_ref, ai_ref, over_ref, ir_ref, ii_ref, *refs,
):
    packs = refs[:parts]
    h_re_out, h_im_out, c_re_out, c_im_out, end_ref = refs[parts : parts + 5]
    hr_ref, hi_ref, cr_ref, ci_ref, sems = refs[parts + 5 :]
    rows, feats = x_ref.shape
    flat = ar_ref.shape[1]
    states = ir_ref.shape[1]
    inner = feats // (flat // states)
    steps = rows // LANES
    order = reorder(rows, False)
    packed = packs[0][:, : 2 * rows]
    for other in packs[1:]:
        packed = packed + other[:, : 2 * rows]
    mean = packed[:, :rows] / total
    scale = lax.rsqrt(packed[:, rows:] / total - mean * mean + norm_eps)
    match = iota((rows, rows), 1) == (iota((rows, rows), 0) % LANES) * steps + iota(
        (rows, rows), 0
    ) // LANES
    mean_col = jnp.sum(jnp.where(match, mean, 0.0), axis=1, keepdims=True)
    scale_col = jnp.sum(jnp.where(match, scale, 0.0), axis=1, keepdims=True)
    cw = min(feats, 256)
    sw = cw // inner * states
    copies = []
    for b in range(feats // cw):
        chans = pl.ds(b * cw, cw)
        cols = pl.ds(b * sw, sw)
        rows_in = mm(order, x_ref[:, chans])
        normed = split2((rows_in - mean_col) * scale_col * gain_ref[:, chans])
        real = split2(spread_table(ir_ref[chans, :], states, inner, states, sw))
        imag = split2(spread_table(ii_ref[chans, :], states, inner, states, sw))
        hr_ref[:, cols], hi_ref[:, cols] = mul(
            mm3(normed, real, NN), mm3(normed, imag, NN), over_ref[0:1, cols], over_ref[1:2, cols]
        )

        def body(j, carry):
            h_re, h_im, c_re, c_im = carry
            here = pl.ds(pl.multiple_of(j * LANES, LANES), LANES)
            a_re, a_im = ar_ref[here, cols], ai_ref[here, cols]
            d_re, d_im = hr_ref[here, cols], hi_ref[here, cols]
            h_re, h_im = mul(a_re, a_im, h_re + d_re, h_im + d_im)
            h_re, h_im = h_re - d_re, h_im - d_im
            c_re, c_im = mul(a_re, a_im, c_re, c_im)
            hr_ref[here, cols], hi_ref[here, cols] = h_re, h_im
            cr_ref[here, cols], ci_ref[here, cols] = c_re, c_im
            return h_re, h_im, c_re, c_im

        zero = jnp.zeros((LANES, sw), f32)
        lax.fori_loop(0, steps, body, (zero, zero, zero + 1.0, zero), unroll=2)
        for n, (ref, out) in enumerate((
            (hr_ref, h_re_out), (hi_ref, h_im_out), (cr_ref, c_re_out), (ci_ref, c_im_out),
        )):
            copies.append(
                pltpu.make_async_copy(ref.at[:, cols], out.at[:, cols], sems.at[b, n])
            )
            copies[-1].start()
    last = pl.ds(rows - LANES, LANES)
    h_re, h_im, c_re, c_im = hr_ref[last, :], hi_ref[last, :], cr_ref[last, :], ci_ref[last, :]
    p_re, p_im = c_re[0:1], c_im[0:1]
    s_re, s_im = h_re[0:1], h_im[0:1]
    for c in range(1, LANES):
        k_re, k_im = c_re[c : c + 1], c_im[c : c + 1]
        p_re, p_im = mul(k_re, k_im, p_re, p_im)
        s_re, s_im = mul(k_re, k_im, s_re, s_im)
        s_re, s_im = s_re + h_re[c : c + 1], s_im + h_im[c : c + 1]
    ends = jnp.concatenate([p_re, p_im, s_re, s_im], axis=0)
    for i in range(end_ref.shape[0]):
        end_ref[i] = ends
    for copy in copies:
        copy.wait()


def read_kernel(
    me_ref, got_ref, h_re_in, h_im_in, c_re_in, c_im_in, rr_ref, ri_ref, out_ref,
    hr_ref, hi_ref, cr_ref, ci_ref, sems,
):
    rows, flat = hr_ref.shape
    feats = out_ref.shape[1]
    states = rr_ref.shape[1]
    inner = feats // (flat // states)
    steps = rows // LANES
    me = me_ref[0]
    cw = min(feats, 256)
    sw = cw // inner * states
    last = pl.ds(rows - LANES, LANES)
    pairs = ((h_re_in, hr_ref), (h_im_in, hi_ref), (c_re_in, cr_ref), (c_im_in, ci_ref))
    loads = []
    for b in range(feats // cw):
        cols = pl.ds(b * sw, sw)
        loads.append([
            pltpu.make_async_copy(src.at[:, cols], ref.at[:, cols], sems.at[b, n])
            for n, (src, ref) in enumerate(pairs)
        ])
        for copy in loads[-1]:
            copy.start()
    s_re = jnp.zeros((1, flat), f32)
    s_im = jnp.zeros((1, flat), f32)
    for i in range(got_ref.shape[0] - 1):
        ends = got_ref[i]
        n_re, n_im = mul(ends[0:1], ends[1:2], s_re, s_im)
        s_re = jnp.where(i < me, n_re + ends[2:3], s_re)
        s_im = jnp.where(i < me, n_im + ends[3:4], s_im)
    back = reorder(rows, True)
    for b in range(feats // cw):
        chans = pl.ds(b * cw, cw)
        lo = b * sw
        cols = pl.ds(lo, sw)
        real = split2(spread_table(rr_ref[chans, :], states, inner, states, sw))
        imag = split2(spread_table(ri_ref[chans, :], states, inner, states, sw))
        for copy in loads[b]:
            copy.wait()
        h_re, h_im, c_re, c_im = (
            ref[last, cols] for ref in (hr_ref, hi_ref, cr_ref, ci_ref)
        )
        in_re, in_im = [s_re[:, lo : lo + sw]], [s_im[:, lo : lo + sw]]
        for c in range(LANES - 1):
            n_re, n_im = mul(c_re[c : c + 1], c_im[c : c + 1], in_re[-1], in_im[-1])
            in_re.append(n_re + h_re[c : c + 1])
            in_im.append(n_im + h_im[c : c + 1])
        g_re = jnp.concatenate(in_re, axis=0)[None]
        g_im = jnp.concatenate(in_im, axis=0)[None]
        shape = (steps, LANES, sw)
        c_re, c_im = cr_ref[:, cols].reshape(shape), ci_ref[:, cols].reshape(shape)
        f_re = hr_ref[:, cols].reshape(shape) + (c_re * g_re - c_im * g_im)
        f_im = hi_ref[:, cols].reshape(shape) + (c_re * g_im + c_im * g_re)
        response = mm3(split2(f_re.reshape(rows, sw)), real, NT) - mm3(
            split2(f_im.reshape(rows, sw)), imag, NT
        )
        cube = response + 0.044715 * (response * response * response)
        mixed = 0.5 * response * (1.0 + jnp.tanh(0.7978845608028654 * cube))
        out_ref[:, chans] = mm(back, mixed.astype(bf16)).astype(bf16)


def output_kernel(parts, me_ref, *refs):
    pieces = refs[:parts]
    value_ref, gate_ref, out_ref = refs[parts:]
    feats = pieces[0].shape[1]
    value = gate = None
    for k, piece in enumerate(pieces):
        at = pl.ds(pl.multiple_of((me_ref[0] ^ k) * feats, feats), feats)
        rows = piece[...]
        v, g = mm(rows, value_ref[at, :]), mm(rows, gate_ref[at, :])
        value, gate = (v, g) if value is None else (value + v, gate + g)
    out_ref[...] = (value * jax.nn.sigmoid(gate)).astype(bf16)


vmem = pl.BlockSpec(memory_space=pltpu.VMEM)
hbm = pl.BlockSpec(memory_space=pltpu.HBM)
smem = pl.BlockSpec(memory_space=pltpu.SMEM)


def stay(value):
    return pltpu.with_memory_space_constraint(value, pltpu.HBM)


def params(mib):
    return pltpu.CompilerParams(vmem_limit_bytes=mib << 20)


def swap(value, bit):
    count = lax.axis_size("tp")
    return lax.ppermute(value, "tp", [(i, i ^ bit) for i in range(count)])


def gather_tp(value):
    count = lax.axis_size("tp")
    blocks = {0: value}
    bit = count // 2
    while bit >= 1:
        blocks.update({k ^ bit: swap(block, bit) for k, block in list(blocks.items())})
        bit //= 2
    return [blocks[k] for k in range(count)]


def shards(
    mixer_input, mixer_gain, time_step, pole_real, pole_imag, input_real, input_imag,
    read_real, read_imag, out_value, out_gate, expert_input, expert_gain, routes,
    route_weight, expert_gate, expert_up, expert_down,
):
    n_tp, n_ep = lax.axis_size("tp"), lax.axis_size("ep")
    tp_at = lax.axis_index("tp").astype(jnp.int32).reshape(1)
    ep_at = lax.axis_index("ep").astype(jnp.int32).reshape(1)
    tokens, feats = expert_input.shape
    top = routes.shape[1]
    capacity = 2 * top * tokens // n_ep
    slots = n_ep * capacity
    routes_t = routes.T
    weight_t = route_weight.T

    rows, chans = mixer_input.shape
    send, packed = pl.pallas_call(
        functools.partial(send_kernel, n_ep, capacity),
        out_shape=(
            jax.ShapeDtypeStruct((slots, feats), bf16),
            jax.ShapeDtypeStruct((1, 2 * rows + feats), f32),
        ),
        in_specs=[vmem] * 4, out_specs=(vmem, vmem), compiler_params=params(60),
        name="send_rows",
    )(routes_t, expert_input, mixer_input, expert_gain.reshape(1, feats))
    arrived = lax.all_to_all(send, "ep", split_axis=0, concat_axis=0, tiled=True)
    packed, tp_at, ep_at = lax.optimization_barrier((packed, tp_at, ep_at))
    packs = gather_tp(packed)
    packs[0] = stay(packed)

    groups, states = pole_real.shape
    flat = groups * states
    big = jax.ShapeDtypeStruct((rows, flat), f32)
    a_re, a_im, over = pl.pallas_call(
        poles_kernel,
        out_shape=(big, big, jax.ShapeDtypeStruct((2, flat), f32)),
        in_specs=[vmem] * 3, out_specs=(vmem,) * 3, compiler_params=params(20),
        name="mixer_poles",
    )(stay(time_step.T), stay(pole_real), stay(pole_imag))
    n_block = max(1, chans // 256)
    far_big = pltpu.HBM((rows, flat), f32)
    *carried, ends = pl.pallas_call(
        functools.partial(scan_kernel, float(chans * n_tp), n_tp),
        out_shape=(far_big,) * 4 + (jax.ShapeDtypeStruct((n_ep, 4, flat), f32),),
        in_specs=[vmem] * (7 + n_tp), out_specs=(hbm,) * 4 + (vmem,),
        scratch_shapes=[pltpu.VMEM((rows, flat), f32)] * 4
        + [pltpu.SemaphoreType.DMA((n_block, 4))],
        compiler_params=params(24), name="mixer_scan",
    )(
        stay(mixer_input), stay(mixer_gain.reshape(1, chans)), a_re, a_im, over,
        stay(jnp.swapaxes(input_real, 1, 2).reshape(chans, states)),
        stay(jnp.swapaxes(input_imag, 1, 2).reshape(chans, states)),
        *packs,
    )
    n_half = 2 if capacity % 32 == 0 else 1
    half = capacity // n_half
    share = pl.pallas_call(
        functools.partial(share_kernel, n_ep, capacity),
        out_shape=jax.ShapeDtypeStruct((3, tokens, slots), bf16),
        in_specs=[vmem, vmem], out_specs=vmem, compiler_params=params(8), name="route_share",
    )(stay(routes_t), stay(weight_t))
    got = lax.all_to_all(ends, "ep", split_axis=0, concat_axis=0)

    units = expert_gate.shape[2]
    n_far = n_tp // 2 - 1
    part = n_ep * half
    by_sender = arrived.reshape(n_ep, capacity, feats)
    halves = [by_sender[:, c * half : (c + 1) * half].reshape(part, feats) for c in range(n_half)]
    far_blocks = []
    for c in range(n_half):
        evens = {0: halves[c]}
        bit = n_tp // 2
        while bit > 1:
            evens.update({k ^ bit: swap(b, bit) for k, b in list(evens.items())})
            bit //= 2
        far_blocks.append(evens)
    partner = swap(arrived, 1)
    weights = tuple(stay(w) for w in (expert_gate, expert_up, expert_down))
    n_unit = max(1, units // 256)
    hiddens, sums = [], []
    for c in range(n_half):
        blocks = [arrived, partner]
        for k in range(2, n_tp, 2):
            blocks += [far_blocks[c][k], swap(far_blocks[c][k], 1)]
        far_shape = jax.ShapeDtypeStruct((n_far, part, feats), bf16)
        load = c == 0
        kept = tuple(jax.ShapeDtypeStruct(w.shape, w.dtype) for w in weights) if load else ()
        hidden, odd_far, even_far, *held = pl.pallas_call(
            functools.partial(hidden_kernel, n_tp, n_ep, c * half, load),
            in_specs=[smem] + [vmem] * (2 * n_tp) + [hbm if load else vmem] * 3,
            out_specs=(vmem,) * (3 + len(kept)),
            scratch_shapes=[pltpu.VMEM((part, n_tp * feats), bf16)]
            + ([pltpu.SemaphoreType.DMA((3, n_unit))] if load else []),
            out_shape=(jax.ShapeDtypeStruct((part, units), bf16), far_shape, far_shape, *kept),
            compiler_params=params(12),
        )(tp_at, *packs, *blocks, *weights)
        weights = held or weights
        hiddens.append(hidden)
        theirs = swap(odd_far, 1)
        far = even_far.astype(f32) + theirs.astype(f32)
        come = []
        bit = n_tp // 4
        while bit >= 1:
            got_far = swap(far[bit - 1 :].astype(bf16), 2 * bit)
            come.append(got_far[0])
            far = far[: bit - 1] + got_far[1:].astype(f32)
            bit //= 2
        sums.append(come)
    near, *owns = pl.pallas_call(
        functools.partial(near_kernel, n_half),
        in_specs=[smem] + [vmem] * (n_half + 1), out_specs=(vmem,) * (n_half + 1),
        out_shape=(jax.ShapeDtypeStruct((slots, feats), bf16),)
        + (jax.ShapeDtypeStruct((part, feats), bf16),) * n_half,
        compiler_params=params(8), name="expert_near",
    )(tp_at, *hiddens, weights[2])
    near = swap(near, 1)
    terms = [term for own, come in zip(owns, sums) for term in (own, *come)]
    result = pl.pallas_call(
        functools.partial(join_kernel, n_half, n_ep),
        out_shape=jax.ShapeDtypeStruct((slots, feats), bf16),
        in_specs=[vmem] * (len(terms) + 1), out_specs=vmem, compiler_params=params(8),
        name="expert_join",
    )(near, *terms)
    back = lax.all_to_all(result, "ep", split_axis=0, concat_axis=0, tiled=True)

    mixed = pl.pallas_call(
        read_kernel,
        out_shape=jax.ShapeDtypeStruct((rows, chans), bf16),
        in_specs=[smem, vmem] + [hbm] * 4 + [vmem] * 2, out_specs=vmem,
        scratch_shapes=[pltpu.VMEM((rows, flat), f32)] * 4
        + [pltpu.SemaphoreType.DMA((n_block, 4))],
        compiler_params=params(20), name="mixer_read",
    )(
        ep_at, got, *(stay(x) for x in carried),
        stay(read_real.reshape(chans, states)), stay(read_imag.reshape(chans, states)),
    )
    pieces = gather_tp(mixed)
    value_w, gate_w = pl.pallas_call(
        fetch_kernel,
        out_shape=tuple(jax.ShapeDtypeStruct(w.shape, bf16) for w in (out_value, out_gate)),
        in_specs=[hbm] * 2, out_specs=(vmem,) * 2,
        scratch_shapes=[pltpu.SemaphoreType.DMA((2,))],
        compiler_params=params(10), name="out_fetch",
    )(stay(out_value), stay(out_gate))
    mixer_output = pl.pallas_call(
        functools.partial(output_kernel, n_tp),
        out_shape=jax.ShapeDtypeStruct((rows, out_value.shape[1]), bf16),
        in_specs=[smem] + [vmem] * (n_tp + 2), out_specs=vmem, compiler_params=params(10),
        name="mixer_out",
    )(tp_at, *pieces, value_w, gate_w)
    expert_output = pl.pallas_call(
        combine_kernel,
        out_shape=jax.ShapeDtypeStruct((tokens, feats), bf16),
        in_specs=[vmem] * 2, out_specs=vmem, compiler_params=params(8), name="combine",
    )(share, back)
    return mixer_output, expert_output


def solution(mesh):
    return jax.shard_map(
        shards,
        mesh=mesh,
        in_specs=(
            P("ep", "tp"), P("tp"), P("ep", "tp"), P("tp", None), P("tp", None),
            P("tp", None, None), P("tp", None, None), P("tp", None, None), P("tp", None, None),
            P(None, "tp"), P(None, "tp"), P("ep", "tp"), P("tp"), P("ep", None), P("ep", None),
            P("ep", None, "tp"), P("ep", None, "tp"), P("ep", "tp", None),
        ),
        out_specs=(P("ep", "tp"), P("ep", "tp")),
        check_vma=False,
    )
```

time: 103 us -> 102 us (level)
  blocking collectives: 27.1 us -> 21.8 us
  waiting for transfers between devices: 21.9 us -> 27 us
  Pallas kernels: 37.6 us -> 35.8 us
    all_gather x1 -> x0, blocking collectives: 5.32 us -> none  [shards(): packed = lax.all_gather(packed, 'tp')]
    ppermute x13 -> x16, waiting for transfers between devices: 15.6 us -> 20.7 us  [swap(): return lax.ppermute(value, 'tp', [(i, i ^ bit) for i in range(count)])]
    ppermute x13 -> x16, starting transfers between devices: 6.84 us -> 8.41 us  [swap(): return lax.ppermute(value, 'tp', [(i, i ^ bit) for i in range(count)])]
    pallas_call x1, Pallas kernels: 2.81 us -> 1.26 us  [shards(): pl.pallas_call(functools.partial(near_kernel, n_half), in_specs=[smem] +...]
    pallas_call x4 -> x5, Pallas kernels: 20.8 us -> 22.2 us  [the longest x2 10.7 us: shards(): pl.pallas_call(functools.partial(hidden_kernel, n_tp, n_ep, c * half, loa...]
    pallas_call x1, Pallas kernels: 2.28 us -> 1.1 us  [shards(): pl.pallas_call(functools.partial(share_kernel, n_ep, capacity), out_shape...]
  transfers between devices with their start and end apart: 15 -> 18, of which waited for: 4 -> 6; matrix products, arithmetic and copies ran while one was open for 0% -> 0% of each run, Pallas kernels for 34% -> 28%
where the time goes in v3:
time: 102 us; the launch traced here: 101 us
  Pallas kernels  35.8 us (35%)
  waiting for transfers between devices  27 us (26%)
  blocking collectives  21.8 us (21%)
  starting transfers between devices  15.7 us (15%)
    all_to_all x1, blocking collectives, shards(): lax.all_to_all(send, 'ep', split_axis=0, concat_axis=0, tiled=True)  21.8 us
    ppermute x16, waiting for transfers between devices, swap(): return lax.ppermute(value, 'tp', [(i, i ^ bit) for i in range(count)])  20.7 us
    pallas_call x2, Pallas kernels, shards(): pl.pallas_call(functools.partial(hidden_kernel, n_tp, n_ep, c * half, loa...  10.7 us
    ppermute x16, starting transfers between devices, swap(): return lax.ppermute(value, 'tp', [(i, i ^ bit) for i in range(count)])  8.41 us
    all_to_all x1, waiting for transfers between devices, shards(): got = lax.all_to_all(ends, 'ep', split_axis=0, concat_axis=0)  6.32 us
    pallas_call x1, Pallas kernels, shards(): pl.pallas_call(functools.partial(scan_kernel, float(chans * n_tp), n_tp),...  6.19 us
    pallas_call x1, Pallas kernels, shards(): pl.pallas_call(read_kernel, out_shape=jax.ShapeDtypeStruct((rows, chans),...  4.88 us
    all_to_all x1, starting transfers between devices, shards(): back = lax.all_to_all(result, 'ep', split_axis=0, concat_axis=0, tiled=True)  3.67 us
  transfers between devices with their start and end apart: 18, of which 6 were waited for; matrix products, arithmetic and copies ran while one was open for 0% of the time, Pallas kernels for 28%

profile of v3, /device:TPU:0, one launch (start us, length us, event | category | flops | bytes accessed | tf_op | source)
XLA Modules:
  0.0 101.3 jit_solution(15323782010875868631)
XLA Ops:
  0.6 2.3 %send_rows.1 = (bf16[512,512]{1,0:T(8,128)(2,1)}, f32[1,1024]{1,0:T(1,128)}) custom-call(s32[2,128]{1,0:T(2,128)} %bitcast.37, bf16[128,512]{1,0:T(8,128)(2,1)} %rows_ref.1, bf16[256,512]{1,0:T(8,128)(2,1)} %x_ref.3, f32[1,512]{1,0:T(1,128)} %bitcast.39), custom_call_target="tpu_custom_call" | custom-call | tf_op jit(solution)/shard_map/send_rows/pallas_call | solution.py:476
  3.0 21.8 %all_to_all.27 = bf16[8,64,512]{2,1,0:T(8,128)(2,1)S(1)} all-to-all(bf16[8,64,512]{2,1,0:T(8,128)(2,1)} %bitcast.29), channel_id=1, replica_groups=mesh['ep'=8,'tp'=4] {'ep'}, dimensions={0} | all-to-all | bytes 1048576 | tf_op jit(solution)/shard_map/all_to_all | solution.py:485
  24.8 0.0 collective-permute-start.6
  24.8 1.6 %collective-permute-start.7 = (bf16[256,512]{1,0:T(8,128)(2,1)S(1)}, bf16[256,512]{1,0:T(8,128)(2,1)S(1)}, u32[]{:S(2)}, u32[]{:S(2)}) collective-permute-start(bf16[256,512]{1,0:T(8,128)(2,1)S(1)} %bitcast.33), channel_id=1, source_target_pairs={{0,2},{1,3},{2,0},{3,1},{4,6},{5,7},{6,4},{7,5},{8,10},{9,11},{10,... | collective-permute-start | bytes 786440 | tf_op jit(solution)/shard_map/ppermute | solution.py:447
  26.4 0.5 collective-permute-start.9
  26.9 7.2 %collective-permute-done.7.refs_6_ = bf16[256,512]{1,0:T(8,128)(2,1)S(1)} collective-permute-done((bf16[256,512]{1,0:T(8,128)(2,1)S(1)}, bf16[256,512]{1,0:T(8,128)(2,1)S(1)}, u32[]{:S(2)}, u32[]{:S(2)}) %collective-permute-start.7) | collective-permute-done | bytes 262176 | tf_op jit(solution)/shard_map/ppermute | solution.py:447
  34.1 0.0 collective-permute-start.8
  34.1 5.2 %collective-permute-done.9.refs_6_ = bf16[256,512]{1,0:T(8,128)(2,1)S(1)} collective-permute-done((bf16[256,512]{1,0:T(8,128)(2,1)S(1)}, bf16[256,512]{1,0:T(8,128)(2,1)S(1)}, u32[]{:S(2)}, u32[]{:S(2)}) %collective-permute-start.9) | collective-permute-done | bytes 262176 | tf_op jit(solution)/shard_map/ppermute | solution.py:447
  39.2 0.0 collective-permute-start.10
  39.2 1.5 %collective-permute-start.1 = (f32[1,1024]{1,0:T(1,128)}, f32[1,1024]{1,0:T(1,128)S(1)}, u32[]{:S(2)}, u32[]{:S(2)}) collective-permute-start(f32[1,1024]{1,0:T(1,128)} %get-tuple-element.35.refs_0_), channel_id=1, source_target_pairs={{0,2},{1,3},{2,0},{3,1},{4,6},{5,7},{6,4},{7,5},{8,10},{9,11},{10,... | collective-permute-start | bytes 12296 | tf_op jit(solution)/shard_map/ppermute | solution.py:447
  40.7 0.2 collective-permute-start
  41.0 2.1 %collective-permute-done.1.refs_2_ = f32[1,1024]{1,0:T(1,128)S(1)} collective-permute-done((f32[1,1024]{1,0:T(1,128)}, f32[1,1024]{1,0:T(1,128)S(1)}, u32[]{:S(2)}, u32[]{:S(2)}) %collective-permute-start.1) | collective-permute-done | bytes 4128 | tf_op jit(solution)/shard_map/ppermute | solution.py:447
  43.0 0.0 collective-permute-start.2
  43.0 0.0 collective-permute-done.refs_1_
  43.0 1.2 %collective-permute-done.2.refs_3_ = f32[1,1024]{1,0:T(1,128)S(1)} collective-permute-done((f32[1,1024]{1,0:T(1,128)S(1)}, f32[1,1024]{1,0:T(1,128)S(1)}, u32[]{:S(2)}, u32[]{:S(2)}) %collective-permute-start.2) | collective-permute-done | bytes 4128 | tf_op jit(solution)/shard_map/ppermute | solution.py:447
  44.2 0.0 collective-permute-done.6.refs_5_
  44.2 0.0 collective-permute-done.8.refs_7_
  44.2 6.3 %shard_map.185 = (bf16[256,1024]{1,0:T(8,128)(2,1)S(1)}, bf16[1,256,512]{2,1,0:T(8,128)(2,1)S(1)}, bf16[1,256,512]{2,1,0:T(8,128)(2,1)S(1)}, bf16[1,2048,1024]{2...) custom-call(s32[1]{0:T(128)} %bitcast.2.me_ref, ...), custom_call_target="tpu_custom_call" | custom-call | tf_op jit(solution)/shard_map/pallas_call | solution.py:547
  50.5 0.0 collective-permute-done.10.refs_7_
  50.5 4.4 %shard_map.186 = (bf16[256,1024]{1,0:T(8,128)(2,1)S(1)}, bf16[1,256,512]{2,1,0:T(8,128)(2,1)S(1)}, bf16[1,256,512]{2,1,0:T(8,128)(2,1)S(1)}) custom-call(s32[1]{0:T(128)} %bitcast.2.me_ref, f32[1,1024]{1,0:T(1,128)} %get-tuple-element.35.refs_0_, f32[1,1024]{1,0:T(1,128)S(1)} %collective-permute-done.refs_1_, f32[1,1024]{1,0:T(1,128)S(1)} %collective-permute-done.1.refs_2_, ...), custom_call_target="tpu_custom_call" | custom-call | tf_op jit(solution)/shard_map/pallas_call | solution.py:547
  55.0 0.2 collective-permute-start.14
  55.2 0.3 collective-permute-start.12
  55.5 1.3 %expert_near.1 = (bf16[512,512]{1,0:T(8,128)(2,1)S(1)}, bf16[256,512]{1,0:T(8,128)(2,1)S(1)}, bf16[256,512]{1,0:T(8,128)(2,1)S(1)}) custom-call(s32[1]{0:T(128)} %bitcast.2.me_ref, bf16[256,1024]{1,0:T(8,128)(2,1)S(1)} %get-tuple-element.44.refs_0_, bf16[256,1024]{1,0:T(8,128)(2,1)S(1)} %get-tuple-element.48.refs_1_, ...), custom_call_target="tpu_custom_call" | custom-call | tf_op jit(solution)/shard_map/expert_near/pallas_call | solution.py:568
  56.8 0.2 collective-permute-start.11
  57.1 0.0 collective-permute-done.14
  57.1 0.1 add_convert_fusion
  57.1 1.6 %collective-permute-start.15 = (bf16[1,256,512]{2,1,0:T(8,128)(2,1)S(1)}, bf16[1,256,512]{2,1,0:T(8,128)(2,1)S(1)}, u32[]{:S(2)}, u32[]{:S(2)}) collective-permute-start(bf16[1,256,512]{2,1,0:T(8,128)(2,1)S(1)} %add_convert_fusion), channel_id=1, source_target_pairs={{0,2},{1,3},{2,0},{3,1},{4,6},{5,7},{6,4},{7,5},{8,10},{9,11},{10,... | collective-permute-start | bytes 786440 | tf_op jit(solution)/shard_map/ppermute | solution.py:447
  58.7 0.0 collective-permute-done.12
  58.7 0.1 add_convert_fusion.1
  58.8 0.6 collective-permute-start.13
  59.4 3.1 %mixer_poles.1 = (f32[256,1024]{1,0:T(8,128)S(1)}, f32[256,1024]{1,0:T(8,128)S(1)}, f32[2,1024]{1,0:T(2,128)S(1)}) custom-call(f32[32,256]{1,0:T(8,128)} %bitcast.36, f32[32,32]{1,0:T(8,128)} %pr_ref.1, f32[32,32]{1,0:T(8,128)} %pi_ref.1), custom_call_target="tpu_custom_call" | custom-call | tf_op jit(solution)/shard_map/mixer_poles/pallas_call | solution.py:493
  62.4 6.2 %mixer_scan.1 = (f32[256,1024]{1,0:T(8,128)}, f32[256,1024]{1,0:T(8,128)}, f32[256,1024]{1,0:T(8,128)}, f32[256,1024]{1,0:T(8,128)}, f32[8,4,1024]{2,1,0:T(4,128)}) custom-call(bf16[256,512]{1,0:T(8,128)(2,1)} %x_ref.3, f32[1,512]{1,0:T(1,128)} %bitcast.40, f32[256,1024]{1,0:T(8,128)S(1)} %get-tuple-element.32.ar_ref, ...), custom_call_target="tpu_custom_call" | custom-call | tf_op jit(solution)/shard_map/mixer_scan/pallas_call | solution.py:501
  68.6 3.6 %all-to-all-start = ((f32[8,4,1024]{2,1,0:T(4,128)}), f32[8,4,1024]{2,1,0:T(4,128)S(1)}, u32[]{:S(2)}, u32[]{:S(2)}) async-start(f32[8,4,1024]{2,1,0:T(4,128)} %get-tuple-element.36), calls=%async_computation | async-start | bytes 262144 | tf_op jit(solution)/shard_map/all_to_all | solution.py:521
  72.2 0.0 collective-permute-done.15
  72.2 0.0 collective-permute-done.13
  72.2 0.0 collective-permute-done.11.near_ref
  72.2 1.0 expert_join.1
  73.2 6.3 %all-to-all-done.got_ref = f32[8,4,1024]{2,1,0:T(4,128)S(1)} async-done(((f32[8,4,1024]{2,1,0:T(4,128)}), f32[8,4,1024]{2,1,0:T(4,128)S(1)}, u32[]{:S(2)}, u32[]{:S(2)}) %all-to-all-start) | async-done | bytes 131104 | tf_op jit(solution)/shard_map/all_to_all | solution.py:521
  79.6 3.7 %all-to-all-start.2 = ((bf16[8,64,512]{2,1,0:T(8,128)(2,1)}), bf16[8,64,512]{2,1,0:T(8,128)(2,1)S(1)}, u32[]{:S(2)}, u32[]{:S(2)}) async-start(bf16[8,64,512]{2,1,0:T(8,128)(2,1)} %bitcast.19), calls=%async_computation.2 | async-start | bytes 1048576 | tf_op jit(solution)/shard_map/all_to_all | solution.py:583
  83.2 4.9 %mixer_read.1.refs_0_ = bf16[256,512]{1,0:T(8,128)(2,1)S(1)} custom-call(s32[1]{0:T(128)} %bitcast.3.me_ref, f32[8,4,1024]{2,1,0:T(4,128)S(1)} %all-to-all-done.got_ref, f32[256,1024]{1,0:T(8,128)} %get-tuple-element.37.h_re_in, f32[256,1024]{1,0:T(8,128)} %get-tuple-element.38.h_im_in, f32[256,1024]{1,0:T(8,128)} %get-tuple-element.39.c_re_in, ...), custom_call_target="tpu_custom_call" | custom-call | tf_op jit(solution)/shard_map/mixer_read/pallas_call | solution.py:585
  88.1 1.6 %collective-permute-start.4 = (bf16[256,512]{1,0:T(8,128)(2,1)S(1)}, bf16[256,512]{1,0:T(8,128)(2,1)S(1)}, u32[]{:S(2)}, u32[]{:S(2)}) collective-permute-start(bf16[256,512]{1,0:T(8,128)(2,1)S(1)} %mixer_read.1.refs_0_), channel_id=1, source_target_pairs={{0,2},{1,3},{2,0},{3,1},{4,6},{5,7},{6,4},{7,5},{8,10},{9,11},{10,... | collective-permute-start | bytes 786440 | tf_op jit(solution)/shard_map/ppermute | solution.py:447
  89.7 0.0 collective-permute-start.3
  89.7 5.1 %collective-permute-done.4.refs_2_ = bf16[256,512]{1,0:T(8,128)(2,1)S(1)} collective-permute-done((bf16[256,512]{1,0:T(8,128)(2,1)S(1)}, bf16[256,512]{1,0:T(8,128)(2,1)S(1)}, u32[]{:S(2)}, u32[]{:S(2)}) %collective-permute-start.4) | collective-permute-done | bytes 262176 | tf_op jit(solution)/shard_map/ppermute | solution.py:447
  94.9 0.0 collective-permute-start.5
  94.9 1.1 %route_share.1.share_ref = bf16[3,128,512]{2,1,0:T(8,128)(2,1)S(1)} custom-call(s32[2,128]{1,0:T(2,128)} %bitcast.38, f32[2,128]{1,0:T(2,128)} %bitcast.41), custom_call_target="tpu_custom_call" | custom-call | tf_op jit(solution)/shard_map/route_share/pallas_call | solution.py:516
  96.0 2.2 %out_fetch.1 = (bf16[2048,512]{1,0:T(8,128)(2,1)S(1)}, bf16[2048,512]{1,0:T(8,128)(2,1)S(1)}) custom-call(bf16[2048,512]{1,0:T(8,128)(2,1)} %refs_0_.1, bf16[2048,512]{1,0:T(8,128)(2,1)} %refs_1_.1), custom_call_target="tpu_custom_call" | custom-call | tf_op jit(solution)/shard_map/out_fetch/pallas_call | solution.py:597
  98.2 0.0 collective-permute-done.3.refs_1_
  98.2 0.0 collective-permute-done.5.refs_3_
  98.2 2.0 %mixer_out.1 = bf16[256,512]{1,0:T(8,128)(2,1)} custom-call(s32[1]{0:T(128)} %bitcast.2.me_ref, bf16[256,512]{1,0:T(8,128)(2,1)S(1)} %mixer_read.1.refs_0_, bf16[256,512]{1,0:T(8,128)(2,1)S(1)} %collective-permute-done.3.refs_1_, bf16[256,512]{1,0:T(8,128)(2,1)S(1)} %collective-permute-done.4.refs_2_, bf16[256,512]{1,0:T(8,128)(2,1)S(1)} %collective-permute-done.5.refs_3_, ...), custom_call_target="tpu_custom_call" | custom-call | tf_op jit(solution)/shard_map/mixer_out/pallas_call | solution.py:604
  100.2 0.0 all-to-all-done.2
  100.2 1.0 %combine.1 = bf16[128,512]{1,0:T(8,128)(2,1)} custom-call(bf16[3,128,512]{2,1,0:T(8,128)(2,1)S(1)} %route_share.1.share_ref, bf16[512,512]{1,0:T(8,128)(2,1)S(1)} %bitcast.26), custom_call_target="tpu_custom_call" | custom-call | tf_op jit(solution)/shard_map/combine/pallas_call | solution.py:610
  (1 shorter events, 0.0 us)
Async XLA Ops:
  24.8 19.4 %collective-permute-start.6 = (bf16[512,512]{1,0:T(8,128)(2,1)S(1)}, bf16[512,512]{1,0:T(8,128)(2,1)S(1)}, u32[]{:S(2)}, u32[]{:S(2)}) collective-permute-start(bf16[512,512]{1,0:T(8,128)(2,1)S(1)} %bitcast.23), channel_id=1, source_target_pairs={{0,1},{1,0},{2,3},{3,2},{4,5},{5,4},{6,7},{7,6},{8,9},{9,8},{10,11... | collective-permute-start | bytes 1572872 | tf_op jit(solution)/shard_map/ppermute | solution.py:447
  24.8 9.2 %collective-permute-start.7 = (bf16[256,512]{1,0:T(8,128)(2,1)S(1)}, bf16[256,512]{1,0:T(8,128)(2,1)S(1)}, u32[]{:S(2)}, u32[]{:S(2)}) collective-permute-start(bf16[256,512]{1,0:T(8,128)(2,1)S(1)} %bitcast.33), channel_id=1, source_target_pairs={{0,2},{1,3},{2,0},{3,1},{4,6},{5,7},{6,4},{7,5},{8,10},{9,11},{10,... | collective-permute-start | bytes 786440 | tf_op jit(solution)/shard_map/ppermute | solution.py:447
  26.4 12.8 %collective-permute-start.9 = (bf16[256,512]{1,0:T(8,128)(2,1)S(1)}, bf16[256,512]{1,0:T(8,128)(2,1)S(1)}, u32[]{:S(2)}, u32[]{:S(2)}) collective-permute-start(bf16[256,512]{1,0:T(8,128)(2,1)S(1)} %bitcast.32), channel_id=1, source_target_pairs={{0,2},{1,3},{2,0},{3,1},{4,6},{5,7},{6,4},{7,5},{8,10},{9,11},{10,... | collective-permute-start | bytes 786440 | tf_op jit(solution)/shard_map/ppermute | solution.py:447
  34.1 10.2 %collective-permute-start.8 = (bf16[256,512]{1,0:T(8,128)(2,1)S(1)}, bf16[256,512]{1,0:T(8,128)(2,1)S(1)}, u32[]{:S(2)}, u32[]{:S(2)}) collective-permute-start(bf16[256,512]{1,0:T(8,128)(2,1)S(1)} %collective-permute-done.7.refs_6_), channel_id=1, source_target_pairs={{0,1},{1,0},{2,3},{3,2},{4,5},{5,4},{6,7},{7,6},{8,9},{9,8},{10,11... | collective-permute-start | bytes 786440 | tf_op jit(solution)/shard_map/ppermute | solution.py:447
  39.2 11.3 %collective-permute-start.10 = (bf16[256,512]{1,0:T(8,128)(2,1)S(1)}, bf16[256,512]{1,0:T(8,128)(2,1)S(1)}, u32[]{:S(2)}, u32[]{:S(2)}) collective-permute-start(bf16[256,512]{1,0:T(8,128)(2,1)S(1)} %collective-permute-done.9.refs_6_), channel_id=1, source_target_pairs={{0,1},{1,0},{2,3},{3,2},{4,5},{5,4},{6,7},{7,6},{8,9},{9,8},{10,11... | collective-permute-start | bytes 786440 | tf_op jit(solution)/shard_map/ppermute | solution.py:447
  39.2 3.8 %collective-permute-start.1 = (f32[1,1024]{1,0:T(1,128)}, f32[1,1024]{1,0:T(1,128)S(1)}, u32[]{:S(2)}, u32[]{:S(2)}) collective-permute-start(f32[1,1024]{1,0:T(1,128)} %get-tuple-element.35.refs_0_), channel_id=1, source_target_pairs={{0,2},{1,3},{2,0},{3,1},{4,6},{5,7},{6,4},{7,5},{8,10},{9,11},{10,... | collective-permute-start | bytes 12296 | tf_op jit(solution)/shard_map/ppermute | solution.py:447
  40.7 2.3 %collective-permute-start = (f32[1,1024]{1,0:T(1,128)}, f32[1,1024]{1,0:T(1,128)S(1)}, u32[]{:S(2)}, u32[]{:S(2)}) collective-permute-start(f32[1,1024]{1,0:T(1,128)} %get-tuple-element.35.refs_0_), channel_id=1, source_target_pairs={{0,1},{1,0},{2,3},{3,2},{4,5},{5,4},{6,7},{7,6},{8,9},{9,8},{10,11... | collective-permute-start | bytes 12296 | tf_op jit(solution)/shard_map/ppermute | solution.py:447
  43.0 1.2 %collective-permute-start.2 = (f32[1,1024]{1,0:T(1,128)S(1)}, f32[1,1024]{1,0:T(1,128)S(1)}, u32[]{:S(2)}, u32[]{:S(2)}) collective-permute-start(f32[1,1024]{1,0:T(1,128)S(1)} %collective-permute-done.1.refs_2_), channel_id=1, source_target_pairs={{0,1},{1,0},{2,3},{3,2},{4,5},{5,4},{6,7},{7,6},{8,9},{9,8},{10,11... | collective-permute-start | bytes 12296 | tf_op jit(solution)/shard_map/ppermute | solution.py:447
  55.0 2.1 %collective-permute-start.14 = (bf16[1,256,512]{2,1,0:T(8,128)(2,1)S(1)}, bf16[1,256,512]{2,1,0:T(8,128)(2,1)S(1)}, u32[]{:S(2)}, u32[]{:S(2)}) collective-permute-start(bf16[1,256,512]{2,1,0:T(8,128)(2,1)S(1)} %get-tuple-element.55), channel_id=1, source_target_pairs={{0,1},{1,0},{2,3},{3,2},{4,5},{5,4},{6,7},{7,6},{8,9},{9,8},{10,11... | collective-permute-start | bytes 786440 | tf_op jit(solution)/shard_map/ppermute | solution.py:447
  55.2 3.5 %collective-permute-start.12 = (bf16[1,256,512]{2,1,0:T(8,128)(2,1)S(1)}, bf16[1,256,512]{2,1,0:T(8,128)(2,1)S(1)}, u32[]{:S(2)}, u32[]{:S(2)}) collective-permute-start(bf16[1,256,512]{2,1,0:T(8,128)(2,1)S(1)} %get-tuple-element.52), channel_id=1, source_target_pairs={{0,1},{1,0},{2,3},{3,2},{4,5},{5,4},{6,7},{7,6},{8,9},{9,8},{10,11... | collective-permute-start | bytes 786440 | tf_op jit(solution)/shard_map/ppermute | solution.py:447
  56.8 15.4 %collective-permute-start.11 = (bf16[512,512]{1,0:T(8,128)(2,1)S(1)}, bf16[512,512]{1,0:T(8,128)(2,1)S(1)}, u32[]{:S(2)}, u32[]{:S(2)}) collective-permute-start(bf16[512,512]{1,0:T(8,128)(2,1)S(1)} %get-tuple-element.49), channel_id=1, source_target_pairs={{0,1},{1,0},{2,3},{3,2},{4,5},{5,4},{6,7},{7,6},{8,9},{9,8},{10,11... | collective-permute-start | bytes 1572872 | tf_op jit(solution)/shard_map/ppermute | solution.py:447
  57.1 15.1 %collective-permute-start.15 = (bf16[1,256,512]{2,1,0:T(8,128)(2,1)S(1)}, bf16[1,256,512]{2,1,0:T(8,128)(2,1)S(1)}, u32[]{:S(2)}, u32[]{:S(2)}) collective-permute-start(bf16[1,256,512]{2,1,0:T(8,128)(2,1)S(1)} %add_convert_fusion), channel_id=1, source_target_pairs={{0,2},{1,3},{2,0},{3,1},{4,6},{5,7},{6,4},{7,5},{8,10},{9,11},{10,... | collective-permute-start | bytes 786440 | tf_op jit(solution)/shard_map/ppermute | solution.py:447
  58.8 13.4 %collective-permute-start.13 = (bf16[1,256,512]{2,1,0:T(8,128)(2,1)S(1)}, bf16[1,256,512]{2,1,0:T(8,128)(2,1)S(1)}, u32[]{:S(2)}, u32[]{:S(2)}) collective-permute-start(bf16[1,256,512]{2,1,0:T(8,128)(2,1)S(1)} %add_convert_fusion.1), channel_id=1, source_target_pairs={{0,2},{1,3},{2,0},{3,1},{4,6},{5,7},{6,4},{7,5},{8,10},{9,11},{10,... | collective-permute-start | bytes 786440 | tf_op jit(solution)/shard_map/ppermute | solution.py:447
  68.6 10.9 %all-to-all-start = ((f32[8,4,1024]{2,1,0:T(4,128)}), f32[8,4,1024]{2,1,0:T(4,128)S(1)}, u32[]{:S(2)}, u32[]{:S(2)}) async-start(f32[8,4,1024]{2,1,0:T(4,128)} %get-tuple-element.36), calls=%async_computation | async-start | bytes 262144 | tf_op jit(solution)/shard_map/all_to_all | solution.py:521
  79.6 20.7 %all-to-all-start.2 = ((bf16[8,64,512]{2,1,0:T(8,128)(2,1)}), bf16[8,64,512]{2,1,0:T(8,128)(2,1)S(1)}, u32[]{:S(2)}, u32[]{:S(2)}) async-start(bf16[8,64,512]{2,1,0:T(8,128)(2,1)} %bitcast.19), calls=%async_computation.2 | async-start | bytes 1048576 | tf_op jit(solution)/shard_map/all_to_all | solution.py:583
  88.1 6.7 %collective-permute-start.4 = (bf16[256,512]{1,0:T(8,128)(2,1)S(1)}, bf16[256,512]{1,0:T(8,128)(2,1)S(1)}, u32[]{:S(2)}, u32[]{:S(2)}) collective-permute-start(bf16[256,512]{1,0:T(8,128)(2,1)S(1)} %mixer_read.1.refs_0_), channel_id=1, source_target_pairs={{0,2},{1,3},{2,0},{3,1},{4,6},{5,7},{6,4},{7,5},{8,10},{9,11},{10,... | collective-permute-start | bytes 786440 | tf_op jit(solution)/shard_map/ppermute | solution.py:447
  89.7 8.5 %collective-permute-start.3 = (bf16[256,512]{1,0:T(8,128)(2,1)S(1)}, bf16[256,512]{1,0:T(8,128)(2,1)S(1)}, u32[]{:S(2)}, u32[]{:S(2)}) collective-permute-start(bf16[256,512]{1,0:T(8,128)(2,1)S(1)} %mixer_read.1.refs_0_), channel_id=1, source_target_pairs={{0,1},{1,0},{2,3},{3,2},{4,5},{5,4},{6,7},{7,6},{8,9},{9,8},{10,11... | collective-permute-start | bytes 786440 | tf_op jit(solution)/shard_map/ppermute | solution.py:447
  94.9 3.4 %collective-permute-start.5 = (bf16[256,512]{1,0:T(8,128)(2,1)S(1)}, bf16[256,512]{1,0:T(8,128)(2,1)S(1)}, u32[]{:S(2)}, u32[]{:S(2)}) collective-permute-start(bf16[256,512]{1,0:T(8,128)(2,1)S(1)} %collective-permute-done.4.refs_2_), channel_id=1, source_target_pairs={{0,1},{1,0},{2,3},{3,2},{4,5},{5,4},{6,7},{7,6},{8,9},{9,8},{10,11... | collective-permute-start | bytes 786440 | tf_op jit(solution)/shard_map/ppermute | solution.py:447

commit v4 on v3

--- a/solution.py
+++ b/solution.py
@@ -115,19 +115,10 @@
     out_ref[...] = out.astype(bf16)
 
 
-def hidden_kernel(parts, senders, start, load, me_ref, *refs):
+def hidden_kernel(parts, senders, start, me_ref, *refs):
     packs = refs[:parts]
     blocks = refs[parts : 2 * parts]
-    if load:
-        sources = refs[2 * parts : 2 * parts + 3]
-        hidden_ref, odd_ref, even_ref, gate_ref, up_ref, down_ref = refs[
-            2 * parts + 3 : 2 * parts + 9
-        ]
-        normed_ref, sems = refs[2 * parts + 9 :]
-    else:
-        gate_ref, up_ref, down_ref, hidden_ref, odd_ref, even_ref, normed_ref = refs[
-            2 * parts :
-        ]
+    gate_ref, up_ref, down_ref, hidden_ref, odd_ref, normed_ref = refs[2 * parts :]
     rows, units = hidden_ref.shape
     full, feats = blocks[0].shape
     width = parts * feats
@@ -135,20 +126,6 @@
     me = me_ref[0]
     lead = packs[0].shape[1] - feats
     size = min(units, 256)
-    loads = []
-    if load:
-        for n in range(units // size):
-            cols = pl.ds(n * size, size)
-            loads.append([
-                pltpu.make_async_copy(
-                    sources[m].at[0, :, cols], ref.at[0, :, cols], sems.at[m, n]
-                )
-                for m, ref in enumerate((gate_ref, up_ref))
-            ])
-        loads.append([pltpu.make_async_copy(sources[2], down_ref, sems.at[2, 0])])
-        for group in loads:
-            for copy in group:
-                copy.start()
 
     def body(sender, unused):
         here = pl.ds(pl.multiple_of(sender * chunk, chunk), chunk)
@@ -169,21 +146,15 @@
             normed_ref[here, cols] = value.astype(bf16)
         return unused
 
-    lax.fori_loop(0, senders, body, 0, unroll=2)
+    lax.fori_loop(0, senders, body, 0, unroll=4)
     for at in range(0, units, size):
         cols = pl.ds(at, size)
-        if load:
-            for copy in loads[at // size]:
-                copy.wait()
         normed = normed_ref[...]
         gate = mm(normed, gate_ref[0, :, cols])
         up = mm(normed, up_ref[0, :, cols])
         hidden_ref[:, cols] = (gate * jax.nn.sigmoid(gate) * up).astype(bf16)
-    if load:
-        loads[-1][0].wait()
-    for first, out in ((3, odd_ref), (2, even_ref)):
-        for n in range(out.shape[0]):
-            out[n] = down_part(me ^ (2 * n + first), hidden_ref, down_ref, feats)
+    for n in range(odd_ref.shape[0]):
+        odd_ref[n] = down_part(me ^ (2 * n + 3), hidden_ref, down_ref, feats)
 
 
 def down_part(which, hidden_ref, weight_ref, feats):
@@ -191,27 +162,25 @@
     return mm(hidden_ref[...], weight_ref[0, :, cols]).astype(bf16)
 
 
-def near_kernel(count, me_ref, *refs):
-    hiddens = refs[:count]
-    down_ref, near_ref, *owns = refs[count:]
+def rest_kernel(me_ref, hidden_ref, down_ref, even_ref, near_ref, own_ref):
+    me = me_ref[0]
     feats = near_ref.shape[1]
-    rows = near_ref.shape[0] // count
-    for c, hidden in enumerate(hiddens):
-        near_ref[pl.ds(c * rows, rows), :] = down_part(me_ref[0] ^ 1, hidden, down_ref, feats)
-    for own, hidden in zip(owns, hiddens):
-        own[...] = down_part(me_ref[0], hidden, down_ref, feats)
-
-
-def join_kernel(count, senders, near_ref, *refs):
+    for n in range(even_ref.shape[0]):
+        even_ref[n] = down_part(me ^ (2 * n + 2), hidden_ref, down_ref, feats)
+    near_ref[...] = down_part(me ^ 1, hidden_ref, down_ref, feats)
+    own_ref[...] = down_part(me, hidden_ref, down_ref, feats)
+
+
+def join_kernel(count, senders, *refs):
     out_ref = refs[-1]
     terms = (len(refs) - 1) // count
-    part = near_ref.shape[0] // count
-    chunk = part // senders
+    chunk = refs[0].shape[0] // senders
     for c in range(count):
         for e in range(senders):
-            total = near_ref[pl.ds(c * part + e * chunk, chunk), :].astype(f32)
+            total = None
             for ref in refs[c * terms : (c + 1) * terms]:
-                total = total + ref[pl.ds(e * chunk, chunk), :].astype(f32)
+                term = ref[pl.ds(e * chunk, chunk), :].astype(f32)
+                total = term if total is None else total + term
             out_ref[pl.ds((e * count + c) * chunk, chunk), :] = total.astype(bf16)
 
 
@@ -534,52 +503,53 @@
             bit //= 2
         far_blocks.append(evens)
     partner = swap(arrived, 1)
-    weights = tuple(stay(w) for w in (expert_gate, expert_up, expert_down))
-    n_unit = max(1, units // 256)
-    hiddens, sums = [], []
+
+    def fetch(*weights):
+        return pl.pallas_call(
+            fetch_kernel,
+            out_shape=tuple(jax.ShapeDtypeStruct(w.shape, w.dtype) for w in weights),
+            in_specs=[hbm] * len(weights), out_specs=(vmem,) * len(weights),
+            scratch_shapes=[pltpu.SemaphoreType.DMA((len(weights),))],
+            compiler_params=params(10),
+        )(*(stay(w) for w in weights))
+
+    gate_w, up_w = fetch(expert_gate, expert_up)
+    (down_w,) = fetch(expert_down)
+    terms = []
     for c in range(n_half):
         blocks = [arrived, partner]
         for k in range(2, n_tp, 2):
             blocks += [far_blocks[c][k], swap(far_blocks[c][k], 1)]
         far_shape = jax.ShapeDtypeStruct((n_far, part, feats), bf16)
-        load = c == 0
-        kept = tuple(jax.ShapeDtypeStruct(w.shape, w.dtype) for w in weights) if load else ()
-        hidden, odd_far, even_far, *held = pl.pallas_call(
-            functools.partial(hidden_kernel, n_tp, n_ep, c * half, load),
-            in_specs=[smem] + [vmem] * (2 * n_tp) + [hbm if load else vmem] * 3,
-            out_specs=(vmem,) * (3 + len(kept)),
-            scratch_shapes=[pltpu.VMEM((part, n_tp * feats), bf16)]
-            + ([pltpu.SemaphoreType.DMA((3, n_unit))] if load else []),
-            out_shape=(jax.ShapeDtypeStruct((part, units), bf16), far_shape, far_shape, *kept),
+        part_shape = jax.ShapeDtypeStruct((part, feats), bf16)
+        hidden, odd_far = pl.pallas_call(
+            functools.partial(hidden_kernel, n_tp, n_ep, c * half),
+            in_specs=[smem] + [vmem] * (2 * n_tp + 3), out_specs=(vmem,) * 2,
+            scratch_shapes=[pltpu.VMEM((part, n_tp * feats), bf16)],
+            out_shape=(jax.ShapeDtypeStruct((part, units), bf16), far_shape),
             compiler_params=params(12),
-        )(tp_at, *packs, *blocks, *weights)
-        weights = held or weights
-        hiddens.append(hidden)
+        )(tp_at, *packs, *blocks, gate_w, up_w, down_w)
         theirs = swap(odd_far, 1)
+        even_far, near, own = pl.pallas_call(
+            rest_kernel,
+            in_specs=[smem] + [vmem] * 2, out_specs=(vmem,) * 3,
+            out_shape=(far_shape, part_shape, part_shape),
+            compiler_params=params(8),
+        )(tp_at, hidden, down_w)
         far = even_far.astype(f32) + theirs.astype(f32)
-        come = []
+        terms += [own, swap(near, 1)]
         bit = n_tp // 4
         while bit >= 1:
-            got_far = swap(far[bit - 1 :].astype(bf16), 2 * bit)
-            come.append(got_far[0])
-            far = far[: bit - 1] + got_far[1:].astype(f32)
+            come = swap(far[bit - 1 :].astype(bf16), 2 * bit)
+            terms.append(come[0])
+            far = far[: bit - 1] + come[1:].astype(f32)
             bit //= 2
-        sums.append(come)
-    near, *owns = pl.pallas_call(
-        functools.partial(near_kernel, n_half),
-        in_specs=[smem] + [vmem] * (n_half + 1), out_specs=(vmem,) * (n_half + 1),
-        out_shape=(jax.ShapeDtypeStruct((slots, feats), bf16),)
-        + (jax.ShapeDtypeStruct((part, feats), bf16),) * n_half,
-        compiler_params=params(8), name="expert_near",
-    )(tp_at, *hiddens, weights[2])
-    near = swap(near, 1)
-    terms = [term for own, come in zip(owns, sums) for term in (own, *come)]
     result = pl.pallas_call(
         functools.partial(join_kernel, n_half, n_ep),
         out_shape=jax.ShapeDtypeStruct((slots, feats), bf16),
-        in_specs=[vmem] * (len(terms) + 1), out_specs=vmem, compiler_params=params(8),
+        in_specs=[vmem] * len(terms), out_specs=vmem, compiler_params=params(8),
         name="expert_join",
-    )(near, *terms)
+    )(*terms)
     back = lax.all_to_all(result, "ep", split_axis=0, concat_axis=0, tiled=True)
 
     mixed = pl.pallas_call(
@@ -594,13 +564,7 @@
         stay(read_real.reshape(chans, states)), stay(read_imag.reshape(chans, states)),
     )
     pieces = gather_tp(mixed)
-    value_w, gate_w = pl.pallas_call(
-        fetch_kernel,
-        out_shape=tuple(jax.ShapeDtypeStruct(w.shape, bf16) for w in (out_value, out_gate)),
-        in_specs=[hbm] * 2, out_specs=(vmem,) * 2,
-        scratch_shapes=[pltpu.SemaphoreType.DMA((2,))],
-        compiler_params=params(10), name="out_fetch",
-    )(stay(out_value), stay(out_gate))
+    value_w, gate_w = fetch(out_value, out_gate)
     mixer_output = pl.pallas_call(
         functools.partial(output_kernel, n_tp),
         out_shape=jax.ShapeDtypeStruct((rows, out_value.shape[1]), bf16),

time: 102 us -> 105 us (1.029)
  Pallas kernels: 35.8 us -> 39.4 us
  waiting for transfers between devices: 27 us -> 25.8 us
    pallas_call x4 -> x7, Pallas kernels: 14.2 us -> 17.8 us  [the longest x2 7.95 us: shards(): pl.pallas_call(functools.partial(hidden_kernel, n_tp, n_ep, c * half), in...]
    ppermute x16 -> x17, waiting for transfers between devices: 20.7 us -> 19.6 us  [swap(): return lax.ppermute(value, 'tp', [(i, i ^ bit) for i in range(count)])]
    ppermute x16 -> x17, starting transfers between devices: 8.41 us -> 8.88 us  [swap(): return lax.ppermute(value, 'tp', [(i, i ^ bit) for i in range(count)])]
  transfers between devices with their start and end apart: 18 -> 19, of which waited for: 6 -> 5; matrix products, arithmetic and copies ran while one was open for 0% -> 0% of each run, Pallas kernels for 28% -> 35%
where the time goes in v4:
time: 105 us; the launch traced here: 104 us
  Pallas kernels  39.4 us (38%)
  waiting for transfers between devices  25.8 us (25%)
  blocking collectives  21.8 us (21%)
  starting transfers between devices  16.1 us (15%)
    all_to_all x1, blocking collectives, shards(): lax.all_to_all(send, 'ep', split_axis=0, concat_axis=0, tiled=True)  21.8 us
    ppermute x17, waiting for transfers between devices, swap(): return lax.ppermute(value, 'tp', [(i, i ^ bit) for i in range(count)])  19.6 us
    ppermute x17, starting transfers between devices, swap(): return lax.ppermute(value, 'tp', [(i, i ^ bit) for i in range(count)])  8.88 us
    pallas_call x2, Pallas kernels, shards(): pl.pallas_call(functools.partial(hidden_kernel, n_tp, n_ep, c * half), in...  7.95 us
    pallas_call x3, Pallas kernels, fetch(): pl.pallas_call(fetch_kernel, out_shape=tuple((jax.ShapeDtypeStruct(w.shap...  7.93 us
    all_to_all x1, waiting for transfers between devices, shards(): got = lax.all_to_all(ends, 'ep', split_axis=0, concat_axis=0)  6.29 us
    pallas_call x1, Pallas kernels, shards(): pl.pallas_call(functools.partial(scan_kernel, float(chans * n_tp), n_tp),...  6.15 us
    pallas_call x1, Pallas kernels, shards(): pl.pallas_call(read_kernel, out_shape=jax.ShapeDtypeStruct((rows, chans),...  4.87 us
  transfers between devices with their start and end apart: 19, of which 5 were waited for; matrix products, arithmetic and copies ran while one was open for 0% of the time, Pallas kernels for 35%

profile of v4, /device:TPU:0, one launch (start us, length us, event | category | flops | bytes accessed | tf_op | source)
XLA Modules:
  0.0 104.2 jit_solution(14336128379461416994)
XLA Ops:
  0.6 2.3 %send_rows.1 = (bf16[512,512]{1,0:T(8,128)(2,1)}, f32[1,1024]{1,0:T(1,128)}) custom-call(s32[2,128]{1,0:T(2,128)} %bitcast.37, bf16[128,512]{1,0:T(8,128)(2,1)} %rows_ref.1, bf16[256,512]{1,0:T(8,128)(2,1)} %x_ref.3, f32[1,512]{1,0:T(1,128)} %bitcast.39), custom_call_target="tpu_custom_call" | custom-call | tf_op jit(solution)/shard_map/send_rows/pallas_call | solution.py:445
  3.0 21.8 %all_to_all.27 = bf16[8,64,512]{2,1,0:T(8,128)(2,1)S(1)} all-to-all(bf16[8,64,512]{2,1,0:T(8,128)(2,1)} %bitcast.29), channel_id=1, replica_groups=mesh['ep'=8,'tp'=4] {'ep'}, dimensions={0} | all-to-all | bytes 1048576 | tf_op jit(solution)/shard_map/all_to_all | solution.py:454
  24.8 0.0 collective-permute-start.6
  24.8 1.6 %collective-permute-start.12 = (bf16[256,512]{1,0:T(8,128)(2,1)S(1)}, bf16[256,512]{1,0:T(8,128)(2,1)S(1)}, u32[]{:S(2)}, u32[]{:S(2)}) collective-permute-start(bf16[256,512]{1,0:T(8,128)(2,1)S(1)} %bitcast.33), channel_id=1, source_target_pairs={{0,2},{1,3},{2,0},{3,1},{4,6},{5,7},{6,4},{7,5},{8,10},{9,11},{10,... | collective-permute-start | bytes 786440 | tf_op jit(solution)/shard_map/ppermute | solution.py:416
  26.4 0.5 collective-permute-start.7
  26.9 7.2 %collective-permute-done.12.refs_6_ = bf16[256,512]{1,0:T(8,128)(2,1)S(1)} collective-permute-done((bf16[256,512]{1,0:T(8,128)(2,1)S(1)}, bf16[256,512]{1,0:T(8,128)(2,1)S(1)}, u32[]{:S(2)}, u32[]{:S(2)}) %collective-permute-start.12) | collective-permute-done | bytes 262176 | tf_op jit(solution)/shard_map/ppermute | solution.py:416
  34.1 0.0 collective-permute-start.13
  34.1 5.2 %collective-permute-done.7.refs_6_ = bf16[256,512]{1,0:T(8,128)(2,1)S(1)} collective-permute-done((bf16[256,512]{1,0:T(8,128)(2,1)S(1)}, bf16[256,512]{1,0:T(8,128)(2,1)S(1)}, u32[]{:S(2)}, u32[]{:S(2)}) %collective-permute-start.7) | collective-permute-done | bytes 262176 | tf_op jit(solution)/shard_map/ppermute | solution.py:416
  39.2 0.0 collective-permute-start.8
  39.2 1.5 %collective-permute-start.1 = (f32[1,1024]{1,0:T(1,128)}, f32[1,1024]{1,0:T(1,128)S(1)}, u32[]{:S(2)}, u32[]{:S(2)}) collective-permute-start(f32[1,1024]{1,0:T(1,128)} %get-tuple-element.35.refs_0_), channel_id=1, source_target_pairs={{0,2},{1,3},{2,0},{3,1},{4,6},{5,7},{6,4},{7,5},{8,10},{9,11},{10,... | collective-permute-start | bytes 12296 | tf_op jit(solution)/shard_map/ppermute | solution.py:416
  40.8 0.2 collective-permute-start
  41.0 2.1 %collective-permute-done.1.refs_2_ = f32[1,1024]{1,0:T(1,128)S(1)} collective-permute-done((f32[1,1024]{1,0:T(1,128)}, f32[1,1024]{1,0:T(1,128)S(1)}, u32[]{:S(2)}, u32[]{:S(2)}) %collective-permute-start.1) | collective-permute-done | bytes 4128 | tf_op jit(solution)/shard_map/ppermute | solution.py:416
  43.0 0.0 collective-permute-start.2
  43.0 2.2 %shard_map.187.refs_10_.down_ref = bf16[1,1024,2048]{2,1,0:T(8,128)(2,1)S(1)} custom-call(bf16[1,1024,2048]{2,1,0:T(8,128)(2,1)} %refs_0_.5), custom_call_target="tpu_custom_call" | custom-call | tf_op jit(solution)/shard_map/pallas_call | solution.py:508
  45.3 3.5 %shard_map.186 = (bf16[1,2048,1024]{2,1,0:T(8,128)(2,1)S(1)}, bf16[1,2048,1024]{2,1,0:T(8,128)(2,1)S(1)}) custom-call(bf16[1,2048,1024]{2,1,0:T(8,128)(2,1)} %refs_0_.4, bf16[1,2048,1024]{2,1,0:T(8,128)(2,1)} %refs_1_.3), custom_call_target="tpu_custom_call" | custom-call | tf_op jit(solution)/shard_map/pallas_call | solution.py:508
  48.7 0.0 collective-permute-done.refs_1_
  48.8 0.0 collective-permute-done.2.refs_3_
  48.8 0.0 collective-permute-done.6.refs_5_
  48.8 0.0 collective-permute-done.13.refs_7_
  48.8 4.0 %shard_map.190 = (bf16[256,1024]{1,0:T(8,128)(2,1)S(1)}, bf16[1,256,512]{2,1,0:T(8,128)(2,1)S(1)}) custom-call(s32[1]{0:T(128)} %bitcast.2.me_ref, f32[1,1024]{1,0:T(1,128)} %get-tuple-element.35.refs_0_, f32[1,1024]{1,0:T(1,128)S(1)} %collective-permute-done.refs_1_, f32[1,1024]{1,0:T(1,128)S(1)} %collective-permute-done.1.refs_2_, ...), custom_call_target="tpu_custom_call" | custom-call | tf_op jit(solution)/shard_map/pallas_call | solution.py:525
  52.8 0.6 collective-permute-start.15
  53.3 0.0 collective-permute-done.8.refs_7_
  53.3 4.0 %shard_map.188 = (bf16[256,1024]{1,0:T(8,128)(2,1)S(1)}, bf16[1,256,512]{2,1,0:T(8,128)(2,1)S(1)}) custom-call(s32[1]{0:T(128)} %bitcast.2.me_ref, f32[1,1024]{1,0:T(1,128)} %get-tuple-element.35.refs_0_, f32[1,1024]{1,0:T(1,128)S(1)} %collective-permute-done.refs_1_, f32[1,1024]{1,0:T(1,128)S(1)} %collective-permute-done.1.refs_2_, ...), custom_call_target="tpu_custom_call" | custom-call | tf_op jit(solution)/shard_map/pallas_call | solution.py:525
  57.3 0.1 collective-permute-start.10
  57.4 1.0 shard_map.191
  58.4 1.0 shard_map.189
  59.4 0.6 collective-permute-start.14
  59.9 0.1 collective-permute-start.9
  60.0 0.0 collective-permute-done.15
  60.0 0.1 add_convert_fusion
  60.1 1.6 %collective-permute-start.16 = (bf16[1,256,512]{2,1,0:T(8,128)(2,1)S(1)}, bf16[1,256,512]{2,1,0:T(8,128)(2,1)S(1)}, u32[]{:S(2)}, u32[]{:S(2)}) collective-permute-start(bf16[1,256,512]{2,1,0:T(8,128)(2,1)S(1)} %add_convert_fusion), channel_id=1, source_target_pairs={{0,2},{1,3},{2,0},{3,1},{4,6},{5,7},{6,4},{7,5},{8,10},{9,11},{10,... | collective-permute-start | bytes 786440 | tf_op jit(solution)/shard_map/ppermute | solution.py:416
  61.7 0.0 collective-permute-done.10
  61.7 0.1 add_convert_fusion.1
  61.8 0.6 collective-permute-start.11
  62.3 3.1 %mixer_poles.1 = (f32[256,1024]{1,0:T(8,128)S(1)}, f32[256,1024]{1,0:T(8,128)S(1)}, f32[2,1024]{1,0:T(2,128)S(1)}) custom-call(f32[32,256]{1,0:T(8,128)} %bitcast.36, f32[32,32]{1,0:T(8,128)} %pr_ref.1, f32[32,32]{1,0:T(8,128)} %pi_ref.1), custom_call_target="tpu_custom_call" | custom-call | tf_op jit(solution)/shard_map/mixer_poles/pallas_call | solution.py:462
  65.4 6.1 %mixer_scan.1 = (f32[256,1024]{1,0:T(8,128)}, f32[256,1024]{1,0:T(8,128)}, f32[256,1024]{1,0:T(8,128)}, f32[256,1024]{1,0:T(8,128)}, f32[8,4,1024]{2,1,0:T(4,128)}) custom-call(bf16[256,512]{1,0:T(8,128)(2,1)} %x_ref.3, f32[1,512]{1,0:T(1,128)} %bitcast.40, f32[256,1024]{1,0:T(8,128)S(1)} %get-tuple-element.32.ar_ref, ...), custom_call_target="tpu_custom_call" | custom-call | tf_op jit(solution)/shard_map/mixer_scan/pallas_call | solution.py:470
  71.5 3.6 %all-to-all-start = ((f32[8,4,1024]{2,1,0:T(4,128)}), f32[8,4,1024]{2,1,0:T(4,128)S(1)}, u32[]{:S(2)}, u32[]{:S(2)}) async-start(f32[8,4,1024]{2,1,0:T(4,128)} %get-tuple-element.36), calls=%async_computation | async-start | bytes 262144 | tf_op jit(solution)/shard_map/all_to_all | solution.py:490
  75.1 0.0 collective-permute-done.14.refs_4_
  75.2 0.0 collective-permute-done.9.refs_1_
  75.2 0.0 collective-permute-done.16
  75.2 0.0 collective-permute-done.11
  75.2 1.0 expert_join.1
  76.2 6.3 %all-to-all-done.got_ref = f32[8,4,1024]{2,1,0:T(4,128)S(1)} async-done(((f32[8,4,1024]{2,1,0:T(4,128)}), f32[8,4,1024]{2,1,0:T(4,128)S(1)}, u32[]{:S(2)}, u32[]{:S(2)}) %all-to-all-start) | async-done | bytes 131104 | tf_op jit(solution)/shard_map/all_to_all | solution.py:490
  82.5 3.7 %all-to-all-start.2 = ((bf16[8,64,512]{2,1,0:T(8,128)(2,1)}), bf16[8,64,512]{2,1,0:T(8,128)(2,1)S(1)}, u32[]{:S(2)}, u32[]{:S(2)}) async-start(bf16[8,64,512]{2,1,0:T(8,128)(2,1)} %bitcast.19), calls=%async_computation.2 | async-start | bytes 1048576 | tf_op jit(solution)/shard_map/all_to_all | solution.py:553
  86.2 4.9 %mixer_read.1.refs_0_ = bf16[256,512]{1,0:T(8,128)(2,1)S(1)} custom-call(s32[1]{0:T(128)} %bitcast.3.me_ref, f32[8,4,1024]{2,1,0:T(4,128)S(1)} %all-to-all-done.got_ref, f32[256,1024]{1,0:T(8,128)} %get-tuple-element.37.h_re_in, f32[256,1024]{1,0:T(8,128)} %get-tuple-element.38.h_im_in, f32[256,1024]{1,0:T(8,128)} %get-tuple-element.39.c_re_in, ...), custom_call_target="tpu_custom_call" | custom-call | tf_op jit(solution)/shard_map/mixer_read/pallas_call | solution.py:555
  91.1 1.6 %collective-permute-start.4 = (bf16[256,512]{1,0:T(8,128)(2,1)S(1)}, bf16[256,512]{1,0:T(8,128)(2,1)S(1)}, u32[]{:S(2)}, u32[]{:S(2)}) collective-permute-start(bf16[256,512]{1,0:T(8,128)(2,1)S(1)} %mixer_read.1.refs_0_), channel_id=1, source_target_pairs={{0,2},{1,3},{2,0},{3,1},{4,6},{5,7},{6,4},{7,5},{8,10},{9,11},{10,... | collective-permute-start | bytes 786440 | tf_op jit(solution)/shard_map/ppermute | solution.py:416
  92.6 0.0 collective-permute-start.3
  92.6 5.2 %collective-permute-done.4.refs_2_ = bf16[256,512]{1,0:T(8,128)(2,1)S(1)} collective-permute-done((bf16[256,512]{1,0:T(8,128)(2,1)S(1)}, bf16[256,512]{1,0:T(8,128)(2,1)S(1)}, u32[]{:S(2)}, u32[]{:S(2)}) %collective-permute-start.4) | collective-permute-done | bytes 262176 | tf_op jit(solution)/shard_map/ppermute | solution.py:416
  97.8 0.0 collective-permute-start.5
  97.8 1.1 %route_share.1.share_ref = bf16[3,128,512]{2,1,0:T(8,128)(2,1)S(1)} custom-call(s32[2,128]{1,0:T(2,128)} %bitcast.38, f32[2,128]{1,0:T(2,128)} %bitcast.41), custom_call_target="tpu_custom_call" | custom-call | tf_op jit(solution)/shard_map/route_share/pallas_call | solution.py:485
  98.9 2.2 %shard_map.185 = (bf16[2048,512]{1,0:T(8,128)(2,1)S(1)}, bf16[2048,512]{1,0:T(8,128)(2,1)S(1)}) custom-call(bf16[2048,512]{1,0:T(8,128)(2,1)} %refs_0_.3, bf16[2048,512]{1,0:T(8,128)(2,1)} %refs_1_.2), custom_call_target="tpu_custom_call" | custom-call | tf_op jit(solution)/shard_map/pallas_call | solution.py:508
  101.2 0.0 collective-permute-done.3.refs_1_
  101.2 0.0 collective-permute-done.5.refs_3_
  101.2 2.0 %mixer_out.1 = bf16[256,512]{1,0:T(8,128)(2,1)} custom-call(s32[1]{0:T(128)} %bitcast.2.me_ref, bf16[256,512]{1,0:T(8,128)(2,1)S(1)} %mixer_read.1.refs_0_, bf16[256,512]{1,0:T(8,128)(2,1)S(1)} %collective-permute-done.3.refs_1_, bf16[256,512]{1,0:T(8,128)(2,1)S(1)} %collective-permute-done.4.refs_2_, bf16[256,512]{1,0:T(8,128)(2,1)S(1)} %collective-permute-done.5.refs_3_, ...), custom_call_target="tpu_custom_call" | custom-call | tf_op jit(solution)/shard_map/mixer_out/pallas_call | solution.py:568
  103.1 0.0 all-to-all-done.2
  103.1 1.0 combine.1
  (1 shorter events, 0.0 us)
Async XLA Ops:
  24.8 24.0 %collective-permute-start.6 = (bf16[512,512]{1,0:T(8,128)(2,1)S(1)}, bf16[512,512]{1,0:T(8,128)(2,1)S(1)}, u32[]{:S(2)}, u32[]{:S(2)}) collective-permute-start(bf16[512,512]{1,0:T(8,128)(2,1)S(1)} %bitcast.23), channel_id=1, source_target_pairs={{0,1},{1,0},{2,3},{3,2},{4,5},{5,4},{6,7},{7,6},{8,9},{9,8},{10,11... | collective-permute-start | bytes 1572872 | tf_op jit(solution)/shard_map/ppermute | solution.py:416
  24.8 9.2 %collective-permute-start.12 = (bf16[256,512]{1,0:T(8,128)(2,1)S(1)}, bf16[256,512]{1,0:T(8,128)(2,1)S(1)}, u32[]{:S(2)}, u32[]{:S(2)}) collective-permute-start(bf16[256,512]{1,0:T(8,128)(2,1)S(1)} %bitcast.33), channel_id=1, source_target_pairs={{0,2},{1,3},{2,0},{3,1},{4,6},{5,7},{6,4},{7,5},{8,10},{9,11},{10,... | collective-permute-start | bytes 786440 | tf_op jit(solution)/shard_map/ppermute | solution.py:416
  26.4 12.8 %collective-permute-start.7 = (bf16[256,512]{1,0:T(8,128)(2,1)S(1)}, bf16[256,512]{1,0:T(8,128)(2,1)S(1)}, u32[]{:S(2)}, u32[]{:S(2)}) collective-permute-start(bf16[256,512]{1,0:T(8,128)(2,1)S(1)} %bitcast.32), channel_id=1, source_target_pairs={{0,2},{1,3},{2,0},{3,1},{4,6},{5,7},{6,4},{7,5},{8,10},{9,11},{10,... | collective-permute-start | bytes 786440 | tf_op jit(solution)/shard_map/ppermute | solution.py:416
  34.1 14.7 %collective-permute-start.13 = (bf16[256,512]{1,0:T(8,128)(2,1)S(1)}, bf16[256,512]{1,0:T(8,128)(2,1)S(1)}, u32[]{:S(2)}, u32[]{:S(2)}) collective-permute-start(bf16[256,512]{1,0:T(8,128)(2,1)S(1)} %collective-permute-done.12.refs_6_), channel_id=1, source_target_pairs={{0,1},{1,0},{2,3},{3,2},{4,5},{5,4},{6,7},{7,6},{8,9},{9,8},{10,11... | collective-permute-start | bytes 786440 | tf_op jit(solution)/shard_map/ppermute | solution.py:416
  39.2 14.1 %collective-permute-start.8 = (bf16[256,512]{1,0:T(8,128)(2,1)S(1)}, bf16[256,512]{1,0:T(8,128)(2,1)S(1)}, u32[]{:S(2)}, u32[]{:S(2)}) collective-permute-start(bf16[256,512]{1,0:T(8,128)(2,1)S(1)} %collective-permute-done.7.refs_6_), channel_id=1, source_target_pairs={{0,1},{1,0},{2,3},{3,2},{4,5},{5,4},{6,7},{7,6},{8,9},{9,8},{10,11... | collective-permute-start | bytes 786440 | tf_op jit(solution)/shard_map/ppermute | solution.py:416
  39.2 3.8 %collective-permute-start.1 = (f32[1,1024]{1,0:T(1,128)}, f32[1,1024]{1,0:T(1,128)S(1)}, u32[]{:S(2)}, u32[]{:S(2)}) collective-permute-start(f32[1,1024]{1,0:T(1,128)} %get-tuple-element.35.refs_0_), channel_id=1, source_target_pairs={{0,2},{1,3},{2,0},{3,1},{4,6},{5,7},{6,4},{7,5},{8,10},{9,11},{10,... | collective-permute-start | bytes 12296 | tf_op jit(solution)/shard_map/ppermute | solution.py:416
  40.8 8.0 %collective-permute-start = (f32[1,1024]{1,0:T(1,128)}, f32[1,1024]{1,0:T(1,128)S(1)}, u32[]{:S(2)}, u32[]{:S(2)}) collective-permute-start(f32[1,1024]{1,0:T(1,128)} %get-tuple-element.35.refs_0_), channel_id=1, source_target_pairs={{0,1},{1,0},{2,3},{3,2},{4,5},{5,4},{6,7},{7,6},{8,9},{9,8},{10,11... | collective-permute-start | bytes 12296 | tf_op jit(solution)/shard_map/ppermute | solution.py:416
  43.0 5.7 %collective-permute-start.2 = (f32[1,1024]{1,0:T(1,128)S(1)}, f32[1,1024]{1,0:T(1,128)S(1)}, u32[]{:S(2)}, u32[]{:S(2)}) collective-permute-start(f32[1,1024]{1,0:T(1,128)S(1)} %collective-permute-done.1.refs_2_), channel_id=1, source_target_pairs={{0,1},{1,0},{2,3},{3,2},{4,5},{5,4},{6,7},{7,6},{8,9},{9,8},{10,11... | collective-permute-start | bytes 12296 | tf_op jit(solution)/shard_map/ppermute | solution.py:416
  52.8 7.2 %collective-permute-start.15 = (bf16[1,256,512]{2,1,0:T(8,128)(2,1)S(1)}, bf16[1,256,512]{2,1,0:T(8,128)(2,1)S(1)}, u32[]{:S(2)}, u32[]{:S(2)}) collective-permute-start(bf16[1,256,512]{2,1,0:T(8,128)(2,1)S(1)} %get-tuple-element.55), channel_id=1, source_target_pairs={{0,1},{1,0},{2,3},{3,2},{4,5},{5,4},{6,7},{7,6},{8,9},{9,8},{10,11... | collective-permute-start | bytes 786440 | tf_op jit(solution)/shard_map/ppermute | solution.py:416
  57.3 4.4 %collective-permute-start.10 = (bf16[1,256,512]{2,1,0:T(8,128)(2,1)S(1)}, bf16[1,256,512]{2,1,0:T(8,128)(2,1)S(1)}, u32[]{:S(2)}, u32[]{:S(2)}) collective-permute-start(bf16[1,256,512]{2,1,0:T(8,128)(2,1)S(1)} %get-tuple-element.50), channel_id=1, source_target_pairs={{0,1},{1,0},{2,3},{3,2},{4,5},{5,4},{6,7},{7,6},{8,9},{9,8},{10,11... | collective-permute-start | bytes 786440 | tf_op jit(solution)/shard_map/ppermute | solution.py:416
  59.4 15.8 %collective-permute-start.14 = (bf16[256,512]{1,0:T(8,128)(2,1)S(1)}, bf16[256,512]{1,0:T(8,128)(2,1)S(1)}, u32[]{:S(2)}, u32[]{:S(2)}) collective-permute-start(bf16[256,512]{1,0:T(8,128)(2,1)S(1)} %get-tuple-element.53), channel_id=1, source_target_pairs={{0,1},{1,0},{2,3},{3,2},{4,5},{5,4},{6,7},{7,6},{8,9},{9,8},{10,11... | collective-permute-start | bytes 786440 | tf_op jit(solution)/shard_map/ppermute | solution.py:416
  59.9 15.2 %collective-permute-start.9 = (bf16[256,512]{1,0:T(8,128)(2,1)S(1)}, bf16[256,512]{1,0:T(8,128)(2,1)S(1)}, u32[]{:S(2)}, u32[]{:S(2)}) collective-permute-start(bf16[256,512]{1,0:T(8,128)(2,1)S(1)} %get-tuple-element.48), channel_id=1, source_target_pairs={{0,1},{1,0},{2,3},{3,2},{4,5},{5,4},{6,7},{7,6},{8,9},{9,8},{10,11... | collective-permute-start | bytes 786440 | tf_op jit(solution)/shard_map/ppermute | solution.py:416
  60.1 15.1 %collective-permute-start.16 = (bf16[1,256,512]{2,1,0:T(8,128)(2,1)S(1)}, bf16[1,256,512]{2,1,0:T(8,128)(2,1)S(1)}, u32[]{:S(2)}, u32[]{:S(2)}) collective-permute-start(bf16[1,256,512]{2,1,0:T(8,128)(2,1)S(1)} %add_convert_fusion), channel_id=1, source_target_pairs={{0,2},{1,3},{2,0},{3,1},{4,6},{5,7},{6,4},{7,5},{8,10},{9,11},{10,... | collective-permute-start | bytes 786440 | tf_op jit(solution)/shard_map/ppermute | solution.py:416
  61.8 13.4 %collective-permute-start.11 = (bf16[1,256,512]{2,1,0:T(8,128)(2,1)S(1)}, bf16[1,256,512]{2,1,0:T(8,128)(2,1)S(1)}, u32[]{:S(2)}, u32[]{:S(2)}) collective-permute-start(bf16[1,256,512]{2,1,0:T(8,128)(2,1)S(1)} %add_convert_fusion.1), channel_id=1, source_target_pairs={{0,2},{1,3},{2,0},{3,1},{4,6},{5,7},{6,4},{7,5},{8,10},{9,11},{10,... | collective-permute-start | bytes 786440 | tf_op jit(solution)/shard_map/ppermute | solution.py:416
  71.5 10.9 %all-to-all-start = ((f32[8,4,1024]{2,1,0:T(4,128)}), f32[8,4,1024]{2,1,0:T(4,128)S(1)}, u32[]{:S(2)}, u32[]{:S(2)}) async-start(f32[8,4,1024]{2,1,0:T(4,128)} %get-tuple-element.36), calls=%async_computation | async-start | bytes 262144 | tf_op jit(solution)/shard_map/all_to_all | solution.py:490
  82.5 20.7 %all-to-all-start.2 = ((bf16[8,64,512]{2,1,0:T(8,128)(2,1)}), bf16[8,64,512]{2,1,0:T(8,128)(2,1)S(1)}, u32[]{:S(2)}, u32[]{:S(2)}) async-start(bf16[8,64,512]{2,1,0:T(8,128)(2,1)} %bitcast.19), calls=%async_computation.2 | async-start | bytes 1048576 | tf_op jit(solution)/shard_map/all_to_all | solution.py:553
  91.1 6.7 %collective-permute-start.4 = (bf16[256,512]{1,0:T(8,128)(2,1)S(1)}, bf16[256,512]{1,0:T(8,128)(2,1)S(1)}, u32[]{:S(2)}, u32[]{:S(2)}) collective-permute-start(bf16[256,512]{1,0:T(8,128)(2,1)S(1)} %mixer_read.1.refs_0_), channel_id=1, source_target_pairs={{0,2},{1,3},{2,0},{3,1},{4,6},{5,7},{6,4},{7,5},{8,10},{9,11},{10,... | collective-permute-start | bytes 786440 | tf_op jit(solution)/shard_map/ppermute | solution.py:416
  92.6 8.5 %collective-permute-start.3 = (bf16[256,512]{1,0:T(8,128)(2,1)S(1)}, bf16[256,512]{1,0:T(8,128)(2,1)S(1)}, u32[]{:S(2)}, u32[]{:S(2)}) collective-permute-start(bf16[256,512]{1,0:T(8,128)(2,1)S(1)} %mixer_read.1.refs_0_), channel_id=1, source_target_pairs={{0,1},{1,0},{2,3},{3,2},{4,5},{5,4},{6,7},{7,6},{8,9},{9,8},{10,11... | collective-permute-start | bytes 786440 | tf_op jit(solution)/shard_map/ppermute | solution.py:416
  97.8 3.4 %collective-permute-start.5 = (bf16[256,512]{1,0:T(8,128)(2,1)S(1)}, bf16[256,512]{1,0:T(8,128)(2,1)S(1)}, u32[]{:S(2)}, u32[]{:S(2)}) collective-permute-start(bf16[256,512]{1,0:T(8,128)(2,1)S(1)} %collective-permute-done.4.refs_2_), channel_id=1, source_target_pairs={{0,1},{1,0},{2,3},{3,2},{4,5},{5,4},{6,7},{7,6},{8,9},{9,8},{10,11... | collective-permute-start | bytes 786440 | tf_op jit(solution)/shard_map/ppermute | solution.py:416

commit v5 on v4

--- a/solution.py
+++ b/solution.py
@@ -115,10 +115,19 @@
     out_ref[...] = out.astype(bf16)
 
 
-def hidden_kernel(parts, senders, start, me_ref, *refs):
+def columns(source, which, feats):
+    return source.at[0, :, pl.ds(pl.multiple_of(which * feats, feats), feats)]
+
+
+def hidden_kernel(parts, senders, start, load, me_ref, *refs):
     packs = refs[:parts]
     blocks = refs[parts : 2 * parts]
-    gate_ref, up_ref, down_ref, hidden_ref, odd_ref, normed_ref = refs[2 * parts :]
+    refs = refs[2 * parts :]
+    if load:
+        sources = refs[:3]
+        hidden_ref, odd_ref, gate_ref, up_ref, down_ref, normed_ref, sems = refs[3:]
+    else:
+        gate_ref, up_ref, down_ref, hidden_ref, odd_ref, normed_ref = refs
     rows, units = hidden_ref.shape
     full, feats = blocks[0].shape
     width = parts * feats
@@ -126,6 +135,24 @@
     me = me_ref[0]
     lead = packs[0].shape[1] - feats
     size = min(units, 256)
+    unit_loads, down_loads = [], []
+    if load:
+        for n in range(units // size):
+            cols = pl.ds(n * size, size)
+            unit_loads.append([
+                pltpu.make_async_copy(
+                    source.at[0, :, cols], ref.at[0, :, cols], sems.at[m, n]
+                )
+                for m, (source, ref) in enumerate(zip(sources, (gate_ref, up_ref)))
+            ])
+        for n in range(odd_ref.shape[0]):
+            down_loads.append(
+                pltpu.make_async_copy(
+                    columns(sources[2], me ^ (2 * n + 3), feats), down_ref.at[n], sems.at[2, n]
+                )
+            )
+        for copy in sum(unit_loads, down_loads[:0]) + down_loads:
+            copy.start()
 
     def body(sender, unused):
         here = pl.ds(pl.multiple_of(sender * chunk, chunk), chunk)
@@ -149,26 +176,40 @@
     lax.fori_loop(0, senders, body, 0, unroll=4)
     for at in range(0, units, size):
         cols = pl.ds(at, size)
+        for copy in unit_loads[at // size] if load else ():
+            copy.wait()
         normed = normed_ref[...]
         gate = mm(normed, gate_ref[0, :, cols])
         up = mm(normed, up_ref[0, :, cols])
         hidden_ref[:, cols] = (gate * jax.nn.sigmoid(gate) * up).astype(bf16)
+    for copy in down_loads:
+        copy.wait()
     for n in range(odd_ref.shape[0]):
-        odd_ref[n] = down_part(me ^ (2 * n + 3), hidden_ref, down_ref, feats)
-
-
-def down_part(which, hidden_ref, weight_ref, feats):
-    cols = pl.ds(pl.multiple_of(which * feats, feats), feats)
-    return mm(hidden_ref[...], weight_ref[0, :, cols]).astype(bf16)
-
-
-def rest_kernel(me_ref, hidden_ref, down_ref, even_ref, near_ref, own_ref):
-    me = me_ref[0]
+        odd_ref[n] = mm(hidden_ref[...], down_ref[n]).astype(bf16)
+
+
+def rest_kernel(load, me_ref, hidden_ref, *refs):
+    if load:
+        source, even_ref, near_ref, own_ref, down_ref, sems = refs
+    else:
+        down_ref, even_ref, near_ref, own_ref = refs
     feats = near_ref.shape[1]
-    for n in range(even_ref.shape[0]):
-        even_ref[n] = down_part(me ^ (2 * n + 2), hidden_ref, down_ref, feats)
-    near_ref[...] = down_part(me ^ 1, hidden_ref, down_ref, feats)
-    own_ref[...] = down_part(me, hidden_ref, down_ref, feats)
+    outs = [even_ref.at[n] for n in range(even_ref.shape[0])] + [near_ref, own_ref]
+    offsets = [2 * n + 2 for n in range(even_ref.shape[0])] + [1, 0]
+    loads = []
+    if load:
+        for n, offset in enumerate(offsets):
+            loads.append(
+                pltpu.make_async_copy(
+                    columns(source, me_ref[0] ^ offset, feats), down_ref.at[n], sems.at[n]
+                )
+            )
+        for copy in loads:
+            copy.start()
+    for n, out in enumerate(outs):
+        if load:
+            loads[n].wait()
+        out[...] = mm(hidden_ref[...], down_ref[n]).astype(bf16)
 
 
 def join_kernel(count, senders, *refs):
@@ -448,13 +489,15 @@
             jax.ShapeDtypeStruct((slots, feats), bf16),
             jax.ShapeDtypeStruct((1, 2 * rows + feats), f32),
         ),
-        in_specs=[vmem] * 4, out_specs=(vmem, vmem), compiler_params=params(60),
+        in_specs=[vmem] * 4, out_specs=(vmem, vmem), compiler_params=params(8),
         name="send_rows",
-    )(routes_t, expert_input, mixer_input, expert_gain.reshape(1, feats))
+    )(
+        stay(routes_t), stay(expert_input), stay(mixer_input),
+        stay(expert_gain.reshape(1, feats)),
+    )
     arrived = lax.all_to_all(send, "ep", split_axis=0, concat_axis=0, tiled=True)
     packed, tp_at, ep_at = lax.optimization_barrier((packed, tp_at, ep_at))
     packs = gather_tp(packed)
-    packs[0] = stay(packed)
 
     groups, states = pole_real.shape
     flat = groups * states
@@ -513,8 +556,10 @@
             compiler_params=params(10),
         )(*(stay(w) for w in weights))
 
-    gate_w, up_w = fetch(expert_gate, expert_up)
-    (down_w,) = fetch(expert_down)
+    weights = (stay(expert_gate), stay(expert_up), stay(expert_down))
+    down_rest = weights[2]
+    n_unit = max(1, units // 256)
+    n_rest = n_far + 2
     terms = []
     for c in range(n_half):
         blocks = [arrived, partner]
@@ -522,20 +567,30 @@
             blocks += [far_blocks[c][k], swap(far_blocks[c][k], 1)]
         far_shape = jax.ShapeDtypeStruct((n_far, part, feats), bf16)
         part_shape = jax.ShapeDtypeStruct((part, feats), bf16)
-        hidden, odd_far = pl.pallas_call(
-            functools.partial(hidden_kernel, n_tp, n_ep, c * half),
-            in_specs=[smem] + [vmem] * (2 * n_tp + 3), out_specs=(vmem,) * 2,
-            scratch_shapes=[pltpu.VMEM((part, n_tp * feats), bf16)],
-            out_shape=(jax.ShapeDtypeStruct((part, units), bf16), far_shape),
+        load = c == 0
+        kept = [jax.ShapeDtypeStruct(w.shape, bf16) for w in (expert_gate, expert_up)]
+        kept = kept + [jax.ShapeDtypeStruct((n_far, units, feats), bf16)] if load else []
+        hidden, odd_far, *held = pl.pallas_call(
+            functools.partial(hidden_kernel, n_tp, n_ep, c * half, load),
+            in_specs=[smem] + [vmem] * (2 * n_tp) + [hbm if load else vmem] * 3,
+            out_specs=(vmem,) * (2 + len(kept)),
+            scratch_shapes=[pltpu.VMEM((part, n_tp * feats), bf16)]
+            + ([pltpu.SemaphoreType.DMA((3, max(n_unit, n_far)))] if load else []),
+            out_shape=(jax.ShapeDtypeStruct((part, units), bf16), far_shape, *kept),
             compiler_params=params(12),
-        )(tp_at, *packs, *blocks, gate_w, up_w, down_w)
+        )(tp_at, *packs, *blocks, *weights)
+        weights = held or weights
         theirs = swap(odd_far, 1)
-        even_far, near, own = pl.pallas_call(
-            rest_kernel,
-            in_specs=[smem] + [vmem] * 2, out_specs=(vmem,) * 3,
-            out_shape=(far_shape, part_shape, part_shape),
+        kept = [jax.ShapeDtypeStruct((n_rest, units, feats), bf16)] if load else []
+        even_far, near, own, *held = pl.pallas_call(
+            functools.partial(rest_kernel, load),
+            in_specs=[smem, vmem, hbm if load else vmem],
+            out_specs=(vmem,) * (3 + len(kept)),
+            scratch_shapes=[pltpu.SemaphoreType.DMA((n_rest,))] if load else [],
+            out_shape=(far_shape, part_shape, part_shape, *kept),
             compiler_params=params(8),
-        )(tp_at, hidden, down_w)
+        )(tp_at, hidden, down_rest)
+        down_rest = held[0] if held else down_rest
         far = even_far.astype(f32) + theirs.astype(f32)
         terms += [own, swap(near, 1)]
         bit = n_tp // 4

time: 105 us -> 101 us (0.962)
  Pallas kernels: 39.4 us -> 35 us
    pallas_call x3 -> x1, Pallas kernels: 7.93 us -> 2.24 us  [fetch(): pl.pallas_call(fetch_kernel, out_shape=tuple((jax.ShapeDtypeStruct(w.shap...]
    pallas_call x4, Pallas kernels: 9.92 us -> 12 us  [the longest x2 8.45 us: shards(): pl.pallas_call(functools.partial(hidden_kernel, n_tp, n_ep, c * half, loa...]
  transfers between devices with their start and end apart: 19 -> 19, of which waited for: 5 -> 6; matrix products, arithmetic and copies ran while one was open for 0% -> 0% of each run, Pallas kernels for 35% -> 29%
where the time goes in v5:
time: 101 us; the launch traced here: 100 us
  Pallas kernels  35 us (35%)
  waiting for transfers between devices  26.8 us (27%)
  blocking collectives  21.6 us (21%)
  starting transfers between devices  15.9 us (16%)
    all_to_all x1, blocking collectives, shards(): lax.all_to_all(send, 'ep', split_axis=0, concat_axis=0, tiled=True)  21.6 us
    ppermute x17, waiting for transfers between devices, swap(): return lax.ppermute(value, 'tp', [(i, i ^ bit) for i in range(count)])  20.5 us
    ppermute x17, starting transfers between devices, swap(): return lax.ppermute(value, 'tp', [(i, i ^ bit) for i in range(count)])  8.75 us
    pallas_call x2, Pallas kernels, shards(): pl.pallas_call(functools.partial(hidden_kernel, n_tp, n_ep, c * half, loa...  8.45 us
    all_to_all x1, waiting for transfers between devices, shards(): got = lax.all_to_all(ends, 'ep', split_axis=0, concat_axis=0)  6.31 us
    pallas_call x1, Pallas kernels, shards(): pl.pallas_call(functools.partial(scan_kernel, float(chans * n_tp), n_tp),...  6.18 us
    pallas_call x1, Pallas kernels, shards(): pl.pallas_call(read_kernel, out_shape=jax.ShapeDtypeStruct((rows, chans),...  4.88 us
    all_to_all x1, starting transfers between devices, shards(): got = lax.all_to_all(ends, 'ep', split_axis=0, concat_axis=0)  3.61 us
  transfers between devices with their start and end apart: 19, of which 6 were waited for; matrix products, arithmetic and copies ran while one was open for 0% of the time, Pallas kernels for 29%

profile of v5, /device:TPU:0, one launch (start us, length us, event | category | flops | bytes accessed | tf_op | source)
XLA Modules:
  0.0 100.2 jit_solution(13267402409754806878)
XLA Ops:
  0.6 1.6 %send_rows.1 = (bf16[512,512]{1,0:T(8,128)(2,1)S(1)}, f32[1,1024]{1,0:T(1,128)S(1)}) custom-call(s32[2,128]{1,0:T(2,128)} %bitcast.37, bf16[128,512]{1,0:T(8,128)(2,1)} %rows_ref.1, bf16[256,512]{1,0:T(8,128)(2,1)} %x_ref.3, f32[1,512]{1,0:T(1,128)} %bitcast.39), custom_call_target="tpu_custom_call" | custom-call | tf_op jit(solution)/shard_map/send_rows/pallas_call | solution.py:486
  2.2 21.6 %all_to_all.27 = bf16[8,64,512]{2,1,0:T(8,128)(2,1)S(1)} all-to-all(bf16[8,64,512]{2,1,0:T(8,128)(2,1)S(1)} %bitcast.27), channel_id=1, replica_groups=mesh['ep'=8,'tp'=4] {'ep'}, dimensions={0} | all-to-all | bytes 1048576 | tf_op jit(solution)/shard_map/all_to_all | solution.py:498
  23.8 0.0 collective-permute-start.6
  23.9 1.6 %collective-permute-start.7 = (bf16[256,512]{1,0:T(8,128)(2,1)S(1)}, bf16[256,512]{1,0:T(8,128)(2,1)S(1)}, u32[]{:S(2)}, u32[]{:S(2)}) collective-permute-start(bf16[256,512]{1,0:T(8,128)(2,1)S(1)} %bitcast.33), channel_id=1, source_target_pairs={{0,2},{1,3},{2,0},{3,1},{4,6},{5,7},{6,4},{7,5},{8,10},{9,11},{10,... | collective-permute-start | bytes 786440 | tf_op jit(solution)/shard_map/ppermute | solution.py:457
  25.5 0.5 collective-permute-start.12
  26.0 7.2 %collective-permute-done.7.refs_6_ = bf16[256,512]{1,0:T(8,128)(2,1)S(1)} collective-permute-done((bf16[256,512]{1,0:T(8,128)(2,1)S(1)}, bf16[256,512]{1,0:T(8,128)(2,1)S(1)}, u32[]{:S(2)}, u32[]{:S(2)}) %collective-permute-start.7) | collective-permute-done | bytes 262176 | tf_op jit(solution)/shard_map/ppermute | solution.py:457
  33.1 0.0 collective-permute-start.8
  33.1 5.2 %collective-permute-done.12.refs_6_ = bf16[256,512]{1,0:T(8,128)(2,1)S(1)} collective-permute-done((bf16[256,512]{1,0:T(8,128)(2,1)S(1)}, bf16[256,512]{1,0:T(8,128)(2,1)S(1)}, u32[]{:S(2)}, u32[]{:S(2)}) %collective-permute-start.12) | collective-permute-done | bytes 262176 | tf_op jit(solution)/shard_map/ppermute | solution.py:457
  38.3 0.0 collective-permute-start.13
  38.3 1.5 %collective-permute-start.1 = (f32[1,1024]{1,0:T(1,128)S(1)}, f32[1,1024]{1,0:T(1,128)S(1)}, u32[]{:S(2)}, u32[]{:S(2)}) collective-permute-start(f32[1,1024]{1,0:T(1,128)S(1)} %get-tuple-element.37.refs_0_), channel_id=1, source_target_pairs={{0,2},{1,3},{2,0},{3,1},{4,6},{5,7},{6,4},{7,5},{8,10},{9,11},{10,... | collective-permute-start | bytes 12296 | tf_op jit(solution)/shard_map/ppermute | solution.py:457
  39.8 0.2 collective-permute-start
  40.0 1.9 %collective-permute-done.1.refs_2_ = f32[1,1024]{1,0:T(1,128)S(1)} collective-permute-done((f32[1,1024]{1,0:T(1,128)S(1)}, f32[1,1024]{1,0:T(1,128)S(1)}, u32[]{:S(2)}, u32[]{:S(2)}) %collective-permute-start.1) | collective-permute-done | bytes 4128 | tf_op jit(solution)/shard_map/ppermute | solution.py:457
  41.9 0.0 collective-permute-start.2
  41.9 0.0 collective-permute-done.refs_1_
  41.9 1.2 %collective-permute-done.2.refs_3_ = f32[1,1024]{1,0:T(1,128)S(1)} collective-permute-done((f32[1,1024]{1,0:T(1,128)S(1)}, f32[1,1024]{1,0:T(1,128)S(1)}, u32[]{:S(2)}, u32[]{:S(2)}) %collective-permute-start.2) | collective-permute-done | bytes 4128 | tf_op jit(solution)/shard_map/ppermute | solution.py:457
  43.0 0.0 collective-permute-done.6.refs_5_
  43.0 0.0 collective-permute-done.8.refs_7_
  43.1 5.1 %shard_map.186 = (bf16[256,1024]{1,0:T(8,128)(2,1)S(1)}, bf16[1,256,512]{2,1,0:T(8,128)(2,1)S(1)}, bf16[1,2048,1024]{2,1,0:T(8,128)(2,1)S(1)}, bf16[1,2048,1024]...) custom-call(s32[1]{0:T(128)} %bitcast.2.me_ref, f32[1,1024]{1,0:T(1,128)S(1)} %get-tuple-element.37.refs_0_, ...), custom_call_target="tpu_custom_call" | custom-call | tf_op jit(solution)/shard_map/pallas_call | solution.py:573
  48.2 0.0 collective-permute-done.13.refs_7_
  48.2 3.3 %shard_map.188 = (bf16[256,1024]{1,0:T(8,128)(2,1)S(1)}, bf16[1,256,512]{2,1,0:T(8,128)(2,1)S(1)}) custom-call(s32[1]{0:T(128)} %bitcast.2.me_ref, f32[1,1024]{1,0:T(1,128)S(1)} %get-tuple-element.37.refs_0_, f32[1,1024]{1,0:T(1,128)S(1)} %collective-permute-done.refs_1_, f32[1,1024]{1,0:T(1,128)S(1)} %collective-permute-done.1.refs_2_, ...), custom_call_target="tpu_custom_call" | custom-call | tf_op jit(solution)/shard_map/pallas_call | solution.py:573
  51.5 0.2 collective-permute-start.15
  51.8 0.4 collective-permute-start.10
  52.1 2.6 %shard_map.187 = (bf16[1,256,512]{2,1,0:T(8,128)(2,1)S(1)}, bf16[256,512]{1,0:T(8,128)(2,1)S(1)}, bf16[256,512]{1,0:T(8,128)(2,1)S(1)}, bf16[3,1024,512]{2,1,0:T(8,128)(2,1)S(1)}) custom-call(s32[1]{0:T(128)} %bitcast.2.me_ref, bf16[256,1024]{1,0:T(8,128)(2,1)S(1)} %get-tuple-element.46.hidden_ref, bf16[1,1024,2048]{2,1,0:T(8,128)(2,1)} %refs_0_.3), custom_call_target="tpu_custom_call" | custom-call | tf_op jit(solution)/shard_map/pallas_call | solution.py:585
  54.7 1.0 shard_map.189
  55.7 0.2 collective-permute-start.14
  55.9 0.4 collective-permute-start.9
  56.2 0.0 collective-permute-done.15
  56.2 0.1 add_convert_fusion
  56.3 1.6 %collective-permute-start.16 = (bf16[1,256,512]{2,1,0:T(8,128)(2,1)S(1)}, bf16[1,256,512]{2,1,0:T(8,128)(2,1)S(1)}, u32[]{:S(2)}, u32[]{:S(2)}) collective-permute-start(bf16[1,256,512]{2,1,0:T(8,128)(2,1)S(1)} %add_convert_fusion), channel_id=1, source_target_pairs={{0,2},{1,3},{2,0},{3,1},{4,6},{5,7},{6,4},{7,5},{8,10},{9,11},{10,... | collective-permute-start | bytes 786440 | tf_op jit(solution)/shard_map/ppermute | solution.py:457
  57.9 0.0 collective-permute-done.10
  57.9 0.1 add_convert_fusion.1
  58.0 0.6 collective-permute-start.11
  58.5 3.1 %mixer_poles.1 = (f32[256,1024]{1,0:T(8,128)S(1)}, f32[256,1024]{1,0:T(8,128)S(1)}, f32[2,1024]{1,0:T(2,128)S(1)}) custom-call(f32[32,256]{1,0:T(8,128)} %bitcast.36, f32[32,32]{1,0:T(8,128)} %pr_ref.1, f32[32,32]{1,0:T(8,128)} %pi_ref.1), custom_call_target="tpu_custom_call" | custom-call | tf_op jit(solution)/shard_map/mixer_poles/pallas_call | solution.py:505
  61.6 6.2 %mixer_scan.1 = (f32[256,1024]{1,0:T(8,128)}, f32[256,1024]{1,0:T(8,128)}, f32[256,1024]{1,0:T(8,128)}, f32[256,1024]{1,0:T(8,128)}, f32[8,4,1024]{2,1,0:T(4,128)}) custom-call(bf16[256,512]{1,0:T(8,128)(2,1)} %x_ref.3, f32[1,512]{1,0:T(1,128)} %bitcast.40, f32[256,1024]{1,0:T(8,128)S(1)} %get-tuple-element.34.ar_ref, ...), custom_call_target="tpu_custom_call" | custom-call | tf_op jit(solution)/shard_map/mixer_scan/pallas_call | solution.py:513
  67.8 3.6 %all-to-all-start = ((f32[8,4,1024]{2,1,0:T(4,128)}), f32[8,4,1024]{2,1,0:T(4,128)S(1)}, u32[]{:S(2)}, u32[]{:S(2)}) async-start(f32[8,4,1024]{2,1,0:T(4,128)} %get-tuple-element.38), calls=%async_computation | async-start | bytes 262144 | tf_op jit(solution)/shard_map/all_to_all | solution.py:533
  71.4 0.0 collective-permute-done.14.refs_4_
  71.4 0.0 collective-permute-done.9.refs_1_
  71.4 0.0 collective-permute-done.16
  71.4 0.0 collective-permute-done.11
  71.4 1.0 expert_join.1
  72.4 6.3 %all-to-all-done.got_ref = f32[8,4,1024]{2,1,0:T(4,128)S(1)} async-done(((f32[8,4,1024]{2,1,0:T(4,128)}), f32[8,4,1024]{2,1,0:T(4,128)S(1)}, u32[]{:S(2)}, u32[]{:S(2)}) %all-to-all-start) | async-done | bytes 131104 | tf_op jit(solution)/shard_map/all_to_all | solution.py:533
  78.7 3.5 %all-to-all-start.2 = ((bf16[8,64,512]{2,1,0:T(8,128)(2,1)}), bf16[8,64,512]{2,1,0:T(8,128)(2,1)S(1)}, u32[]{:S(2)}, u32[]{:S(2)}) async-start(bf16[8,64,512]{2,1,0:T(8,128)(2,1)} %bitcast.19), calls=%async_computation.2 | async-start | bytes 1048576 | tf_op jit(solution)/shard_map/all_to_all | solution.py:608
  82.2 4.9 %mixer_read.1.refs_0_ = bf16[256,512]{1,0:T(8,128)(2,1)S(1)} custom-call(s32[1]{0:T(128)} %bitcast.3.me_ref, f32[8,4,1024]{2,1,0:T(4,128)S(1)} %all-to-all-done.got_ref, f32[256,1024]{1,0:T(8,128)} %get-tuple-element.39.h_re_in, f32[256,1024]{1,0:T(8,128)} %get-tuple-element.40.h_im_in, f32[256,1024]{1,0:T(8,128)} %get-tuple-element.41.c_re_in, ...), custom_call_target="tpu_custom_call" | custom-call | tf_op jit(solution)/shard_map/mixer_read/pallas_call | solution.py:610
  87.1 1.6 %collective-permute-start.4 = (bf16[256,512]{1,0:T(8,128)(2,1)S(1)}, bf16[256,512]{1,0:T(8,128)(2,1)S(1)}, u32[]{:S(2)}, u32[]{:S(2)}) collective-permute-start(bf16[256,512]{1,0:T(8,128)(2,1)S(1)} %mixer_read.1.refs_0_), channel_id=1, source_target_pairs={{0,2},{1,3},{2,0},{3,1},{4,6},{5,7},{6,4},{7,5},{8,10},{9,11},{10,... | collective-permute-start | bytes 786440 | tf_op jit(solution)/shard_map/ppermute | solution.py:457
  88.7 0.0 collective-permute-start.3
  88.7 5.1 %collective-permute-done.4.refs_2_ = bf16[256,512]{1,0:T(8,128)(2,1)S(1)} collective-permute-done((bf16[256,512]{1,0:T(8,128)(2,1)S(1)}, bf16[256,512]{1,0:T(8,128)(2,1)S(1)}, u32[]{:S(2)}, u32[]{:S(2)}) %collective-permute-start.4) | collective-permute-done | bytes 262176 | tf_op jit(solution)/shard_map/ppermute | solution.py:457
  93.9 0.0 collective-permute-start.5
  93.9 1.1 %route_share.1.share_ref = bf16[3,128,512]{2,1,0:T(8,128)(2,1)S(1)} custom-call(s32[2,128]{1,0:T(2,128)} %bitcast.38, f32[2,128]{1,0:T(2,128)} %bitcast.41), custom_call_target="tpu_custom_call" | custom-call | tf_op jit(solution)/shard_map/route_share/pallas_call | solution.py:528
  95.0 2.2 %shard_map.185 = (bf16[2048,512]{1,0:T(8,128)(2,1)S(1)}, bf16[2048,512]{1,0:T(8,128)(2,1)S(1)}) custom-call(bf16[2048,512]{1,0:T(8,128)(2,1)} %refs_0_.2, bf16[2048,512]{1,0:T(8,128)(2,1)} %refs_1_.1), custom_call_target="tpu_custom_call" | custom-call | tf_op jit(solution)/shard_map/pallas_call | solution.py:551
  97.2 0.0 collective-permute-done.3.refs_1_
  97.2 0.0 collective-permute-done.5.refs_3_
  97.2 2.0 %mixer_out.1 = bf16[256,512]{1,0:T(8,128)(2,1)} custom-call(s32[1]{0:T(128)} %bitcast.2.me_ref, bf16[256,512]{1,0:T(8,128)(2,1)S(1)} %mixer_read.1.refs_0_, bf16[256,512]{1,0:T(8,128)(2,1)S(1)} %collective-permute-done.3.refs_1_, bf16[256,512]{1,0:T(8,128)(2,1)S(1)} %collective-permute-done.4.refs_2_, bf16[256,512]{1,0:T(8,128)(2,1)S(1)} %collective-permute-done.5.refs_3_, ...), custom_call_target="tpu_custom_call" | custom-call | tf_op jit(solution)/shard_map/mixer_out/pallas_call | solution.py:623
  99.2 0.0 all-to-all-done.2
  99.2 1.0 %combine.1 = bf16[128,512]{1,0:T(8,128)(2,1)} custom-call(bf16[3,128,512]{2,1,0:T(8,128)(2,1)S(1)} %route_share.1.share_ref, bf16[512,512]{1,0:T(8,128)(2,1)S(1)} %bitcast.26), custom_call_target="tpu_custom_call" | custom-call | tf_op jit(solution)/shard_map/combine/pallas_call | solution.py:629
  (1 shorter events, 0.0 us)
Async XLA Ops:
  23.8 19.2 %collective-permute-start.6 = (bf16[512,512]{1,0:T(8,128)(2,1)S(1)}, bf16[512,512]{1,0:T(8,128)(2,1)S(1)}, u32[]{:S(2)}, u32[]{:S(2)}) collective-permute-start(bf16[512,512]{1,0:T(8,128)(2,1)S(1)} %bitcast.23), channel_id=1, source_target_pairs={{0,1},{1,0},{2,3},{3,2},{4,5},{5,4},{6,7},{7,6},{8,9},{9,8},{10,11... | collective-permute-start | bytes 1572872 | tf_op jit(solution)/shard_map/ppermute | solution.py:457
  23.9 9.2 %collective-permute-start.7 = (bf16[256,512]{1,0:T(8,128)(2,1)S(1)}, bf16[256,512]{1,0:T(8,128)(2,1)S(1)}, u32[]{:S(2)}, u32[]{:S(2)}) collective-permute-start(bf16[256,512]{1,0:T(8,128)(2,1)S(1)} %bitcast.33), channel_id=1, source_target_pairs={{0,2},{1,3},{2,0},{3,1},{4,6},{5,7},{6,4},{7,5},{8,10},{9,11},{10,... | collective-permute-start | bytes 786440 | tf_op jit(solution)/shard_map/ppermute | solution.py:457
  25.5 12.8 %collective-permute-start.12 = (bf16[256,512]{1,0:T(8,128)(2,1)S(1)}, bf16[256,512]{1,0:T(8,128)(2,1)S(1)}, u32[]{:S(2)}, u32[]{:S(2)}) collective-permute-start(bf16[256,512]{1,0:T(8,128)(2,1)S(1)} %bitcast.32), channel_id=1, source_target_pairs={{0,2},{1,3},{2,0},{3,1},{4,6},{5,7},{6,4},{7,5},{8,10},{9,11},{10,... | collective-permute-start | bytes 786440 | tf_op jit(solution)/shard_map/ppermute | solution.py:457
  33.1 9.9 %collective-permute-start.8 = (bf16[256,512]{1,0:T(8,128)(2,1)S(1)}, bf16[256,512]{1,0:T(8,128)(2,1)S(1)}, u32[]{:S(2)}, u32[]{:S(2)}) collective-permute-start(bf16[256,512]{1,0:T(8,128)(2,1)S(1)} %collective-permute-done.7.refs_6_), channel_id=1, source_target_pairs={{0,1},{1,0},{2,3},{3,2},{4,5},{5,4},{6,7},{7,6},{8,9},{9,8},{10,11... | collective-permute-start | bytes 786440 | tf_op jit(solution)/shard_map/ppermute | solution.py:457
  38.3 9.9 %collective-permute-start.13 = (bf16[256,512]{1,0:T(8,128)(2,1)S(1)}, bf16[256,512]{1,0:T(8,128)(2,1)S(1)}, u32[]{:S(2)}, u32[]{:S(2)}) collective-permute-start(bf16[256,512]{1,0:T(8,128)(2,1)S(1)} %collective-permute-done.12.refs_6_), channel_id=1, source_target_pairs={{0,1},{1,0},{2,3},{3,2},{4,5},{5,4},{6,7},{7,6},{8,9},{9,8},{10,11... | collective-permute-start | bytes 786440 | tf_op jit(solution)/shard_map/ppermute | solution.py:457
  38.3 3.6 %collective-permute-start.1 = (f32[1,1024]{1,0:T(1,128)S(1)}, f32[1,1024]{1,0:T(1,128)S(1)}, u32[]{:S(2)}, u32[]{:S(2)}) collective-permute-start(f32[1,1024]{1,0:T(1,128)S(1)} %get-tuple-element.37.refs_0_), channel_id=1, source_target_pairs={{0,2},{1,3},{2,0},{3,1},{4,6},{5,7},{6,4},{7,5},{8,10},{9,11},{10,... | collective-permute-start | bytes 12296 | tf_op jit(solution)/shard_map/ppermute | solution.py:457
  39.8 2.1 %collective-permute-start = (f32[1,1024]{1,0:T(1,128)S(1)}, f32[1,1024]{1,0:T(1,128)S(1)}, u32[]{:S(2)}, u32[]{:S(2)}) collective-permute-start(f32[1,1024]{1,0:T(1,128)S(1)} %get-tuple-element.37.refs_0_), channel_id=1, source_target_pairs={{0,1},{1,0},{2,3},{3,2},{4,5},{5,4},{6,7},{7,6},{8,9},{9,8},{10,11... | collective-permute-start | bytes 12296 | tf_op jit(solution)/shard_map/ppermute | solution.py:457
  41.9 1.2 %collective-permute-start.2 = (f32[1,1024]{1,0:T(1,128)S(1)}, f32[1,1024]{1,0:T(1,128)S(1)}, u32[]{:S(2)}, u32[]{:S(2)}) collective-permute-start(f32[1,1024]{1,0:T(1,128)S(1)} %collective-permute-done.1.refs_2_), channel_id=1, source_target_pairs={{0,1},{1,0},{2,3},{3,2},{4,5},{5,4},{6,7},{7,6},{8,9},{9,8},{10,11... | collective-permute-start | bytes 12296 | tf_op jit(solution)/shard_map/ppermute | solution.py:457
  51.5 4.7 %collective-permute-start.15 = (bf16[1,256,512]{2,1,0:T(8,128)(2,1)S(1)}, bf16[1,256,512]{2,1,0:T(8,128)(2,1)S(1)}, u32[]{:S(2)}, u32[]{:S(2)}) collective-permute-start(bf16[1,256,512]{2,1,0:T(8,128)(2,1)S(1)} %get-tuple-element.59), channel_id=1, source_target_pairs={{0,1},{1,0},{2,3},{3,2},{4,5},{5,4},{6,7},{7,6},{8,9},{9,8},{10,11... | collective-permute-start | bytes 786440 | tf_op jit(solution)/shard_map/ppermute | solution.py:457
  51.8 6.2 %collective-permute-start.10 = (bf16[1,256,512]{2,1,0:T(8,128)(2,1)S(1)}, bf16[1,256,512]{2,1,0:T(8,128)(2,1)S(1)}, u32[]{:S(2)}, u32[]{:S(2)}) collective-permute-start(bf16[1,256,512]{2,1,0:T(8,128)(2,1)S(1)} %get-tuple-element.50), channel_id=1, source_target_pairs={{0,1},{1,0},{2,3},{3,2},{4,5},{5,4},{6,7},{7,6},{8,9},{9,8},{10,11... | collective-permute-start | bytes 786440 | tf_op jit(solution)/shard_map/ppermute | solution.py:457
  55.7 15.7 %collective-permute-start.14 = (bf16[256,512]{1,0:T(8,128)(2,1)S(1)}, bf16[256,512]{1,0:T(8,128)(2,1)S(1)}, u32[]{:S(2)}, u32[]{:S(2)}) collective-permute-start(bf16[256,512]{1,0:T(8,128)(2,1)S(1)} %get-tuple-element.57), channel_id=1, source_target_pairs={{0,1},{1,0},{2,3},{3,2},{4,5},{5,4},{6,7},{7,6},{8,9},{9,8},{10,11... | collective-permute-start | bytes 786440 | tf_op jit(solution)/shard_map/ppermute | solution.py:457
  55.9 15.5 %collective-permute-start.9 = (bf16[256,512]{1,0:T(8,128)(2,1)S(1)}, bf16[256,512]{1,0:T(8,128)(2,1)S(1)}, u32[]{:S(2)}, u32[]{:S(2)}) collective-permute-start(bf16[256,512]{1,0:T(8,128)(2,1)S(1)} %get-tuple-element.48), channel_id=1, source_target_pairs={{0,1},{1,0},{2,3},{3,2},{4,5},{5,4},{6,7},{7,6},{8,9},{9,8},{10,11... | collective-permute-start | bytes 786440 | tf_op jit(solution)/shard_map/ppermute | solution.py:457
  56.3 15.1 %collective-permute-start.16 = (bf16[1,256,512]{2,1,0:T(8,128)(2,1)S(1)}, bf16[1,256,512]{2,1,0:T(8,128)(2,1)S(1)}, u32[]{:S(2)}, u32[]{:S(2)}) collective-permute-start(bf16[1,256,512]{2,1,0:T(8,128)(2,1)S(1)} %add_convert_fusion), channel_id=1, source_target_pairs={{0,2},{1,3},{2,0},{3,1},{4,6},{5,7},{6,4},{7,5},{8,10},{9,11},{10,... | collective-permute-start | bytes 786440 | tf_op jit(solution)/shard_map/ppermute | solution.py:457
  58.0 13.5 %collective-permute-start.11 = (bf16[1,256,512]{2,1,0:T(8,128)(2,1)S(1)}, bf16[1,256,512]{2,1,0:T(8,128)(2,1)S(1)}, u32[]{:S(2)}, u32[]{:S(2)}) collective-permute-start(bf16[1,256,512]{2,1,0:T(8,128)(2,1)S(1)} %add_convert_fusion.1), channel_id=1, source_target_pairs={{0,2},{1,3},{2,0},{3,1},{4,6},{5,7},{6,4},{7,5},{8,10},{9,11},{10,... | collective-permute-start | bytes 786440 | tf_op jit(solution)/shard_map/ppermute | solution.py:457
  67.8 11.0 %all-to-all-start = ((f32[8,4,1024]{2,1,0:T(4,128)}), f32[8,4,1024]{2,1,0:T(4,128)S(1)}, u32[]{:S(2)}, u32[]{:S(2)}) async-start(f32[8,4,1024]{2,1,0:T(4,128)} %get-tuple-element.38), calls=%async_computation | async-start | bytes 262144 | tf_op jit(solution)/shard_map/all_to_all | solution.py:533
  78.7 20.5 %all-to-all-start.2 = ((bf16[8,64,512]{2,1,0:T(8,128)(2,1)}), bf16[8,64,512]{2,1,0:T(8,128)(2,1)S(1)}, u32[]{:S(2)}, u32[]{:S(2)}) async-start(bf16[8,64,512]{2,1,0:T(8,128)(2,1)} %bitcast.19), calls=%async_computation.2 | async-start | bytes 1048576 | tf_op jit(solution)/shard_map/all_to_all | solution.py:608
  87.1 6.7 %collective-permute-start.4 = (bf16[256,512]{1,0:T(8,128)(2,1)S(1)}, bf16[256,512]{1,0:T(8,128)(2,1)S(1)}, u32[]{:S(2)}, u32[]{:S(2)}) collective-permute-start(bf16[256,512]{1,0:T(8,128)(2,1)S(1)} %mixer_read.1.refs_0_), channel_id=1, source_target_pairs={{0,2},{1,3},{2,0},{3,1},{4,6},{5,7},{6,4},{7,5},{8,10},{9,11},{10,... | collective-permute-start | bytes 786440 | tf_op jit(solution)/shard_map/ppermute | solution.py:457
  88.7 8.5 %collective-permute-start.3 = (bf16[256,512]{1,0:T(8,128)(2,1)S(1)}, bf16[256,512]{1,0:T(8,128)(2,1)S(1)}, u32[]{:S(2)}, u32[]{:S(2)}) collective-permute-start(bf16[256,512]{1,0:T(8,128)(2,1)S(1)} %mixer_read.1.refs_0_), channel_id=1, source_target_pairs={{0,1},{1,0},{2,3},{3,2},{4,5},{5,4},{6,7},{7,6},{8,9},{9,8},{10,11... | collective-permute-start | bytes 786440 | tf_op jit(solution)/shard_map/ppermute | solution.py:457
  93.9 3.4 %collective-permute-start.5 = (bf16[256,512]{1,0:T(8,128)(2,1)S(1)}, bf16[256,512]{1,0:T(8,128)(2,1)S(1)}, u32[]{:S(2)}, u32[]{:S(2)}) collective-permute-start(bf16[256,512]{1,0:T(8,128)(2,1)S(1)} %collective-permute-done.4.refs_2_), channel_id=1, source_target_pairs={{0,1},{1,0},{2,3},{3,2},{4,5},{5,4},{6,7},{7,6},{8,9},{9,8},{10,11... | collective-permute-start | bytes 786440 | tf_op jit(solution)/shard_map/ppermute | solution.py:457

commit v6 on v4

--- a/solution.py
+++ b/solution.py
@@ -62,12 +62,20 @@
     return jnp.where(hit, place, -1.0)
 
 
-def send_kernel(experts, capacity, routes_ref, rows_ref, x_ref, gain_ref, out_ref, sums_ref):
+def send_kernel(
+    experts, capacity, routes_ref, rows_ref, x_hbm, gain_ref, out_hbm, sums_ref,
+    x_ref, out_ref, sems,
+):
+    come = pltpu.make_async_copy(x_hbm, x_ref, sems.at[0])
+    leave = pltpu.make_async_copy(out_ref, out_hbm, sems.at[1])
+    come.start()
     keys = slot_keys(routes_ref[...], experts)
     tokens = keys.shape[1]
     slot = iota((capacity, tokens), 0).astype(f32)
     chosen = [ones_where(slot == keys[e : e + 1, :]) for e in range(experts)]
     out_ref[...] = mm(jnp.concatenate(chosen, axis=0), rows_ref[...]).astype(bf16)
+    leave.start()
+    come.wait()
     rows = x_ref[...]
     count = rows.shape[0]
     ones = jnp.ones((8, rows.shape[1]), bf16)
@@ -76,6 +84,7 @@
     sums_ref[:, :count] = mm(ones, rows, NT)[0:1]
     sums_ref[:, count : 2 * count] = (mm(ones, high, NT) + mm(ones, low, NT))[0:1]
     sums_ref[:, 2 * count :] = gain_ref[...]
+    leave.wait()
 
 
 def share_kernel(experts, capacity, routes_ref, weight_ref, out_ref):
@@ -115,17 +124,55 @@
     out_ref[...] = out.astype(bf16)
 
 
-def hidden_kernel(parts, senders, start, me_ref, *refs):
+def first_kernel(*refs):
+    count = (len(refs) - 1) // 2
+    sems = refs[-1]
+    copies = []
+    for n in range(count):
+        out = refs[count + n]
+        copies.append(
+            pltpu.make_async_copy(
+                refs[n].at[0, :, pl.ds(0, out.shape[1])], out, sems.at[n]
+            )
+        )
+        copies[-1].start()
+    for copy in copies:
+        copy.wait()
+
+
+def hidden_kernel(parts, senders, start, load, me_ref, *refs):
     packs = refs[:parts]
     blocks = refs[parts : 2 * parts]
-    gate_ref, up_ref, down_ref, hidden_ref, odd_ref, normed_ref = refs[2 * parts :]
+    firsts = refs[2 * parts : 2 * parts + 2]
+    refs = refs[2 * parts + 2 :]
+    if load:
+        sources = refs[:3]
+        hidden_ref, odd_ref, gate_ref, up_ref, down_ref, normed_ref, sems = refs[3:]
+    else:
+        gate_ref, up_ref, down_ref, hidden_ref, odd_ref, normed_ref = refs
     rows, units = hidden_ref.shape
     full, feats = blocks[0].shape
     width = parts * feats
     chunk = rows // senders
     me = me_ref[0]
     lead = packs[0].shape[1] - feats
-    size = min(units, 256)
+    middle = firsts[0].shape[1]
+    size = min(middle, 256)
+    loads = []
+    if load:
+        for n in range((units - middle) // size):
+            cols = pl.ds(n * size, size)
+            loads.append([
+                pltpu.make_async_copy(
+                    source.at[0, :, pl.ds(middle + n * size, size)], ref.at[:, cols],
+                    sems.at[m, n],
+                )
+                for m, (source, ref) in enumerate(zip(sources, (gate_ref, up_ref)))
+            ])
+        loads.append([pltpu.make_async_copy(sources[2], down_ref, sems.at[2, 0])])
+        for group in loads:
+            for copy in group:
+                copy.start()
 
     def body(sender, unused):
         here = pl.ds(pl.multiple_of(sender * chunk, chunk), chunk)
@@ -148,11 +195,16 @@
 
     lax.fori_loop(0, senders, body, 0, unroll=4)
     for at in range(0, units, size):
-        cols = pl.ds(at, size)
+        tables, where = (firsts, at) if at < middle else ((gate_ref, up_ref), at - middle)
+        if load and at >= middle:
+            for copy in loads[where // size]:
+                copy.wait()
         normed = normed_ref[...]
-        gate = mm(normed, gate_ref[0, :, cols])
-        up = mm(normed, up_ref[0, :, cols])
-        hidden_ref[:, cols] = (gate * jax.nn.sigmoid(gate) * up).astype(bf16)
+        gate = mm(normed, tables[0][:, pl.ds(where, size)])
+        up = mm(normed, tables[1][:, pl.ds(where, size)])
+        hidden_ref[:, pl.ds(at, size)] = (gate * jax.nn.sigmoid(gate) * up).astype(bf16)
+    if load:
+        loads[-1][0].wait()
     for n in range(odd_ref.shape[0]):
         odd_ref[n] = down_part(me ^ (2 * n + 3), hidden_ref, down_ref, feats)
 
@@ -445,16 +497,22 @@
     send, packed = pl.pallas_call(
         functools.partial(send_kernel, n_ep, capacity),
         out_shape=(
-            jax.ShapeDtypeStruct((slots, feats), bf16),
+            pltpu.HBM((slots, feats), bf16),
             jax.ShapeDtypeStruct((1, 2 * rows + feats), f32),
         ),
-        in_specs=[vmem] * 4, out_specs=(vmem, vmem), compiler_params=params(60),
-        name="send_rows",
-    )(routes_t, expert_input, mixer_input, expert_gain.reshape(1, feats))
+        in_specs=[vmem, vmem, hbm, vmem], out_specs=(hbm, vmem),
+        scratch_shapes=[
+            pltpu.VMEM((rows, chans), bf16), pltpu.VMEM((slots, feats), bf16),
+            pltpu.SemaphoreType.DMA((2,)),
+        ],
+        compiler_params=params(8), name="send_rows",
+    )(
+        stay(routes_t), stay(expert_input), stay(mixer_input),
+        stay(expert_gain.reshape(1, feats)),
+    )
     arrived = lax.all_to_all(send, "ep", split_axis=0, concat_axis=0, tiled=True)
     packed, tp_at, ep_at = lax.optimization_barrier((packed, tp_at, ep_at))
     packs = gather_tp(packed)
-    packs[0] = stay(packed)
 
     groups, states = pole_real.shape
     flat = groups * states
@@ -513,8 +571,17 @@
             compiler_params=params(10),
         )(*(stay(w) for w in weights))
 
-    gate_w, up_w = fetch(expert_gate, expert_up)
-    (down_w,) = fetch(expert_down)
+    weights = (stay(expert_gate), stay(expert_up), stay(expert_down))
+    middle = units // 2
+    half_shape = jax.ShapeDtypeStruct((n_tp * feats, middle), bf16)
+    rest_shape = jax.ShapeDtypeStruct((n_tp * feats, units - middle), bf16)
+    firsts = pl.pallas_call(
+        first_kernel,
+        out_shape=(half_shape, half_shape), in_specs=[hbm] * 2, out_specs=(vmem,) * 2,
+        scratch_shapes=[pltpu.SemaphoreType.DMA((2,))],
+        compiler_params=params(10), name="fetch_first",
+    )(*weights[:2])
+    n_unit = max(1, (units - middle) // 256)
     terms = []
     for c in range(n_half):
         blocks = [arrived, partner]
@@ -522,20 +589,26 @@
             blocks += [far_blocks[c][k], swap(far_blocks[c][k], 1)]
         far_shape = jax.ShapeDtypeStruct((n_far, part, feats), bf16)
         part_shape = jax.ShapeDtypeStruct((part, feats), bf16)
-        hidden, odd_far = pl.pallas_call(
-            functools.partial(hidden_kernel, n_tp, n_ep, c * half),
-            in_specs=[smem] + [vmem] * (2 * n_tp + 3), out_specs=(vmem,) * 2,
-            scratch_shapes=[pltpu.VMEM((part, n_tp * feats), bf16)],
-            out_shape=(jax.ShapeDtypeStruct((part, units), bf16), far_shape),
+        load = c == 0
+        kept = [rest_shape, rest_shape, jax.ShapeDtypeStruct(expert_down.shape, bf16)]
+        kept = kept if load else []
+        hidden, odd_far, *held = pl.pallas_call(
+            functools.partial(hidden_kernel, n_tp, n_ep, c * half, load),
+            in_specs=[smem] + [vmem] * (2 * n_tp + 2) + [hbm if load else vmem] * 3,
+            out_specs=(vmem,) * (2 + len(kept)),
+            scratch_shapes=[pltpu.VMEM((part, n_tp * feats), bf16)]
+            + ([pltpu.SemaphoreType.DMA((3, n_unit))] if load else []),
+            out_shape=(jax.ShapeDtypeStruct((part, units), bf16), far_shape, *kept),
             compiler_params=params(12),
-        )(tp_at, *packs, *blocks, gate_w, up_w, down_w)
+        )(tp_at, *packs, *blocks, *firsts, *weights)
+        weights = held or weights
         theirs = swap(odd_far, 1)
         even_far, near, own = pl.pallas_call(
             rest_kernel,
             in_specs=[smem] + [vmem] * 2, out_specs=(vmem,) * 3,
             out_shape=(far_shape, part_shape, part_shape),
             compiler_params=params(8),
-        )(tp_at, hidden, down_w)
+        )(tp_at, hidden, weights[2])
         far = even_far.astype(f32) + theirs.astype(f32)
         terms += [own, swap(near, 1)]
         bit = n_tp // 4

time: 105 us -> 101 us (0.962)
  Pallas kernels: 39.4 us -> 35.4 us
    pallas_call x3 -> x1, Pallas kernels: 7.93 us -> 2.24 us  [fetch(): pl.pallas_call(fetch_kernel, out_shape=tuple((jax.ShapeDtypeStruct(w.shap...]
    pallas_call x2 -> x3, Pallas kernels: 7.95 us -> 9.73 us  [the longest x2 7.43 us: shards(): pl.pallas_call(functools.partial(hidden_kernel, n_tp, n_ep, c * half, loa...]
  transfers between devices with their start and end apart: 19 -> 19, of which waited for: 5 -> 5; matrix products, arithmetic and copies ran while one was open for 0% -> 0% of each run, Pallas kernels for 35% -> 29%
where the time goes in v6:
time: 101 us; the launch traced here: 100 us
  Pallas kernels  35.4 us (35%)
  waiting for transfers between devices  25.6 us (25%)
  blocking collectives  21.8 us (22%)
  starting transfers between devices  16.1 us (16%)
    all_to_all x1, blocking collectives, shards(): lax.all_to_all(send, 'ep', split_axis=0, concat_axis=0, tiled=True)  21.8 us
    ppermute x17, waiting for transfers between devices, swap(): return lax.ppermute(value, 'tp', [(i, i ^ bit) for i in range(count)])  19.3 us
    ppermute x17, starting transfers between devices, swap(): return lax.ppermute(value, 'tp', [(i, i ^ bit) for i in range(count)])  8.87 us
    pallas_call x2, Pallas kernels, shards(): pl.pallas_call(functools.partial(hidden_kernel, n_tp, n_ep, c * half, loa...  7.43 us
    all_to_all x1, waiting for transfers between devices, shards(): got = lax.all_to_all(ends, 'ep', split_axis=0, concat_axis=0)  6.29 us
    pallas_call x1, Pallas kernels, shards(): pl.pallas_call(functools.partial(scan_kernel, float(chans * n_tp), n_tp),...  6.15 us
    pallas_call x1, Pallas kernels, shards(): pl.pallas_call(read_kernel, out_shape=jax.ShapeDtypeStruct((rows, chans),...  4.88 us
    all_to_all x1, starting transfers between devices, shards(): back = lax.all_to_all(result, 'ep', split_axis=0, concat_axis=0, tiled=True)  3.67 us
  transfers between devices with their start and end apart: 19, of which 5 were waited for; matrix products, arithmetic and copies ran while one was open for 0% of the time, Pallas kernels for 29%

profile of v6, /device:TPU:0, one launch (start us, length us, event | category | flops | bytes accessed | tf_op | source)
XLA Modules:
  0.0 100.0 jit_solution(7730100204719573677)
XLA Ops:
  0.6 2.3 %send_rows.1 = (bf16[512,512]{1,0:T(8,128)(2,1)}, f32[1,1024]{1,0:T(1,128)S(1)}) custom-call(s32[2,128]{1,0:T(2,128)} %bitcast.37, bf16[128,512]{1,0:T(8,128)(2,1)} %rows_ref.1, bf16[256,512]{1,0:T(8,128)(2,1)} %x_ref.1, f32[1,512]{1,0:T(1,128)} %bitcast.39), custom_call_target="tpu_custom_call" | custom-call | tf_op jit(solution)/shard_map/send_rows/pallas_call | solution.py:497
  2.9 21.8 %all_to_all.27 = bf16[8,64,512]{2,1,0:T(8,128)(2,1)S(1)} all-to-all(bf16[8,64,512]{2,1,0:T(8,128)(2,1)} %bitcast.29), channel_id=1, replica_groups=mesh['ep'=8,'tp'=4] {'ep'}, dimensions={0} | all-to-all | bytes 1048576 | tf_op jit(solution)/shard_map/all_to_all | solution.py:513
  24.7 0.0 collective-permute-start.6
  24.8 1.6 %collective-permute-start.7 = (bf16[256,512]{1,0:T(8,128)(2,1)S(1)}, bf16[256,512]{1,0:T(8,128)(2,1)S(1)}, u32[]{:S(2)}, u32[]{:S(2)}) collective-permute-start(bf16[256,512]{1,0:T(8,128)(2,1)S(1)} %bitcast.33), channel_id=1, source_target_pairs={{0,2},{1,3},{2,0},{3,1},{4,6},{5,7},{6,4},{7,5},{8,10},{9,11},{10,... | collective-permute-start | bytes 786440 | tf_op jit(solution)/shard_map/ppermute | solution.py:468
  26.4 0.5 collective-permute-start.12
  26.9 7.2 %collective-permute-done.7.refs_6_ = bf16[256,512]{1,0:T(8,128)(2,1)S(1)} collective-permute-done((bf16[256,512]{1,0:T(8,128)(2,1)S(1)}, bf16[256,512]{1,0:T(8,128)(2,1)S(1)}, u32[]{:S(2)}, u32[]{:S(2)}) %collective-permute-start.7) | collective-permute-done | bytes 262176 | tf_op jit(solution)/shard_map/ppermute | solution.py:468
  34.0 0.0 collective-permute-start.8
  34.0 5.2 %collective-permute-done.12.refs_6_ = bf16[256,512]{1,0:T(8,128)(2,1)S(1)} collective-permute-done((bf16[256,512]{1,0:T(8,128)(2,1)S(1)}, bf16[256,512]{1,0:T(8,128)(2,1)S(1)}, u32[]{:S(2)}, u32[]{:S(2)}) %collective-permute-start.12) | collective-permute-done | bytes 262176 | tf_op jit(solution)/shard_map/ppermute | solution.py:468
  39.2 0.0 collective-permute-start.13
  39.2 1.5 %collective-permute-start.1 = (f32[1,1024]{1,0:T(1,128)S(1)}, f32[1,1024]{1,0:T(1,128)S(1)}, u32[]{:S(2)}, u32[]{:S(2)}) collective-permute-start(f32[1,1024]{1,0:T(1,128)S(1)} %get-tuple-element.38.refs_0_), channel_id=1, source_target_pairs={{0,2},{1,3},{2,0},{3,1},{4,6},{5,7},{6,4},{7,5},{8,10},{9,11},{10,... | collective-permute-start | bytes 12296 | tf_op jit(solution)/shard_map/ppermute | solution.py:468
  40.7 0.2 collective-permute-start
  40.9 1.9 %collective-permute-done.1.refs_2_ = f32[1,1024]{1,0:T(1,128)S(1)} collective-permute-done((f32[1,1024]{1,0:T(1,128)S(1)}, f32[1,1024]{1,0:T(1,128)S(1)}, u32[]{:S(2)}, u32[]{:S(2)}) %collective-permute-start.1) | collective-permute-done | bytes 4128 | tf_op jit(solution)/shard_map/ppermute | solution.py:468
  42.8 0.0 collective-permute-start.2
  42.8 2.3 %fetch_first.1 = (bf16[2048,512]{1,0:T(8,128)(2,1)S(1)}, bf16[2048,512]{1,0:T(8,128)(2,1)S(1)}) custom-call(bf16[1,2048,1024]{2,1,0:T(8,128)(2,1)} %refs_10_.1, bf16[1,2048,1024]{2,1,0:T(8,128)(2,1)} %refs_11_.1), custom_call_target="tpu_custom_call" | custom-call | tf_op jit(solution)/shard_map/fetch_first/pallas_call | solution.py:578
  45.1 0.0 collective-permute-done.refs_1_
  45.1 0.0 collective-permute-done.2.refs_3_
  45.1 0.0 collective-permute-done.6.refs_5_
  45.1 0.0 collective-permute-done.8.refs_7_
  45.1 4.0 %shard_map.186 = (bf16[256,1024]{1,0:T(8,128)(2,1)S(1)}, bf16[1,256,512]{2,1,0:T(8,128)(2,1)S(1)}, bf16[2048,512]{1,0:T(8,128)(2,1)S(1)}, bf16[2048,512]{1,0:T(8,128)(2,1)S(1)}, bf16[1,1024,2048]{2,1,0:T(8,128)(2,1)S(1)}) custom-call(s32[1]{0:T(128)} %bitcast.2.me_ref, f32[1,1024]{1,0:T(1,128)S(1)} %get-tuple-element.38.refs_0_, ...), custom_call_target="tpu_custom_call" | custom-call | tf_op jit(solution)/shard_map/pallas_call | solution.py:595
  49.2 0.0 collective-permute-done.13.refs_7_
  49.2 3.4 %shard_map.188 = (bf16[256,1024]{1,0:T(8,128)(2,1)S(1)}, bf16[1,256,512]{2,1,0:T(8,128)(2,1)S(1)}) custom-call(s32[1]{0:T(128)} %bitcast.2.me_ref, f32[1,1024]{1,0:T(1,128)S(1)} %get-tuple-element.38.refs_0_, f32[1,1024]{1,0:T(1,128)S(1)} %collective-permute-done.refs_1_, f32[1,1024]{1,0:T(1,128)S(1)} %collective-permute-done.1.refs_2_, ...), custom_call_target="tpu_custom_call" | custom-call | tf_op jit(solution)/shard_map/pallas_call | solution.py:595
  52.6 0.6 collective-permute-start.15
  53.2 0.1 collective-permute-start.10
  53.2 1.0 shard_map.189
  54.2 0.5 collective-permute-start.14
  54.7 1.0 shard_map.187
  55.7 0.1 collective-permute-start.9
  55.9 0.0 collective-permute-done.15
  55.9 0.1 add_convert_fusion
  55.9 1.6 %collective-permute-start.16 = (bf16[1,256,512]{2,1,0:T(8,128)(2,1)S(1)}, bf16[1,256,512]{2,1,0:T(8,128)(2,1)S(1)}, u32[]{:S(2)}, u32[]{:S(2)}) collective-permute-start(bf16[1,256,512]{2,1,0:T(8,128)(2,1)S(1)} %add_convert_fusion), channel_id=1, source_target_pairs={{0,2},{1,3},{2,0},{3,1},{4,6},{5,7},{6,4},{7,5},{8,10},{9,11},{10,... | collective-permute-start | bytes 786440 | tf_op jit(solution)/shard_map/ppermute | solution.py:468
  57.5 0.0 collective-permute-done.10
  57.5 0.1 add_convert_fusion.1
  57.6 0.6 collective-permute-start.11
  58.2 3.0 %mixer_poles.1 = (f32[256,1024]{1,0:T(8,128)S(1)}, f32[256,1024]{1,0:T(8,128)S(1)}, f32[2,1024]{1,0:T(2,128)S(1)}) custom-call(f32[32,256]{1,0:T(8,128)} %bitcast.36, f32[32,32]{1,0:T(8,128)} %pr_ref.1, f32[32,32]{1,0:T(8,128)} %pi_ref.1), custom_call_target="tpu_custom_call" | custom-call | tf_op jit(solution)/shard_map/mixer_poles/pallas_call | solution.py:520
  61.2 6.1 %mixer_scan.1 = (f32[256,1024]{1,0:T(8,128)}, f32[256,1024]{1,0:T(8,128)}, f32[256,1024]{1,0:T(8,128)}, f32[256,1024]{1,0:T(8,128)}, f32[8,4,1024]{2,1,0:T(4,128)}) custom-call(bf16[256,512]{1,0:T(8,128)(2,1)} %x_ref.1, f32[1,512]{1,0:T(1,128)} %bitcast.40, f32[256,1024]{1,0:T(8,128)S(1)} %get-tuple-element.35.ar_ref, ...), custom_call_target="tpu_custom_call" | custom-call | tf_op jit(solution)/shard_map/mixer_scan/pallas_call | solution.py:528
  67.4 3.6 %all-to-all-start = ((f32[8,4,1024]{2,1,0:T(4,128)}), f32[8,4,1024]{2,1,0:T(4,128)S(1)}, u32[]{:S(2)}, u32[]{:S(2)}) async-start(f32[8,4,1024]{2,1,0:T(4,128)} %get-tuple-element.39), calls=%async_computation | async-start | bytes 262144 | tf_op jit(solution)/shard_map/all_to_all | solution.py:548
  71.0 0.0 collective-permute-done.14.refs_4_
  71.0 0.0 collective-permute-done.9.refs_1_
  71.0 0.0 collective-permute-done.16
  71.0 0.0 collective-permute-done.11
  71.0 1.0 %expert_join.1 = bf16[512,512]{1,0:T(8,128)(2,1)} custom-call(bf16[256,512]{1,0:T(8,128)(2,1)S(1)} %get-tuple-element.51.refs_0_, bf16[256,512]{1,0:T(8,128)(2,1)S(1)} %collective-permute-done.9.refs_1_, bf16[256,512]{1,0:T(8,128)(2,1)S(1)} %bitcast.28, bf16[256,512]{1,0:T(8,128)(2,1)S(1)} %get-tuple-element.58.refs_3_, ...), custom_call_target="tpu_custom_call" | custom-call | tf_op jit(solution)/shard_map/expert_join/pallas_call | solution.py:620
  72.0 6.3 %all-to-all-done.got_ref = f32[8,4,1024]{2,1,0:T(4,128)S(1)} async-done(((f32[8,4,1024]{2,1,0:T(4,128)}), f32[8,4,1024]{2,1,0:T(4,128)S(1)}, u32[]{:S(2)}, u32[]{:S(2)}) %all-to-all-start) | async-done | bytes 131104 | tf_op jit(solution)/shard_map/all_to_all | solution.py:548
  78.3 3.7 %all-to-all-start.2 = ((bf16[8,64,512]{2,1,0:T(8,128)(2,1)}), bf16[8,64,512]{2,1,0:T(8,128)(2,1)S(1)}, u32[]{:S(2)}, u32[]{:S(2)}) async-start(bf16[8,64,512]{2,1,0:T(8,128)(2,1)} %bitcast.19), calls=%async_computation.2 | async-start | bytes 1048576 | tf_op jit(solution)/shard_map/all_to_all | solution.py:626
  82.0 4.9 %mixer_read.1.refs_0_ = bf16[256,512]{1,0:T(8,128)(2,1)S(1)} custom-call(s32[1]{0:T(128)} %bitcast.3.me_ref, f32[8,4,1024]{2,1,0:T(4,128)S(1)} %all-to-all-done.got_ref, f32[256,1024]{1,0:T(8,128)} %get-tuple-element.40.h_re_in, f32[256,1024]{1,0:T(8,128)} %get-tuple-element.41.h_im_in, f32[256,1024]{1,0:T(8,128)} %get-tuple-element.42.c_re_in, ...), custom_call_target="tpu_custom_call" | custom-call | tf_op jit(solution)/shard_map/mixer_read/pallas_call | solution.py:628
  86.9 1.6 %collective-permute-start.4 = (bf16[256,512]{1,0:T(8,128)(2,1)S(1)}, bf16[256,512]{1,0:T(8,128)(2,1)S(1)}, u32[]{:S(2)}, u32[]{:S(2)}) collective-permute-start(bf16[256,512]{1,0:T(8,128)(2,1)S(1)} %mixer_read.1.refs_0_), channel_id=1, source_target_pairs={{0,2},{1,3},{2,0},{3,1},{4,6},{5,7},{6,4},{7,5},{8,10},{9,11},{10,... | collective-permute-start | bytes 786440 | tf_op jit(solution)/shard_map/ppermute | solution.py:468
  88.5 0.0 collective-permute-start.3
  88.5 5.1 %collective-permute-done.4.refs_2_ = bf16[256,512]{1,0:T(8,128)(2,1)S(1)} collective-permute-done((bf16[256,512]{1,0:T(8,128)(2,1)S(1)}, bf16[256,512]{1,0:T(8,128)(2,1)S(1)}, u32[]{:S(2)}, u32[]{:S(2)}) %collective-permute-start.4) | collective-permute-done | bytes 262176 | tf_op jit(solution)/shard_map/ppermute | solution.py:468
  93.6 0.0 collective-permute-start.5
  93.6 1.1 %route_share.1.share_ref = bf16[3,128,512]{2,1,0:T(8,128)(2,1)S(1)} custom-call(s32[2,128]{1,0:T(2,128)} %bitcast.38, f32[2,128]{1,0:T(2,128)} %bitcast.41), custom_call_target="tpu_custom_call" | custom-call | tf_op jit(solution)/shard_map/route_share/pallas_call | solution.py:543
  94.7 2.2 %shard_map.185 = (bf16[2048,512]{1,0:T(8,128)(2,1)S(1)}, bf16[2048,512]{1,0:T(8,128)(2,1)S(1)}) custom-call(bf16[2048,512]{1,0:T(8,128)(2,1)} %refs_0_.2, bf16[2048,512]{1,0:T(8,128)(2,1)} %refs_1_.2), custom_call_target="tpu_custom_call" | custom-call | tf_op jit(solution)/shard_map/pallas_call | solution.py:566
  97.0 0.0 collective-permute-done.3.refs_1_
  97.0 0.0 collective-permute-done.5.refs_3_
  97.0 2.0 %mixer_out.1 = bf16[256,512]{1,0:T(8,128)(2,1)} custom-call(s32[1]{0:T(128)} %bitcast.2.me_ref, bf16[256,512]{1,0:T(8,128)(2,1)S(1)} %mixer_read.1.refs_0_, bf16[256,512]{1,0:T(8,128)(2,1)S(1)} %collective-permute-done.3.refs_1_, bf16[256,512]{1,0:T(8,128)(2,1)S(1)} %collective-permute-done.4.refs_2_, bf16[256,512]{1,0:T(8,128)(2,1)S(1)} %collective-permute-done.5.refs_3_, ...), custom_call_target="tpu_custom_call" | custom-call | tf_op jit(solution)/shard_map/mixer_out/pallas_call | solution.py:641
  99.0 0.0 all-to-all-done.2
  99.0 1.0 %combine.1 = bf16[128,512]{1,0:T(8,128)(2,1)} custom-call(bf16[3,128,512]{2,1,0:T(8,128)(2,1)S(1)} %route_share.1.share_ref, bf16[512,512]{1,0:T(8,128)(2,1)S(1)} %bitcast.26), custom_call_target="tpu_custom_call" | custom-call | tf_op jit(solution)/shard_map/combine/pallas_call | solution.py:647
  (1 shorter events, 0.0 us)
Async XLA Ops:
  24.7 20.4 %collective-permute-start.6 = (bf16[512,512]{1,0:T(8,128)(2,1)S(1)}, bf16[512,512]{1,0:T(8,128)(2,1)S(1)}, u32[]{:S(2)}, u32[]{:S(2)}) collective-permute-start(bf16[512,512]{1,0:T(8,128)(2,1)S(1)} %bitcast.23), channel_id=1, source_target_pairs={{0,1},{1,0},{2,3},{3,2},{4,5},{5,4},{6,7},{7,6},{8,9},{9,8},{10,11... | collective-permute-start | bytes 1572872 | tf_op jit(solution)/shard_map/ppermute | solution.py:468
  24.8 9.2 %collective-permute-start.7 = (bf16[256,512]{1,0:T(8,128)(2,1)S(1)}, bf16[256,512]{1,0:T(8,128)(2,1)S(1)}, u32[]{:S(2)}, u32[]{:S(2)}) collective-permute-start(bf16[256,512]{1,0:T(8,128)(2,1)S(1)} %bitcast.33), channel_id=1, source_target_pairs={{0,2},{1,3},{2,0},{3,1},{4,6},{5,7},{6,4},{7,5},{8,10},{9,11},{10,... | collective-permute-start | bytes 786440 | tf_op jit(solution)/shard_map/ppermute | solution.py:468
  26.4 12.8 %collective-permute-start.12 = (bf16[256,512]{1,0:T(8,128)(2,1)S(1)}, bf16[256,512]{1,0:T(8,128)(2,1)S(1)}, u32[]{:S(2)}, u32[]{:S(2)}) collective-permute-start(bf16[256,512]{1,0:T(8,128)(2,1)S(1)} %bitcast.32), channel_id=1, source_target_pairs={{0,2},{1,3},{2,0},{3,1},{4,6},{5,7},{6,4},{7,5},{8,10},{9,11},{10,... | collective-permute-start | bytes 786440 | tf_op jit(solution)/shard_map/ppermute | solution.py:468
  34.0 11.1 %collective-permute-start.8 = (bf16[256,512]{1,0:T(8,128)(2,1)S(1)}, bf16[256,512]{1,0:T(8,128)(2,1)S(1)}, u32[]{:S(2)}, u32[]{:S(2)}) collective-permute-start(bf16[256,512]{1,0:T(8,128)(2,1)S(1)} %collective-permute-done.7.refs_6_), channel_id=1, source_target_pairs={{0,1},{1,0},{2,3},{3,2},{4,5},{5,4},{6,7},{7,6},{8,9},{9,8},{10,11... | collective-permute-start | bytes 786440 | tf_op jit(solution)/shard_map/ppermute | solution.py:468
  39.2 10.0 %collective-permute-start.13 = (bf16[256,512]{1,0:T(8,128)(2,1)S(1)}, bf16[256,512]{1,0:T(8,128)(2,1)S(1)}, u32[]{:S(2)}, u32[]{:S(2)}) collective-permute-start(bf16[256,512]{1,0:T(8,128)(2,1)S(1)} %collective-permute-done.12.refs_6_), channel_id=1, source_target_pairs={{0,1},{1,0},{2,3},{3,2},{4,5},{5,4},{6,7},{7,6},{8,9},{9,8},{10,11... | collective-permute-start | bytes 786440 | tf_op jit(solution)/shard_map/ppermute | solution.py:468
  39.2 3.6 %collective-permute-start.1 = (f32[1,1024]{1,0:T(1,128)S(1)}, f32[1,1024]{1,0:T(1,128)S(1)}, u32[]{:S(2)}, u32[]{:S(2)}) collective-permute-start(f32[1,1024]{1,0:T(1,128)S(1)} %get-tuple-element.38.refs_0_), channel_id=1, source_target_pairs={{0,2},{1,3},{2,0},{3,1},{4,6},{5,7},{6,4},{7,5},{8,10},{9,11},{10,... | collective-permute-start | bytes 12296 | tf_op jit(solution)/shard_map/ppermute | solution.py:468
  40.7 4.4 %collective-permute-start = (f32[1,1024]{1,0:T(1,128)S(1)}, f32[1,1024]{1,0:T(1,128)S(1)}, u32[]{:S(2)}, u32[]{:S(2)}) collective-permute-start(f32[1,1024]{1,0:T(1,128)S(1)} %get-tuple-element.38.refs_0_), channel_id=1, source_target_pairs={{0,1},{1,0},{2,3},{3,2},{4,5},{5,4},{6,7},{7,6},{8,9},{9,8},{10,11... | collective-permute-start | bytes 12296 | tf_op jit(solution)/shard_map/ppermute | solution.py:468
  42.8 2.3 %collective-permute-start.2 = (f32[1,1024]{1,0:T(1,128)S(1)}, f32[1,1024]{1,0:T(1,128)S(1)}, u32[]{:S(2)}, u32[]{:S(2)}) collective-permute-start(f32[1,1024]{1,0:T(1,128)S(1)} %collective-permute-done.1.refs_2_), channel_id=1, source_target_pairs={{0,1},{1,0},{2,3},{3,2},{4,5},{5,4},{6,7},{7,6},{8,9},{9,8},{10,11... | collective-permute-start | bytes 12296 | tf_op jit(solution)/shard_map/ppermute | solution.py:468
  52.6 3.3 %collective-permute-start.15 = (bf16[1,256,512]{2,1,0:T(8,128)(2,1)S(1)}, bf16[1,256,512]{2,1,0:T(8,128)(2,1)S(1)}, u32[]{:S(2)}, u32[]{:S(2)}) collective-permute-start(bf16[1,256,512]{2,1,0:T(8,128)(2,1)S(1)} %get-tuple-element.61), channel_id=1, source_target_pairs={{0,1},{1,0},{2,3},{3,2},{4,5},{5,4},{6,7},{7,6},{8,9},{9,8},{10,11... | collective-permute-start | bytes 786440 | tf_op jit(solution)/shard_map/ppermute | solution.py:468
  53.2 4.4 %collective-permute-start.10 = (bf16[1,256,512]{2,1,0:T(8,128)(2,1)S(1)}, bf16[1,256,512]{2,1,0:T(8,128)(2,1)S(1)}, u32[]{:S(2)}, u32[]{:S(2)}) collective-permute-start(bf16[1,256,512]{2,1,0:T(8,128)(2,1)S(1)} %get-tuple-element.54), channel_id=1, source_target_pairs={{0,1},{1,0},{2,3},{3,2},{4,5},{5,4},{6,7},{7,6},{8,9},{9,8},{10,11... | collective-permute-start | bytes 786440 | tf_op jit(solution)/shard_map/ppermute | solution.py:468
  54.2 16.8 %collective-permute-start.14 = (bf16[256,512]{1,0:T(8,128)(2,1)S(1)}, bf16[256,512]{1,0:T(8,128)(2,1)S(1)}, u32[]{:S(2)}, u32[]{:S(2)}) collective-permute-start(bf16[256,512]{1,0:T(8,128)(2,1)S(1)} %get-tuple-element.59), channel_id=1, source_target_pairs={{0,1},{1,0},{2,3},{3,2},{4,5},{5,4},{6,7},{7,6},{8,9},{9,8},{10,11... | collective-permute-start | bytes 786440 | tf_op jit(solution)/shard_map/ppermute | solution.py:468
  55.7 15.3 %collective-permute-start.9 = (bf16[256,512]{1,0:T(8,128)(2,1)S(1)}, bf16[256,512]{1,0:T(8,128)(2,1)S(1)}, u32[]{:S(2)}, u32[]{:S(2)}) collective-permute-start(bf16[256,512]{1,0:T(8,128)(2,1)S(1)} %get-tuple-element.52), channel_id=1, source_target_pairs={{0,1},{1,0},{2,3},{3,2},{4,5},{5,4},{6,7},{7,6},{8,9},{9,8},{10,11... | collective-permute-start | bytes 786440 | tf_op jit(solution)/shard_map/ppermute | solution.py:468
  55.9 15.1 %collective-permute-start.16 = (bf16[1,256,512]{2,1,0:T(8,128)(2,1)S(1)}, bf16[1,256,512]{2,1,0:T(8,128)(2,1)S(1)}, u32[]{:S(2)}, u32[]{:S(2)}) collective-permute-start(bf16[1,256,512]{2,1,0:T(8,128)(2,1)S(1)} %add_convert_fusion), channel_id=1, source_target_pairs={{0,2},{1,3},{2,0},{3,1},{4,6},{5,7},{6,4},{7,5},{8,10},{9,11},{10,... | collective-permute-start | bytes 786440 | tf_op jit(solution)/shard_map/ppermute | solution.py:468
  57.6 13.4 %collective-permute-start.11 = (bf16[1,256,512]{2,1,0:T(8,128)(2,1)S(1)}, bf16[1,256,512]{2,1,0:T(8,128)(2,1)S(1)}, u32[]{:S(2)}, u32[]{:S(2)}) collective-permute-start(bf16[1,256,512]{2,1,0:T(8,128)(2,1)S(1)} %add_convert_fusion.1), channel_id=1, source_target_pairs={{0,2},{1,3},{2,0},{3,1},{4,6},{5,7},{6,4},{7,5},{8,10},{9,11},{10,... | collective-permute-start | bytes 786440 | tf_op jit(solution)/shard_map/ppermute | solution.py:468
  67.4 10.9 %all-to-all-start = ((f32[8,4,1024]{2,1,0:T(4,128)}), f32[8,4,1024]{2,1,0:T(4,128)S(1)}, u32[]{:S(2)}, u32[]{:S(2)}) async-start(f32[8,4,1024]{2,1,0:T(4,128)} %get-tuple-element.39), calls=%async_computation | async-start | bytes 262144 | tf_op jit(solution)/shard_map/all_to_all | solution.py:548
  78.3 20.7 %all-to-all-start.2 = ((bf16[8,64,512]{2,1,0:T(8,128)(2,1)}), bf16[8,64,512]{2,1,0:T(8,128)(2,1)S(1)}, u32[]{:S(2)}, u32[]{:S(2)}) async-start(bf16[8,64,512]{2,1,0:T(8,128)(2,1)} %bitcast.19), calls=%async_computation.2 | async-start | bytes 1048576 | tf_op jit(solution)/shard_map/all_to_all | solution.py:626
  86.9 6.7 %collective-permute-start.4 = (bf16[256,512]{1,0:T(8,128)(2,1)S(1)}, bf16[256,512]{1,0:T(8,128)(2,1)S(1)}, u32[]{:S(2)}, u32[]{:S(2)}) collective-permute-start(bf16[256,512]{1,0:T(8,128)(2,1)S(1)} %mixer_read.1.refs_0_), channel_id=1, source_target_pairs={{0,2},{1,3},{2,0},{3,1},{4,6},{5,7},{6,4},{7,5},{8,10},{9,11},{10,... | collective-permute-start | bytes 786440 | tf_op jit(solution)/shard_map/ppermute | solution.py:468
  88.5 8.5 %collective-permute-start.3 = (bf16[256,512]{1,0:T(8,128)(2,1)S(1)}, bf16[256,512]{1,0:T(8,128)(2,1)S(1)}, u32[]{:S(2)}, u32[]{:S(2)}) collective-permute-start(bf16[256,512]{1,0:T(8,128)(2,1)S(1)} %mixer_read.1.refs_0_), channel_id=1, source_target_pairs={{0,1},{1,0},{2,3},{3,2},{4,5},{5,4},{6,7},{7,6},{8,9},{9,8},{10,11... | collective-permute-start | bytes 786440 | tf_op jit(solution)/shard_map/ppermute | solution.py:468
  93.6 3.4 %collective-permute-start.5 = (bf16[256,512]{1,0:T(8,128)(2,1)S(1)}, bf16[256,512]{1,0:T(8,128)(2,1)S(1)}, u32[]{:S(2)}, u32[]{:S(2)}) collective-permute-start(bf16[256,512]{1,0:T(8,128)(2,1)S(1)} %collective-permute-done.4.refs_2_), channel_id=1, source_target_pairs={{0,1},{1,0},{2,3},{3,2},{4,5},{5,4},{6,7},{7,6},{8,9},{9,8},{10,11... | collective-permute-start | bytes 786440 | tf_op jit(solution)/shard_map/ppermute | solution.py:468

commit v7 on v6

--- a/solution.py
+++ b/solution.py
@@ -224,16 +224,25 @@
 
 
 def join_kernel(count, senders, *refs):
-    out_ref = refs[-1]
-    terms = (len(refs) - 1) // count
+    out_hbm, sum_ref, sems = refs[-3:]
+    terms = (len(refs) - 3) // count
     chunk = refs[0].shape[0] // senders
+    copies = []
     for c in range(count):
         for e in range(senders):
             total = None
             for ref in refs[c * terms : (c + 1) * terms]:
                 term = ref[pl.ds(e * chunk, chunk), :].astype(f32)
                 total = term if total is None else total + term
-            out_ref[pl.ds((e * count + c) * chunk, chunk), :] = total.astype(bf16)
+            sum_ref[c, e] = total.astype(bf16)
+        copies.append(
+            pltpu.make_async_copy(
+                sum_ref.at[c], out_hbm.at[:, pl.ds(c * chunk, chunk), :], sems.at[c]
+            )
+        )
+        copies[-1].start()
+    for copy in copies:
+        copy.wait()
 
 
 def reorder(rows, back):
@@ -278,7 +287,14 @@
     return jnp.where(same, wide, 0.0)
 
 
-def poles_kernel(step_ref, pr_ref, pi_ref, ar_ref, ai_ref, over_ref):
+def poles_kernel(count, step_ref, pr_ref, pi_ref, *refs):
+    ar_ref, ai_ref, over_ref = refs[count : count + 3]
+    copies = [
+        pltpu.make_async_copy(refs[n], refs[count + 3 + n], refs[-1].at[n])
+        for n in range(count)
+    ]
+    for copy in copies:
+        copy.start()
     groups, states = pr_ref.shape
     rows, flat = ar_ref.shape
     order = reorder(rows, False)
@@ -301,6 +317,8 @@
         sine, cosine = sin_cos(poles_im[:, at : at + piece] * delta)
         ar_ref[:, cols] = size * cosine
         ai_ref[:, cols] = size * sine
+    for copy in copies:
+        copy.wait()
 
 
 def scan_kernel(
@@ -512,17 +530,24 @@
     )
     arrived = lax.all_to_all(send, "ep", split_axis=0, concat_axis=0, tiled=True)
     packed, tp_at, ep_at = lax.optimization_barrier((packed, tp_at, ep_at))
-    packs = gather_tp(packed)
+    packs = [packed] + [swap(packed, k) for k in range(1, n_tp)]
 
     groups, states = pole_real.shape
     flat = groups * states
     big = jax.ShapeDtypeStruct((rows, flat), f32)
-    a_re, a_im, over = pl.pallas_call(
-        poles_kernel,
-        out_shape=(big, big, jax.ShapeDtypeStruct((2, flat), f32)),
-        in_specs=[vmem] * 3, out_specs=(vmem,) * 3, compiler_params=params(20),
-        name="mixer_poles",
-    )(stay(time_step.T), stay(pole_real), stay(pole_imag))
+    inputs = (
+        mixer_input,
+        jnp.swapaxes(input_real, 1, 2).reshape(chans, states),
+        jnp.swapaxes(input_imag, 1, 2).reshape(chans, states),
+    )
+    a_re, a_im, over, x_here, real_here, imag_here = pl.pallas_call(
+        functools.partial(poles_kernel, len(inputs)),
+        out_shape=(big, big, jax.ShapeDtypeStruct((2, flat), f32))
+        + tuple(jax.ShapeDtypeStruct(x.shape, x.dtype) for x in inputs),
+        in_specs=[vmem] * 3 + [hbm] * len(inputs), out_specs=(vmem,) * (3 + len(inputs)),
+        scratch_shapes=[pltpu.SemaphoreType.DMA((len(inputs),))],
+        compiler_params=params(20), name="mixer_poles",
+    )(stay(time_step.T), stay(pole_real), stay(pole_imag), *(stay(x) for x in inputs))
     n_block = max(1, chans // 256)
     far_big = pltpu.HBM((rows, flat), f32)
     *carried, ends = pl.pallas_call(
@@ -533,9 +558,7 @@
         + [pltpu.SemaphoreType.DMA((n_block, 4))],
         compiler_params=params(24), name="mixer_scan",
     )(
-        stay(mixer_input), stay(mixer_gain.reshape(1, chans)), a_re, a_im, over,
-        stay(jnp.swapaxes(input_real, 1, 2).reshape(chans, states)),
-        stay(jnp.swapaxes(input_imag, 1, 2).reshape(chans, states)),
+        x_here, stay(mixer_gain.reshape(1, chans)), a_re, a_im, over, real_here, imag_here,
         *packs,
     )
     n_half = 2 if capacity % 32 == 0 else 1
@@ -619,10 +642,14 @@
             bit //= 2
     result = pl.pallas_call(
         functools.partial(join_kernel, n_half, n_ep),
-        out_shape=jax.ShapeDtypeStruct((slots, feats), bf16),
-        in_specs=[vmem] * len(terms), out_specs=vmem, compiler_params=params(8),
-        name="expert_join",
-    )(*terms)
+        out_shape=pltpu.HBM((n_ep, capacity, feats), bf16),
+        in_specs=[vmem] * len(terms), out_specs=hbm,
+        scratch_shapes=[
+            pltpu.VMEM((n_half, n_ep, half, feats), bf16),
+            pltpu.SemaphoreType.DMA((n_half,)),
+        ],
+        compiler_params=params(8), name="expert_join",
+    )(*terms).reshape(slots, feats)
     back = lax.all_to_all(result, "ep", split_axis=0, concat_axis=0, tiled=True)
 
     mixed = pl.pallas_call(

time: 101 us -> 99.2 us (0.982)
  waiting for transfers between devices: 25.6 us -> 24.5 us
    ppermute x17, waiting for transfers between devices: 19.3 us -> 18.1 us  [swap(): return lax.ppermute(value, 'tp', [(i, i ^ bit) for i in range(count)])]
  transfers between devices with their start and end apart: 19 -> 19, of which waited for: 5 -> 4; matrix products, arithmetic and copies ran while one was open for 0% -> 0% of each run, Pallas kernels for 29% -> 29%
where the time goes in v7:
time: 99.2 us; the launch traced here: 98.7 us
  Pallas kernels  34.8 us (35%)
  waiting for transfers between devices  24.5 us (25%)
  blocking collectives  21.8 us (22%)
  starting transfers between devices  16.5 us (17%)
    all_to_all x1, blocking collectives, shards(): lax.all_to_all(send, 'ep', split_axis=0, concat_axis=0, tiled=True)  21.8 us
    ppermute x17, waiting for transfers between devices, swap(): return lax.ppermute(value, 'tp', [(i, i ^ bit) for i in range(count)])  18.1 us
    ppermute x17, starting transfers between devices, swap(): return lax.ppermute(value, 'tp', [(i, i ^ bit) for i in range(count)])  9.28 us
    pallas_call x2, Pallas kernels, shards(): pl.pallas_call(functools.partial(hidden_kernel, n_tp, n_ep, c * half, loa...  7.33 us
    all_to_all x1, waiting for transfers between devices, shards(): got = lax.all_to_all(ends, 'ep', split_axis=0, concat_axis=0)  6.36 us
    pallas_call x1, Pallas kernels, shards(): pl.pallas_call(functools.partial(scan_kernel, float(chans * n_tp), n_tp),...  5.7 us
    pallas_call x1, Pallas kernels, shards(): pl.pallas_call(read_kernel, out_shape=jax.ShapeDtypeStruct((rows, chans),...  4.88 us
    all_to_all x1, starting transfers between devices, shards(): back = lax.all_to_all(result, 'ep', split_axis=0, concat_axis=0, tiled=True)  3.67 us
  transfers between devices with their start and end apart: 19, of which 4 were waited for; matrix products, arithmetic and copies ran while one was open for 0% of the time, Pallas kernels for 29%

profile of v7, /device:TPU:0, one launch (start us, length us, event | category | flops | bytes accessed | tf_op | source)
XLA Modules:
  0.0 98.7 jit_solution(6554687754635300008)
XLA Ops:
  0.6 2.3 %send_rows.1 = (bf16[512,512]{1,0:T(8,128)(2,1)}, f32[1,1024]{1,0:T(1,128)S(1)}) custom-call(s32[2,128]{1,0:T(2,128)} %bitcast.36, bf16[128,512]{1,0:T(8,128)(2,1)} %rows_ref.1, bf16[256,512]{1,0:T(8,128)(2,1)} %refs_0_.3, f32[1,512]{1,0:T(1,128)} %bitcast.38), custom_call_target="tpu_custom_call" | custom-call | tf_op jit(solution)/shard_map/send_rows/pallas_call | solution.py:515
  2.9 21.8 %all_to_all.24 = bf16[8,64,512]{2,1,0:T(8,128)(2,1)S(1)} all-to-all(bf16[8,64,512]{2,1,0:T(8,128)(2,1)} %bitcast.28), channel_id=1, replica_groups=mesh['ep'=8,'tp'=4] {'ep'}, dimensions={0} | all-to-all | bytes 1048576 | tf_op jit(solution)/shard_map/all_to_all | solution.py:531
  24.7 0.0 collective-permute-start.6
  24.8 1.6 %collective-permute-start.7 = (bf16[256,512]{1,0:T(8,128)(2,1)S(1)}, bf16[256,512]{1,0:T(8,128)(2,1)S(1)}, u32[]{:S(2)}, u32[]{:S(2)}) collective-permute-start(bf16[256,512]{1,0:T(8,128)(2,1)S(1)} %bitcast.32), channel_id=1, source_target_pairs={{0,2},{1,3},{2,0},{3,1},{4,6},{5,7},{6,4},{7,5},{8,10},{9,11},{10,... | collective-permute-start | bytes 786440 | tf_op jit(solution)/shard_map/ppermute | solution.py:486
  26.4 0.5 collective-permute-start.12
  26.9 7.2 %collective-permute-done.7.refs_6_ = bf16[256,512]{1,0:T(8,128)(2,1)S(1)} collective-permute-done((bf16[256,512]{1,0:T(8,128)(2,1)S(1)}, bf16[256,512]{1,0:T(8,128)(2,1)S(1)}, u32[]{:S(2)}, u32[]{:S(2)}) %collective-permute-start.7) | collective-permute-done | bytes 262176 | tf_op jit(solution)/shard_map/ppermute | solution.py:486
  34.0 0.0 collective-permute-start.8
  34.0 5.2 %collective-permute-done.12.refs_6_ = bf16[256,512]{1,0:T(8,128)(2,1)S(1)} collective-permute-done((bf16[256,512]{1,0:T(8,128)(2,1)S(1)}, bf16[256,512]{1,0:T(8,128)(2,1)S(1)}, u32[]{:S(2)}, u32[]{:S(2)}) %collective-permute-start.12) | collective-permute-done | bytes 262176 | tf_op jit(solution)/shard_map/ppermute | solution.py:486
  39.2 0.0 collective-permute-start.13
  39.2 0.5 collective-permute-start
  39.7 1.5 %collective-permute-start.1 = (f32[1,1024]{1,0:T(1,128)S(1)}, f32[1,1024]{1,0:T(1,128)S(1)}, u32[]{:S(2)}, u32[]{:S(2)}) collective-permute-start(f32[1,1024]{1,0:T(1,128)S(1)} %get-tuple-element.44.refs_0_), channel_id=1, source_target_pairs={{0,2},{1,3},{2,0},{3,1},{4,6},{5,7},{6,4},{7,5},{8,10},{9,11},{10,... | collective-permute-start | bytes 12296 | tf_op jit(solution)/shard_map/ppermute | solution.py:486
  41.2 0.0 collective-permute-done.refs_1_
  41.2 0.8 collective-permute-start.2
  42.0 2.3 %fetch_first.1 = (bf16[2048,512]{1,0:T(8,128)(2,1)S(1)}, bf16[2048,512]{1,0:T(8,128)(2,1)S(1)}) custom-call(bf16[1,2048,1024]{2,1,0:T(8,128)(2,1)} %refs_10_.1, bf16[1,2048,1024]{2,1,0:T(8,128)(2,1)} %refs_11_.1), custom_call_target="tpu_custom_call" | custom-call | tf_op jit(solution)/shard_map/fetch_first/pallas_call | solution.py:601
  44.3 0.0 collective-permute-done.1.refs_2_
  44.3 0.0 collective-permute-done.2.refs_3_
  44.3 0.0 collective-permute-done.6.refs_5_
  44.3 0.0 collective-permute-done.8.refs_7_
  44.3 4.0 %shard_map.186 = (bf16[256,1024]{1,0:T(8,128)(2,1)S(1)}, bf16[1,256,512]{2,1,0:T(8,128)(2,1)S(1)}, bf16[2048,512]{1,0:T(8,128)(2,1)S(1)}, bf16[2048,512]{1,0:T(8,128)(2,1)S(1)}, bf16[1,1024,2048]{2,1,0:T(8,128)(2,1)S(1)}) custom-call(s32[1]{0:T(128)} %bitcast.2.me_ref, f32[1,1024]{1,0:T(1,128)S(1)} %get-tuple-element.44.refs_0_, ...), custom_call_target="tpu_custom_call" | custom-call | tf_op jit(solution)/shard_map/pallas_call | solution.py:618
  48.4 0.0 collective-permute-done.13.refs_7_
  48.4 3.3 %shard_map.188 = (bf16[256,1024]{1,0:T(8,128)(2,1)S(1)}, bf16[1,256,512]{2,1,0:T(8,128)(2,1)S(1)}) custom-call(s32[1]{0:T(128)} %bitcast.2.me_ref, f32[1,1024]{1,0:T(1,128)S(1)} %get-tuple-element.44.refs_0_, f32[1,1024]{1,0:T(1,128)S(1)} %collective-permute-done.refs_1_, f32[1,1024]{1,0:T(1,128)S(1)} %collective-permute-done.1.refs_2_, ...), custom_call_target="tpu_custom_call" | custom-call | tf_op jit(solution)/shard_map/pallas_call | solution.py:618
  51.7 0.4 collective-permute-start.15
  52.1 0.1 collective-permute-start.10
  52.3 1.0 shard_map.189
  53.2 0.4 collective-permute-start.14
  53.7 1.0 shard_map.187
  54.7 0.2 collective-permute-start.9
  54.9 0.0 collective-permute-done.15
  54.9 0.1 add_convert_fusion
  55.0 1.0 %collective-permute-start.16 = (bf16[1,256,512]{2,1,0:T(8,128)(2,1)S(1)}, bf16[1,256,512]{2,1,0:T(8,128)(2,1)S(1)}, u32[]{:S(2)}, u32[]{:S(2)}) collective-permute-start(bf16[1,256,512]{2,1,0:T(8,128)(2,1)S(1)} %add_convert_fusion), channel_id=1, source_target_pairs={{0,2},{1,3},{2,0},{3,1},{4,6},{5,7},{6,4},{7,5},{8,10},{9,11},{10,... | collective-permute-start | bytes 786440 | tf_op jit(solution)/shard_map/ppermute | solution.py:486
  56.0 0.0 collective-permute-done.10
  56.0 0.1 add_convert_fusion.1
  56.0 1.2 %collective-permute-start.11 = (bf16[1,256,512]{2,1,0:T(8,128)(2,1)S(1)}, bf16[1,256,512]{2,1,0:T(8,128)(2,1)S(1)}, u32[]{:S(2)}, u32[]{:S(2)}) collective-permute-start(bf16[1,256,512]{2,1,0:T(8,128)(2,1)S(1)} %add_convert_fusion.1), channel_id=1, source_target_pairs={{0,2},{1,3},{2,0},{3,1},{4,6},{5,7},{6,4},{7,5},{8,10},{9,11},{10,... | collective-permute-start | bytes 786440 | tf_op jit(solution)/shard_map/ppermute | solution.py:486
  57.2 3.1 %mixer_poles.1 = (f32[256,1024]{1,0:T(8,128)S(1)}, f32[256,1024]{1,0:T(8,128)S(1)}, f32[2,1024]{1,0:T(2,128)S(1)}, bf16[256,512]{1,0:T(8,128)(2,1)S(1)}, f32[512,32]{1,0:T(8,128)S(1)}, /*index=5*/f32[512,32]{1,0:T(8,128)S(1)}) custom-call(f32[32,256]{1,0:T(8,128)} %bitcast.35, f32[32,32]{1,0:T(8,128)} %pr_ref.1, f32[32,32]{1,0:T(8,128)} %pi_ref.1, ...), custom_call_target="tpu_custom_call" | custom-call | tf_op jit(solution)/shard_map/mixer_poles/pallas_call | solution.py:543
  60.3 5.7 %mixer_scan.1 = (f32[256,1024]{1,0:T(8,128)}, f32[256,1024]{1,0:T(8,128)}, f32[256,1024]{1,0:T(8,128)}, f32[256,1024]{1,0:T(8,128)}, f32[8,4,1024]{2,1,0:T(4,128)}) custom-call(bf16[256,512]{1,0:T(8,128)(2,1)S(1)} %get-tuple-element.38.x_ref, f32[1,512]{1,0:T(1,128)} %bitcast.39, f32[256,1024]{1,0:T(8,128)S(1)} %get-tuple-element.39.ar_ref, ...), custom_call_target="tpu_custom_call" | custom-call | tf_op jit(solution)/shard_map/mixer_scan/pallas_call | solution.py:553
  66.0 3.6 %all-to-all-start = ((f32[8,4,1024]{2,1,0:T(4,128)}), f32[8,4,1024]{2,1,0:T(4,128)S(1)}, u32[]{:S(2)}, u32[]{:S(2)}) async-start(f32[8,4,1024]{2,1,0:T(4,128)} %get-tuple-element.45), calls=%async_computation | async-start | bytes 262144 | tf_op jit(solution)/shard_map/all_to_all | solution.py:571
  69.6 0.0 collective-permute-done.14.refs_4_
  69.6 0.0 collective-permute-done.9.refs_1_
  69.6 0.0 collective-permute-done.16
  69.6 0.0 collective-permute-done.11
  69.6 0.9 expert_join.1
  70.6 6.4 %all-to-all-done.got_ref = f32[8,4,1024]{2,1,0:T(4,128)S(1)} async-done(((f32[8,4,1024]{2,1,0:T(4,128)}), f32[8,4,1024]{2,1,0:T(4,128)S(1)}, u32[]{:S(2)}, u32[]{:S(2)}) %all-to-all-start) | async-done | bytes 131104 | tf_op jit(solution)/shard_map/all_to_all | solution.py:571
  76.9 3.7 %all-to-all-start.2 = ((bf16[8,64,512]{2,1,0:T(8,128)(2,1)}), bf16[8,64,512]{2,1,0:T(8,128)(2,1)S(1)}, u32[]{:S(2)}, u32[]{:S(2)}) async-start(bf16[8,64,512]{2,1,0:T(8,128)(2,1)} %expert_join.1), calls=%async_computation.2 | async-start | bytes 1048576 | tf_op jit(solution)/shard_map/all_to_all | solution.py:653
  80.6 4.9 %mixer_read.1.refs_0_ = bf16[256,512]{1,0:T(8,128)(2,1)S(1)} custom-call(s32[1]{0:T(128)} %bitcast.3.me_ref, f32[8,4,1024]{2,1,0:T(4,128)S(1)} %all-to-all-done.got_ref, f32[256,1024]{1,0:T(8,128)} %get-tuple-element.46.h_re_in, f32[256,1024]{1,0:T(8,128)} %get-tuple-element.47.h_im_in, f32[256,1024]{1,0:T(8,128)} %get-tuple-element.48.c_re_in, ...), custom_call_target="tpu_custom_call" | custom-call | tf_op jit(solution)/shard_map/mixer_read/pallas_call | solution.py:655
  85.5 1.0 %collective-permute-start.4 = (bf16[256,512]{1,0:T(8,128)(2,1)S(1)}, bf16[256,512]{1,0:T(8,128)(2,1)S(1)}, u32[]{:S(2)}, u32[]{:S(2)}) collective-permute-start(bf16[256,512]{1,0:T(8,128)(2,1)S(1)} %mixer_read.1.refs_0_), channel_id=1, source_target_pairs={{0,2},{1,3},{2,0},{3,1},{4,6},{5,7},{6,4},{7,5},{8,10},{9,11},{10,... | collective-permute-start | bytes 786440 | tf_op jit(solution)/shard_map/ppermute | solution.py:486
  86.5 0.0 collective-permute-start.3
  86.5 5.8 %collective-permute-done.4.refs_2_ = bf16[256,512]{1,0:T(8,128)(2,1)S(1)} collective-permute-done((bf16[256,512]{1,0:T(8,128)(2,1)S(1)}, bf16[256,512]{1,0:T(8,128)(2,1)S(1)}, u32[]{:S(2)}, u32[]{:S(2)}) %collective-permute-start.4) | collective-permute-done | bytes 262176 | tf_op jit(solution)/shard_map/ppermute | solution.py:486
  92.3 0.0 collective-permute-start.5
  92.3 1.1 %route_share.1.share_ref = bf16[3,128,512]{2,1,0:T(8,128)(2,1)S(1)} custom-call(s32[2,128]{1,0:T(2,128)} %bitcast.37, f32[2,128]{1,0:T(2,128)} %bitcast.40), custom_call_target="tpu_custom_call" | custom-call | tf_op jit(solution)/shard_map/route_share/pallas_call | solution.py:566
  93.4 2.2 %shard_map.185 = (bf16[2048,512]{1,0:T(8,128)(2,1)S(1)}, bf16[2048,512]{1,0:T(8,128)(2,1)S(1)}) custom-call(bf16[2048,512]{1,0:T(8,128)(2,1)} %refs_0_.4, bf16[2048,512]{1,0:T(8,128)(2,1)} %refs_1_.2), custom_call_target="tpu_custom_call" | custom-call | tf_op jit(solution)/shard_map/pallas_call | solution.py:589
  95.6 0.0 collective-permute-done.3.refs_1_
  95.6 0.0 collective-permute-done.5.refs_3_
  95.7 2.0 %mixer_out.1 = bf16[256,512]{1,0:T(8,128)(2,1)} custom-call(s32[1]{0:T(128)} %bitcast.2.me_ref, bf16[256,512]{1,0:T(8,128)(2,1)S(1)} %mixer_read.1.refs_0_, bf16[256,512]{1,0:T(8,128)(2,1)S(1)} %collective-permute-done.3.refs_1_, bf16[256,512]{1,0:T(8,128)(2,1)S(1)} %collective-permute-done.4.refs_2_, bf16[256,512]{1,0:T(8,128)(2,1)S(1)} %collective-permute-done.5.refs_3_, ...), custom_call_target="tpu_custom_call" | custom-call | tf_op jit(solution)/shard_map/mixer_out/pallas_call | solution.py:668
  97.6 0.0 all-to-all-done.2
  97.6 1.0 %combine.1 = bf16[128,512]{1,0:T(8,128)(2,1)} custom-call(bf16[3,128,512]{2,1,0:T(8,128)(2,1)S(1)} %route_share.1.share_ref, bf16[512,512]{1,0:T(8,128)(2,1)S(1)} %bitcast.25), custom_call_target="tpu_custom_call" | custom-call | tf_op jit(solution)/shard_map/combine/pallas_call | solution.py:674
  (1 shorter events, 0.0 us)
Async XLA Ops:
  24.7 19.6 %collective-permute-start.6 = (bf16[512,512]{1,0:T(8,128)(2,1)S(1)}, bf16[512,512]{1,0:T(8,128)(2,1)S(1)}, u32[]{:S(2)}, u32[]{:S(2)}) collective-permute-start(bf16[512,512]{1,0:T(8,128)(2,1)S(1)} %bitcast.22), channel_id=1, source_target_pairs={{0,1},{1,0},{2,3},{3,2},{4,5},{5,4},{6,7},{7,6},{8,9},{9,8},{10,11... | collective-permute-start | bytes 1572872 | tf_op jit(solution)/shard_map/ppermute | solution.py:486
  24.8 9.2 %collective-permute-start.7 = (bf16[256,512]{1,0:T(8,128)(2,1)S(1)}, bf16[256,512]{1,0:T(8,128)(2,1)S(1)}, u32[]{:S(2)}, u32[]{:S(2)}) collective-permute-start(bf16[256,512]{1,0:T(8,128)(2,1)S(1)} %bitcast.32), channel_id=1, source_target_pairs={{0,2},{1,3},{2,0},{3,1},{4,6},{5,7},{6,4},{7,5},{8,10},{9,11},{10,... | collective-permute-start | bytes 786440 | tf_op jit(solution)/shard_map/ppermute | solution.py:486
  26.4 12.8 %collective-permute-start.12 = (bf16[256,512]{1,0:T(8,128)(2,1)S(1)}, bf16[256,512]{1,0:T(8,128)(2,1)S(1)}, u32[]{:S(2)}, u32[]{:S(2)}) collective-permute-start(bf16[256,512]{1,0:T(8,128)(2,1)S(1)} %bitcast.31), channel_id=1, source_target_pairs={{0,2},{1,3},{2,0},{3,1},{4,6},{5,7},{6,4},{7,5},{8,10},{9,11},{10,... | collective-permute-start | bytes 786440 | tf_op jit(solution)/shard_map/ppermute | solution.py:486
  34.0 10.3 %collective-permute-start.8 = (bf16[256,512]{1,0:T(8,128)(2,1)S(1)}, bf16[256,512]{1,0:T(8,128)(2,1)S(1)}, u32[]{:S(2)}, u32[]{:S(2)}) collective-permute-start(bf16[256,512]{1,0:T(8,128)(2,1)S(1)} %collective-permute-done.7.refs_6_), channel_id=1, source_target_pairs={{0,1},{1,0},{2,3},{3,2},{4,5},{5,4},{6,7},{7,6},{8,9},{9,8},{10,11... | collective-permute-start | bytes 786440 | tf_op jit(solution)/shard_map/ppermute | solution.py:486
  39.2 9.2 %collective-permute-start.13 = (bf16[256,512]{1,0:T(8,128)(2,1)S(1)}, bf16[256,512]{1,0:T(8,128)(2,1)S(1)}, u32[]{:S(2)}, u32[]{:S(2)}) collective-permute-start(bf16[256,512]{1,0:T(8,128)(2,1)S(1)} %collective-permute-done.12.refs_6_), channel_id=1, source_target_pairs={{0,1},{1,0},{2,3},{3,2},{4,5},{5,4},{6,7},{7,6},{8,9},{9,8},{10,11... | collective-permute-start | bytes 786440 | tf_op jit(solution)/shard_map/ppermute | solution.py:486
  39.2 2.0 %collective-permute-start = (f32[1,1024]{1,0:T(1,128)S(1)}, f32[1,1024]{1,0:T(1,128)S(1)}, u32[]{:S(2)}, u32[]{:S(2)}) collective-permute-start(f32[1,1024]{1,0:T(1,128)S(1)} %get-tuple-element.44.refs_0_), channel_id=1, source_target_pairs={{0,1},{1,0},{2,3},{3,2},{4,5},{5,4},{6,7},{7,6},{8,9},{9,8},{10,11... | collective-permute-start | bytes 12296 | tf_op jit(solution)/shard_map/ppermute | solution.py:486
  39.7 4.6 %collective-permute-start.1 = (f32[1,1024]{1,0:T(1,128)S(1)}, f32[1,1024]{1,0:T(1,128)S(1)}, u32[]{:S(2)}, u32[]{:S(2)}) collective-permute-start(f32[1,1024]{1,0:T(1,128)S(1)} %get-tuple-element.44.refs_0_), channel_id=1, source_target_pairs={{0,2},{1,3},{2,0},{3,1},{4,6},{5,7},{6,4},{7,5},{8,10},{9,11},{10,... | collective-permute-start | bytes 12296 | tf_op jit(solution)/shard_map/ppermute | solution.py:486
  41.2 3.1 %collective-permute-start.2 = (f32[1,1024]{1,0:T(1,128)S(1)}, f32[1,1024]{1,0:T(1,128)S(1)}, u32[]{:S(2)}, u32[]{:S(2)}) collective-permute-start(f32[1,1024]{1,0:T(1,128)S(1)} %get-tuple-element.44.refs_0_), channel_id=1, source_target_pairs={{0,3},{1,2},{2,1},{3,0},{4,7},{5,6},{6,5},{7,4},{8,11},{9,10},{10,... | collective-permute-start | bytes 12296 | tf_op jit(solution)/shard_map/ppermute | solution.py:486
  51.7 3.2 %collective-permute-start.15 = (bf16[1,256,512]{2,1,0:T(8,128)(2,1)S(1)}, bf16[1,256,512]{2,1,0:T(8,128)(2,1)S(1)}, u32[]{:S(2)}, u32[]{:S(2)}) collective-permute-start(bf16[1,256,512]{2,1,0:T(8,128)(2,1)S(1)} %get-tuple-element.67), channel_id=1, source_target_pairs={{0,1},{1,0},{2,3},{3,2},{4,5},{5,4},{6,7},{7,6},{8,9},{9,8},{10,11... | collective-permute-start | bytes 786440 | tf_op jit(solution)/shard_map/ppermute | solution.py:486
  52.1 3.9 %collective-permute-start.10 = (bf16[1,256,512]{2,1,0:T(8,128)(2,1)S(1)}, bf16[1,256,512]{2,1,0:T(8,128)(2,1)S(1)}, u32[]{:S(2)}, u32[]{:S(2)}) collective-permute-start(bf16[1,256,512]{2,1,0:T(8,128)(2,1)S(1)} %get-tuple-element.60), channel_id=1, source_target_pairs={{0,1},{1,0},{2,3},{3,2},{4,5},{5,4},{6,7},{7,6},{8,9},{9,8},{10,11... | collective-permute-start | bytes 786440 | tf_op jit(solution)/shard_map/ppermute | solution.py:486
  53.2 16.4 %collective-permute-start.14 = (bf16[256,512]{1,0:T(8,128)(2,1)S(1)}, bf16[256,512]{1,0:T(8,128)(2,1)S(1)}, u32[]{:S(2)}, u32[]{:S(2)}) collective-permute-start(bf16[256,512]{1,0:T(8,128)(2,1)S(1)} %get-tuple-element.65), channel_id=1, source_target_pairs={{0,1},{1,0},{2,3},{3,2},{4,5},{5,4},{6,7},{7,6},{8,9},{9,8},{10,11... | collective-permute-start | bytes 786440 | tf_op jit(solution)/shard_map/ppermute | solution.py:486
  54.7 14.9 %collective-permute-start.9 = (bf16[256,512]{1,0:T(8,128)(2,1)S(1)}, bf16[256,512]{1,0:T(8,128)(2,1)S(1)}, u32[]{:S(2)}, u32[]{:S(2)}) collective-permute-start(bf16[256,512]{1,0:T(8,128)(2,1)S(1)} %get-tuple-element.58), channel_id=1, source_target_pairs={{0,1},{1,0},{2,3},{3,2},{4,5},{5,4},{6,7},{7,6},{8,9},{9,8},{10,11... | collective-permute-start | bytes 786440 | tf_op jit(solution)/shard_map/ppermute | solution.py:486
  55.0 14.7 %collective-permute-start.16 = (bf16[1,256,512]{2,1,0:T(8,128)(2,1)S(1)}, bf16[1,256,512]{2,1,0:T(8,128)(2,1)S(1)}, u32[]{:S(2)}, u32[]{:S(2)}) collective-permute-start(bf16[1,256,512]{2,1,0:T(8,128)(2,1)S(1)} %add_convert_fusion), channel_id=1, source_target_pairs={{0,2},{1,3},{2,0},{3,1},{4,6},{5,7},{6,4},{7,5},{8,10},{9,11},{10,... | collective-permute-start | bytes 786440 | tf_op jit(solution)/shard_map/ppermute | solution.py:486
  56.0 13.6 %collective-permute-start.11 = (bf16[1,256,512]{2,1,0:T(8,128)(2,1)S(1)}, bf16[1,256,512]{2,1,0:T(8,128)(2,1)S(1)}, u32[]{:S(2)}, u32[]{:S(2)}) collective-permute-start(bf16[1,256,512]{2,1,0:T(8,128)(2,1)S(1)} %add_convert_fusion.1), channel_id=1, source_target_pairs={{0,2},{1,3},{2,0},{3,1},{4,6},{5,7},{6,4},{7,5},{8,10},{9,11},{10,... | collective-permute-start | bytes 786440 | tf_op jit(solution)/shard_map/ppermute | solution.py:486
  66.0 10.9 %all-to-all-start = ((f32[8,4,1024]{2,1,0:T(4,128)}), f32[8,4,1024]{2,1,0:T(4,128)S(1)}, u32[]{:S(2)}, u32[]{:S(2)}) async-start(f32[8,4,1024]{2,1,0:T(4,128)} %get-tuple-element.45), calls=%async_computation | async-start | bytes 262144 | tf_op jit(solution)/shard_map/all_to_all | solution.py:571
  76.9 20.7 %all-to-all-start.2 = ((bf16[8,64,512]{2,1,0:T(8,128)(2,1)}), bf16[8,64,512]{2,1,0:T(8,128)(2,1)S(1)}, u32[]{:S(2)}, u32[]{:S(2)}) async-start(bf16[8,64,512]{2,1,0:T(8,128)(2,1)} %expert_join.1), calls=%async_computation.2 | async-start | bytes 1048576 | tf_op jit(solution)/shard_map/all_to_all | solution.py:653
  85.5 6.8 %collective-permute-start.4 = (bf16[256,512]{1,0:T(8,128)(2,1)S(1)}, bf16[256,512]{1,0:T(8,128)(2,1)S(1)}, u32[]{:S(2)}, u32[]{:S(2)}) collective-permute-start(bf16[256,512]{1,0:T(8,128)(2,1)S(1)} %mixer_read.1.refs_0_), channel_id=1, source_target_pairs={{0,2},{1,3},{2,0},{3,1},{4,6},{5,7},{6,4},{7,5},{8,10},{9,11},{10,... | collective-permute-start | bytes 786440 | tf_op jit(solution)/shard_map/ppermute | solution.py:486
  86.5 9.1 %collective-permute-start.3 = (bf16[256,512]{1,0:T(8,128)(2,1)S(1)}, bf16[256,512]{1,0:T(8,128)(2,1)S(1)}, u32[]{:S(2)}, u32[]{:S(2)}) collective-permute-start(bf16[256,512]{1,0:T(8,128)(2,1)S(1)} %mixer_read.1.refs_0_), channel_id=1, source_target_pairs={{0,1},{1,0},{2,3},{3,2},{4,5},{5,4},{6,7},{7,6},{8,9},{9,8},{10,11... | collective-permute-start | bytes 786440 | tf_op jit(solution)/shard_map/ppermute | solution.py:486
  92.3 3.4 %collective-permute-start.5 = (bf16[256,512]{1,0:T(8,128)(2,1)S(1)}, bf16[256,512]{1,0:T(8,128)(2,1)S(1)}, u32[]{:S(2)}, u32[]{:S(2)}) collective-permute-start(bf16[256,512]{1,0:T(8,128)(2,1)S(1)} %collective-permute-done.4.refs_2_), channel_id=1, source_target_pairs={{0,1},{1,0},{2,3},{3,2},{4,5},{5,4},{6,7},{7,6},{8,9},{9,8},{10,11... | collective-permute-start | bytes 786440 | tf_op jit(solution)/shard_map/ppermute | solution.py:486

commit v8 on v7

--- a/solution.py
+++ b/solution.py
@@ -124,18 +124,28 @@
     out_ref[...] = out.astype(bf16)
 
 
+CUTS = 4
+
+
+def in_pieces(source, target, sems):
+    rows = target.shape[0] // CUTS
+    return [
+        pltpu.make_async_copy(
+            source.at[pl.ds(n * rows, rows), :], target.at[pl.ds(n * rows, rows), :], sems.at[n]
+        )
+        for n in range(CUTS)
+    ]
+
+
 def first_kernel(*refs):
     count = (len(refs) - 1) // 2
     sems = refs[-1]
     copies = []
     for n in range(count):
         out = refs[count + n]
-        copies.append(
-            pltpu.make_async_copy(
-                refs[n].at[0, :, pl.ds(0, out.shape[1])], out, sems.at[n]
-            )
-        )
-        copies[-1].start()
+        copies += in_pieces(refs[n].at[0, :, pl.ds(0, out.shape[1])], out, sems.at[n])
+    for copy in copies:
+        copy.start()
     for copy in copies:
         copy.wait()
 
@@ -163,13 +173,14 @@
         for n in range((units - middle) // size):
             cols = pl.ds(n * size, size)
             loads.append([
-                pltpu.make_async_copy(
+                copy
+                for m, (source, ref) in enumerate(zip(sources, (gate_ref, up_ref)))
+                for copy in in_pieces(
                     source.at[0, :, pl.ds(middle + n * size, size)], ref.at[:, cols],
                     sems.at[m, n],
                 )
-                for m, (source, ref) in enumerate(zip(sources, (gate_ref, up_ref)))
             ])
-        loads.append([pltpu.make_async_copy(sources[2], down_ref, sems.at[2, 0])])
+        loads.append(in_pieces(sources[2].at[0], down_ref.at[0], sems.at[2, 0]))
         for group in loads:
             for copy in group:
                 copy.start()
@@ -204,7 +215,8 @@
         up = mm(normed, tables[1][:, pl.ds(where, size)])
         hidden_ref[:, pl.ds(at, size)] = (gate * jax.nn.sigmoid(gate) * up).astype(bf16)
     if load:
-        loads[-1][0].wait()
+        for copy in loads[-1]:
+            copy.wait()
     for n in range(odd_ref.shape[0]):
         odd_ref[n] = down_part(me ^ (2 * n + 3), hidden_ref, down_ref, feats)
 
@@ -601,7 +613,7 @@
     firsts = pl.pallas_call(
         first_kernel,
         out_shape=(half_shape, half_shape), in_specs=[hbm] * 2, out_specs=(vmem,) * 2,
-        scratch_shapes=[pltpu.SemaphoreType.DMA((2,))],
+        scratch_shapes=[pltpu.SemaphoreType.DMA((2, CUTS))],
         compiler_params=params(10), name="fetch_first",
     )(*weights[:2])
     n_unit = max(1, (units - middle) // 256)
@@ -620,7 +632,7 @@
             in_specs=[smem] + [vmem] * (2 * n_tp + 2) + [hbm if load else vmem] * 3,
             out_specs=(vmem,) * (2 + len(kept)),
             scratch_shapes=[pltpu.VMEM((part, n_tp * feats), bf16)]
-            + ([pltpu.SemaphoreType.DMA((3, n_unit))] if load else []),
+            + ([pltpu.SemaphoreType.DMA((3, n_unit, CUTS))] if load else []),
             out_shape=(jax.ShapeDtypeStruct((part, units), bf16), far_shape, *kept),
             compiler_params=params(12),
         )(tp_at, *packs, *blocks, *firsts, *weights)

time: 99.2 us -> 99.2 us (level)
  no operation moved by 1% of the time
where the time goes in v8:
time: 99.2 us; the launch traced here: 98.6 us
  Pallas kernels  35 us (35%)
  waiting for transfers between devices  24.5 us (25%)
  blocking collectives  21.8 us (22%)
  starting transfers between devices  16.4 us (17%)
    all_to_all x1, blocking collectives, shards(): lax.all_to_all(send, 'ep', split_axis=0, concat_axis=0, tiled=True)  21.8 us
    ppermute x17, waiting for transfers between devices, swap(): return lax.ppermute(value, 'tp', [(i, i ^ bit) for i in range(count)])  18.1 us
    ppermute x17, starting transfers between devices, swap(): return lax.ppermute(value, 'tp', [(i, i ^ bit) for i in range(count)])  9.28 us
    pallas_call x2, Pallas kernels, shards(): pl.pallas_call(functools.partial(hidden_kernel, n_tp, n_ep, c * half, loa...  7.43 us
    all_to_all x1, waiting for transfers between devices, shards(): got = lax.all_to_all(ends, 'ep', split_axis=0, concat_axis=0)  6.36 us
    pallas_call x1, Pallas kernels, shards(): pl.pallas_call(functools.partial(scan_kernel, float(chans * n_tp), n_tp),...  5.7 us
    pallas_call x1, Pallas kernels, shards(): pl.pallas_call(read_kernel, out_shape=jax.ShapeDtypeStruct((rows, chans),...  4.88 us
    all_to_all x1, starting transfers between devices, shards(): got = lax.all_to_all(ends, 'ep', split_axis=0, concat_axis=0)  3.61 us
  transfers between devices with their start and end apart: 19, of which 4 were waited for; matrix products, arithmetic and copies ran while one was open for 0% of the time, Pallas kernels for 29%

profile of v8, /device:TPU:0, one launch (start us, length us, event | category | flops | bytes accessed | tf_op | source)
XLA Modules:
  0.0 98.6 jit_solution(8839060818531049787)
XLA Ops:
  0.6 2.3 %send_rows.1 = (bf16[512,512]{1,0:T(8,128)(2,1)}, f32[1,1024]{1,0:T(1,128)S(1)}) custom-call(s32[2,128]{1,0:T(2,128)} %bitcast.36, bf16[128,512]{1,0:T(8,128)(2,1)} %rows_ref.1, bf16[256,512]{1,0:T(8,128)(2,1)} %refs_0_.3, f32[1,512]{1,0:T(1,128)} %bitcast.38), custom_call_target="tpu_custom_call" | custom-call | tf_op jit(solution)/shard_map/send_rows/pallas_call | solution.py:527
  2.9 21.8 %all_to_all.24 = bf16[8,64,512]{2,1,0:T(8,128)(2,1)S(1)} all-to-all(bf16[8,64,512]{2,1,0:T(8,128)(2,1)} %bitcast.28), channel_id=1, replica_groups=mesh['ep'=8,'tp'=4] {'ep'}, dimensions={0} | all-to-all | bytes 1048576 | tf_op jit(solution)/shard_map/all_to_all | solution.py:543
  24.7 0.0 collective-permute-start.6
  24.8 1.6 %collective-permute-start.7 = (bf16[256,512]{1,0:T(8,128)(2,1)S(1)}, bf16[256,512]{1,0:T(8,128)(2,1)S(1)}, u32[]{:S(2)}, u32[]{:S(2)}) collective-permute-start(bf16[256,512]{1,0:T(8,128)(2,1)S(1)} %bitcast.32), channel_id=1, source_target_pairs={{0,2},{1,3},{2,0},{3,1},{4,6},{5,7},{6,4},{7,5},{8,10},{9,11},{10,... | collective-permute-start | bytes 786440 | tf_op jit(solution)/shard_map/ppermute | solution.py:498
  26.4 0.5 collective-permute-start.12
  26.9 7.2 %collective-permute-done.7.refs_6_ = bf16[256,512]{1,0:T(8,128)(2,1)S(1)} collective-permute-done((bf16[256,512]{1,0:T(8,128)(2,1)S(1)}, bf16[256,512]{1,0:T(8,128)(2,1)S(1)}, u32[]{:S(2)}, u32[]{:S(2)}) %collective-permute-start.7) | collective-permute-done | bytes 262176 | tf_op jit(solution)/shard_map/ppermute | solution.py:498
  34.0 0.0 collective-permute-start.8
  34.0 5.2 %collective-permute-done.12.refs_6_ = bf16[256,512]{1,0:T(8,128)(2,1)S(1)} collective-permute-done((bf16[256,512]{1,0:T(8,128)(2,1)S(1)}, bf16[256,512]{1,0:T(8,128)(2,1)S(1)}, u32[]{:S(2)}, u32[]{:S(2)}) %collective-permute-start.12) | collective-permute-done | bytes 262176 | tf_op jit(solution)/shard_map/ppermute | solution.py:498
  39.2 0.0 collective-permute-start.13
  39.2 0.5 collective-permute-start
  39.7 1.5 %collective-permute-start.1 = (f32[1,1024]{1,0:T(1,128)S(1)}, f32[1,1024]{1,0:T(1,128)S(1)}, u32[]{:S(2)}, u32[]{:S(2)}) collective-permute-start(f32[1,1024]{1,0:T(1,128)S(1)} %get-tuple-element.44.refs_0_), channel_id=1, source_target_pairs={{0,2},{1,3},{2,0},{3,1},{4,6},{5,7},{6,4},{7,5},{8,10},{9,11},{10,... | collective-permute-start | bytes 12296 | tf_op jit(solution)/shard_map/ppermute | solution.py:498
  41.2 0.0 collective-permute-done.refs_1_
  41.2 0.8 collective-permute-start.2
  42.0 2.4 %fetch_first.1 = (bf16[2048,512]{1,0:T(8,128)(2,1)S(1)}, bf16[2048,512]{1,0:T(8,128)(2,1)S(1)}) custom-call(bf16[1,2048,1024]{2,1,0:T(8,128)(2,1)} %refs_10_.1, bf16[1,2048,1024]{2,1,0:T(8,128)(2,1)} %refs_11_.1), custom_call_target="tpu_custom_call" | custom-call | tf_op jit(solution)/shard_map/fetch_first/pallas_call | solution.py:613
  44.3 0.0 collective-permute-done.1.refs_2_
  44.3 0.0 collective-permute-done.2.refs_3_
  44.4 0.0 collective-permute-done.6.refs_5_
  44.4 0.0 collective-permute-done.8.refs_7_
  44.4 4.1 %shard_map.186 = (bf16[256,1024]{1,0:T(8,128)(2,1)S(1)}, bf16[1,256,512]{2,1,0:T(8,128)(2,1)S(1)}, bf16[2048,512]{1,0:T(8,128)(2,1)S(1)}, bf16[2048,512]{1,0:T(8,128)(2,1)S(1)}, bf16[1,1024,2048]{2,1,0:T(8,128)(2,1)S(1)}) custom-call(s32[1]{0:T(128)} %bitcast.2.me_ref, f32[1,1024]{1,0:T(1,128)S(1)} %get-tuple-element.44.refs_0_, ...), custom_call_target="tpu_custom_call" | custom-call | tf_op jit(solution)/shard_map/pallas_call | solution.py:630
  48.5 0.0 collective-permute-done.13.refs_7_
  48.5 3.3 %shard_map.188 = (bf16[256,1024]{1,0:T(8,128)(2,1)S(1)}, bf16[1,256,512]{2,1,0:T(8,128)(2,1)S(1)}) custom-call(s32[1]{0:T(128)} %bitcast.2.me_ref, f32[1,1024]{1,0:T(1,128)S(1)} %get-tuple-element.44.refs_0_, f32[1,1024]{1,0:T(1,128)S(1)} %collective-permute-done.refs_1_, f32[1,1024]{1,0:T(1,128)S(1)} %collective-permute-done.1.refs_2_, ...), custom_call_target="tpu_custom_call" | custom-call | tf_op jit(solution)/shard_map/pallas_call | solution.py:630
  51.8 0.4 collective-permute-start.15
  52.3 0.1 collective-permute-start.10
  52.4 1.0 shard_map.189
  53.4 0.4 collective-permute-start.14
  53.8 1.0 shard_map.187
  54.8 0.2 collective-permute-start.9
  55.0 0.0 collective-permute-done.15
  55.0 0.1 add_convert_fusion
  55.1 1.0 %collective-permute-start.16 = (bf16[1,256,512]{2,1,0:T(8,128)(2,1)S(1)}, bf16[1,256,512]{2,1,0:T(8,128)(2,1)S(1)}, u32[]{:S(2)}, u32[]{:S(2)}) collective-permute-start(bf16[1,256,512]{2,1,0:T(8,128)(2,1)S(1)} %add_convert_fusion), channel_id=1, source_target_pairs={{0,2},{1,3},{2,0},{3,1},{4,6},{5,7},{6,4},{7,5},{8,10},{9,11},{10,... | collective-permute-start | bytes 786440 | tf_op jit(solution)/shard_map/ppermute | solution.py:498
  56.1 0.0 collective-permute-done.10
  56.1 0.1 add_convert_fusion.1
  56.2 1.2 %collective-permute-start.11 = (bf16[1,256,512]{2,1,0:T(8,128)(2,1)S(1)}, bf16[1,256,512]{2,1,0:T(8,128)(2,1)S(1)}, u32[]{:S(2)}, u32[]{:S(2)}) collective-permute-start(bf16[1,256,512]{2,1,0:T(8,128)(2,1)S(1)} %add_convert_fusion.1), channel_id=1, source_target_pairs={{0,2},{1,3},{2,0},{3,1},{4,6},{5,7},{6,4},{7,5},{8,10},{9,11},{10,... | collective-permute-start | bytes 786440 | tf_op jit(solution)/shard_map/ppermute | solution.py:498
  57.3 3.1 %mixer_poles.1 = (f32[256,1024]{1,0:T(8,128)S(1)}, f32[256,1024]{1,0:T(8,128)S(1)}, f32[2,1024]{1,0:T(2,128)S(1)}, bf16[256,512]{1,0:T(8,128)(2,1)S(1)}, f32[512,32]{1,0:T(8,128)S(1)}, /*index=5*/f32[512,32]{1,0:T(8,128)S(1)}) custom-call(f32[32,256]{1,0:T(8,128)} %bitcast.35, f32[32,32]{1,0:T(8,128)} %pr_ref.1, f32[32,32]{1,0:T(8,128)} %pi_ref.1, ...), custom_call_target="tpu_custom_call" | custom-call | tf_op jit(solution)/shard_map/mixer_poles/pallas_call | solution.py:555
  60.4 5.7 %mixer_scan.1 = (f32[256,1024]{1,0:T(8,128)}, f32[256,1024]{1,0:T(8,128)}, f32[256,1024]{1,0:T(8,128)}, f32[256,1024]{1,0:T(8,128)}, f32[8,4,1024]{2,1,0:T(4,128)}) custom-call(bf16[256,512]{1,0:T(8,128)(2,1)S(1)} %get-tuple-element.38.x_ref, f32[1,512]{1,0:T(1,128)} %bitcast.39, f32[256,1024]{1,0:T(8,128)S(1)} %get-tuple-element.39.ar_ref, ...), custom_call_target="tpu_custom_call" | custom-call | tf_op jit(solution)/shard_map/mixer_scan/pallas_call | solution.py:565
  66.1 3.6 %all-to-all-start = ((f32[8,4,1024]{2,1,0:T(4,128)}), f32[8,4,1024]{2,1,0:T(4,128)S(1)}, u32[]{:S(2)}, u32[]{:S(2)}) async-start(f32[8,4,1024]{2,1,0:T(4,128)} %get-tuple-element.45), calls=%async_computation | async-start | bytes 262144 | tf_op jit(solution)/shard_map/all_to_all | solution.py:583
  69.7 0.0 collective-permute-done.14.refs_4_
  69.8 0.0 collective-permute-done.9.refs_1_
  69.8 0.0 collective-permute-done.16
  69.8 0.0 collective-permute-done.11
  69.8 0.9 expert_join.1
  70.7 6.4 %all-to-all-done.got_ref = f32[8,4,1024]{2,1,0:T(4,128)S(1)} async-done(((f32[8,4,1024]{2,1,0:T(4,128)}), f32[8,4,1024]{2,1,0:T(4,128)S(1)}, u32[]{:S(2)}, u32[]{:S(2)}) %all-to-all-start) | async-done | bytes 131104 | tf_op jit(solution)/shard_map/all_to_all | solution.py:583
  77.1 3.5 %all-to-all-start.2 = ((bf16[8,64,512]{2,1,0:T(8,128)(2,1)}), bf16[8,64,512]{2,1,0:T(8,128)(2,1)S(1)}, u32[]{:S(2)}, u32[]{:S(2)}) async-start(bf16[8,64,512]{2,1,0:T(8,128)(2,1)} %expert_join.1), calls=%async_computation.2 | async-start | bytes 1048576 | tf_op jit(solution)/shard_map/all_to_all | solution.py:665
  80.6 4.9 %mixer_read.1.refs_0_ = bf16[256,512]{1,0:T(8,128)(2,1)S(1)} custom-call(s32[1]{0:T(128)} %bitcast.3.me_ref, f32[8,4,1024]{2,1,0:T(4,128)S(1)} %all-to-all-done.got_ref, f32[256,1024]{1,0:T(8,128)} %get-tuple-element.46.h_re_in, f32[256,1024]{1,0:T(8,128)} %get-tuple-element.47.h_im_in, f32[256,1024]{1,0:T(8,128)} %get-tuple-element.48.c_re_in, ...), custom_call_target="tpu_custom_call" | custom-call | tf_op jit(solution)/shard_map/mixer_read/pallas_call | solution.py:667
  85.5 1.0 %collective-permute-start.4 = (bf16[256,512]{1,0:T(8,128)(2,1)S(1)}, bf16[256,512]{1,0:T(8,128)(2,1)S(1)}, u32[]{:S(2)}, u32[]{:S(2)}) collective-permute-start(bf16[256,512]{1,0:T(8,128)(2,1)S(1)} %mixer_read.1.refs_0_), channel_id=1, source_target_pairs={{0,2},{1,3},{2,0},{3,1},{4,6},{5,7},{6,4},{7,5},{8,10},{9,11},{10,... | collective-permute-start | bytes 786440 | tf_op jit(solution)/shard_map/ppermute | solution.py:498
  86.5 0.0 collective-permute-start.3
  86.5 5.8 %collective-permute-done.4.refs_2_ = bf16[256,512]{1,0:T(8,128)(2,1)S(1)} collective-permute-done((bf16[256,512]{1,0:T(8,128)(2,1)S(1)}, bf16[256,512]{1,0:T(8,128)(2,1)S(1)}, u32[]{:S(2)}, u32[]{:S(2)}) %collective-permute-start.4) | collective-permute-done | bytes 262176 | tf_op jit(solution)/shard_map/ppermute | solution.py:498
  92.2 0.0 collective-permute-start.5
  92.2 1.1 %route_share.1.share_ref = bf16[3,128,512]{2,1,0:T(8,128)(2,1)S(1)} custom-call(s32[2,128]{1,0:T(2,128)} %bitcast.37, f32[2,128]{1,0:T(2,128)} %bitcast.40), custom_call_target="tpu_custom_call" | custom-call | tf_op jit(solution)/shard_map/route_share/pallas_call | solution.py:578
  93.4 2.2 %shard_map.185 = (bf16[2048,512]{1,0:T(8,128)(2,1)S(1)}, bf16[2048,512]{1,0:T(8,128)(2,1)S(1)}) custom-call(bf16[2048,512]{1,0:T(8,128)(2,1)} %refs_0_.4, bf16[2048,512]{1,0:T(8,128)(2,1)} %refs_1_.2), custom_call_target="tpu_custom_call" | custom-call | tf_op jit(solution)/shard_map/pallas_call | solution.py:601
  95.6 0.0 collective-permute-done.3.refs_1_
  95.6 0.0 collective-permute-done.5.refs_3_
  95.6 2.0 %mixer_out.1 = bf16[256,512]{1,0:T(8,128)(2,1)} custom-call(s32[1]{0:T(128)} %bitcast.2.me_ref, bf16[256,512]{1,0:T(8,128)(2,1)S(1)} %mixer_read.1.refs_0_, bf16[256,512]{1,0:T(8,128)(2,1)S(1)} %collective-permute-done.3.refs_1_, bf16[256,512]{1,0:T(8,128)(2,1)S(1)} %collective-permute-done.4.refs_2_, bf16[256,512]{1,0:T(8,128)(2,1)S(1)} %collective-permute-done.5.refs_3_, ...), custom_call_target="tpu_custom_call" | custom-call | tf_op jit(solution)/shard_map/mixer_out/pallas_call | solution.py:680
  97.6 0.0 all-to-all-done.2
  97.6 1.0 %combine.1 = bf16[128,512]{1,0:T(8,128)(2,1)} custom-call(bf16[3,128,512]{2,1,0:T(8,128)(2,1)S(1)} %route_share.1.share_ref, bf16[512,512]{1,0:T(8,128)(2,1)S(1)} %bitcast.25), custom_call_target="tpu_custom_call" | custom-call | tf_op jit(solution)/shard_map/combine/pallas_call | solution.py:686
  (1 shorter events, 0.0 us)
Async XLA Ops:
  24.7 19.6 %collective-permute-start.6 = (bf16[512,512]{1,0:T(8,128)(2,1)S(1)}, bf16[512,512]{1,0:T(8,128)(2,1)S(1)}, u32[]{:S(2)}, u32[]{:S(2)}) collective-permute-start(bf16[512,512]{1,0:T(8,128)(2,1)S(1)} %bitcast.22), channel_id=1, source_target_pairs={{0,1},{1,0},{2,3},{3,2},{4,5},{5,4},{6,7},{7,6},{8,9},{9,8},{10,11... | collective-permute-start | bytes 1572872 | tf_op jit(solution)/shard_map/ppermute | solution.py:498
  24.8 9.2 %collective-permute-start.7 = (bf16[256,512]{1,0:T(8,128)(2,1)S(1)}, bf16[256,512]{1,0:T(8,128)(2,1)S(1)}, u32[]{:S(2)}, u32[]{:S(2)}) collective-permute-start(bf16[256,512]{1,0:T(8,128)(2,1)S(1)} %bitcast.32), channel_id=1, source_target_pairs={{0,2},{1,3},{2,0},{3,1},{4,6},{5,7},{6,4},{7,5},{8,10},{9,11},{10,... | collective-permute-start | bytes 786440 | tf_op jit(solution)/shard_map/ppermute | solution.py:498
  26.4 12.8 %collective-permute-start.12 = (bf16[256,512]{1,0:T(8,128)(2,1)S(1)}, bf16[256,512]{1,0:T(8,128)(2,1)S(1)}, u32[]{:S(2)}, u32[]{:S(2)}) collective-permute-start(bf16[256,512]{1,0:T(8,128)(2,1)S(1)} %bitcast.31), channel_id=1, source_target_pairs={{0,2},{1,3},{2,0},{3,1},{4,6},{5,7},{6,4},{7,5},{8,10},{9,11},{10,... | collective-permute-start | bytes 786440 | tf_op jit(solution)/shard_map/ppermute | solution.py:498
  34.0 10.4 %collective-permute-start.8 = (bf16[256,512]{1,0:T(8,128)(2,1)S(1)}, bf16[256,512]{1,0:T(8,128)(2,1)S(1)}, u32[]{:S(2)}, u32[]{:S(2)}) collective-permute-start(bf16[256,512]{1,0:T(8,128)(2,1)S(1)} %collective-permute-done.7.refs_6_), channel_id=1, source_target_pairs={{0,1},{1,0},{2,3},{3,2},{4,5},{5,4},{6,7},{7,6},{8,9},{9,8},{10,11... | collective-permute-start | bytes 786440 | tf_op jit(solution)/shard_map/ppermute | solution.py:498
  39.2 9.4 %collective-permute-start.13 = (bf16[256,512]{1,0:T(8,128)(2,1)S(1)}, bf16[256,512]{1,0:T(8,128)(2,1)S(1)}, u32[]{:S(2)}, u32[]{:S(2)}) collective-permute-start(bf16[256,512]{1,0:T(8,128)(2,1)S(1)} %collective-permute-done.12.refs_6_), channel_id=1, source_target_pairs={{0,1},{1,0},{2,3},{3,2},{4,5},{5,4},{6,7},{7,6},{8,9},{9,8},{10,11... | collective-permute-start | bytes 786440 | tf_op jit(solution)/shard_map/ppermute | solution.py:498
  39.2 2.0 %collective-permute-start = (f32[1,1024]{1,0:T(1,128)S(1)}, f32[1,1024]{1,0:T(1,128)S(1)}, u32[]{:S(2)}, u32[]{:S(2)}) collective-permute-start(f32[1,1024]{1,0:T(1,128)S(1)} %get-tuple-element.44.refs_0_), channel_id=1, source_target_pairs={{0,1},{1,0},{2,3},{3,2},{4,5},{5,4},{6,7},{7,6},{8,9},{9,8},{10,11... | collective-permute-start | bytes 12296 | tf_op jit(solution)/shard_map/ppermute | solution.py:498
  39.7 4.7 %collective-permute-start.1 = (f32[1,1024]{1,0:T(1,128)S(1)}, f32[1,1024]{1,0:T(1,128)S(1)}, u32[]{:S(2)}, u32[]{:S(2)}) collective-permute-start(f32[1,1024]{1,0:T(1,128)S(1)} %get-tuple-element.44.refs_0_), channel_id=1, source_target_pairs={{0,2},{1,3},{2,0},{3,1},{4,6},{5,7},{6,4},{7,5},{8,10},{9,11},{10,... | collective-permute-start | bytes 12296 | tf_op jit(solution)/shard_map/ppermute | solution.py:498
  41.2 3.1 %collective-permute-start.2 = (f32[1,1024]{1,0:T(1,128)S(1)}, f32[1,1024]{1,0:T(1,128)S(1)}, u32[]{:S(2)}, u32[]{:S(2)}) collective-permute-start(f32[1,1024]{1,0:T(1,128)S(1)} %get-tuple-element.44.refs_0_), channel_id=1, source_target_pairs={{0,3},{1,2},{2,1},{3,0},{4,7},{5,6},{6,5},{7,4},{8,11},{9,10},{10,... | collective-permute-start | bytes 12296 | tf_op jit(solution)/shard_map/ppermute | solution.py:498
  51.8 3.2 %collective-permute-start.15 = (bf16[1,256,512]{2,1,0:T(8,128)(2,1)S(1)}, bf16[1,256,512]{2,1,0:T(8,128)(2,1)S(1)}, u32[]{:S(2)}, u32[]{:S(2)}) collective-permute-start(bf16[1,256,512]{2,1,0:T(8,128)(2,1)S(1)} %get-tuple-element.67), channel_id=1, source_target_pairs={{0,1},{1,0},{2,3},{3,2},{4,5},{5,4},{6,7},{7,6},{8,9},{9,8},{10,11... | collective-permute-start | bytes 786440 | tf_op jit(solution)/shard_map/ppermute | solution.py:498
  52.3 3.9 %collective-permute-start.10 = (bf16[1,256,512]{2,1,0:T(8,128)(2,1)S(1)}, bf16[1,256,512]{2,1,0:T(8,128)(2,1)S(1)}, u32[]{:S(2)}, u32[]{:S(2)}) collective-permute-start(bf16[1,256,512]{2,1,0:T(8,128)(2,1)S(1)} %get-tuple-element.60), channel_id=1, source_target_pairs={{0,1},{1,0},{2,3},{3,2},{4,5},{5,4},{6,7},{7,6},{8,9},{9,8},{10,11... | collective-permute-start | bytes 786440 | tf_op jit(solution)/shard_map/ppermute | solution.py:498
  53.4 16.4 %collective-permute-start.14 = (bf16[256,512]{1,0:T(8,128)(2,1)S(1)}, bf16[256,512]{1,0:T(8,128)(2,1)S(1)}, u32[]{:S(2)}, u32[]{:S(2)}) collective-permute-start(bf16[256,512]{1,0:T(8,128)(2,1)S(1)} %get-tuple-element.65), channel_id=1, source_target_pairs={{0,1},{1,0},{2,3},{3,2},{4,5},{5,4},{6,7},{7,6},{8,9},{9,8},{10,11... | collective-permute-start | bytes 786440 | tf_op jit(solution)/shard_map/ppermute | solution.py:498
  54.8 14.9 %collective-permute-start.9 = (bf16[256,512]{1,0:T(8,128)(2,1)S(1)}, bf16[256,512]{1,0:T(8,128)(2,1)S(1)}, u32[]{:S(2)}, u32[]{:S(2)}) collective-permute-start(bf16[256,512]{1,0:T(8,128)(2,1)S(1)} %get-tuple-element.58), channel_id=1, source_target_pairs={{0,1},{1,0},{2,3},{3,2},{4,5},{5,4},{6,7},{7,6},{8,9},{9,8},{10,11... | collective-permute-start | bytes 786440 | tf_op jit(solution)/shard_map/ppermute | solution.py:498
  55.1 14.7 %collective-permute-start.16 = (bf16[1,256,512]{2,1,0:T(8,128)(2,1)S(1)}, bf16[1,256,512]{2,1,0:T(8,128)(2,1)S(1)}, u32[]{:S(2)}, u32[]{:S(2)}) collective-permute-start(bf16[1,256,512]{2,1,0:T(8,128)(2,1)S(1)} %add_convert_fusion), channel_id=1, source_target_pairs={{0,2},{1,3},{2,0},{3,1},{4,6},{5,7},{6,4},{7,5},{8,10},{9,11},{10,... | collective-permute-start | bytes 786440 | tf_op jit(solution)/shard_map/ppermute | solution.py:498
  56.2 13.6 %collective-permute-start.11 = (bf16[1,256,512]{2,1,0:T(8,128)(2,1)S(1)}, bf16[1,256,512]{2,1,0:T(8,128)(2,1)S(1)}, u32[]{:S(2)}, u32[]{:S(2)}) collective-permute-start(bf16[1,256,512]{2,1,0:T(8,128)(2,1)S(1)} %add_convert_fusion.1), channel_id=1, source_target_pairs={{0,2},{1,3},{2,0},{3,1},{4,6},{5,7},{6,4},{7,5},{8,10},{9,11},{10,... | collective-permute-start | bytes 786440 | tf_op jit(solution)/shard_map/ppermute | solution.py:498
  66.1 11.0 %all-to-all-start = ((f32[8,4,1024]{2,1,0:T(4,128)}), f32[8,4,1024]{2,1,0:T(4,128)S(1)}, u32[]{:S(2)}, u32[]{:S(2)}) async-start(f32[8,4,1024]{2,1,0:T(4,128)} %get-tuple-element.45), calls=%async_computation | async-start | bytes 262144 | tf_op jit(solution)/shard_map/all_to_all | solution.py:583
  77.1 20.5 %all-to-all-start.2 = ((bf16[8,64,512]{2,1,0:T(8,128)(2,1)}), bf16[8,64,512]{2,1,0:T(8,128)(2,1)S(1)}, u32[]{:S(2)}, u32[]{:S(2)}) async-start(bf16[8,64,512]{2,1,0:T(8,128)(2,1)} %expert_join.1), calls=%async_computation.2 | async-start | bytes 1048576 | tf_op jit(solution)/shard_map/all_to_all | solution.py:665
  85.5 6.8 %collective-permute-start.4 = (bf16[256,512]{1,0:T(8,128)(2,1)S(1)}, bf16[256,512]{1,0:T(8,128)(2,1)S(1)}, u32[]{:S(2)}, u32[]{:S(2)}) collective-permute-start(bf16[256,512]{1,0:T(8,128)(2,1)S(1)} %mixer_read.1.refs_0_), channel_id=1, source_target_pairs={{0,2},{1,3},{2,0},{3,1},{4,6},{5,7},{6,4},{7,5},{8,10},{9,11},{10,... | collective-permute-start | bytes 786440 | tf_op jit(solution)/shard_map/ppermute | solution.py:498
  86.5 9.1 %collective-permute-start.3 = (bf16[256,512]{1,0:T(8,128)(2,1)S(1)}, bf16[256,512]{1,0:T(8,128)(2,1)S(1)}, u32[]{:S(2)}, u32[]{:S(2)}) collective-permute-start(bf16[256,512]{1,0:T(8,128)(2,1)S(1)} %mixer_read.1.refs_0_), channel_id=1, source_target_pairs={{0,1},{1,0},{2,3},{3,2},{4,5},{5,4},{6,7},{7,6},{8,9},{9,8},{10,11... | collective-permute-start | bytes 786440 | tf_op jit(solution)/shard_map/ppermute | solution.py:498
  92.2 3.4 %collective-permute-start.5 = (bf16[256,512]{1,0:T(8,128)(2,1)S(1)}, bf16[256,512]{1,0:T(8,128)(2,1)S(1)}, u32[]{:S(2)}, u32[]{:S(2)}) collective-permute-start(bf16[256,512]{1,0:T(8,128)(2,1)S(1)} %collective-permute-done.4.refs_2_), channel_id=1, source_target_pairs={{0,1},{1,0},{2,3},{3,2},{4,5},{5,4},{6,7},{7,6},{8,9},{9,8},{10,11... | collective-permute-start | bytes 786440 | tf_op jit(solution)/shard_map/ppermute | solution.py:498

commit v9 on v6

--- a/solution.py
+++ b/solution.py
@@ -124,7 +124,7 @@
     out_ref[...] = out.astype(bf16)
 
 
-def first_kernel(*refs):
+def first_kernel(skip, *refs):
     count = (len(refs) - 1) // 2
     sems = refs[-1]
     copies = []
@@ -132,7 +132,7 @@
         out = refs[count + n]
         copies.append(
             pltpu.make_async_copy(
-                refs[n].at[0, :, pl.ds(0, out.shape[1])], out, sems.at[n]
+                refs[n].at[0, :, pl.ds(skip, out.shape[1])], out, sems.at[n]
             )
         )
         copies[-1].start()
@@ -140,11 +140,11 @@
         copy.wait()
 
 
-def hidden_kernel(parts, senders, start, load, me_ref, *refs):
+def hidden_kernel(parts, senders, start, load, early, me_ref, *refs):
     packs = refs[:parts]
     blocks = refs[parts : 2 * parts]
-    firsts = refs[2 * parts : 2 * parts + 2]
-    refs = refs[2 * parts + 2 :]
+    heads, firsts, refs = refs[2 * parts :][:early], refs[2 * parts + early :], None
+    firsts, refs = firsts[:2], firsts[2:]
     if load:
         sources = refs[:3]
         hidden_ref, odd_ref, gate_ref, up_ref, down_ref, normed_ref, sems = refs[3:]
@@ -156,7 +156,8 @@
     chunk = rows // senders
     me = me_ref[0]
     lead = packs[0].shape[1] - feats
-    middle = firsts[0].shape[1]
+    skip = heads[0].shape[1] if heads else 0
+    middle = skip + firsts[0].shape[1]
     size = min(middle, 256)
     loads = []
     if load:
@@ -195,7 +196,12 @@
 
     lax.fori_loop(0, senders, body, 0, unroll=4)
     for at in range(0, units, size):
-        tables, where = (firsts, at) if at < middle else ((gate_ref, up_ref), at - middle)
+        if at < skip:
+            tables, where = heads, at
+        elif at < middle:
+            tables, where = firsts, at - skip
+        else:
+            tables, where = (gate_ref, up_ref), at - middle
         if load and at >= middle:
             for copy in loads[where // size]:
                 copy.wait()
@@ -304,11 +310,22 @@
 
 
 def scan_kernel(
-    total, parts, x_ref, gain_ref, ar_ref, ai_ref, over_ref, ir_ref, ii_ref, *refs,
+    total, parts, early, x_ref, gain_ref, ar_ref, ai_ref, over_ref, ir_ref, ii_ref, *refs,
 ):
     packs = refs[:parts]
-    h_re_out, h_im_out, c_re_out, c_im_out, end_ref = refs[parts : parts + 5]
-    hr_ref, hi_ref, cr_ref, ci_ref, sems = refs[parts + 5 :]
+    refs = refs[parts:]
+    sources, refs = refs[:early], refs[early:]
+    h_re_out, h_im_out, c_re_out, c_im_out, end_ref = refs[:5]
+    heads, refs = refs[5 : 5 + early], refs[5 + early :]
+    hr_ref, hi_ref, cr_ref, ci_ref, sems, head_sems = refs
+    head_copies = [
+        pltpu.make_async_copy(
+            source.at[0, :, pl.ds(0, head.shape[1])], head, head_sems.at[n]
+        )
+        for n, (source, head) in enumerate(zip(sources, heads))
+    ]
+    for copy in head_copies:
+        copy.start()
     rows, feats = x_ref.shape
     flat = ar_ref.shape[1]
     states = ir_ref.shape[1]
@@ -372,7 +389,7 @@
     ends = jnp.concatenate([p_re, p_im, s_re, s_im], axis=0)
     for i in range(end_ref.shape[0]):
         end_ref[i] = ends
-    for copy in copies:
+    for copy in copies + head_copies:
         copy.wait()
 
 
@@ -525,19 +542,27 @@
     )(stay(time_step.T), stay(pole_real), stay(pole_imag))
     n_block = max(1, chans // 256)
     far_big = pltpu.HBM((rows, flat), f32)
+    middle = expert_gate.shape[2] // 2
+    head = 256 if middle > 256 else 0
+    early = [stay(expert_gate), stay(expert_up)] if head else []
+    head_shape = jax.ShapeDtypeStruct((n_tp * feats, head), bf16)
     *carried, ends = pl.pallas_call(
-        functools.partial(scan_kernel, float(chans * n_tp), n_tp),
-        out_shape=(far_big,) * 4 + (jax.ShapeDtypeStruct((n_ep, 4, flat), f32),),
-        in_specs=[vmem] * (7 + n_tp), out_specs=(hbm,) * 4 + (vmem,),
+        functools.partial(scan_kernel, float(chans * n_tp), n_tp, len(early)),
+        out_shape=(far_big,) * 4
+        + (jax.ShapeDtypeStruct((n_ep, 4, flat), f32),)
+        + (head_shape,) * len(early),
+        in_specs=[vmem] * (7 + n_tp) + [hbm] * len(early),
+        out_specs=(hbm,) * 4 + (vmem,) * (1 + len(early)),
         scratch_shapes=[pltpu.VMEM((rows, flat), f32)] * 4
-        + [pltpu.SemaphoreType.DMA((n_block, 4))],
+        + [pltpu.SemaphoreType.DMA((n_block, 4)), pltpu.SemaphoreType.DMA((2,))],
         compiler_params=params(24), name="mixer_scan",
     )(
         stay(mixer_input), stay(mixer_gain.reshape(1, chans)), a_re, a_im, over,
         stay(jnp.swapaxes(input_real, 1, 2).reshape(chans, states)),
         stay(jnp.swapaxes(input_imag, 1, 2).reshape(chans, states)),
-        *packs,
+        *packs, *early,
     )
+    carried, ends, heads = carried[:4], (carried + [ends])[4], (carried + [ends])[5:]
     n_half = 2 if capacity % 32 == 0 else 1
     half = capacity // n_half
     share = pl.pallas_call(
@@ -572,11 +597,10 @@
         )(*(stay(w) for w in weights))
 
     weights = (stay(expert_gate), stay(expert_up), stay(expert_down))
-    middle = units // 2
-    half_shape = jax.ShapeDtypeStruct((n_tp * feats, middle), bf16)
+    half_shape = jax.ShapeDtypeStruct((n_tp * feats, middle - head), bf16)
     rest_shape = jax.ShapeDtypeStruct((n_tp * feats, units - middle), bf16)
     firsts = pl.pallas_call(
-        first_kernel,
+        functools.partial(first_kernel, head),
         out_shape=(half_shape, half_shape), in_specs=[hbm] * 2, out_specs=(vmem,) * 2,
         scratch_shapes=[pltpu.SemaphoreType.DMA((2,))],
         compiler_params=params(10), name="fetch_first",
@@ -593,14 +617,16 @@
         kept = [rest_shape, rest_shape, jax.ShapeDtypeStruct(expert_down.shape, bf16)]
         kept = kept if load else []
         hidden, odd_far, *held = pl.pallas_call(
-            functools.partial(hidden_kernel, n_tp, n_ep, c * half, load),
-            in_specs=[smem] + [vmem] * (2 * n_tp + 2) + [hbm if load else vmem] * 3,
+            functools.partial(hidden_kernel, n_tp, n_ep, c * half, load, len(early)),
+            in_specs=[smem]
+            + [vmem] * (2 * n_tp + 2 + len(early))
+            + [hbm if load else vmem] * 3,
             out_specs=(vmem,) * (2 + len(kept)),
             scratch_shapes=[pltpu.VMEM((part, n_tp * feats), bf16)]
             + ([pltpu.SemaphoreType.DMA((3, n_unit))] if load else []),
             out_shape=(jax.ShapeDtypeStruct((part, units), bf16), far_shape, *kept),
             compiler_params=params(12),
-        )(tp_at, *packs, *blocks, *firsts, *weights)
+        )(tp_at, *packs, *blocks, *heads, *firsts, *weights)
         weights = held or weights
         theirs = swap(odd_far, 1)
         even_far, near, own = pl.pallas_call(

time: 101 us -> 103 us (1.020)
  waiting for transfers between devices: 25.6 us -> 29.1 us
    ppermute x17, waiting for transfers between devices: 19.3 us -> 29 us  [swap(): return lax.ppermute(value, 'tp', [(i, i ^ bit) for i in range(count)])]
    all_to_all x1, waiting for transfers between devices: 6.29 us -> 0.01 us  [shards(): got = lax.all_to_all(ends, 'ep', split_axis=0, concat_axis=0)]
  transfers between devices with their start and end apart: 19 -> 19, of which waited for: 5 -> 6; matrix products, arithmetic and copies ran while one was open for 0% -> 0% of each run, Pallas kernels for 29% -> 31%
where the time goes in v9:
time: 103 us
  Pallas kernels  34.7 us (34%)
  waiting for transfers between devices  29.1 us (28%)
  blocking collectives  21.8 us (21%)
  starting transfers between devices  16.2 us (16%)
    ppermute x17, waiting for transfers between devices, swap(): return lax.ppermute(value, 'tp', [(i, i ^ bit) for i in range(count)])  29 us
    all_to_all x1, blocking collectives, shards(): lax.all_to_all(send, 'ep', split_axis=0, concat_axis=0, tiled=True)  21.8 us
    ppermute x17, starting transfers between devices, swap(): return lax.ppermute(value, 'tp', [(i, i ^ bit) for i in range(count)])  8.89 us
    pallas_call x2, Pallas kernels, shards(): pl.pallas_call(functools.partial(hidden_kernel, n_tp, n_ep, c * half, loa...  7.38 us
    pallas_call x1, Pallas kernels, shards(): pl.pallas_call(functools.partial(scan_kernel, float(chans * n_tp), n_tp,...  6.19 us
    pallas_call x1, Pallas kernels, shards(): pl.pallas_call(read_kernel, out_shape=jax.ShapeDtypeStruct((rows, chans),...  4.88 us
    all_to_all x1, starting transfers between devices, shards(): back = lax.all_to_all(result, 'ep', split_axis=0, concat_axis=0, tiled=True)  3.67 us
    all_to_all x1, starting transfers between devices, shards(): got = lax.all_to_all(ends, 'ep', split_axis=0, concat_axis=0)  3.59 us
  transfers between devices with their start and end apart: 19, of which 6 were waited for; matrix products, arithmetic and copies ran while one was open for 0% of the time, Pallas kernels for 31%

profile of v9, /device:TPU:0, one launch (start us, length us, event | category | flops | bytes accessed | tf_op | source)
XLA Modules:
  0.0 102.7 jit_solution(5667044506398036479)
XLA Ops:
  0.6 2.3 %send_rows.1 = (bf16[512,512]{1,0:T(8,128)(2,1)}, f32[1,1024]{1,0:T(1,128)S(1)}) custom-call(s32[2,128]{1,0:T(2,128)} %bitcast.37, bf16[128,512]{1,0:T(8,128)(2,1)} %rows_ref.1, bf16[256,512]{1,0:T(8,128)(2,1)} %x_ref.1, f32[1,512]{1,0:T(1,128)} %bitcast.39), custom_call_target="tpu_custom_call" | custom-call | tf_op jit(solution)/shard_map/send_rows/pallas_call | solution.py:514
  2.9 21.8 %all_to_all.27 = bf16[8,64,512]{2,1,0:T(8,128)(2,1)S(1)} all-to-all(bf16[8,64,512]{2,1,0:T(8,128)(2,1)} %bitcast.29), channel_id=1, replica_groups=mesh['ep'=8,'tp'=4] {'ep'}, dimensions={0} | all-to-all | bytes 1048576 | tf_op jit(solution)/shard_map/all_to_all | solution.py:530
  24.7 0.0 collective-permute-start.6
  24.8 1.6 %collective-permute-start.7 = (bf16[256,512]{1,0:T(8,128)(2,1)S(1)}, bf16[256,512]{1,0:T(8,128)(2,1)S(1)}, u32[]{:S(2)}, u32[]{:S(2)}) collective-permute-start(bf16[256,512]{1,0:T(8,128)(2,1)S(1)} %bitcast.33), channel_id=1, source_target_pairs={{0,2},{1,3},{2,0},{3,1},{4,6},{5,7},{6,4},{7,5},{8,10},{9,11},{10,... | collective-permute-start | bytes 786440 | tf_op jit(solution)/shard_map/ppermute | solution.py:485
  26.4 0.5 collective-permute-start.12
  26.9 7.2 %collective-permute-done.7.refs_6_ = bf16[256,512]{1,0:T(8,128)(2,1)S(1)} collective-permute-done((bf16[256,512]{1,0:T(8,128)(2,1)S(1)}, bf16[256,512]{1,0:T(8,128)(2,1)S(1)}, u32[]{:S(2)}, u32[]{:S(2)}) %collective-permute-start.7) | collective-permute-done | bytes 262176 | tf_op jit(solution)/shard_map/ppermute | solution.py:485
  34.0 0.0 collective-permute-start.8
  34.0 5.2 %collective-permute-done.12.refs_6_ = bf16[256,512]{1,0:T(8,128)(2,1)S(1)} collective-permute-done((bf16[256,512]{1,0:T(8,128)(2,1)S(1)}, bf16[256,512]{1,0:T(8,128)(2,1)S(1)}, u32[]{:S(2)}, u32[]{:S(2)}) %collective-permute-start.12) | collective-permute-done | bytes 262176 | tf_op jit(solution)/shard_map/ppermute | solution.py:485
  39.2 0.0 collective-permute-start.13
  39.2 1.5 %collective-permute-start.1 = (f32[1,1024]{1,0:T(1,128)S(1)}, f32[1,1024]{1,0:T(1,128)S(1)}, u32[]{:S(2)}, u32[]{:S(2)}) collective-permute-start(f32[1,1024]{1,0:T(1,128)S(1)} %get-tuple-element.40.refs_0_), channel_id=1, source_target_pairs={{0,2},{1,3},{2,0},{3,1},{4,6},{5,7},{6,4},{7,5},{8,10},{9,11},{10,... | collective-permute-start | bytes 12296 | tf_op jit(solution)/shard_map/ppermute | solution.py:485
  40.7 0.2 collective-permute-start
  40.9 1.9 %collective-permute-done.1.refs_2_ = f32[1,1024]{1,0:T(1,128)S(1)} collective-permute-done((f32[1,1024]{1,0:T(1,128)S(1)}, f32[1,1024]{1,0:T(1,128)S(1)}, u32[]{:S(2)}, u32[]{:S(2)}) %collective-permute-start.1) | collective-permute-done | bytes 4128 | tf_op jit(solution)/shard_map/ppermute | solution.py:485
  42.8 0.0 collective-permute-start.2
  42.8 1.6 %fetch_first.1 = (bf16[2048,256]{1,0:T(8,128)(2,1)S(1)}, bf16[2048,256]{1,0:T(8,128)(2,1)S(1)}) custom-call(bf16[1,2048,1024]{2,1,0:T(8,128)(2,1)} %refs_12_.1, bf16[1,2048,1024]{2,1,0:T(8,128)(2,1)} %refs_13_.1), custom_call_target="tpu_custom_call" | custom-call | tf_op jit(solution)/shard_map/fetch_first/pallas_call | solution.py:602
  44.4 3.1 %mixer_poles.1 = (f32[256,1024]{1,0:T(8,128)S(1)}, f32[256,1024]{1,0:T(8,128)S(1)}, f32[2,1024]{1,0:T(2,128)S(1)}) custom-call(f32[32,256]{1,0:T(8,128)} %bitcast.36, f32[32,32]{1,0:T(8,128)} %pr_ref.1, f32[32,32]{1,0:T(8,128)} %pi_ref.1), custom_call_target="tpu_custom_call" | custom-call | tf_op jit(solution)/shard_map/mixer_poles/pallas_call | solution.py:537
  47.4 0.0 collective-permute-done.refs_1_
  47.5 0.0 collective-permute-done.2.refs_3_
  47.5 6.2 %mixer_scan.1 = (f32[256,1024]{1,0:T(8,128)}, f32[256,1024]{1,0:T(8,128)}, f32[256,1024]{1,0:T(8,128)}, f32[256,1024]{1,0:T(8,128)}, f32[8,4,1024]{2,1,0:T(4,128...) custom-call(bf16[256,512]{1,0:T(8,128)(2,1)} %x_ref.1, f32[1,512]{1,0:T(1,128)} %bitcast.40, ...), custom_call_target="tpu_custom_call" | custom-call | tf_op jit(solution)/shard_map/mixer_scan/pallas_call | solution.py:549
  53.7 0.0 collective-permute-done.6.refs_5_
  53.7 0.0 collective-permute-done.8.refs_7_
  53.7 4.0 %shard_map.186 = (bf16[256,1024]{1,0:T(8,128)(2,1)S(1)}, bf16[1,256,512]{2,1,0:T(8,128)(2,1)S(1)}, bf16[2048,512]{1,0:T(8,128)(2,1)S(1)}, bf16[2048,512]{1,0:T(8,128)(2,1)S(1)}, bf16[1,1024,2048]{2,1,0:T(8,128)(2,1)S(1)}) custom-call(s32[1]{0:T(128)} %bitcast.2.me_ref, f32[1,1024]{1,0:T(1,128)S(1)} %get-tuple-element.40.refs_0_, ...), custom_call_target="tpu_custom_call" | custom-call | tf_op jit(solution)/shard_map/pallas_call | solution.py:619
  57.7 0.6 collective-permute-start.10
  58.3 0.0 collective-permute-done.13.refs_7_
  58.3 3.3 %shard_map.188 = (bf16[256,1024]{1,0:T(8,128)(2,1)S(1)}, bf16[1,256,512]{2,1,0:T(8,128)(2,1)S(1)}) custom-call(s32[1]{0:T(128)} %bitcast.2.me_ref, f32[1,1024]{1,0:T(1,128)S(1)} %get-tuple-element.40.refs_0_, f32[1,1024]{1,0:T(1,128)S(1)} %collective-permute-done.refs_1_, f32[1,1024]{1,0:T(1,128)S(1)} %collective-permute-done.1.refs_2_, ...), custom_call_target="tpu_custom_call" | custom-call | tf_op jit(solution)/shard_map/pallas_call | solution.py:619
  61.6 0.1 collective-permute-start.15
  61.7 1.0 shard_map.187
  62.7 0.6 collective-permute-start.9
  63.3 1.0 shard_map.189
  64.3 0.1 collective-permute-start.14
  64.4 0.0 collective-permute-done.10
  64.4 0.1 add_convert_fusion.1
  64.4 1.6 %collective-permute-start.11 = (bf16[1,256,512]{2,1,0:T(8,128)(2,1)S(1)}, bf16[1,256,512]{2,1,0:T(8,128)(2,1)S(1)}, u32[]{:S(2)}, u32[]{:S(2)}) collective-permute-start(bf16[1,256,512]{2,1,0:T(8,128)(2,1)S(1)} %add_convert_fusion.1), channel_id=1, source_target_pairs={{0,2},{1,3},{2,0},{3,1},{4,6},{5,7},{6,4},{7,5},{8,10},{9,11},{10,... | collective-permute-start | bytes 786440 | tf_op jit(solution)/shard_map/ppermute | solution.py:485
  66.0 0.0 collective-permute-done.15
  66.0 0.1 add_convert_fusion
  66.1 0.6 collective-permute-start.16
  66.7 3.6 %all-to-all-start = ((f32[8,4,1024]{2,1,0:T(4,128)}), f32[8,4,1024]{2,1,0:T(4,128)S(1)}, u32[]{:S(2)}, u32[]{:S(2)}) async-start(f32[8,4,1024]{2,1,0:T(4,128)} %get-tuple-element.41), calls=%async_computation | async-start | bytes 262144 | tf_op jit(solution)/shard_map/all_to_all | solution.py:573
  70.3 0.0 collective-permute-done.9.refs_1_
  70.3 0.0 collective-permute-done.14.refs_4_
  70.3 3.4 %collective-permute-done.11 = bf16[1,256,512]{2,1,0:T(8,128)(2,1)S(1)} collective-permute-done((bf16[1,256,512]{2,1,0:T(8,128)(2,1)S(1)}, bf16[1,256,512]{2,1,0:T(8,128)(2,1)S(1)}, u32[]{:S(2)}, u32[]{:S(2)}) %collective-permute-start.11) | collective-permute-done | bytes 262176 | tf_op jit(solution)/shard_map/ppermute | solution.py:485
  73.7 5.1 %collective-permute-done.16 = bf16[1,256,512]{2,1,0:T(8,128)(2,1)S(1)} collective-permute-done((bf16[1,256,512]{2,1,0:T(8,128)(2,1)S(1)}, bf16[1,256,512]{2,1,0:T(8,128)(2,1)S(1)}, u32[]{:S(2)}, u32[]{:S(2)}) %collective-permute-start.16) | collective-permute-done | bytes 262176 | tf_op jit(solution)/shard_map/ppermute | solution.py:485
  78.8 1.0 expert_join.1
  79.8 0.0 all-to-all-done.got_ref
  79.8 3.7 %all-to-all-start.2 = ((bf16[8,64,512]{2,1,0:T(8,128)(2,1)}), bf16[8,64,512]{2,1,0:T(8,128)(2,1)S(1)}, u32[]{:S(2)}, u32[]{:S(2)}) async-start(bf16[8,64,512]{2,1,0:T(8,128)(2,1)} %bitcast.19), calls=%async_computation.2 | async-start | bytes 1048576 | tf_op jit(solution)/shard_map/all_to_all | solution.py:652
  83.5 4.9 %mixer_read.1.refs_0_ = bf16[256,512]{1,0:T(8,128)(2,1)S(1)} custom-call(s32[1]{0:T(128)} %bitcast.3.me_ref, f32[8,4,1024]{2,1,0:T(4,128)S(1)} %all-to-all-done.got_ref, f32[256,1024]{1,0:T(8,128)} %get-tuple-element.42.h_re_in, f32[256,1024]{1,0:T(8,128)} %get-tuple-element.43.h_im_in, f32[256,1024]{1,0:T(8,128)} %get-tuple-element.44.c_re_in, ...), custom_call_target="tpu_custom_call" | custom-call | tf_op jit(solution)/shard_map/mixer_read/pallas_call | solution.py:654
  88.4 1.6 %collective-permute-start.4 = (bf16[256,512]{1,0:T(8,128)(2,1)S(1)}, bf16[256,512]{1,0:T(8,128)(2,1)S(1)}, u32[]{:S(2)}, u32[]{:S(2)}) collective-permute-start(bf16[256,512]{1,0:T(8,128)(2,1)S(1)} %mixer_read.1.refs_0_), channel_id=1, source_target_pairs={{0,2},{1,3},{2,0},{3,1},{4,6},{5,7},{6,4},{7,5},{8,10},{9,11},{10,... | collective-permute-start | bytes 786440 | tf_op jit(solution)/shard_map/ppermute | solution.py:485
  90.0 0.0 collective-permute-start.3
  90.0 6.3 %collective-permute-done.4.refs_2_ = bf16[256,512]{1,0:T(8,128)(2,1)S(1)} collective-permute-done((bf16[256,512]{1,0:T(8,128)(2,1)S(1)}, bf16[256,512]{1,0:T(8,128)(2,1)S(1)}, u32[]{:S(2)}, u32[]{:S(2)}) %collective-permute-start.4) | collective-permute-done | bytes 262176 | tf_op jit(solution)/shard_map/ppermute | solution.py:485
  96.3 0.0 collective-permute-start.5
  96.3 1.1 %route_share.1.share_ref = bf16[3,128,512]{2,1,0:T(8,128)(2,1)S(1)} custom-call(s32[2,128]{1,0:T(2,128)} %bitcast.38, f32[2,128]{1,0:T(2,128)} %bitcast.41), custom_call_target="tpu_custom_call" | custom-call | tf_op jit(solution)/shard_map/route_share/pallas_call | solution.py:568
  97.4 2.2 %shard_map.185 = (bf16[2048,512]{1,0:T(8,128)(2,1)S(1)}, bf16[2048,512]{1,0:T(8,128)(2,1)S(1)}) custom-call(bf16[2048,512]{1,0:T(8,128)(2,1)} %refs_0_.2, bf16[2048,512]{1,0:T(8,128)(2,1)} %refs_1_.2), custom_call_target="tpu_custom_call" | custom-call | tf_op jit(solution)/shard_map/pallas_call | solution.py:591
  99.7 0.0 collective-permute-done.3.refs_1_
  99.7 0.0 collective-permute-done.5.refs_3_
  99.7 2.0 %mixer_out.1 = bf16[256,512]{1,0:T(8,128)(2,1)} custom-call(s32[1]{0:T(128)} %bitcast.2.me_ref, bf16[256,512]{1,0:T(8,128)(2,1)S(1)} %mixer_read.1.refs_0_, bf16[256,512]{1,0:T(8,128)(2,1)S(1)} %collective-permute-done.3.refs_1_, bf16[256,512]{1,0:T(8,128)(2,1)S(1)} %collective-permute-done.4.refs_2_, bf16[256,512]{1,0:T(8,128)(2,1)S(1)} %collective-permute-done.5.refs_3_, ...), custom_call_target="tpu_custom_call" | custom-call | tf_op jit(solution)/shard_map/mixer_out/pallas_call | solution.py:667
  101.7 0.0 all-to-all-done.2
  101.7 1.0 %combine.1 = bf16[128,512]{1,0:T(8,128)(2,1)} custom-call(bf16[3,128,512]{2,1,0:T(8,128)(2,1)S(1)} %route_share.1.share_ref, bf16[512,512]{1,0:T(8,128)(2,1)S(1)} %bitcast.26), custom_call_target="tpu_custom_call" | custom-call | tf_op jit(solution)/shard_map/combine/pallas_call | solution.py:673
  (1 shorter events, 0.0 us)
Async XLA Ops:
  24.7 28.9 %collective-permute-start.6 = (bf16[512,512]{1,0:T(8,128)(2,1)S(1)}, bf16[512,512]{1,0:T(8,128)(2,1)S(1)}, u32[]{:S(2)}, u32[]{:S(2)}) collective-permute-start(bf16[512,512]{1,0:T(8,128)(2,1)S(1)} %bitcast.23), channel_id=1, source_target_pairs={{0,1},{1,0},{2,3},{3,2},{4,5},{5,4},{6,7},{7,6},{8,9},{9,8},{10,11... | collective-permute-start | bytes 1572872 | tf_op jit(solution)/shard_map/ppermute | solution.py:485
  24.8 9.2 %collective-permute-start.7 = (bf16[256,512]{1,0:T(8,128)(2,1)S(1)}, bf16[256,512]{1,0:T(8,128)(2,1)S(1)}, u32[]{:S(2)}, u32[]{:S(2)}) collective-permute-start(bf16[256,512]{1,0:T(8,128)(2,1)S(1)} %bitcast.33), channel_id=1, source_target_pairs={{0,2},{1,3},{2,0},{3,1},{4,6},{5,7},{6,4},{7,5},{8,10},{9,11},{10,... | collective-permute-start | bytes 786440 | tf_op jit(solution)/shard_map/ppermute | solution.py:485
  26.4 12.8 %collective-permute-start.12 = (bf16[256,512]{1,0:T(8,128)(2,1)S(1)}, bf16[256,512]{1,0:T(8,128)(2,1)S(1)}, u32[]{:S(2)}, u32[]{:S(2)}) collective-permute-start(bf16[256,512]{1,0:T(8,128)(2,1)S(1)} %bitcast.32), channel_id=1, source_target_pairs={{0,2},{1,3},{2,0},{3,1},{4,6},{5,7},{6,4},{7,5},{8,10},{9,11},{10,... | collective-permute-start | bytes 786440 | tf_op jit(solution)/shard_map/ppermute | solution.py:485
  34.0 19.6 %collective-permute-start.8 = (bf16[256,512]{1,0:T(8,128)(2,1)S(1)}, bf16[256,512]{1,0:T(8,128)(2,1)S(1)}, u32[]{:S(2)}, u32[]{:S(2)}) collective-permute-start(bf16[256,512]{1,0:T(8,128)(2,1)S(1)} %collective-permute-done.7.refs_6_), channel_id=1, source_target_pairs={{0,1},{1,0},{2,3},{3,2},{4,5},{5,4},{6,7},{7,6},{8,9},{9,8},{10,11... | collective-permute-start | bytes 786440 | tf_op jit(solution)/shard_map/ppermute | solution.py:485
  39.2 19.1 %collective-permute-start.13 = (bf16[256,512]{1,0:T(8,128)(2,1)S(1)}, bf16[256,512]{1,0:T(8,128)(2,1)S(1)}, u32[]{:S(2)}, u32[]{:S(2)}) collective-permute-start(bf16[256,512]{1,0:T(8,128)(2,1)S(1)} %collective-permute-done.12.refs_6_), channel_id=1, source_target_pairs={{0,1},{1,0},{2,3},{3,2},{4,5},{5,4},{6,7},{7,6},{8,9},{9,8},{10,11... | collective-permute-start | bytes 786440 | tf_op jit(solution)/shard_map/ppermute | solution.py:485
  39.2 3.6 %collective-permute-start.1 = (f32[1,1024]{1,0:T(1,128)S(1)}, f32[1,1024]{1,0:T(1,128)S(1)}, u32[]{:S(2)}, u32[]{:S(2)}) collective-permute-start(f32[1,1024]{1,0:T(1,128)S(1)} %get-tuple-element.40.refs_0_), channel_id=1, source_target_pairs={{0,2},{1,3},{2,0},{3,1},{4,6},{5,7},{6,4},{7,5},{8,10},{9,11},{10,... | collective-permute-start | bytes 12296 | tf_op jit(solution)/shard_map/ppermute | solution.py:485
  40.7 6.7 %collective-permute-start = (f32[1,1024]{1,0:T(1,128)S(1)}, f32[1,1024]{1,0:T(1,128)S(1)}, u32[]{:S(2)}, u32[]{:S(2)}) collective-permute-start(f32[1,1024]{1,0:T(1,128)S(1)} %get-tuple-element.40.refs_0_), channel_id=1, source_target_pairs={{0,1},{1,0},{2,3},{3,2},{4,5},{5,4},{6,7},{7,6},{8,9},{9,8},{10,11... | collective-permute-start | bytes 12296 | tf_op jit(solution)/shard_map/ppermute | solution.py:485
  42.8 4.7 %collective-permute-start.2 = (f32[1,1024]{1,0:T(1,128)S(1)}, f32[1,1024]{1,0:T(1,128)S(1)}, u32[]{:S(2)}, u32[]{:S(2)}) collective-permute-start(f32[1,1024]{1,0:T(1,128)S(1)} %collective-permute-done.1.refs_2_), channel_id=1, source_target_pairs={{0,1},{1,0},{2,3},{3,2},{4,5},{5,4},{6,7},{7,6},{8,9},{9,8},{10,11... | collective-permute-start | bytes 12296 | tf_op jit(solution)/shard_map/ppermute | solution.py:485
  57.7 6.6 %collective-permute-start.10 = (bf16[1,256,512]{2,1,0:T(8,128)(2,1)S(1)}, bf16[1,256,512]{2,1,0:T(8,128)(2,1)S(1)}, u32[]{:S(2)}, u32[]{:S(2)}) collective-permute-start(bf16[1,256,512]{2,1,0:T(8,128)(2,1)S(1)} %get-tuple-element.58), channel_id=1, source_target_pairs={{0,1},{1,0},{2,3},{3,2},{4,5},{5,4},{6,7},{7,6},{8,9},{9,8},{10,11... | collective-permute-start | bytes 786440 | tf_op jit(solution)/shard_map/ppermute | solution.py:485
  61.6 4.4 %collective-permute-start.15 = (bf16[1,256,512]{2,1,0:T(8,128)(2,1)S(1)}, bf16[1,256,512]{2,1,0:T(8,128)(2,1)S(1)}, u32[]{:S(2)}, u32[]{:S(2)}) collective-permute-start(bf16[1,256,512]{2,1,0:T(8,128)(2,1)S(1)} %get-tuple-element.65), channel_id=1, source_target_pairs={{0,1},{1,0},{2,3},{3,2},{4,5},{5,4},{6,7},{7,6},{8,9},{9,8},{10,11... | collective-permute-start | bytes 786440 | tf_op jit(solution)/shard_map/ppermute | solution.py:485
  62.7 7.5 %collective-permute-start.9 = (bf16[256,512]{1,0:T(8,128)(2,1)S(1)}, bf16[256,512]{1,0:T(8,128)(2,1)S(1)}, u32[]{:S(2)}, u32[]{:S(2)}) collective-permute-start(bf16[256,512]{1,0:T(8,128)(2,1)S(1)} %get-tuple-element.56), channel_id=1, source_target_pairs={{0,1},{1,0},{2,3},{3,2},{4,5},{5,4},{6,7},{7,6},{8,9},{9,8},{10,11... | collective-permute-start | bytes 786440 | tf_op jit(solution)/shard_map/ppermute | solution.py:485
  64.3 6.0 %collective-permute-start.14 = (bf16[256,512]{1,0:T(8,128)(2,1)S(1)}, bf16[256,512]{1,0:T(8,128)(2,1)S(1)}, u32[]{:S(2)}, u32[]{:S(2)}) collective-permute-start(bf16[256,512]{1,0:T(8,128)(2,1)S(1)} %get-tuple-element.63), channel_id=1, source_target_pairs={{0,1},{1,0},{2,3},{3,2},{4,5},{5,4},{6,7},{7,6},{8,9},{9,8},{10,11... | collective-permute-start | bytes 786440 | tf_op jit(solution)/shard_map/ppermute | solution.py:485
  64.4 9.2 %collective-permute-start.11 = (bf16[1,256,512]{2,1,0:T(8,128)(2,1)S(1)}, bf16[1,256,512]{2,1,0:T(8,128)(2,1)S(1)}, u32[]{:S(2)}, u32[]{:S(2)}) collective-permute-start(bf16[1,256,512]{2,1,0:T(8,128)(2,1)S(1)} %add_convert_fusion.1), channel_id=1, source_target_pairs={{0,2},{1,3},{2,0},{3,1},{4,6},{5,7},{6,4},{7,5},{8,10},{9,11},{10,... | collective-permute-start | bytes 786440 | tf_op jit(solution)/shard_map/ppermute | solution.py:485
  66.1 12.7 %collective-permute-start.16 = (bf16[1,256,512]{2,1,0:T(8,128)(2,1)S(1)}, bf16[1,256,512]{2,1,0:T(8,128)(2,1)S(1)}, u32[]{:S(2)}, u32[]{:S(2)}) collective-permute-start(bf16[1,256,512]{2,1,0:T(8,128)(2,1)S(1)} %add_convert_fusion), channel_id=1, source_target_pairs={{0,2},{1,3},{2,0},{3,1},{4,6},{5,7},{6,4},{7,5},{8,10},{9,11},{10,... | collective-permute-start | bytes 786440 | tf_op jit(solution)/shard_map/ppermute | solution.py:485
  66.7 13.2 %all-to-all-start = ((f32[8,4,1024]{2,1,0:T(4,128)}), f32[8,4,1024]{2,1,0:T(4,128)S(1)}, u32[]{:S(2)}, u32[]{:S(2)}) async-start(f32[8,4,1024]{2,1,0:T(4,128)} %get-tuple-element.41), calls=%async_computation | async-start | bytes 262144 | tf_op jit(solution)/shard_map/all_to_all | solution.py:573
  79.8 21.8 %all-to-all-start.2 = ((bf16[8,64,512]{2,1,0:T(8,128)(2,1)}), bf16[8,64,512]{2,1,0:T(8,128)(2,1)S(1)}, u32[]{:S(2)}, u32[]{:S(2)}) async-start(bf16[8,64,512]{2,1,0:T(8,128)(2,1)} %bitcast.19), calls=%async_computation.2 | async-start | bytes 1048576 | tf_op jit(solution)/shard_map/all_to_all | solution.py:652
  88.4 7.9 %collective-permute-start.4 = (bf16[256,512]{1,0:T(8,128)(2,1)S(1)}, bf16[256,512]{1,0:T(8,128)(2,1)S(1)}, u32[]{:S(2)}, u32[]{:S(2)}) collective-permute-start(bf16[256,512]{1,0:T(8,128)(2,1)S(1)} %mixer_read.1.refs_0_), channel_id=1, source_target_pairs={{0,2},{1,3},{2,0},{3,1},{4,6},{5,7},{6,4},{7,5},{8,10},{9,11},{10,... | collective-permute-start | bytes 786440 | tf_op jit(solution)/shard_map/ppermute | solution.py:485
  90.0 9.7 %collective-permute-start.3 = (bf16[256,512]{1,0:T(8,128)(2,1)S(1)}, bf16[256,512]{1,0:T(8,128)(2,1)S(1)}, u32[]{:S(2)}, u32[]{:S(2)}) collective-permute-start(bf16[256,512]{1,0:T(8,128)(2,1)S(1)} %mixer_read.1.refs_0_), channel_id=1, source_target_pairs={{0,1},{1,0},{2,3},{3,2},{4,5},{5,4},{6,7},{7,6},{8,9},{9,8},{10,11... | collective-permute-start | bytes 786440 | tf_op jit(solution)/shard_map/ppermute | solution.py:485
  96.3 3.4 %collective-permute-start.5 = (bf16[256,512]{1,0:T(8,128)(2,1)S(1)}, bf16[256,512]{1,0:T(8,128)(2,1)S(1)}, u32[]{:S(2)}, u32[]{:S(2)}) collective-permute-start(bf16[256,512]{1,0:T(8,128)(2,1)S(1)} %collective-permute-done.4.refs_2_), channel_id=1, source_target_pairs={{0,1},{1,0},{2,3},{3,2},{4,5},{5,4},{6,7},{7,6},{8,9},{9,8},{10,11... | collective-permute-start | bytes 786440 | tf_op jit(solution)/shard_map/ppermute | solution.py:485
